TPU v7x, 128 devices: a whole 4x4x4 slice. The times are simulated.
128 devices in a mesh: sp: 32 (over z, y, core), tp: 4 (over x).
Axes of the slice: x: 4, y: 4, z: 4, core: 2. Of those that a mesh axis runs over, the one named last changes fastest.
Arguments:
- residual_in: bfloat16 [32768, 2048], P(('sp', 'tp')), may hold values from -6 to 6
- queries: bfloat16 [32768, 2048], P('sp', 'tp'), may hold values from -200 to 200, as said below
- keys_values: bfloat16 [2, 32768, 1024], P(None, 'sp', 'tp'), may hold values from -6 to 6
- sink_logit: float32 [32], P('tp'), may hold values from -2 to 6
- out_weight: bfloat16 [2048, 2048], P('tp'), may hold values from -2 to 2
- norm1_gain: float32 [2048], replicated, may hold values from 0.1 to 1.9
- norm1_bias: float32 [2048], replicated, may hold values from -3 to 3
- up_weight: bfloat16 [2048, 8192], P('sp', 'tp'), may hold values from -0.125 to 0.125
- down_weight: bfloat16 [8192, 2048], P('tp', 'sp'), may hold values from -0.0625 to 0.0625
- norm2_gain: float32 [2048], replicated, may hold values from 0.1 to 1.9
- norm2_bias: float32 [2048], replicated, may hold values from -3 to 3
Outputs:
- stream_out: bfloat16 [32768, 2048], P(('sp', 'tp'))
Inputs may be any that keep to these rules, and one draw needn't show every extreme that they name: `queries`: of order one mostly; some rows may be large multiples of a nearby key row.
All inputs are finite; a program needn't handle non-finite values.
Results may differ from a plain program's by a relative error of at most 0.014.
Values may be sent and summed in bfloat16 or wider, within the bound.
No kernel may reach another device: no remote copies, remote signals or barrier semaphores. Data moves between devices by JAX's collectives and lax.ppermute only.
A program may use at most 128 MiB of HBM per device.

v0:
```python
import jax
import jax.numpy as jnp
from jax import lax
from jax.sharding import PartitionSpec as P

HEAD_DIM = 64
WINDOW = 128


def in_order(pieces, dim):
    dims = list(pieces.shape[1:])
    dims[dim] *= pieces.shape[0]
    return jnp.moveaxis(pieces, 0, dim).reshape(dims)


def one_gather(arrays, axis, dims):
    flat = jnp.concatenate([a.reshape(-1) for a in arrays])
    lines, at, finished = (lax.all_gather(flat, axis), 0, [])
    for a, dim in zip(arrays, dims):
        pieces = lines[:, at : at + a.size].reshape(-1, *a.shape)
        finished.append(in_order(pieces, dim))
        at += a.size
    return tuple(finished)


def with_halo(shard, sides, width):
    for axis, dim in sides:
        devices, length = (lax.axis_size(axis), shard.shape[dim])
        up = [(i, (i + 1) % devices) for i in range(devices - 1)]
        down = [(j, i) for i, j in up]
        last = lax.slice_in_dim(shard, length - width, length, axis=dim)
        first = lax.slice_in_dim(shard, 0, width, axis=dim)
        before = lax.ppermute(last, axis, up)
        after = lax.ppermute(first, axis, down)
        shard = jnp.concatenate([before, shard, after], axis=dim)
    return shard


def in_blocks(shard, dim, devices):
    dims = shard.shape
    pieces = shard.reshape(*dims[:dim], devices, dims[dim] // devices, *dims[dim + 1 :])
    return jnp.moveaxis(pieces, dim, 0)


def sent_and_summed(shard, axis, dim):
    pieces = in_blocks(shard, dim, lax.axis_size(axis))
    arrived = lax.all_to_all(pieces, axis, split_axis=0, concat_axis=0, tiled=True)
    return arrived.astype(jnp.float32).sum(axis=0)


def sent_to_all(shard, axis):
    devices = lax.axis_size(axis)
    return lax.all_to_all(
        jnp.broadcast_to(shard[None], (devices, *shard.shape)), axis, 0, 0, tiled=True
    )


def gathered_copies(shard, axis, dim):
    pieces = sent_to_all(shard, axis)
    return in_order(pieces, dim)


def norm_rows(values, gain, bias):
    mean = jnp.mean(values, axis=-1, keepdims=True)
    centred = values - mean
    variance = jnp.mean(centred * centred, axis=-1, keepdims=True)
    return (centred * lax.rsqrt(variance + 1e-06) * gain + bias).astype(jnp.bfloat16)


def attend(queries, padded, sink_logit, offset, total):
    tok_rows = queries.shape[0]
    block = min(512, tok_rows)
    span = block + 2 * WINDOW
    kv_local = padded.shape[2] // HEAD_DIM
    heads_local = queries.shape[1] // HEAD_DIM
    group = heads_local // kv_local
    sink = sink_logit.reshape(kv_local, group, 1, 1)

    def one_block(index):
        start = index * block
        query = lax.dynamic_slice_in_dim(queries, start, block, 0).reshape(
            block, kv_local, group, HEAD_DIM
        )
        keys = lax.dynamic_slice_in_dim(padded[0], start, span, 0).reshape(span, kv_local, HEAD_DIM)
        values = lax.dynamic_slice_in_dim(padded[1], start, span, 0).reshape(
            span, kv_local, HEAD_DIM
        )
        scores = jnp.einsum(
            "qhgd,khd->hgqk", query, keys, preferred_element_type=jnp.float32
        ) * HEAD_DIM ** (-0.5)
        query_pos = offset + start + jnp.arange(block, dtype=jnp.int32)
        key_pos = offset + start - WINDOW + jnp.arange(span, dtype=jnp.int32)
        valid = (
            (jnp.abs(key_pos[None, :] - query_pos[:, None]) <= WINDOW)
            & (key_pos[None, :] >= 0)
            & (key_pos[None, :] < total)
        )
        scores = jnp.where(valid, scores, -jnp.inf)
        top = jnp.maximum(jnp.max(scores, axis=-1, keepdims=True), sink)
        expd = jnp.exp(scores - top)
        denom = jnp.sum(expd, axis=-1, keepdims=True) + jnp.exp(sink - top)
        weights = (expd / denom).astype(jnp.bfloat16)
        mixed = jnp.einsum("hgqk,khd->qhgd", weights, values, preferred_element_type=jnp.float32)
        return mixed.reshape(block, heads_local * HEAD_DIM).astype(jnp.bfloat16)

    blocks = lax.map(one_block, jnp.arange(tok_rows // block, dtype=jnp.int32))
    return blocks.reshape(tok_rows, heads_local * HEAD_DIM)


def activate(rows, up_full):
    hidden = jnp.dot(rows, up_full, preferred_element_type=jnp.float32)
    return jnp.square(jnp.maximum(hidden, 0.0)).astype(jnp.bfloat16)


def on_device(
    residual_in,
    queries,
    keys_values,
    sink_logit,
    out_weight,
    norm1_gain,
    norm1_bias,
    up_weight,
    down_weight,
    norm2_gain,
    norm2_bias,
):
    up_full, down_full = one_gather((up_weight, down_weight), "sp", (0, 1))
    tok_rows = queries.shape[0]
    padded = with_halo(keys_values, (("sp", 1),), WINDOW)
    offset = lax.axis_index("sp") * tok_rows
    attended = attend(queries, padded, sink_logit, offset, tok_rows * lax.axis_size("sp"))
    rows = attended
    projected = sent_and_summed(
        jnp.dot(rows, out_weight, preferred_element_type=jnp.float32)
        .astype(jnp.bfloat16)
        .astype(jnp.float32)
        .astype(jnp.bfloat16),
        "tp",
        0,
    )
    first = norm_rows(residual_in.astype(jnp.float32) + projected, norm1_gain, norm1_bias)
    activation = activate(gathered_copies(first, "tp", 0), up_full)
    rows = activation
    branch = lax.psum_scatter(
        jnp.dot(rows, down_full, preferred_element_type=jnp.float32)
        .astype(jnp.bfloat16)
        .astype(jnp.float32)
        .astype(jnp.bfloat16),
        "tp",
        scatter_dimension=0,
        tiled=True,
    ).astype(jnp.float32)
    return norm_rows(first.astype(jnp.float32) + branch, norm2_gain, norm2_bias)


def solution(mesh):
    return jax.shard_map(
        on_device,
        mesh=mesh,
        in_specs=(
            P(("sp", "tp"), None),
            P("sp", "tp"),
            P(None, "sp", "tp"),
            P("tp"),
            P("tp", None),
            P(),
            P(),
            P("sp", "tp"),
            P("tp", "sp"),
            P(),
            P(),
        ),
        out_specs=P(("sp", "tp"), None),
        check_vma=False,
    )
```

profile of v0, /device:TPU:1, one launch (start us, length us, event | category | flops | bytes accessed | tf_op | source)
XLA Modules:
  0.0 300.6 jit_solution(18373947099800134417)
XLA Ops:
  6.5 1.4 copy.37
  10.0 1.5 copy.31
  12.2 3.3 %collective-permute-start.1 = (bf16[2,128,256]{1,2,0:T(8,128)(2,1)}, bf16[2,128,256]{1,2,0:T(8,128)(2,1)S(1)}, u32[]{:S(2)}, u32[]{:S(2)}) collective-permute-start(bf16[2,128,256]{1,2,0:T(8,128)(2,1)} %get-tuple-element.141), channel_id=1, source_target_pairs={{4,0},{8,4},{12,8},{16,12},{20,16},{24,20},{28,24},{32,28},{36,32}... | collective-permute-start | bytes 393224 | tf_op jit(solution)/shard_map/ppermute | solution.py:34
  15.5 3.2 %collective-permute-start = (bf16[2,128,256]{1,2,0:T(8,128)(2,1)S(1)}, bf16[2,128,256]{1,2,0:T(8,128)(2,1)S(1)}, u32[]{:S(2)}, u32[]{:S(2)}) collective-permute-start(bf16[2,128,256]{1,2,0:T(8,128)(2,1)S(1)} %get-tuple-element.140), channel_id=1, source_target_pairs={{0,4},{4,8},{8,12},{12,16},{16,20},{20,24},{24,28},{28,32},{32,36}... | collective-permute-start | bytes 393224 | tf_op jit(solution)/shard_map/ppermute | solution.py:33
  19.6 1.0 collective-permute-done
  20.7 1.2 pad_maximum_fusion
  21.8 53.7 %while.12 = (s32[]{:T(128)}, bf16[2,512,512]{2,1,0:T(8,128)(2,1)}, bf16[2,1280,256]{1,2,0:T(8,128)(2,1)}, s32[2]{0:T(128)S(1)}, s32[]{:T(128)}, /*index=5*/bf16[...) while((s32[]{:T(128)}, bf16[2,512,512]{2,1,0:T(8,128)(2,1)}, ...), condition=%wide.region_3.4_spmd, body=%wide.region_0.3_spmd.sunk | while | flops 845295104 | bytes 101627328 | solution.py:106
  21.8 1.5 fusion.37
  26.3 1.1 constant_dynamic-slice_fusion.6
  27.6 7.7 %fusion.40 = (f32[4,2,512]{2,1,0:T(2,128)S(1)}, f32[4,768,512,2]{2,1,3,0:T(8,128)}) fusion(pred[512,768]{0,1:T(8,128)(4,1)S(1)} %fusion.39, bf16[768,4,64,1]{0,2,3,1:T(8,128)(2,1)} %bitcast.68, bf16[512,4,2,64]{0,3,2,1:T(8,128)(2,1)S(1)} %bitcast.67), kind=kOutput, calls=%fused_computation.4.clone.1 | convolution fusion | flops 412086272 | bytes 13910016 | tf_op jit(solution)/shard_map/while/body/eval_jaxpr/qhgd,khd->hgqk/dot_general | solution.py:88
  35.5 7.3 %fusion.41 = f32[4,2,512]{2,1,0:T(2,128)S(1)} fusion(f32[4,768,512,2]{2,1,3,0:T(8,128)} %get-tuple-element.199, f32[4,2,512]{2,1,0:T(2,128)S(1)} %broadcast_maximum_fusion.2, pred[512,768]{0,1:T(8,128)(4,1)S(1)} %fusion.39), kind=kLoop, calls=%fused_computation.3.clone.1 | loop fusion | flops 12578816 | bytes 13008896 | tf_op jit(solution)/shard_map/while/body/eval_jaxpr/reduce_sum | solution.py:101
  43.6 3.6 %fusion.42 = bf16[4,64,2,512]{3,1,2,0:T(8,128)(2,1)S(1)} fusion(bf16[768,4,64,1]{0,2,3,1:T(8,128)(2,1)S(1)} %bitcast.70, f32[4,768,512,2]{2,1,3,0:T(8,128)S(1)} %copy-done.1, f32[4,2,512]{2,1,0:T(2,128)S(1)} %exponential_add_fusion.2, f32[4,2,512]{2,1,0:T(2,128)S(1)} %broadcast_maximum_fusion.2, pred[512,768]{0,1:T(8,128)(4,1)S(1)} %fusion.39), kind=kOutput, calls=%fused_computation.9.clone.1 | convolution fusion | flops 418643968 | bytes 13926400 | tf_op jit(solution)/shard_map/while/body/eval_jaxpr/hgqk,khd->qhgd/dot_general | solution.py:103
  48.3 1.4 fusion.37
  52.7 1.1 constant_dynamic-slice_fusion.6
  54.0 7.7 %fusion.40 = (f32[4,2,512]{2,1,0:T(2,128)S(1)}, f32[4,768,512,2]{2,1,3,0:T(8,128)}) fusion(pred[512,768]{0,1:T(8,128)(4,1)S(1)} %fusion.39, bf16[768,4,64,1]{0,2,3,1:T(8,128)(2,1)} %bitcast.68, bf16[512,4,2,64]{0,3,2,1:T(8,128)(2,1)S(1)} %bitcast.67), kind=kOutput, calls=%fused_computation.4.clone.1 | convolution fusion | flops 412086272 | bytes 13910016 | tf_op jit(solution)/shard_map/while/body/eval_jaxpr/qhgd,khd->hgqk/dot_general | solution.py:88
  61.8 7.8 %fusion.41 = f32[4,2,512]{2,1,0:T(2,128)S(1)} fusion(f32[4,768,512,2]{2,1,3,0:T(8,128)} %get-tuple-element.199, f32[4,2,512]{2,1,0:T(2,128)S(1)} %broadcast_maximum_fusion.2, pred[512,768]{0,1:T(8,128)(4,1)S(1)} %fusion.39), kind=kLoop, calls=%fused_computation.3.clone.1 | loop fusion | flops 12578816 | bytes 13008896 | tf_op jit(solution)/shard_map/while/body/eval_jaxpr/reduce_sum | solution.py:101
  69.7 1.1 copy-done.1
  70.9 3.6 %fusion.42 = bf16[4,64,2,512]{3,1,2,0:T(8,128)(2,1)S(1)} fusion(bf16[768,4,64,1]{0,2,3,1:T(8,128)(2,1)S(1)} %bitcast.70, f32[4,768,512,2]{2,1,3,0:T(8,128)S(1)} %copy-done.1, f32[4,2,512]{2,1,0:T(2,128)S(1)} %exponential_add_fusion.2, f32[4,2,512]{2,1,0:T(2,128)S(1)} %broadcast_maximum_fusion.2, pred[512,768]{0,1:T(8,128)(4,1)S(1)} %fusion.39), kind=kOutput, calls=%fused_computation.9.clone.1 | convolution fusion | flops 418643968 | bytes 13926400 | tf_op jit(solution)/shard_map/while/body/eval_jaxpr/hgqk,khd->qhgd/dot_general | solution.py:103
  75.5 3.7 %convolution_convert_fusion.1 = bf16[1024,2048]{1,0:T(8,128)(2,1)S(1)} fusion(bf16[1024,512]{1,0:T(8,128)(2,1)} %bitcast.76, bf16[512,2048]{1,0:T(8,128)(2,1)S(1)} %copy-done), kind=kOutput, calls=%fused_computation.25 | convolution fusion | flops 2149580800 | bytes 7340032 | tf_op jit(solution)/shard_map/dot_general | solution.py:135
  79.2 52.5 %all_to_all.10 = bf16[4,256,2048]{2,1,0:T(8,128)(2,1)S(1)} all-to-all(bf16[4,256,2048]{2,1,0:T(8,128)(2,1)S(1)} %bitcast.72), channel_id=1, replica_groups=mesh['sp'=32,'tp'=4] {'tp'}, dimensions={0} | all-to-all | bytes 8388608 | tf_op jit(solution)/shard_map/all_to_all | solution.py:47
  134.3 2.5 broadcast_in_dim.27
  136.9 4.8 %all-to-all-start.1 = ((bf16[4,256,2048]{2,1,0:T(8,128)(2,1)}), bf16[4,256,2048]{2,1,0:T(8,128)(2,1)}, u32[]{:S(2)}, u32[]{:S(2)}) async-start(bf16[4,256,2048]{2,1,0:T(8,128)(2,1)} %broadcast_in_dim.27), calls=%async_computation.1 | async-start | bytes 8388608 | tf_op jit(solution)/shard_map/all_to_all | solution.py:53
  141.8 14.6 %reshape.138 = bf16[32,262144]{1,0:T(8,128)(2,1)} reshape(bf16[8388608]{0:T(1024)(128)(2,1)} %all-gather.3.cloned.1.call-done) | data formatting | bytes 33554432 | tf_op jit(solution)/shard_map/all_gather | solution.py:18
  156.3 11.3 %fusion.15 = (bf16[32,131072]{1,0:T(8,128)(2,1)}, bf16[32,131072]{1,0:T(8,128)(2,1)}) fusion(bf16[32,262144]{1,0:T(8,128)(2,1)} %reshape.138), kind=kLoop, calls=%fused_computation.43 | loop fusion | bytes 33554432 | tf_op jit(solution)/shard_map/slice | solution.py:20
  167.6 19.0 %reshape.136 = bf16[32,2048,64]{2,1,0:T(8,128)(2,1)} reshape(bf16[32,131072]{1,0:T(8,128)(2,1)} %get-tuple-element.139) | data formatting | bytes 16777216 | tf_op jit(solution)/shard_map/reshape | solution.py:20
  186.6 15.8 %copy.38 = bf16[2048,32,64]{0,2,1:T(8,128)(2,1)} copy(bf16[2048,32,64]{2,0,1:T(8,128)(2,1)} %bitcast.66) | data formatting | bytes 16777216 | tf_op jit(solution)/shard_map/transpose | solution.py:13
  202.4 8.9 %reshape_reshape.3 = bf16[2048,2048]{1,0:T(8,128)(2,1)} reshape(bf16[32,131072]{1,0:T(8,128)(2,1)} %get-tuple-element.138) | data formatting | bytes 16777216 | tf_op jit(solution)/shard_map/reshape;reshape | solution.py:13
  211.3 25.7 %convolution_convert_fusion = bf16[1024,2048]{1,0:T(8,128)(2,1)} fusion(bf16[2048,2048]{0,1:T(8,128)(2,1)} %bitcast.71, bf16[1024,2048]{1,0:T(8,128)(2,1)} %bitcast.14, bf16[2048,2048]{1,0:T(8,128)(2,1)} %reshape_reshape.3), kind=kOutput, calls=%fused_computation.24 | convolution fusion | flops 17188257792 | bytes 25165824 | tf_op jit(solution)/shard_map/dot_general | solution.py:146
  237.0 51.8 %reduce-scatter.2.cloned.1.call-done = bf16[256,2048]{1,0:T(8,128)(2,1)} async-done(((bf16[1024,2048]{1,0:T(8,128)(2,1)}), bf16[256,2048]{1,0:T(8,128)(2,1)}) %reduce-scatter.2.cloned.1.call-update) | async-done | bytes 1048592 | tf_op jit(solution)/shard_map/reduce_scatter | solution.py:145
  288.8 1.7 fusion.11
  290.5 1.7 multiply_reduce_fusion
  292.2 1.5 add_convert_fusion
  (70 shorter events, 14.8 us)
Async XLA Ops:
  6.5 69.0 %copy-start = (bf16[512,2048]{1,0:T(8,128)(2,1)S(1)}, bf16[512,2048]{1,0:T(8,128)(2,1)}, u32[]{:S(2)}) copy-start(bf16[512,2048]{1,0:T(8,128)(2,1)} %param.17) | copy-start | bytes 6291460
  6.5 12.2 %copy-start.9 = (f32[8]{0:T(128)S(1)}, f32[8]{0:T(128)}, u32[]{:S(2)}) copy-start(f32[8]{0:T(128)} %param.16) | copy-start | bytes 100
  6.5 135.2 %all-gather.3.cloned.1.call-start = ((), (), s32[]{:S(2)}) async-start(), calls=%async_computation.4 | async-start | bytes 17301504 | tf_op jit(solution)/shard_map/all_gather | solution.py:18
  12.2 7.4 %collective-permute-start.1 = (bf16[2,128,256]{1,2,0:T(8,128)(2,1)}, bf16[2,128,256]{1,2,0:T(8,128)(2,1)S(1)}, u32[]{:S(2)}, u32[]{:S(2)}) collective-permute-start(bf16[2,128,256]{1,2,0:T(8,128)(2,1)} %get-tuple-element.141), channel_id=1, source_target_pairs={{4,0},{8,4},{12,8},{16,12},{20,16},{24,20},{28,24},{32,28},{36,32}... | collective-permute-start | bytes 393224 | tf_op jit(solution)/shard_map/ppermute | solution.py:34
  15.5 5.1 %collective-permute-start = (bf16[2,128,256]{1,2,0:T(8,128)(2,1)S(1)}, bf16[2,128,256]{1,2,0:T(8,128)(2,1)S(1)}, u32[]{:S(2)}, u32[]{:S(2)}) collective-permute-start(bf16[2,128,256]{1,2,0:T(8,128)(2,1)S(1)} %get-tuple-element.140), channel_id=1, source_target_pairs={{0,4},{4,8},{8,12},{12,16},{16,20},{20,24},{24,28},{28,32},{32,36}... | collective-permute-start | bytes 393224 | tf_op jit(solution)/shard_map/ppermute | solution.py:33
  35.5 8.2 %copy-start.1 = (f32[4,768,512,2]{2,1,3,0:T(8,128)S(1)}, f32[4,768,512,2]{2,1,3,0:T(8,128)}, u32[]{:S(2)}) copy-start(f32[4,768,512,2]{2,1,3,0:T(8,128)} %get-tuple-element.199) | copy-start | bytes 37748740 | tf_op jit(solution)/shard_map/while
  35.5 8.2 %copy-start.2 = (bf16[1,768,256]{1,2,0:T(8,128)(2,1)S(1)}, bf16[1,768,256]{1,2,0:T(8,128)(2,1)}, u32[]{:S(2)}) copy-start(bf16[1,768,256]{1,2,0:T(8,128)(2,1)} %get-tuple-element.195) | copy-start | bytes 1179652 | tf_op jit(solution)/shard_map/while
  61.8 9.0 %copy-start.1 = (f32[4,768,512,2]{2,1,3,0:T(8,128)S(1)}, f32[4,768,512,2]{2,1,3,0:T(8,128)}, u32[]{:S(2)}) copy-start(f32[4,768,512,2]{2,1,3,0:T(8,128)} %get-tuple-element.199) | copy-start | bytes 37748740 | tf_op jit(solution)/shard_map/while
  61.8 9.0 %copy-start.2 = (bf16[1,768,256]{1,2,0:T(8,128)(2,1)S(1)}, bf16[1,768,256]{1,2,0:T(8,128)(2,1)}, u32[]{:S(2)}) copy-start(bf16[1,768,256]{1,2,0:T(8,128)(2,1)} %get-tuple-element.195) | copy-start | bytes 1179652 | tf_op jit(solution)/shard_map/while
  131.8 1.2 copy-start.4
  133.0 0.8 copy-start.5
  133.0 0.8 copy-start.6
  136.9 74.5 %all-to-all-start.1 = ((bf16[4,256,2048]{2,1,0:T(8,128)(2,1)}), bf16[4,256,2048]{2,1,0:T(8,128)(2,1)}, u32[]{:S(2)}, u32[]{:S(2)}) async-start(bf16[4,256,2048]{2,1,0:T(8,128)(2,1)} %broadcast_in_dim.27), calls=%async_computation.1 | async-start | bytes 8388608 | tf_op jit(solution)/shard_map/all_to_all | solution.py:53
  141.7 147.1 %reduce-scatter.2.cloned.1.call-start = ((), (), s32[]{:S(2)}) async-start(), calls=%async_computation.3 | async-start | bytes 5242880 | tf_op jit(solution)/shard_map/reduce_scatter | solution.py:145
  237.0 55.2 %copy-start.7 = (f32[2048]{0:T(1024)S(1)}, f32[2048]{0:T(1024)}, u32[]{:S(2)}) copy-start(f32[2048]{0:T(1024)} %param.23) | copy-start | bytes 24580
  237.0 55.2 %copy-start.8 = (f32[2048]{0:T(1024)S(1)}, f32[2048]{0:T(1024)}, u32[]{:S(2)}) copy-start(f32[2048]{0:T(1024)} %param.22) | copy-start | bytes 24580
  288.8 3.4 %copy-start.3 = (bf16[256,2048]{1,0:T(8,128)(2,1)S(1)}, bf16[256,2048]{1,0:T(8,128)(2,1)}, u32[]{:S(2)}) copy-start(bf16[256,2048]{1,0:T(8,128)(2,1)} %reduce-scatter.2.cloned.1.call-done) | copy-start | bytes 3145732
Sparse Core Ops, SparseCore 0:
  10.2 76.2 all-gather.2
  237.1 51.6 reduce-scatter.1
where the time goes:
time: 302 us; the launch traced here: 301 us
  local copies, waits for them, and re-layouts  90.2 us (30%)
  waiting for transfers between devices  53.6 us (18%)
  blocking collectives  52.5 us (17%)
  matrix products  51.9 us (17%)
  other arithmetic  26.1 us (9%)
  between operations  13.6 us (5%)
  starting transfers between devices  11.4 us (4%)
    all_to_all x1, blocking collectives, sent_and_summed(): lax.all_to_all(pieces, axis, split_axis=0, concat_axis=0, tiled=True)  52.5 us
    reduce_scatter x1, waiting for transfers between devices, on_device(): lax.psum_scatter(jnp.dot(rows, down_full, preferred_element_type=jnp.floa...  51.8 us
    dot_general x1, matrix products, on_device(): jnp.dot(rows, down_full, preferred_element_type=jnp.float32)  25.7 us
    reshape x1, local copies, waits for them, and re-layouts, one_gather(): pieces = lines[:, at:at + a.size].reshape(-1, *a.shape)  19 us
    transpose x1, local copies, waits for them, and re-layouts, in_order(): return jnp.moveaxis(pieces, 0, dim).reshape(dims)  15.8 us
    dot_general x2, matrix products, one_block(): jnp.einsum('qhgd,khd->hgqk', query, keys, preferred_element_type=jnp.floa...  15.3 us
    reduce_sum x2, other arithmetic, one_block(): denom = jnp.sum(expd, axis=-1, keepdims=True) + jnp.exp(sink - top)  15.1 us
    all_gather x1, local copies, waits for them, and re-layouts, one_gather(): lines, at, finished = (lax.all_gather(flat, axis), 0, [])  14.6 us
  transfers between devices with their start and end apart: 5, of which 3 were waited for; matrix products, arithmetic and copies ran while one was open for 44% of the time, Pallas kernels for 0%

commit v1 on v0

v1 whole, which is shorter than its diff:
```python
import functools

import jax
import jax.numpy as jnp
from jax import lax
from jax.experimental import pallas as pl
from jax.experimental.pallas import tpu as pltpu
from jax.sharding import PartitionSpec as P

HEAD_DIM = 64
WINDOW = 128
LANES = 128
NEG = -1e30


def shift(value, axis, step):
    devices = lax.axis_size(axis)
    return lax.ppermute(value, axis, [(i, (i + step) % devices) for i in range(devices)])


def halo(shard, axis, width):
    devices, length = (lax.axis_size(axis), shard.shape[1])
    up = [(i, i + 1) for i in range(devices - 1)]
    down = [(j, i) for i, j in up]
    before = lax.ppermute(shard[:, length - width :], axis, up)
    after = lax.ppermute(shard[:, :width], axis, down)
    return jnp.concatenate([before, shard, after], axis=1)


def attend_kernel(place, sink, q_ref, kv_ref, w_ref, out_ref, *, rel, n_sp, tok_rows):
    step = pl.program_id(0)
    rows = q_ref.shape[0]
    quarter = (place[0] + rel(step)) % (tok_rows // rows)
    blocks = rows // WINDOW
    pairs = q_ref.shape[1] // LANES
    row = lax.broadcasted_iota(jnp.int32, (2 * WINDOW, WINDOW), 0) % WINDOW
    col = lax.broadcasted_iota(jnp.int32, (2 * WINDOW, WINDOW), 1)
    low = lax.broadcasted_iota(jnp.int32, (WINDOW, LANES), 1) < HEAD_DIM
    upper = lax.broadcasted_iota(jnp.int32, (2 * WINDOW, 1), 0) < WINDOW
    ones = jnp.ones((3 * WINDOW, LANES), jnp.bfloat16)
    finished = []
    for block in range(blocks):
        index = quarter * blocks + block
        at_start = jnp.where((place[1] == 0) & (index == 0), 4 * WINDOW, 0)
        at_end = jnp.where((place[1] == n_sp - 1) & (index == tok_rows // WINDOW - 1), 4 * WINDOW, 0)
        before_ok = col - row >= at_start
        after_ok = row - col >= at_end
        start = pl.multiple_of(index * WINDOW, WINDOW)
        mixed = []
        for pair in range(pairs):
            tile, half = (pair // 2, pair % 2)
            lanes = slice(tile * LANES, (tile + 1) * LANES)
            query = q_ref[block * WINDOW : (block + 1) * WINDOW, pair * LANES : (pair + 1) * LANES]
            query = query.astype(jnp.float32) * HEAD_DIM**-0.5
            turned = pltpu.roll(query, HEAD_DIM, 1)
            if half == 0:
                both = (jnp.where(low, query, 0.0), jnp.where(low, turned, 0.0))
            else:
                both = (jnp.where(low, 0.0, turned), jnp.where(low, 0.0, query))
            query = jnp.concatenate(both, axis=0).astype(jnp.bfloat16)
            keys = kv_ref[0, pl.ds(start, 3 * WINDOW), lanes]
            values = kv_ref[1, pl.ds(start, 3 * WINDOW), lanes]
            scores = lax.dot_general(
                query, keys, (((1,), (1,)), ((), ())), preferred_element_type=jnp.float32
            )
            before = jnp.where(before_ok, scores[:, :WINDOW], NEG)
            middle = scores[:, WINDOW : 2 * WINDOW]
            after = jnp.where(after_ok, scores[:, 2 * WINDOW :], NEG)
            sink_col = jnp.where(upper, sink[2 * pair], sink[2 * pair + 1])
            top = jnp.max(
                jnp.maximum(jnp.maximum(before, after), middle), axis=-1, keepdims=True
            )
            top = jnp.maximum(top, sink_col)
            expd = jnp.concatenate(
                [jnp.exp(part - top).astype(jnp.bfloat16) for part in (before, middle, after)],
                axis=1,
            )
            summed = jnp.dot(
                expd,
                jnp.concatenate([values, ones], axis=1),
                preferred_element_type=jnp.float32,
            )
            result = summed[:, :LANES] / (summed[:, LANES:] + jnp.exp(sink_col - top))
            first, second = (result[:WINDOW], result[WINDOW:])
            if half == 0:
                second = pltpu.roll(second, HEAD_DIM, 1)
            else:
                first = pltpu.roll(first, HEAD_DIM, 1)
            mixed.append(jnp.where(low, first, second).astype(jnp.bfloat16))
        finished.append(jnp.concatenate(mixed, axis=1))
    attended = jnp.concatenate(finished, axis=0)
    out_ref[...] = jnp.dot(attended, w_ref[...], preferred_element_type=jnp.float32).astype(
        jnp.bfloat16
    )


def attend(place, sink, queries, padded, out_weight, steps, rel, n_tp, n_sp):
    tok_rows, width = queries.shape
    rows = tok_rows // n_tp
    cols = out_weight.shape[1]
    return pl.pallas_call(
        functools.partial(attend_kernel, rel=rel, n_sp=n_sp, tok_rows=tok_rows),
        grid_spec=pltpu.PrefetchScalarGridSpec(
            num_scalar_prefetch=2,
            grid=(steps,),
            in_specs=[
                pl.BlockSpec((rows, width), lambda i, place, sink: ((place[0] + rel(i)) % n_tp, 0)),
                pl.BlockSpec(padded.shape, lambda i, place, sink: (0, 0, 0)),
                pl.BlockSpec(out_weight.shape, lambda i, place, sink: (0, 0)),
            ],
            out_specs=pl.BlockSpec((rows, cols), lambda i, place, sink: (i, 0)),
        ),
        out_shape=jax.ShapeDtypeStruct((steps * rows, cols), jnp.bfloat16),
        name="attend",
    )(place, sink, queries, padded, out_weight)


def norm_kernel(*refs):
    gain, bias, out_ref = refs[-3:]
    values = refs[0][...].astype(jnp.float32)
    for ref in refs[1:-3]:
        values = values + ref[...].astype(jnp.float32)
    width = values.shape[1]
    mean = jnp.sum(values, axis=-1, keepdims=True) * (1.0 / width)
    centred = values - mean
    variance = jnp.sum(centred * centred, axis=-1, keepdims=True) * (1.0 / width)
    out_ref[...] = (centred * lax.rsqrt(variance + 1e-06) * gain[...] + bias[...]).astype(
        jnp.bfloat16
    )


def norm_rows(parts, gain, bias, block=64):
    rows, width = parts[0].shape
    tile = pl.BlockSpec((block, width), lambda i: (i, 0))
    line = pl.BlockSpec((1, width), lambda i: (0, 0))
    return pl.pallas_call(
        norm_kernel,
        grid=(rows // block,),
        in_specs=[tile] * len(parts) + [line, line],
        out_specs=tile,
        out_shape=jax.ShapeDtypeStruct((rows, width), jnp.bfloat16),
        name="norm",
    )(*parts, gain[None], bias[None])


def added(part, arrived, top):
    half = arrived.shape[0]
    mine = part[:half] if top else part[half:]
    total = (mine.astype(jnp.float32) + arrived.astype(jnp.float32)).astype(jnp.bfloat16)
    return jnp.concatenate([total, part[half:]] if top else [part[:half], total], axis=0)


def ring_sum(far, right, left):
    half = far.shape[0] // 2
    from_left = shift(far[:half], "tp", 1)
    from_right = shift(far[half:], "tp", -1)
    return (
        shift(added(right, from_left, True), "tp", 1),
        shift(added(left, from_right, False), "tp", -1),
    )


def feed_forward(rows, up_full, down_full):
    hidden = jnp.dot(rows, up_full, preferred_element_type=jnp.float32)
    activation = jnp.square(jnp.maximum(hidden, 0.0)).astype(jnp.bfloat16)
    return lax.dot_general(
        activation, down_full, (((1,), (1,)), ((), ())), preferred_element_type=jnp.float32
    ).astype(jnp.bfloat16)


def on_device(
    residual_in,
    queries,
    keys_values,
    sink_logit,
    out_weight,
    norm1_gain,
    norm1_bias,
    up_weight,
    down_weight,
    norm2_gain,
    norm2_bias,
):
    n_tp, n_sp = (lax.axis_size("tp"), lax.axis_size("sp"))
    up_full = lax.all_gather(up_weight, "sp", axis=0, tiled=True)
    down_full = lax.all_gather(down_weight.T, "sp", axis=0, tiled=True)
    place = jnp.where(
        jnp.arange(2, dtype=jnp.int32) == 0, lax.axis_index("tp"), lax.axis_index("sp")
    )
    padded = halo(keys_values, "sp", WINDOW)
    run = functools.partial(attend, place, sink_logit, queries, padded, out_weight)
    rows = queries.shape[0] // n_tp
    far = run(1, lambda i: 2, n_tp, n_sp)
    near = run(3, lambda i: 1 + 2 * i - i // 2, n_tp, n_sp)
    right, left, own = (near[:rows], near[rows : 2 * rows], near[2 * rows :])
    arrived = ring_sum(far, right, left)
    first = norm_rows((residual_in, own, *arrived), norm1_gain, norm1_bias)

    half = rows // 2
    of_left, of_right = (shift(first, "tp", 1), shift(first, "tp", -1))
    of_far = jnp.concatenate(
        [shift(of_left[:half], "tp", 1), shift(of_right[half:], "tp", -1)], axis=0
    )
    far = feed_forward(of_far, up_full, down_full)
    right = feed_forward(of_right, up_full, down_full)
    left = feed_forward(of_left, up_full, down_full)
    own = feed_forward(first, up_full, down_full)
    arrived = ring_sum(far, right, left)
    return norm_rows((first, own, *arrived), norm2_gain, norm2_bias)


def solution(mesh):
    return jax.shard_map(
        on_device,
        mesh=mesh,
        in_specs=(
            P(("sp", "tp"), None),
            P("sp", "tp"),
            P(None, "sp", "tp"),
            P("tp"),
            P("tp", None),
            P(),
            P(),
            P("sp", "tp"),
            P("tp", "sp"),
            P(),
            P(),
        ),
        out_specs=P(("sp", "tp"), None),
        check_vma=False,
    )
```

time: 302 us -> 201 us (0.67)
  local copies, waits for them, and re-layouts: 90.2 us -> 11.6 us
  blocking collectives: 52.5 us -> 0 us
  Pallas kernels: 0 us -> 27.1 us
  waiting for transfers between devices: 53.6 us -> 76.7 us
  other arithmetic: 26.1 us -> 5.77 us
  starting transfers between devices: 11.4 us -> 22.1 us
  matrix products: 51.9 us -> 42.4 us
    ppermute x2 -> x14, waiting for transfers between devices: 1.72 us -> 72.9 us  [the longest x12 70.5 us: shift(): lax.ppermute(value, axis, [(i, (i + step) % devices) for i in range(devic...]
    all_to_all x1 -> x0, blocking collectives: 52.5 us -> none  [sent_and_summed(): lax.all_to_all(pieces, axis, split_axis=0, concat_axis=0, tiled=True)]
    reduce_scatter x1 -> x0, waiting for transfers between devices: 51.8 us -> none  [on_device(): lax.psum_scatter(jnp.dot(rows, down_full, preferred_element_type=jnp.floa...]
    pallas_call x0 -> x4, Pallas kernels: none -> 27.1 us  [the longest x2 18 us: attend(): pl.pallas_call(functools.partial(attend_kernel, rel=rel, n_sp=n_sp, tok_r...]
    reduce_sum x7 -> x0, other arithmetic: 20.1 us -> none  [the longest x2 15.1 us: one_block(): denom = jnp.sum(expd, axis=-1, keepdims=True) + jnp.exp(sink - top)]
    reshape x3 -> x0, local copies, waits for them, and re-layouts: 19.3 us -> none  [the longest x1 19 us: one_gather(): pieces = lines[:, at:at + a.size].reshape(-1, *a.shape)]
    transpose x1 -> x0, local copies, waits for them, and re-layouts: 15.8 us -> none  [in_order(): return jnp.moveaxis(pieces, 0, dim).reshape(dims)]
    ppermute x2 -> x14, starting transfers between devices: 6.49 us -> 22 us  [the longest x12 15.5 us: shift(): lax.ppermute(value, axis, [(i, (i + step) % devices) for i in range(devic...]
  transfers between devices with their start and end apart: 5 -> 16, of which waited for: 3 -> 8; matrix products, arithmetic and copies ran while one was open for 44% -> 23% of each run, Pallas kernels for 0% -> 11%
where the time goes in v1:
time: 201 us; the launch traced here: 199 us
  waiting for transfers between devices  76.7 us (38%)
  matrix products  42.4 us (21%)
  Pallas kernels  27.1 us (13%)
  starting transfers between devices  22.1 us (11%)
  between operations  13.6 us (7%)
  local copies, waits for them, and re-layouts  11.6 us (6%)
  other arithmetic  5.77 us (3%)
    ppermute x12, waiting for transfers between devices, shift(): lax.ppermute(value, axis, [(i, (i + step) % devices) for i in range(devic...  70.5 us
    dot_general x4, matrix products, feed_forward(): lax.dot_general(activation, down_full, (((1,), (1,)), ((), ())), preferre...  42.4 us
    pallas_call x2, Pallas kernels, attend(): pl.pallas_call(functools.partial(attend_kernel, rel=rel, n_sp=n_sp, tok_r...  18 us
    ppermute x12, starting transfers between devices, shift(): lax.ppermute(value, axis, [(i, (i + step) % devices) for i in range(devic...  15.5 us
    pallas_call x2, Pallas kernels, norm_rows(): pl.pallas_call(norm_kernel, grid=(rows // block,), in_specs=[tile] * len(...  9.09 us
    ppermute x1, starting transfers between devices, halo(): before = lax.ppermute(shard[:, length - width:], axis, up)  4.58 us
    unnamed x16, local copies, waits for them, and re-layouts  4.32 us
  transfers between devices with their start and end apart: 16, of which 8 were waited for; matrix products, arithmetic and copies ran while one was open for 23% of the time, Pallas kernels for 11%

profile of v1, /device:TPU:1, one launch (start us, length us, event | category | flops | bytes accessed | tf_op | source)
XLA Modules:
  0.0 199.2 jit_solution(17997374950089164702)
XLA Ops:
  9.0 4.6 %collective-permute-start = (bf16[2,128,256]{2,1,0:T(8,128)(2,1)S(1)}, bf16[2,128,256]{2,1,0:T(8,128)(2,1)S(1)}, u32[]{:S(2)}, u32[]{:S(2)}) collective-permute-start(bf16[2,128,256]{2,1,0:T(8,128)(2,1)S(1)} %get-tuple-element.14), channel_id=1, source_target_pairs={{0,4},{4,8},{8,12},{12,16},{16,20},{20,24},{24,28},{28,32},{32,36}... | collective-permute-start | bytes 393224 | tf_op jit(solution)/shard_map/ppermute | solution.py:25
  13.6 1.9 collective-permute-start.1
  16.1 1.3 constant_dynamic-update-slice_fusion.1
  17.4 2.5 %collective-permute-done.1 = bf16[2,128,256]{2,1,0:T(8,128)(2,1)S(1)} collective-permute-done((bf16[2,128,256]{2,1,0:T(8,128)(2,1)S(1)}, bf16[2,128,256]{2,1,0:T(8,128)(2,1)S(1)}, u32[]{:S(2)}, u32[]{:S(2)}) %collective-permute-start.1) | collective-permute-done | bytes 131104 | tf_op jit(solution)/shard_map/ppermute | solution.py:26
  21.0 6.3 %attend.3 = bf16[256,2048]{1,0:T(8,128)(2,1)} custom-call(s32[2]{0:T(128)} %compare_select_fusion.place, f32[8]{0:T(128)} %sink.3, bf16[1024,512]{1,0:T(8,128)(2,1)} %q_ref.3, bf16[2,1280,256]{2,1,0:T(8,128)(2,1)} %copy-done, bf16[512,2048]{1,0:T(8,128)(2,1)} %w_ref.3), custom_call_target="tpu_custom_call" | custom-call | tf_op jit(solution)/shard_map/attend/pallas_call | solution.py:101
  27.3 1.3 fusion.21
  28.6 1.3 collective-permute-start.2
  29.9 1.5 collective-permute-start.4
  31.3 11.7 %attend.2 = bf16[768,2048]{1,0:T(8,128)(2,1)} custom-call(s32[2]{0:T(128)} %compare_select_fusion.place, f32[8]{0:T(128)} %sink.3, bf16[1024,512]{1,0:T(8,128)(2,1)} %q_ref.3, bf16[2,1280,256]{2,1,0:T(8,128)(2,1)} %copy-done, bf16[512,2048]{1,0:T(8,128)(2,1)} %w_ref.3), custom_call_target="tpu_custom_call" | custom-call | tf_op jit(solution)/shard_map/attend/pallas_call | solution.py:101
  43.0 1.4 fusion.19
  44.5 1.6 add_convert_fusion.2
  46.1 1.3 collective-permute-start.5
  47.8 2.3 %slice.74.refs_1_ = bf16[256,2048]{1,0:T(8,128)(2,1)} slice(bf16[768,2048]{1,0:T(8,128)(2,1)} %attend.2), slice={[512:768], [0:2048]} | slice | bytes 2097152 | tf_op jit(solution)/shard_map/slice | solution.py:195
  50.1 18.9 %collective-permute-done.5.refs_3_ = bf16[256,2048]{1,0:T(8,128)(2,1)S(1)} collective-permute-done((bf16[256,2048]{1,0:T(8,128)(2,1)S(1)}, bf16[256,2048]{1,0:T(8,128)(2,1)S(1)}, u32[]{:S(2)}, u32[]{:S(2)}) %collective-permute-start.5) | collective-permute-done | bytes 1048608 | tf_op jit(solution)/shard_map/ppermute | solution.py:18
  69.0 2.7 %collective-permute-done.3.refs_2_ = bf16[256,2048]{1,0:T(8,128)(2,1)S(1)} collective-permute-done((bf16[256,2048]{1,0:T(8,128)(2,1)S(1)}, bf16[256,2048]{1,0:T(8,128)(2,1)S(1)}, u32[]{:S(2)}, u32[]{:S(2)}) %collective-permute-start.3) | collective-permute-done | bytes 1048608 | tf_op jit(solution)/shard_map/ppermute | solution.py:18
  72.7 4.5 %norm.2.refs_0_ = bf16[256,2048]{1,0:T(8,128)(2,1)} custom-call(bf16[256,2048]{1,0:T(8,128)(2,1)} %refs_0_.1, bf16[256,2048]{1,0:T(8,128)(2,1)} %slice.74.refs_1_, bf16[256,2048]{1,0:T(8,128)(2,1)} %copy-done.5, bf16[256,2048]{1,0:T(8,128)(2,1)} %copy-done.3, f32[1,2048]{1,0:T(1,128)} %bitcast.17, f32[1,2048]{1,0:T(1,128)} %bitcast.18), custom_call_target="tpu_custom_call" | custom-call | tf_op jit(solution)/shard_map/norm/pallas_call | solution.py:136
  77.2 2.7 %collective-permute-start.6 = (bf16[256,2048]{1,0:T(8,128)(2,1)}, bf16[256,2048]{1,0:T(8,128)(2,1)S(1)}, u32[]{:S(2)}, u32[]{:S(2)}) collective-permute-start(bf16[256,2048]{1,0:T(8,128)(2,1)} %norm.2.refs_0_), channel_id=1, source_target_pairs={{0,3},{1,0},{2,1},{3,2},{4,7},{5,4},{6,5},{7,6},{8,11},{9,8},{10,9... | collective-permute-start | bytes 3145736 | tf_op jit(solution)/shard_map/ppermute | solution.py:18
  79.9 23.2 %collective-permute-done.7 = bf16[256,2048]{1,0:T(8,128)(2,1)S(1)} collective-permute-done((bf16[256,2048]{1,0:T(8,128)(2,1)}, bf16[256,2048]{1,0:T(8,128)(2,1)S(1)}, u32[]{:S(2)}, u32[]{:S(2)}) %collective-permute-start.7) | collective-permute-done | bytes 1048608 | tf_op jit(solution)/shard_map/ppermute | solution.py:18
  103.3 3.1 %collective-permute-start.9 = (bf16[128,2048]{1,0:T(8,128)(2,1)S(1)}, bf16[128,2048]{1,0:T(8,128)(2,1)S(1)}, u32[]{:S(2)}, u32[]{:S(2)}) collective-permute-start(bf16[128,2048]{1,0:T(8,128)(2,1)S(1)} %slice.83), channel_id=1, source_target_pairs={{0,3},{1,0},{2,1},{3,2},{4,7},{5,4},{6,5},{7,6},{8,11},{9,8},{10,9... | collective-permute-start | bytes 1572872 | tf_op jit(solution)/shard_map/ppermute | solution.py:18
  106.4 12.1 %collective-permute-done.8 = bf16[128,2048]{1,0:T(8,128)(2,1)S(1)} collective-permute-done((bf16[128,2048]{1,0:T(8,128)(2,1)S(1)}, bf16[128,2048]{1,0:T(8,128)(2,1)S(1)}, u32[]{:S(2)}, u32[]{:S(2)}) %collective-permute-start.8) | collective-permute-done | bytes 524320 | tf_op jit(solution)/shard_map/ppermute | solution.py:18
  118.4 2.3 %all-gather.5.cloned.1.call-done = bf16[2048,2048]{1,0:T(8,128)(2,1)} async-done(((bf16[64,2048]{1,0:T(8,128)(2,1)}), bf16[2048,2048]{1,0:T(8,128)(2,1)}) %all-gather.5.cloned.1.call-update) | async-done | bytes 8388624 | tf_op jit(solution)/shard_map/all_gather | solution.py:186
  120.8 10.3 %convolution_convert_fusion.1 = bf16[256,2048]{1,0:T(8,128)(2,1)S(1)} fusion(bf16[2048,2048]{1,0:T(8,128)(2,1)} %all-gather.5.cloned.1.call-done, bf16[2048,2048]{1,0:T(8,128)(2,1)} %all-gather.3.cloned.1.call-done, bf16[128,2048]{1,0:T(8,128)(2,1)S(1)} %collective-permute-done.9, bf16[128,2048]{1,0:T(8,128)(2,1)S(1)} %collective-permute-done.8), kind=kOutput, calls=%fused_computation.13 | convolution fusion | flops 4299161600 | bytes 18874368 | tf_op jit(solution)/shard_map/dot_general | solution.py:166
  131.1 1.1 fusion.20
  132.2 2.4 %collective-permute-start.12 = (bf16[128,2048]{1,0:T(8,128)(2,1)}, bf16[128,2048]{1,0:T(8,128)(2,1)S(1)}, u32[]{:S(2)}, u32[]{:S(2)}) collective-permute-start(bf16[128,2048]{1,0:T(8,128)(2,1)} %get-tuple-element.9), channel_id=1, source_target_pairs={{0,3},{1,0},{2,1},{3,2},{4,7},{5,4},{6,5},{7,6},{8,11},{9,8},{10,9... | collective-permute-start | bytes 1572872 | tf_op jit(solution)/shard_map/ppermute | solution.py:18
  134.6 10.3 %convolution_convert_fusion = bf16[256,2048]{1,0:T(8,128)(2,1)S(1)} fusion(bf16[2048,2048]{1,0:T(8,128)(2,1)} %all-gather.5.cloned.1.call-done, bf16[256,2048]{1,0:T(8,128)(2,1)S(1)} %collective-permute-done.7, bf16[2048,2048]{1,0:T(8,128)(2,1)} %all-gather.3.cloned.1.call-done), kind=kOutput, calls=%fused_computation.12 | convolution fusion | flops 4297064448 | bytes 18874368 | tf_op jit(solution)/shard_map/dot_general | solution.py:166
  145.2 10.6 %convolution_convert_fusion.2 = bf16[256,2048]{1,0:T(8,128)(2,1)S(1)} fusion(bf16[2048,2048]{1,0:T(8,128)(2,1)} %all-gather.5.cloned.1.call-done, bf16[256,2048]{1,0:T(8,128)(2,1)} %copy-done.6, bf16[2048,2048]{1,0:T(8,128)(2,1)} %all-gather.3.cloned.1.call-done), kind=kOutput, calls=%fused_computation.14 | convolution fusion | flops 4297064448 | bytes 18874368 | tf_op jit(solution)/shard_map/dot_general | solution.py:166
  157.1 2.7 %collective-permute-start.13 = (bf16[256,2048]{1,0:T(8,128)(2,1)}, bf16[256,2048]{1,0:T(8,128)(2,1)S(1)}, u32[]{:S(2)}, u32[]{:S(2)}) collective-permute-start(bf16[256,2048]{1,0:T(8,128)(2,1)} %pad_maximum_fusion.3), channel_id=1, source_target_pairs={{0,3},{1,0},{2,1},{3,2},{4,7},{5,4},{6,5},{7,6},{8,11},{9,8},{10,9... | collective-permute-start | bytes 3145736 | tf_op jit(solution)/shard_map/ppermute | solution.py:18
  159.8 1.2 add_convert_fusion.1
  162.0 11.2 %convolution_convert_fusion.3.refs_1_ = bf16[256,2048]{1,0:T(8,128)(2,1)} fusion(bf16[2048,2048]{1,0:T(8,128)(2,1)} %all-gather.5.cloned.1.call-done, bf16[256,2048]{1,0:T(8,128)(2,1)S(1)} %copy-done.1, bf16[2048,2048]{1,0:T(8,128)(2,1)} %all-gather.3.cloned.1.call-done), kind=kOutput, calls=%fused_computation.15 | convolution fusion | flops 4297064448 | bytes 18874368 | tf_op jit(solution)/shard_map/dot_general | solution.py:166
  173.3 8.5 %collective-permute-done.13.refs_3_ = bf16[256,2048]{1,0:T(8,128)(2,1)S(1)} collective-permute-done((bf16[256,2048]{1,0:T(8,128)(2,1)}, bf16[256,2048]{1,0:T(8,128)(2,1)S(1)}, u32[]{:S(2)}, u32[]{:S(2)}) %collective-permute-start.13) | collective-permute-done | bytes 1048608 | tf_op jit(solution)/shard_map/ppermute | solution.py:18
  181.8 5.1 %collective-permute-done.11.refs_2_ = bf16[256,2048]{1,0:T(8,128)(2,1)S(1)} collective-permute-done((bf16[256,2048]{1,0:T(8,128)(2,1)}, bf16[256,2048]{1,0:T(8,128)(2,1)S(1)}, u32[]{:S(2)}, u32[]{:S(2)}) %collective-permute-start.11) | collective-permute-done | bytes 1048608 | tf_op jit(solution)/shard_map/ppermute | solution.py:18
  187.8 4.5 %norm.3 = bf16[256,2048]{1,0:T(8,128)(2,1)} custom-call(bf16[256,2048]{1,0:T(8,128)(2,1)} %norm.2.refs_0_, bf16[256,2048]{1,0:T(8,128)(2,1)} %convolution_convert_fusion.3.refs_1_, bf16[256,2048]{1,0:T(8,128)(2,1)} %copy-done.4, bf16[256,2048]{1,0:T(8,128)(2,1)} %copy-done.2, f32[1,2048]{1,0:T(1,128)} %bitcast.19, f32[1,2048]{1,0:T(1,128)} %bitcast.20), custom_call_target="tpu_custom_call" | custom-call | tf_op jit(solution)/shard_map/norm/pallas_call | solution.py:136
  (44 shorter events, 9.4 us)
Async XLA Ops:
  6.5 111.9 %all-gather.3.cloned.1.call-start = ((), (), s32[]{:S(2)}) async-start(), calls=%async_computation | async-start | bytes 8650752 | tf_op jit(solution)/shard_map/all_gather | solution.py:185
  7.3 113.5 %all-gather.5.cloned.1.call-start = ((), (), s32[]{:S(2)}) async-start(), calls=%async_computation.1 | async-start | bytes 8650752 | tf_op jit(solution)/shard_map/all_gather | solution.py:186
  9.0 7.1 %collective-permute-start = (bf16[2,128,256]{2,1,0:T(8,128)(2,1)S(1)}, bf16[2,128,256]{2,1,0:T(8,128)(2,1)S(1)}, u32[]{:S(2)}, u32[]{:S(2)}) collective-permute-start(bf16[2,128,256]{2,1,0:T(8,128)(2,1)S(1)} %get-tuple-element.14), channel_id=1, source_target_pairs={{0,4},{4,8},{8,12},{12,16},{16,20},{20,24},{24,28},{28,32},{32,36}... | collective-permute-start | bytes 393224 | tf_op jit(solution)/shard_map/ppermute | solution.py:25
  13.6 6.3 %collective-permute-start.1 = (bf16[2,128,256]{2,1,0:T(8,128)(2,1)S(1)}, bf16[2,128,256]{2,1,0:T(8,128)(2,1)S(1)}, u32[]{:S(2)}, u32[]{:S(2)}) collective-permute-start(bf16[2,128,256]{2,1,0:T(8,128)(2,1)S(1)} %get-tuple-element.13), channel_id=1, source_target_pairs={{4,0},{8,4},{12,8},{16,12},{20,16},{24,20},{28,24},{32,28},{36,32}... | collective-permute-start | bytes 393224 | tf_op jit(solution)/shard_map/ppermute | solution.py:26
  19.9 1.1 copy-start
  28.6 15.9 %collective-permute-start.2 = (bf16[128,2048]{1,0:T(8,128)(2,1)S(1)}, bf16[128,2048]{1,0:T(8,128)(2,1)S(1)}, u32[]{:S(2)}, u32[]{:S(2)}) collective-permute-start(bf16[128,2048]{1,0:T(8,128)(2,1)S(1)} %get-tuple-element.12), channel_id=1, source_target_pairs={{0,1},{1,2},{2,3},{3,0},{4,5},{5,6},{6,7},{7,4},{8,9},{9,10},{10,1... | collective-permute-start | bytes 1572872 | tf_op jit(solution)/shard_map/ppermute | solution.py:18
  29.9 14.6 %collective-permute-start.4 = (bf16[128,2048]{1,0:T(8,128)(2,1)S(1)}, bf16[128,2048]{1,0:T(8,128)(2,1)S(1)}, u32[]{:S(2)}, u32[]{:S(2)}) collective-permute-start(bf16[128,2048]{1,0:T(8,128)(2,1)S(1)} %get-tuple-element.11), channel_id=1, source_target_pairs={{0,3},{1,0},{2,1},{3,2},{4,7},{5,4},{6,5},{7,6},{8,11},{9,8},{10,9... | collective-permute-start | bytes 1572872 | tf_op jit(solution)/shard_map/ppermute | solution.py:18
  46.1 22.9 %collective-permute-start.5 = (bf16[256,2048]{1,0:T(8,128)(2,1)S(1)}, bf16[256,2048]{1,0:T(8,128)(2,1)S(1)}, u32[]{:S(2)}, u32[]{:S(2)}) collective-permute-start(bf16[256,2048]{1,0:T(8,128)(2,1)S(1)} %pad_maximum_fusion.1), channel_id=1, source_target_pairs={{0,3},{1,0},{2,1},{3,2},{4,7},{5,4},{6,5},{7,6},{8,11},{9,8},{10,9... | collective-permute-start | bytes 3145736 | tf_op jit(solution)/shard_map/ppermute | solution.py:18
  47.5 24.2 %collective-permute-start.3 = (bf16[256,2048]{1,0:T(8,128)(2,1)S(1)}, bf16[256,2048]{1,0:T(8,128)(2,1)S(1)}, u32[]{:S(2)}, u32[]{:S(2)}) collective-permute-start(bf16[256,2048]{1,0:T(8,128)(2,1)S(1)} %pad_maximum_fusion), channel_id=1, source_target_pairs={{0,1},{1,2},{2,3},{3,0},{4,5},{5,6},{6,7},{7,4},{8,9},{9,10},{10,1... | collective-permute-start | bytes 3145736 | tf_op jit(solution)/shard_map/ppermute | solution.py:18
  69.0 2.7 %copy-start.3 = (bf16[256,2048]{1,0:T(8,128)(2,1)}, bf16[256,2048]{1,0:T(8,128)(2,1)S(1)}, u32[]{:S(2)}) copy-start(bf16[256,2048]{1,0:T(8,128)(2,1)S(1)} %collective-permute-done.5.refs_3_) | copy-start | bytes 3145732
  71.7 1.0 copy-start.5
  77.2 25.9 %collective-permute-start.7 = (bf16[256,2048]{1,0:T(8,128)(2,1)}, bf16[256,2048]{1,0:T(8,128)(2,1)S(1)}, u32[]{:S(2)}, u32[]{:S(2)}) collective-permute-start(bf16[256,2048]{1,0:T(8,128)(2,1)} %norm.2.refs_0_), channel_id=1, source_target_pairs={{0,1},{1,2},{2,3},{3,0},{4,5},{5,6},{6,7},{7,4},{8,9},{9,10},{10,1... | collective-permute-start | bytes 3145736 | tf_op jit(solution)/shard_map/ppermute | solution.py:18
  77.2 26.0 %collective-permute-start.6 = (bf16[256,2048]{1,0:T(8,128)(2,1)}, bf16[256,2048]{1,0:T(8,128)(2,1)S(1)}, u32[]{:S(2)}, u32[]{:S(2)}) collective-permute-start(bf16[256,2048]{1,0:T(8,128)(2,1)} %norm.2.refs_0_), channel_id=1, source_target_pairs={{0,3},{1,0},{2,1},{3,2},{4,7},{5,4},{6,5},{7,6},{8,11},{9,8},{10,9... | collective-permute-start | bytes 3145736 | tf_op jit(solution)/shard_map/ppermute | solution.py:18
  103.2 15.3 %collective-permute-start.8 = (bf16[128,2048]{1,0:T(8,128)(2,1)S(1)}, bf16[128,2048]{1,0:T(8,128)(2,1)S(1)}, u32[]{:S(2)}, u32[]{:S(2)}) collective-permute-start(bf16[128,2048]{1,0:T(8,128)(2,1)S(1)} %slice.82), channel_id=1, source_target_pairs={{0,1},{1,2},{2,3},{3,0},{4,5},{5,6},{6,7},{7,4},{8,9},{9,10},{10,1... | collective-permute-start | bytes 1572872 | tf_op jit(solution)/shard_map/ppermute | solution.py:18
  103.3 15.2 %copy-start.6 = (bf16[256,2048]{1,0:T(8,128)(2,1)}, bf16[256,2048]{1,0:T(8,128)(2,1)S(1)}, u32[]{:S(2)}) copy-start(bf16[256,2048]{1,0:T(8,128)(2,1)S(1)} %collective-permute-done.6) | copy-start | bytes 3145732
  103.3 15.1 %collective-permute-start.9 = (bf16[128,2048]{1,0:T(8,128)(2,1)S(1)}, bf16[128,2048]{1,0:T(8,128)(2,1)S(1)}, u32[]{:S(2)}, u32[]{:S(2)}) collective-permute-start(bf16[128,2048]{1,0:T(8,128)(2,1)S(1)} %slice.83), channel_id=1, source_target_pairs={{0,3},{1,0},{2,1},{3,2},{4,7},{5,4},{6,5},{7,6},{8,11},{9,8},{10,9... | collective-permute-start | bytes 1572872 | tf_op jit(solution)/shard_map/ppermute | solution.py:18
  132.2 23.7 %collective-permute-start.12 = (bf16[128,2048]{1,0:T(8,128)(2,1)}, bf16[128,2048]{1,0:T(8,128)(2,1)S(1)}, u32[]{:S(2)}, u32[]{:S(2)}) collective-permute-start(bf16[128,2048]{1,0:T(8,128)(2,1)} %get-tuple-element.9), channel_id=1, source_target_pairs={{0,3},{1,0},{2,1},{3,2},{4,7},{5,4},{6,5},{7,6},{8,11},{9,8},{10,9... | collective-permute-start | bytes 1572872 | tf_op jit(solution)/shard_map/ppermute | solution.py:18
  144.9 14.8 %collective-permute-start.10 = (bf16[128,2048]{1,0:T(8,128)(2,1)}, bf16[128,2048]{1,0:T(8,128)(2,1)}, u32[]{:S(2)}, u32[]{:S(2)}) collective-permute-start(bf16[128,2048]{1,0:T(8,128)(2,1)} %get-tuple-element.10), channel_id=1, source_target_pairs={{0,1},{1,2},{2,3},{3,0},{4,5},{5,6},{6,7},{7,4},{8,9},{9,10},{10,1... | collective-permute-start | bytes 1572872 | tf_op jit(solution)/shard_map/ppermute | solution.py:18
  157.1 4.9 %copy-start.1 = (bf16[256,2048]{1,0:T(8,128)(2,1)S(1)}, bf16[256,2048]{1,0:T(8,128)(2,1)}, u32[]{:S(2)}) copy-start(bf16[256,2048]{1,0:T(8,128)(2,1)} %norm.2.refs_0_) | copy-start | bytes 3145732
  157.1 24.7 %collective-permute-start.13 = (bf16[256,2048]{1,0:T(8,128)(2,1)}, bf16[256,2048]{1,0:T(8,128)(2,1)S(1)}, u32[]{:S(2)}, u32[]{:S(2)}) collective-permute-start(bf16[256,2048]{1,0:T(8,128)(2,1)} %pad_maximum_fusion.3), channel_id=1, source_target_pairs={{0,3},{1,0},{2,1},{3,2},{4,7},{5,4},{6,5},{7,6},{8,11},{9,8},{10,9... | collective-permute-start | bytes 3145736 | tf_op jit(solution)/shard_map/ppermute | solution.py:18
  162.0 24.8 %collective-permute-start.11 = (bf16[256,2048]{1,0:T(8,128)(2,1)}, bf16[256,2048]{1,0:T(8,128)(2,1)S(1)}, u32[]{:S(2)}, u32[]{:S(2)}) collective-permute-start(bf16[256,2048]{1,0:T(8,128)(2,1)} %pad_maximum_fusion.2), channel_id=1, source_target_pairs={{0,1},{1,2},{2,3},{3,0},{4,5},{5,6},{6,7},{7,4},{8,9},{9,10},{10,1... | collective-permute-start | bytes 3145736 | tf_op jit(solution)/shard_map/ppermute | solution.py:18
  181.8 5.1 %copy-start.2 = (bf16[256,2048]{1,0:T(8,128)(2,1)}, bf16[256,2048]{1,0:T(8,128)(2,1)S(1)}, u32[]{:S(2)}) copy-start(bf16[256,2048]{1,0:T(8,128)(2,1)S(1)} %collective-permute-done.13.refs_3_) | copy-start | bytes 3145732
  186.8 1.0 copy-start.4
Sparse Core Ops, SparseCore 0:
  9.6 56.4 all-gather.2
  68.4 52.3 all-gather.4

commit v2 on v1

--- a/solution.py
+++ b/solution.py
@@ -24,11 +24,21 @@
     down = [(j, i) for i, j in up]
     before = lax.ppermute(shard[:, length - width :], axis, up)
     after = lax.ppermute(shard[:, :width], axis, down)
-    return jnp.concatenate([before, shard, after], axis=1)
-
-
-def attend_kernel(place, sink, q_ref, kv_ref, w_ref, out_ref, *, rel, n_sp, tok_rows):
+    return before, after
+
+
+def attend_kernel(
+    place, sink, q_ref, before_ref, mid_ref, after_ref, w_ref, *refs, rel, n_sp, tok_rows
+):
+    *out_refs, kv_ref = refs
     step = pl.program_id(0)
+
+    @pl.when(step == 0)
+    def _():
+        kv_ref[:, :WINDOW] = before_ref[...]
+        kv_ref[:, WINDOW : WINDOW + tok_rows] = mid_ref[...]
+        kv_ref[:, WINDOW + tok_rows :] = after_ref[...]
+
     rows = q_ref.shape[0]
     quarter = (place[0] + rel(step)) % (tok_rows // rows)
     blocks = rows // WINDOW
@@ -89,15 +99,26 @@
             mixed.append(jnp.where(low, first, second).astype(jnp.bfloat16))
         finished.append(jnp.concatenate(mixed, axis=1))
     attended = jnp.concatenate(finished, axis=0)
-    out_ref[...] = jnp.dot(attended, w_ref[...], preferred_element_type=jnp.float32).astype(
+    projected = jnp.dot(attended, w_ref[...], preferred_element_type=jnp.float32).astype(
         jnp.bfloat16
     )
-
-
-def attend(place, sink, queries, padded, out_weight, steps, rel, n_tp, n_sp):
+    half = rows // 2
+    for turn in range(len(out_refs) // 2):
+
+        @pl.when(step == turn)
+        def _():
+            out_refs[2 * turn][...] = projected[:half]
+            out_refs[2 * turn + 1][...] = projected[half:]
+
+
+def attend(place, sink, queries, before, middle, after, out_weight, steps, rel, n_tp, n_sp):
     tok_rows, width = queries.shape
     rows = tok_rows // n_tp
     cols = out_weight.shape[1]
+
+    def whole(array):
+        return pl.BlockSpec(array.shape, lambda i, place, sink: (0,) * array.ndim)
+
     return pl.pallas_call(
         functools.partial(attend_kernel, rel=rel, n_sp=n_sp, tok_rows=tok_rows),
         grid_spec=pltpu.PrefetchScalarGridSpec(
@@ -105,67 +126,133 @@
             grid=(steps,),
             in_specs=[
                 pl.BlockSpec((rows, width), lambda i, place, sink: ((place[0] + rel(i)) % n_tp, 0)),
-                pl.BlockSpec(padded.shape, lambda i, place, sink: (0, 0, 0)),
-                pl.BlockSpec(out_weight.shape, lambda i, place, sink: (0, 0)),
+                whole(before),
+                whole(middle),
+                whole(after),
+                whole(out_weight),
             ],
-            out_specs=pl.BlockSpec((rows, cols), lambda i, place, sink: (i, 0)),
+            out_specs=[pl.BlockSpec((rows // 2, cols), lambda i, place, sink: (0, 0))] * (2 * steps),
+            scratch_shapes=[
+                pltpu.VMEM((2, tok_rows + 2 * WINDOW, middle.shape[2]), jnp.bfloat16)
+            ],
         ),
-        out_shape=jax.ShapeDtypeStruct((steps * rows, cols), jnp.bfloat16),
+        out_shape=[jax.ShapeDtypeStruct((rows // 2, cols), jnp.bfloat16)] * (2 * steps),
         name="attend",
-    )(place, sink, queries, padded, out_weight)
-
-
-def norm_kernel(*refs):
-    gain, bias, out_ref = refs[-3:]
+    )(place, sink, queries, before, middle, after, out_weight)
+
+
+def normed(refs, gain, bias):
     values = refs[0][...].astype(jnp.float32)
-    for ref in refs[1:-3]:
+    for ref in refs[1:]:
         values = values + ref[...].astype(jnp.float32)
     width = values.shape[1]
     mean = jnp.sum(values, axis=-1, keepdims=True) * (1.0 / width)
     centred = values - mean
     variance = jnp.sum(centred * centred, axis=-1, keepdims=True) * (1.0 / width)
-    out_ref[...] = (centred * lax.rsqrt(variance + 1e-06) * gain[...] + bias[...]).astype(
-        jnp.bfloat16
-    )
-
-
-def norm_rows(parts, gain, bias, block=64):
+    return (centred * lax.rsqrt(variance + 1e-06) * gain[...] + bias[...]).astype(jnp.bfloat16)
+
+
+def norm_kernel(*refs):
+    refs[-1][...] = normed(refs[:-3], *refs[-3:-1])
+
+
+def norm_half(residual, side, parts, gain, bias, block=64):
     rows, width = parts[0].shape
+    steps = rows // block
     tile = pl.BlockSpec((block, width), lambda i: (i, 0))
     line = pl.BlockSpec((1, width), lambda i: (0, 0))
     return pl.pallas_call(
         norm_kernel,
-        grid=(rows // block,),
-        in_specs=[tile] * len(parts) + [line, line],
+        grid=(steps,),
+        in_specs=[pl.BlockSpec((block, width), lambda i: (side * steps + i, 0))]
+        + [tile] * len(parts)
+        + [line, line],
         out_specs=tile,
         out_shape=jax.ShapeDtypeStruct((rows, width), jnp.bfloat16),
         name="norm",
-    )(*parts, gain[None], bias[None])
-
-
-def added(part, arrived, top):
-    half = arrived.shape[0]
-    mine = part[:half] if top else part[half:]
-    total = (mine.astype(jnp.float32) + arrived.astype(jnp.float32)).astype(jnp.bfloat16)
-    return jnp.concatenate([total, part[half:]] if top else [part[:half], total], axis=0)
-
-
-def ring_sum(far, right, left):
-    half = far.shape[0] // 2
-    from_left = shift(far[:half], "tp", 1)
-    from_right = shift(far[half:], "tp", -1)
-    return (
-        shift(added(right, from_left, True), "tp", 1),
-        shift(added(left, from_right, False), "tp", -1),
-    )
-
-
-def feed_forward(rows, up_full, down_full):
-    hidden = jnp.dot(rows, up_full, preferred_element_type=jnp.float32)
+    )(residual, *parts, gain[None], bias[None])
+
+
+def norm_both_kernel(*refs):
+    *halves, gain, bias, out_ref = refs
+    for side in range(2):
+
+        @pl.when(pl.program_id(0) == side)
+        def _():
+            out_ref[...] = normed(halves[side::2], gain, bias)
+
+
+def norm_both(halves, gain, bias):
+    rows, width = halves[0].shape
+    whole = pl.BlockSpec((rows, width), lambda i: (0, 0))
+    line = pl.BlockSpec((1, width), lambda i: (0, 0))
+    return pl.pallas_call(
+        norm_both_kernel,
+        grid=(2,),
+        in_specs=[whole] * len(halves) + [line, line],
+        out_specs=pl.BlockSpec((rows, width), lambda i: (i, 0)),
+        out_shape=jax.ShapeDtypeStruct((2 * rows, width), jnp.bfloat16),
+        name="norm_both",
+    )(*halves, gain[None], bias[None])
+
+
+def added(part, arrived):
+    return (part.astype(jnp.float32) + arrived.astype(jnp.float32)).astype(jnp.bfloat16)
+
+
+def feed_kernel(*refs, count):
+    rows, (up_ref, down_ref), outs, acc = (
+        refs[:count],
+        refs[count : count + 2],
+        refs[count + 2 : -1],
+        refs[-1],
+    )
+    step = pl.program_id(0)
+    width, block = (down_ref.shape[0] * down_ref.shape[2], up_ref.shape[3])
+    tokens = jnp.concatenate([ref[...] for ref in rows], axis=0)
+    hidden = jnp.dot(tokens, up_ref[...].reshape(-1, block), preferred_element_type=jnp.float32)
     activation = jnp.square(jnp.maximum(hidden, 0.0)).astype(jnp.bfloat16)
-    return lax.dot_general(
-        activation, down_full, (((1,), (1,)), ((), ())), preferred_element_type=jnp.float32
-    ).astype(jnp.bfloat16)
+    branch = lax.dot_general(
+        activation,
+        down_ref[...].reshape(width, block),
+        (((1,), (1,)), ((), ())),
+        preferred_element_type=jnp.float32,
+    )
+
+    @pl.when(step == 0)
+    def _():
+        acc[...] = branch
+
+    @pl.when((step > 0) & (step < pl.num_programs(0) - 1))
+    def _():
+        acc[...] += branch
+
+    @pl.when(step == pl.num_programs(0) - 1)
+    def _():
+        total = (acc[...] + branch).astype(jnp.bfloat16)
+        size = rows[0].shape[0]
+        for index, out in enumerate(outs):
+            out[...] = total[index * size : (index + 1) * size]
+
+
+def feed_forward(rows, weights, block=512):
+    size, width = rows[0].shape
+    pieces, _, height, units = weights.shape
+    whole = pl.BlockSpec((size, width), lambda i: (0, 0))
+    return pl.pallas_call(
+        functools.partial(feed_kernel, count=len(rows)),
+        grid=(units // block,),
+        in_specs=[whole] * len(rows)
+        + [
+            pl.BlockSpec((pieces, 1, height, block), lambda i: (0, 0, 0, i)),
+            pl.BlockSpec((pieces, 1, height, block), lambda i: (0, 1, 0, i)),
+        ],
+        out_specs=[whole] * len(rows),
+        out_shape=[jax.ShapeDtypeStruct((size, width), jnp.bfloat16)] * len(rows),
+        scratch_shapes=[pltpu.VMEM((size * len(rows), width), jnp.float32)],
+        compiler_params=pltpu.CompilerParams(vmem_limit_bytes=48 * 1024 * 1024),
+        name="feed",
+    )(*rows, weights, weights)
 
 
 def on_device(
@@ -182,31 +269,52 @@
     norm2_bias,
 ):
     n_tp, n_sp = (lax.axis_size("tp"), lax.axis_size("sp"))
-    up_full = lax.all_gather(up_weight, "sp", axis=0, tiled=True)
-    down_full = lax.all_gather(down_weight.T, "sp", axis=0, tiled=True)
+    before, after = halo(keys_values, "sp", WINDOW)
+    shards = jnp.concatenate([up_weight, down_weight.T], axis=0)
+    weights = lax.all_gather(shards, "sp", axis=0, tiled=True).reshape(
+        n_sp, 2, up_weight.shape[0], up_weight.shape[1]
+    )
     place = jnp.where(
         jnp.arange(2, dtype=jnp.int32) == 0, lax.axis_index("tp"), lax.axis_index("sp")
     )
-    padded = halo(keys_values, "sp", WINDOW)
-    run = functools.partial(attend, place, sink_logit, queries, padded, out_weight)
-    rows = queries.shape[0] // n_tp
-    far = run(1, lambda i: 2, n_tp, n_sp)
-    near = run(3, lambda i: 1 + 2 * i - i // 2, n_tp, n_sp)
-    right, left, own = (near[:rows], near[rows : 2 * rows], near[2 * rows :])
-    arrived = ring_sum(far, right, left)
-    first = norm_rows((residual_in, own, *arrived), norm1_gain, norm1_bias)
-
-    half = rows // 2
-    of_left, of_right = (shift(first, "tp", 1), shift(first, "tp", -1))
-    of_far = jnp.concatenate(
-        [shift(of_left[:half], "tp", 1), shift(of_right[half:], "tp", -1)], axis=0
-    )
-    far = feed_forward(of_far, up_full, down_full)
-    right = feed_forward(of_right, up_full, down_full)
-    left = feed_forward(of_left, up_full, down_full)
-    own = feed_forward(first, up_full, down_full)
-    arrived = ring_sum(far, right, left)
-    return norm_rows((first, own, *arrived), norm2_gain, norm2_bias)
+    run = functools.partial(
+        attend, place, sink_logit, queries, before, keys_values, after, out_weight
+    )
+    far_top, far_bottom = run(1, lambda i: 2, n_tp, n_sp)
+    from_left = shift(far_top, "tp", 1)
+    from_right = shift(far_bottom, "tp", -1)
+    right_top, right_bottom, left_top, left_bottom = run(2, lambda i: 1 + 2 * i, n_tp, n_sp)
+    left_plain = shift(right_bottom, "tp", 1)
+    right_plain = shift(left_top, "tp", -1)
+    own_top, own_bottom = run(1, lambda i: 0, n_tp, n_sp)
+    left_sum = shift(added(right_top, from_left), "tp", 1)
+    right_sum = shift(added(left_bottom, from_right), "tp", -1)
+    norm1 = (norm1_gain, norm1_bias)
+    first_top = norm_half(residual_in, 0, (own_top, left_sum, right_plain), *norm1)
+    first_bottom = norm_half(residual_in, 1, (own_bottom, left_plain, right_sum), *norm1)
+
+    row_lt = shift(first_top, "tp", 1)
+    row_rb = shift(first_bottom, "tp", -1)
+    row_lb = shift(first_bottom, "tp", 1)
+    row_rt = shift(first_top, "tp", -1)
+    row_ft = shift(row_lt, "tp", 1)
+    row_fb = shift(row_rb, "tp", -1)
+    left_top, left_bottom, right_top, right_bottom = feed_forward(
+        (row_lt, row_lb, row_rt, row_rb), weights
+    )
+    left_plain = shift(right_bottom, "tp", 1)
+    right_plain = shift(left_top, "tp", -1)
+    far_top, far_bottom = feed_forward((row_ft, row_fb), weights)
+    from_left = shift(far_top, "tp", 1)
+    from_right = shift(far_bottom, "tp", -1)
+    own_top, own_bottom = feed_forward((first_top, first_bottom), weights)
+    left_sum = shift(added(right_top, from_left), "tp", 1)
+    right_sum = shift(added(left_bottom, from_right), "tp", -1)
+    return norm_both(
+        (first_top, first_bottom, own_top, own_bottom, left_sum, left_plain, right_plain, right_sum),
+        norm2_gain,
+        norm2_bias,
+    )
 
 
 def solution(mesh):

time: 201 us -> 167 us (0.83)
  matrix products: 42.4 us -> 0 us
  Pallas kernels: 27.1 us -> 63.9 us
  waiting for transfers between devices: 76.7 us -> 47.7 us
  local copies, waits for them, and re-layouts: 11.6 us -> 5.07 us
  starting transfers between devices: 22.1 us -> 28.6 us
    dot_general x4 -> x0, matrix products: 42.4 us -> none  [feed_forward(): lax.dot_general(activation, down_full, (((1,), (1,)), ((), ())), preferre...]
    pallas_call x2 -> x6, Pallas kernels: 9.09 us -> 41.2 us  [the longest x3 31.6 us: feed_forward(): pl.pallas_call(functools.partial(feed_kernel, count=len(rows)), grid=(uni...]
    ppermute x12 -> x18, waiting for transfers between devices: 70.5 us -> 43.8 us  [shift(): lax.ppermute(value, axis, [(i, (i + step) % devices) for i in range(devic...]
    ppermute x12 -> x18, starting transfers between devices: 15.5 us -> 22.1 us  [shift(): lax.ppermute(value, axis, [(i, (i + step) % devices) for i in range(devic...]
    slice x8 -> x0, local copies, waits for them, and re-layouts: 6.28 us -> none  [the longest x2 2.39 us: ring_sum(): from_right = shift(far[half:], 'tp', -1)]
    pallas_call x2 -> x3, Pallas kernels: 18 us -> 22.7 us  [attend(): pl.pallas_call(functools.partial(attend_kernel, rel=rel, n_sp=n_sp, tok_r...]
    all_gather x2 -> x1, waiting for transfers between devices: 2.35 us -> 0.01 us  [on_device(): lax.all_gather(shards, 'sp', axis=0, tiled=True)]
    unnamed x16 -> x26, local copies, waits for them, and re-layouts: 4.32 us -> 4.08 us
  transfers between devices with their start and end apart: 16 -> 21, of which waited for: 8 -> 10; matrix products, arithmetic and copies ran while one was open for 23% -> 2% of each run, Pallas kernels for 11% -> 36%
where the time goes in v2:
time: 167 us; the launch traced here: 164 us
  Pallas kernels  63.9 us (38%)
  waiting for transfers between devices  47.7 us (29%)
  starting transfers between devices  28.6 us (17%)
  between operations  13.6 us (8%)
  local copies, waits for them, and re-layouts  5.07 us (3%)
  other arithmetic  4.93 us (3%)
    ppermute x18, waiting for transfers between devices, shift(): lax.ppermute(value, axis, [(i, (i + step) % devices) for i in range(devic...  43.8 us
    pallas_call x3, Pallas kernels, feed_forward(): pl.pallas_call(functools.partial(feed_kernel, count=len(rows)), grid=(uni...  31.6 us
    pallas_call x3, Pallas kernels, attend(): pl.pallas_call(functools.partial(attend_kernel, rel=rel, n_sp=n_sp, tok_r...  22.7 us
    ppermute x18, starting transfers between devices, shift(): lax.ppermute(value, axis, [(i, (i + step) % devices) for i in range(devic...  22.1 us
    pallas_call x2, Pallas kernels, norm_half(): pl.pallas_call(norm_kernel, grid=(steps,), in_specs=[pl.BlockSpec((block,...  5.36 us
    ppermute x1, starting transfers between devices, halo(): before = lax.ppermute(shard[:, length - width:], axis, up)  4.58 us
    pallas_call x1, Pallas kernels, norm_both(): pl.pallas_call(norm_both_kernel, grid=(2,), in_specs=[whole] * len(halves...  4.22 us
    unnamed x26, local copies, waits for them, and re-layouts  4.08 us
  transfers between devices with their start and end apart: 21, of which 10 were waited for; matrix products, arithmetic and copies ran while one was open for 2% of the time, Pallas kernels for 36%

profile of v2, /device:TPU:1, one launch (start us, length us, event | category | flops | bytes accessed | tf_op | source)
XLA Modules:
  0.0 163.8 jit_solution(15557629358564970144)
XLA Ops:
  6.5 1.9 %pad_maximum_fusion = bf16[128,2048]{1,0:T(8,128)(2,1)} fusion(bf16[64,2048]{1,0:T(8,128)(2,1)} %bitcast.12, bf16[64,2048]{1,0:T(8,128)(2,1)} %param.18), kind=kLoop, calls=%fused_computation.4 | loop fusion | flops 1048576 | bytes 1048576 | tf_op jit(solution)/shard_map/concatenate | solution.py:273
  9.4 4.6 %collective-permute-start = (bf16[2,128,256]{2,1,0:T(8,128)(2,1)S(1)}, bf16[2,128,256]{2,1,0:T(8,128)(2,1)S(1)}, u32[]{:S(2)}, u32[]{:S(2)}) collective-permute-start(bf16[2,128,256]{2,1,0:T(8,128)(2,1)S(1)} %get-tuple-element.38), channel_id=1, source_target_pairs={{0,4},{4,8},{8,12},{12,16},{16,20},{20,24},{24,28},{28,32},{32,36}... | collective-permute-start | bytes 393224 | tf_op jit(solution)/shard_map/ppermute | solution.py:25
  14.0 1.9 %collective-permute-start.1 = (bf16[2,128,256]{2,1,0:T(8,128)(2,1)S(1)}, bf16[2,128,256]{2,1,0:T(8,128)(2,1)S(1)}, u32[]{:S(2)}, u32[]{:S(2)}) collective-permute-start(bf16[2,128,256]{2,1,0:T(8,128)(2,1)S(1)} %get-tuple-element.37), channel_id=1, source_target_pairs={{4,0},{8,4},{12,8},{16,12},{20,16},{24,20},{28,24},{32,28},{36,32}... | collective-permute-start | bytes 393224 | tf_op jit(solution)/shard_map/ppermute | solution.py:26
  16.4 3.9 %collective-permute-done.1.after_ref = bf16[2,128,256]{2,1,0:T(8,128)(2,1)S(1)} collective-permute-done((bf16[2,128,256]{2,1,0:T(8,128)(2,1)S(1)}, bf16[2,128,256]{2,1,0:T(8,128)(2,1)S(1)}, u32[]{:S(2)}, u32[]{:S(2)}) %collective-permute-start.1) | collective-permute-done | bytes 131104 | tf_op jit(solution)/shard_map/ppermute | solution.py:26
  21.0 6.6 %attend.5 = (bf16[128,2048]{1,0:T(8,128)(2,1)}, bf16[128,2048]{1,0:T(8,128)(2,1)}) custom-call(s32[2]{0:T(128)} %compare_select_fusion.place, f32[8]{0:T(128)} %sink.5, bf16[1024,512]{1,0:T(8,128)(2,1)} %q_ref.5, bf16[2,128,256]{2,1,0:T(8,128)(2,1)} %copy-done.4, bf16[2,1024,256]{2,1,0:T(8,128)(2,1)} %mid_ref.5, bf16[2,128,256]{2,1,0:T(8,128)(2,1)} %copy-done.5, ...), custom_call_target="tpu_custom_call" | custom-call | tf_op jit(solution)/shard_map/attend/pallas_call | solution.py:122
  27.5 2.5 %collective-permute-start.6 = (bf16[128,2048]{1,0:T(8,128)(2,1)}, bf16[128,2048]{1,0:T(8,128)(2,1)S(1)}, u32[]{:S(2)}, u32[]{:S(2)}) collective-permute-start(bf16[128,2048]{1,0:T(8,128)(2,1)} %get-tuple-element.28), channel_id=1, source_target_pairs={{0,3},{1,0},{2,1},{3,2},{4,7},{5,4},{6,5},{7,6},{8,11},{9,8},{10,9... | collective-permute-start | bytes 1572872 | tf_op jit(solution)/shard_map/ppermute | solution.py:18
  30.0 9.6 %attend.4 = (bf16[128,2048]{1,0:T(8,128)(2,1)}, bf16[128,2048]{1,0:T(8,128)(2,1)}, bf16[128,2048]{1,0:T(8,128)(2,1)}, bf16[128,2048]{1,0:T(8,128)(2,1)}) custom-call(s32[2]{0:T(128)} %compare_select_fusion.place, f32[8]{0:T(128)} %sink.5, bf16[1024,512]{1,0:T(8,128)(2,1)} %q_ref.5, bf16[2,128,256]{2,1,0:T(8,128)(2,1)} %copy-done.4, ...), custom_call_target="tpu_custom_call" | custom-call | tf_op jit(solution)/shard_map/attend/pallas_call | solution.py:122
  39.9 2.4 %collective-permute-start.4 = (bf16[128,2048]{1,0:T(8,128)(2,1)}, bf16[128,2048]{1,0:T(8,128)(2,1)S(1)}, u32[]{:S(2)}, u32[]{:S(2)}) collective-permute-start(bf16[128,2048]{1,0:T(8,128)(2,1)} %get-tuple-element.24), channel_id=1, source_target_pairs={{0,3},{1,0},{2,1},{3,2},{4,7},{5,4},{6,5},{7,6},{8,11},{9,8},{10,9... | collective-permute-start | bytes 1572872 | tf_op jit(solution)/shard_map/ppermute | solution.py:18
  42.3 1.2 add_convert_fusion.2
  43.5 1.5 collective-permute-start.7
  45.0 1.2 add_convert_fusion.3
  46.2 6.6 %attend.3 = (bf16[128,2048]{1,0:T(8,128)(2,1)}, bf16[128,2048]{1,0:T(8,128)(2,1)}) custom-call(s32[2]{0:T(128)} %compare_select_fusion.place, f32[8]{0:T(128)} %sink.5, bf16[1024,512]{1,0:T(8,128)(2,1)} %q_ref.5, bf16[2,128,256]{2,1,0:T(8,128)(2,1)} %copy-done.4, bf16[2,1024,256]{2,1,0:T(8,128)(2,1)} %mid_ref.5, bf16[2,128,256]{2,1,0:T(8,128)(2,1)} %copy-done.5, ...), custom_call_target="tpu_custom_call" | custom-call | tf_op jit(solution)/shard_map/attend/pallas_call | solution.py:122
  52.8 3.0 %collective-permute-done.5.refs_2_ = bf16[128,2048]{1,0:T(8,128)(2,1)S(1)} collective-permute-done((bf16[128,2048]{1,0:T(8,128)(2,1)}, bf16[128,2048]{1,0:T(8,128)(2,1)S(1)}, u32[]{:S(2)}, u32[]{:S(2)}) %collective-permute-start.5) | collective-permute-done | bytes 524320 | tf_op jit(solution)/shard_map/ppermute | solution.py:18
  55.8 7.5 %collective-permute-done.7.refs_3_ = bf16[128,2048]{1,0:T(8,128)(2,1)} collective-permute-done((bf16[128,2048]{1,0:T(8,128)(2,1)S(1)}, bf16[128,2048]{1,0:T(8,128)(2,1)}, u32[]{:S(2)}, u32[]{:S(2)}) %collective-permute-start.7) | collective-permute-done | bytes 524320 | tf_op jit(solution)/shard_map/ppermute | solution.py:18
  63.3 2.7 %norm.3.refs_1_ = bf16[128,2048]{1,0:T(8,128)(2,1)} custom-call(bf16[256,2048]{1,0:T(8,128)(2,1)} %refs_0_.3, bf16[128,2048]{1,0:T(8,128)(2,1)} %get-tuple-element.25.refs_1_, bf16[128,2048]{1,0:T(8,128)(2,1)} %copy-done.11, bf16[128,2048]{1,0:T(8,128)(2,1)} %collective-permute-done.7.refs_3_, f32[1,2048]{1,0:T(1,128)} %bitcast.13, f32[1,2048]{1,0:T(1,128)} %bitcast.15), custom_call_target="tpu_custom_call" | custom-call | tf_op jit(solution)/shard_map/norm/pallas_call | solution.py:164
  66.0 3.4 %collective-permute-start.11 = (bf16[128,2048]{1,0:T(8,128)(2,1)}, bf16[128,2048]{1,0:T(8,128)(2,1)S(1)}, u32[]{:S(2)}, u32[]{:S(2)}) collective-permute-start(bf16[128,2048]{1,0:T(8,128)(2,1)} %norm.3.refs_1_), channel_id=1, source_target_pairs={{0,3},{1,0},{2,1},{3,2},{4,7},{5,4},{6,5},{7,6},{8,11},{9,8},{10,9... | collective-permute-start | bytes 1572872 | tf_op jit(solution)/shard_map/ppermute | solution.py:18
  70.5 2.6 %norm.2.refs_0_ = bf16[128,2048]{1,0:T(8,128)(2,1)} custom-call(bf16[256,2048]{1,0:T(8,128)(2,1)} %refs_0_.3, bf16[128,2048]{1,0:T(8,128)(2,1)} %get-tuple-element.21.refs_1_, bf16[128,2048]{1,0:T(8,128)(2,1)} %copy-done.12, bf16[128,2048]{1,0:T(8,128)(2,1)} %copy-done.10, f32[1,2048]{1,0:T(1,128)} %bitcast.14, f32[1,2048]{1,0:T(1,128)} %bitcast.16), custom_call_target="tpu_custom_call" | custom-call | tf_op jit(solution)/shard_map/norm/pallas_call | solution.py:164
  73.1 7.0 %collective-permute-done.11.refs_3_ = bf16[128,2048]{1,0:T(8,128)(2,1)S(1)} collective-permute-done((bf16[128,2048]{1,0:T(8,128)(2,1)}, bf16[128,2048]{1,0:T(8,128)(2,1)S(1)}, u32[]{:S(2)}, u32[]{:S(2)}) %collective-permute-start.11) | collective-permute-done | bytes 524320 | tf_op jit(solution)/shard_map/ppermute | solution.py:18
  80.1 3.4 %collective-permute-start.13 = (bf16[128,2048]{1,0:T(8,128)(2,1)S(1)}, bf16[128,2048]{1,0:T(8,128)(2,1)S(1)}, u32[]{:S(2)}, u32[]{:S(2)}) collective-permute-start(bf16[128,2048]{1,0:T(8,128)(2,1)S(1)} %collective-permute-done.11.refs_3_), channel_id=1, source_target_pairs={{0,3},{1,0},{2,1},{3,2},{4,7},{5,4},{6,5},{7,6},{8,11},{9,8},{10,9... | collective-permute-start | bytes 1572872 | tf_op jit(solution)/shard_map/ppermute | solution.py:18
  83.5 3.5 %collective-permute-done.8.refs_0_ = bf16[128,2048]{1,0:T(8,128)(2,1)S(1)} collective-permute-done((bf16[128,2048]{1,0:T(8,128)(2,1)}, bf16[128,2048]{1,0:T(8,128)(2,1)S(1)}, u32[]{:S(2)}, u32[]{:S(2)}) %collective-permute-start.8) | collective-permute-done | bytes 524320 | tf_op jit(solution)/shard_map/ppermute | solution.py:18
  87.1 2.7 %collective-permute-start.10 = (bf16[128,2048]{1,0:T(8,128)(2,1)}, bf16[128,2048]{1,0:T(8,128)(2,1)S(1)}, u32[]{:S(2)}, u32[]{:S(2)}) collective-permute-start(bf16[128,2048]{1,0:T(8,128)(2,1)} %norm.2.refs_0_), channel_id=1, source_target_pairs={{0,3},{1,0},{2,1},{3,2},{4,7},{5,4},{6,5},{7,6},{8,11},{9,8},{10,9... | collective-permute-start | bytes 1572872 | tf_op jit(solution)/shard_map/ppermute | solution.py:18
  89.8 5.5 %collective-permute-done.13.refs_1_ = bf16[128,2048]{1,0:T(8,128)(2,1)S(1)} collective-permute-done((bf16[128,2048]{1,0:T(8,128)(2,1)S(1)}, bf16[128,2048]{1,0:T(8,128)(2,1)S(1)}, u32[]{:S(2)}, u32[]{:S(2)}) %collective-permute-start.13) | collective-permute-done | bytes 524320 | tf_op jit(solution)/shard_map/ppermute | solution.py:18
  95.3 6.9 %collective-permute-done.12.refs_0_ = bf16[128,2048]{1,0:T(8,128)(2,1)S(1)} collective-permute-done((bf16[128,2048]{1,0:T(8,128)(2,1)S(1)}, bf16[128,2048]{1,0:T(8,128)(2,1)S(1)}, u32[]{:S(2)}, u32[]{:S(2)}) %collective-permute-start.12) | collective-permute-done | bytes 524320 | tf_op jit(solution)/shard_map/ppermute | solution.py:18
  102.2 9.2 %feed.5 = (bf16[128,2048]{1,0:T(8,128)(2,1)S(1)}, bf16[128,2048]{1,0:T(8,128)(2,1)S(1)}) custom-call(bf16[128,2048]{1,0:T(8,128)(2,1)S(1)} %collective-permute-done.12.refs_0_, bf16[128,2048]{1,0:T(8,128)(2,1)S(1)} %collective-permute-done.13.refs_1_, bf16[32,2,64,2048]{3,2,1,0:T(8,128)(2,1)} %bitcast.6, bf16[32,2,64,2048]{3,2,1,0:T(8,128)(2,1)} %bitcast.7), custom_call_target="tpu_custom_call" | custom-call | tf_op jit(solution)/shard_map/feed/pallas_call | solution.py:242
  111.5 1.4 collective-permute-start.14
  113.4 13.1 %feed.4 = (bf16[128,2048]{1,0:T(8,128)(2,1)S(1)}, bf16[128,2048]{1,0:T(8,128)(2,1)S(1)}, bf16[128,2048]{1,0:T(8,128)(2,1)S(1)}, bf16[128,2048]{1,0:T(8,128)(2,1)S(1)}) custom-call(bf16[128,2048]{1,0:T(8,128)(2,1)S(1)} %collective-permute-done.8.refs_0_, bf16[128,2048]{1,0:T(8,128)(2,1)S(1)} %collective-permute-done.9.refs_1_, ...), custom_call_target="tpu_custom_call" | custom-call | tf_op jit(solution)/shard_map/feed/pallas_call | solution.py:242
  126.7 2.7 %collective-permute-start.17 = (bf16[128,2048]{1,0:T(8,128)(2,1)S(1)}, bf16[128,2048]{1,0:T(8,128)(2,1)S(1)}, u32[]{:S(2)}, u32[]{:S(2)}) collective-permute-start(bf16[128,2048]{1,0:T(8,128)(2,1)S(1)} %get-tuple-element.34), channel_id=1, source_target_pairs={{0,3},{1,0},{2,1},{3,2},{4,7},{5,4},{6,5},{7,6},{8,11},{9,8},{10,9... | collective-permute-start | bytes 1572872 | tf_op jit(solution)/shard_map/ppermute | solution.py:18
  129.7 1.5 collective-permute-start.15
  131.2 9.2 %feed.3 = (bf16[128,2048]{1,0:T(8,128)(2,1)S(1)}, bf16[128,2048]{1,0:T(8,128)(2,1)S(1)}) custom-call(bf16[128,2048]{1,0:T(8,128)(2,1)S(1)} %copy-done.1, bf16[128,2048]{1,0:T(8,128)(2,1)S(1)} %copy-done, bf16[32,2,64,2048]{3,2,1,0:T(8,128)(2,1)} %bitcast.10, bf16[32,2,64,2048]{3,2,1,0:T(8,128)(2,1)} %bitcast.11), custom_call_target="tpu_custom_call" | custom-call | tf_op jit(solution)/shard_map/feed/pallas_call | solution.py:242
  142.1 8.9 %collective-permute-done.19.refs_7_ = bf16[128,2048]{1,0:T(8,128)(2,1)S(1)} collective-permute-done((bf16[128,2048]{1,0:T(8,128)(2,1)S(1)}, bf16[128,2048]{1,0:T(8,128)(2,1)S(1)}, u32[]{:S(2)}, u32[]{:S(2)}) %collective-permute-start.19) | collective-permute-done | bytes 524320 | tf_op jit(solution)/shard_map/ppermute | solution.py:18
  151.0 1.0 collective-permute-done.15.refs_4_
  152.8 4.2 %norm_both.1 = bf16[256,2048]{1,0:T(8,128)(2,1)} custom-call(bf16[128,2048]{1,0:T(8,128)(2,1)} %norm.2.refs_0_, bf16[128,2048]{1,0:T(8,128)(2,1)} %norm.3.refs_1_, bf16[128,2048]{1,0:T(8,128)(2,1)} %copy-done.2, bf16[128,2048]{1,0:T(8,128)(2,1)} %copy-done.3, bf16[128,2048]{1,0:T(8,128)(2,1)} %copy-done.9, bf16[128,2048]{1,0:T(8,128)(2,1)} %copy-done.6, ...), custom_call_target="tpu_custom_call" | custom-call | tf_op jit(solution)/shard_map/norm_both/pallas_call | solution.py:189
  (53 shorter events, 6.9 us)
Async XLA Ops:
  6.5 95.6 %all-gather.2.cloned.1.call-start = ((), (), s32[]{:S(2)}) async-start(), calls=%async_computation | async-start | bytes 17301504 | tf_op jit(solution)/shard_map/all_gather | solution.py:274
  9.4 7.0 %collective-permute-start = (bf16[2,128,256]{2,1,0:T(8,128)(2,1)S(1)}, bf16[2,128,256]{2,1,0:T(8,128)(2,1)S(1)}, u32[]{:S(2)}, u32[]{:S(2)}) collective-permute-start(bf16[2,128,256]{2,1,0:T(8,128)(2,1)S(1)} %get-tuple-element.38), channel_id=1, source_target_pairs={{0,4},{4,8},{8,12},{12,16},{16,20},{20,24},{24,28},{28,32},{32,36}... | collective-permute-start | bytes 393224 | tf_op jit(solution)/shard_map/ppermute | solution.py:25
  14.0 6.3 %collective-permute-start.1 = (bf16[2,128,256]{2,1,0:T(8,128)(2,1)S(1)}, bf16[2,128,256]{2,1,0:T(8,128)(2,1)S(1)}, u32[]{:S(2)}, u32[]{:S(2)}) collective-permute-start(bf16[2,128,256]{2,1,0:T(8,128)(2,1)S(1)} %get-tuple-element.37), channel_id=1, source_target_pairs={{4,0},{8,4},{12,8},{16,12},{20,16},{24,20},{28,24},{32,28},{36,32}... | collective-permute-start | bytes 393224 | tf_op jit(solution)/shard_map/ppermute | solution.py:26
  16.4 3.9 %copy-start.4 = (bf16[2,128,256]{2,1,0:T(8,128)(2,1)}, bf16[2,128,256]{2,1,0:T(8,128)(2,1)S(1)}, u32[]{:S(2)}) copy-start(bf16[2,128,256]{2,1,0:T(8,128)(2,1)S(1)} %collective-permute-done.before_ref) | copy-start | bytes 393220
  27.5 14.7 %collective-permute-start.6 = (bf16[128,2048]{1,0:T(8,128)(2,1)}, bf16[128,2048]{1,0:T(8,128)(2,1)S(1)}, u32[]{:S(2)}, u32[]{:S(2)}) collective-permute-start(bf16[128,2048]{1,0:T(8,128)(2,1)} %get-tuple-element.28), channel_id=1, source_target_pairs={{0,3},{1,0},{2,1},{3,2},{4,7},{5,4},{6,5},{7,6},{8,11},{9,8},{10,9... | collective-permute-start | bytes 1572872 | tf_op jit(solution)/shard_map/ppermute | solution.py:18
  30.0 15.0 %collective-permute-start.2 = (bf16[128,2048]{1,0:T(8,128)(2,1)}, bf16[128,2048]{1,0:T(8,128)(2,1)S(1)}, u32[]{:S(2)}, u32[]{:S(2)}) collective-permute-start(bf16[128,2048]{1,0:T(8,128)(2,1)} %get-tuple-element.23), channel_id=1, source_target_pairs={{0,1},{1,2},{2,3},{3,0},{4,5},{5,6},{6,7},{7,4},{8,9},{9,10},{10,1... | collective-permute-start | bytes 1572872 | tf_op jit(solution)/shard_map/ppermute | solution.py:18
  39.6 16.2 %collective-permute-start.5 = (bf16[128,2048]{1,0:T(8,128)(2,1)}, bf16[128,2048]{1,0:T(8,128)(2,1)S(1)}, u32[]{:S(2)}, u32[]{:S(2)}) collective-permute-start(bf16[128,2048]{1,0:T(8,128)(2,1)} %get-tuple-element.26), channel_id=1, source_target_pairs={{0,1},{1,2},{2,3},{3,0},{4,5},{5,6},{6,7},{7,4},{8,9},{9,10},{10,1... | collective-permute-start | bytes 1572872 | tf_op jit(solution)/shard_map/ppermute | solution.py:18
  39.9 29.6 %collective-permute-start.4 = (bf16[128,2048]{1,0:T(8,128)(2,1)}, bf16[128,2048]{1,0:T(8,128)(2,1)S(1)}, u32[]{:S(2)}, u32[]{:S(2)}) collective-permute-start(bf16[128,2048]{1,0:T(8,128)(2,1)} %get-tuple-element.24), channel_id=1, source_target_pairs={{0,3},{1,0},{2,1},{3,2},{4,7},{5,4},{6,5},{7,6},{8,11},{9,8},{10,9... | collective-permute-start | bytes 1572872 | tf_op jit(solution)/shard_map/ppermute | solution.py:18
  43.5 19.9 %collective-permute-start.7 = (bf16[128,2048]{1,0:T(8,128)(2,1)S(1)}, bf16[128,2048]{1,0:T(8,128)(2,1)}, u32[]{:S(2)}, u32[]{:S(2)}) collective-permute-start(bf16[128,2048]{1,0:T(8,128)(2,1)S(1)} %add_convert_fusion.2), channel_id=1, source_target_pairs={{0,3},{1,0},{2,1},{3,2},{4,7},{5,4},{6,5},{7,6},{8,11},{9,8},{10,9... | collective-permute-start | bytes 1572872 | tf_op jit(solution)/shard_map/ppermute | solution.py:18
  46.1 23.3 %collective-permute-start.3 = (bf16[128,2048]{1,0:T(8,128)(2,1)S(1)}, bf16[128,2048]{1,0:T(8,128)(2,1)S(1)}, u32[]{:S(2)}, u32[]{:S(2)}) collective-permute-start(bf16[128,2048]{1,0:T(8,128)(2,1)S(1)} %add_convert_fusion.3), channel_id=1, source_target_pairs={{0,1},{1,2},{2,3},{3,0},{4,5},{5,6},{6,7},{7,4},{8,9},{9,10},{10,1... | collective-permute-start | bytes 1572872 | tf_op jit(solution)/shard_map/ppermute | solution.py:18
  55.8 7.5 %copy-start.11 = (bf16[128,2048]{1,0:T(8,128)(2,1)}, bf16[128,2048]{1,0:T(8,128)(2,1)S(1)}, u32[]{:S(2)}) copy-start(bf16[128,2048]{1,0:T(8,128)(2,1)S(1)} %collective-permute-done.5.refs_2_) | copy-start | bytes 1572868
  66.0 14.1 %collective-permute-start.11 = (bf16[128,2048]{1,0:T(8,128)(2,1)}, bf16[128,2048]{1,0:T(8,128)(2,1)S(1)}, u32[]{:S(2)}, u32[]{:S(2)}) collective-permute-start(bf16[128,2048]{1,0:T(8,128)(2,1)} %norm.3.refs_1_), channel_id=1, source_target_pairs={{0,3},{1,0},{2,1},{3,2},{4,7},{5,4},{6,5},{7,6},{8,11},{9,8},{10,9... | collective-permute-start | bytes 1572872 | tf_op jit(solution)/shard_map/ppermute | solution.py:18
  69.4 0.8 copy-start.10
  69.5 1.0 copy-start.12
  73.1 14.0 %collective-permute-start.8 = (bf16[128,2048]{1,0:T(8,128)(2,1)}, bf16[128,2048]{1,0:T(8,128)(2,1)S(1)}, u32[]{:S(2)}, u32[]{:S(2)}) collective-permute-start(bf16[128,2048]{1,0:T(8,128)(2,1)} %norm.2.refs_0_), channel_id=1, source_target_pairs={{0,1},{1,2},{2,3},{3,0},{4,5},{5,6},{6,7},{7,4},{8,9},{9,10},{10,1... | collective-permute-start | bytes 1572872 | tf_op jit(solution)/shard_map/ppermute | solution.py:18
  80.1 15.2 %collective-permute-start.13 = (bf16[128,2048]{1,0:T(8,128)(2,1)S(1)}, bf16[128,2048]{1,0:T(8,128)(2,1)S(1)}, u32[]{:S(2)}, u32[]{:S(2)}) collective-permute-start(bf16[128,2048]{1,0:T(8,128)(2,1)S(1)} %collective-permute-done.11.refs_3_), channel_id=1, source_target_pairs={{0,3},{1,0},{2,1},{3,2},{4,7},{5,4},{6,5},{7,6},{8,11},{9,8},{10,9... | collective-permute-start | bytes 1572872 | tf_op jit(solution)/shard_map/ppermute | solution.py:18
  87.1 15.1 %collective-permute-start.12 = (bf16[128,2048]{1,0:T(8,128)(2,1)S(1)}, bf16[128,2048]{1,0:T(8,128)(2,1)S(1)}, u32[]{:S(2)}, u32[]{:S(2)}) collective-permute-start(bf16[128,2048]{1,0:T(8,128)(2,1)S(1)} %collective-permute-done.8.refs_0_), channel_id=1, source_target_pairs={{0,1},{1,2},{2,3},{3,0},{4,5},{5,6},{6,7},{7,4},{8,9},{9,10},{10,1... | collective-permute-start | bytes 1572872 | tf_op jit(solution)/shard_map/ppermute | solution.py:18
  87.1 26.3 %collective-permute-start.9 = (bf16[128,2048]{1,0:T(8,128)(2,1)}, bf16[128,2048]{1,0:T(8,128)(2,1)S(1)}, u32[]{:S(2)}, u32[]{:S(2)}) collective-permute-start(bf16[128,2048]{1,0:T(8,128)(2,1)} %norm.3.refs_1_), channel_id=1, source_target_pairs={{0,1},{1,2},{2,3},{3,0},{4,5},{5,6},{6,7},{7,4},{8,9},{9,10},{10,1... | collective-permute-start | bytes 1572872 | tf_op jit(solution)/shard_map/ppermute | solution.py:18
  87.1 26.3 %collective-permute-start.10 = (bf16[128,2048]{1,0:T(8,128)(2,1)}, bf16[128,2048]{1,0:T(8,128)(2,1)S(1)}, u32[]{:S(2)}, u32[]{:S(2)}) collective-permute-start(bf16[128,2048]{1,0:T(8,128)(2,1)} %norm.2.refs_0_), channel_id=1, source_target_pairs={{0,3},{1,0},{2,1},{3,2},{4,7},{5,4},{6,5},{7,6},{8,11},{9,8},{10,9... | collective-permute-start | bytes 1572872 | tf_op jit(solution)/shard_map/ppermute | solution.py:18
  111.4 17.9 %collective-permute-start.18 = (bf16[128,2048]{1,0:T(8,128)(2,1)S(1)}, bf16[128,2048]{1,0:T(8,128)(2,1)S(1)}, u32[]{:S(2)}, u32[]{:S(2)}) collective-permute-start(bf16[128,2048]{1,0:T(8,128)(2,1)S(1)} %get-tuple-element.36), channel_id=1, source_target_pairs={{0,3},{1,0},{2,1},{3,2},{4,7},{5,4},{6,5},{7,6},{8,11},{9,8},{10,9... | collective-permute-start | bytes 1572872 | tf_op jit(solution)/shard_map/ppermute | solution.py:18
  111.5 19.7 %copy-start = (bf16[128,2048]{1,0:T(8,128)(2,1)S(1)}, bf16[128,2048]{1,0:T(8,128)(2,1)}, u32[]{:S(2)}) copy-start(bf16[128,2048]{1,0:T(8,128)(2,1)} %norm.3.refs_1_) | copy-start | bytes 1572868
  111.5 19.7 %copy-start.1 = (bf16[128,2048]{1,0:T(8,128)(2,1)S(1)}, bf16[128,2048]{1,0:T(8,128)(2,1)}, u32[]{:S(2)}) copy-start(bf16[128,2048]{1,0:T(8,128)(2,1)} %norm.2.refs_0_) | copy-start | bytes 1572868
  111.5 18.0 %collective-permute-start.14 = (bf16[128,2048]{1,0:T(8,128)(2,1)S(1)}, bf16[128,2048]{1,0:T(8,128)(2,1)S(1)}, u32[]{:S(2)}, u32[]{:S(2)}) collective-permute-start(bf16[128,2048]{1,0:T(8,128)(2,1)S(1)} %get-tuple-element.32), channel_id=1, source_target_pairs={{0,1},{1,2},{2,3},{3,0},{4,5},{5,6},{6,7},{7,4},{8,9},{9,10},{10,1... | collective-permute-start | bytes 1572872 | tf_op jit(solution)/shard_map/ppermute | solution.py:18
  126.6 15.5 %collective-permute-start.16 = (bf16[128,2048]{1,0:T(8,128)(2,1)S(1)}, bf16[128,2048]{1,0:T(8,128)(2,1)S(1)}, u32[]{:S(2)}, u32[]{:S(2)}) collective-permute-start(bf16[128,2048]{1,0:T(8,128)(2,1)S(1)} %get-tuple-element.33), channel_id=1, source_target_pairs={{0,1},{1,2},{2,3},{3,0},{4,5},{5,6},{6,7},{7,4},{8,9},{9,10},{10,1... | collective-permute-start | bytes 1572872 | tf_op jit(solution)/shard_map/ppermute | solution.py:18
  126.7 15.4 %collective-permute-start.17 = (bf16[128,2048]{1,0:T(8,128)(2,1)S(1)}, bf16[128,2048]{1,0:T(8,128)(2,1)S(1)}, u32[]{:S(2)}, u32[]{:S(2)}) collective-permute-start(bf16[128,2048]{1,0:T(8,128)(2,1)S(1)} %get-tuple-element.34), channel_id=1, source_target_pairs={{0,3},{1,0},{2,1},{3,2},{4,7},{5,4},{6,5},{7,6},{8,11},{9,8},{10,9... | collective-permute-start | bytes 1572872 | tf_op jit(solution)/shard_map/ppermute | solution.py:18
  129.5 21.5 %collective-permute-start.19 = (bf16[128,2048]{1,0:T(8,128)(2,1)S(1)}, bf16[128,2048]{1,0:T(8,128)(2,1)S(1)}, u32[]{:S(2)}, u32[]{:S(2)}) collective-permute-start(bf16[128,2048]{1,0:T(8,128)(2,1)S(1)} %add_convert_fusion), channel_id=1, source_target_pairs={{0,3},{1,0},{2,1},{3,2},{4,7},{5,4},{6,5},{7,6},{8,11},{9,8},{10,9... | collective-permute-start | bytes 1572872 | tf_op jit(solution)/shard_map/ppermute | solution.py:18
  129.7 22.3 %collective-permute-start.15 = (bf16[128,2048]{1,0:T(8,128)(2,1)S(1)}, bf16[128,2048]{1,0:T(8,128)(2,1)S(1)}, u32[]{:S(2)}, u32[]{:S(2)}) collective-permute-start(bf16[128,2048]{1,0:T(8,128)(2,1)S(1)} %add_convert_fusion.1), channel_id=1, source_target_pairs={{0,1},{1,2},{2,3},{3,0},{4,5},{5,6},{6,7},{7,4},{8,9},{9,10},{10,1... | collective-permute-start | bytes 1572872 | tf_op jit(solution)/shard_map/ppermute | solution.py:18
  141.2 0.8 copy-start.3
  142.1 9.9 %copy-start.6 = (bf16[128,2048]{1,0:T(8,128)(2,1)}, bf16[128,2048]{1,0:T(8,128)(2,1)S(1)}, u32[]{:S(2)}) copy-start(bf16[128,2048]{1,0:T(8,128)(2,1)S(1)} %collective-permute-done.16.refs_5_) | copy-start | bytes 1572868
  142.1 9.9 %copy-start.7 = (bf16[128,2048]{1,0:T(8,128)(2,1)}, bf16[128,2048]{1,0:T(8,128)(2,1)S(1)}, u32[]{:S(2)}) copy-start(bf16[128,2048]{1,0:T(8,128)(2,1)S(1)} %collective-permute-done.17.refs_6_) | copy-start | bytes 1572868
  151.0 1.0 copy-start.8
  152.0 0.8 copy-start.9
  (2 other events, 1.4 us)
Sparse Core Ops, SparseCore 0:
  9.6 76.2 all-gather.1

commit v3 on v2

--- a/solution.py
+++ b/solution.py
@@ -7,13 +7,14 @@
 from jax.experimental.pallas import tpu as pltpu
 from jax.sharding import PartitionSpec as P
 
+
 HEAD_DIM = 64
 WINDOW = 128
 LANES = 128
 NEG = -1e30
 
 
-def shift(value, axis, step):
+def shift(value, step, axis="tp"):
     devices = lax.axis_size(axis)
     return lax.ppermute(value, axis, [(i, (i + step) % devices) for i in range(devices)])
 
@@ -200,62 +201,74 @@
     return (part.astype(jnp.float32) + arrived.astype(jnp.float32)).astype(jnp.bfloat16)
 
 
-def feed_kernel(*refs, count):
-    rows, (up_ref, down_ref), outs, acc = (
-        refs[:count],
-        refs[count : count + 2],
-        refs[count + 2 : -1],
-        refs[-1],
-    )
-    step = pl.program_id(0)
-    width, block = (down_ref.shape[0] * down_ref.shape[2], up_ref.shape[3])
-    tokens = jnp.concatenate([ref[...] for ref in rows], axis=0)
-    hidden = jnp.dot(tokens, up_ref[...].reshape(-1, block), preferred_element_type=jnp.float32)
-    activation = jnp.square(jnp.maximum(hidden, 0.0)).astype(jnp.bfloat16)
-    branch = lax.dot_general(
-        activation,
-        down_ref[...].reshape(width, block),
-        (((1,), (1,)), ((), ())),
-        preferred_element_type=jnp.float32,
-    )
-
-    @pl.when(step == 0)
-    def _():
-        acc[...] = branch
-
-    @pl.when((step > 0) & (step < pl.num_programs(0) - 1))
-    def _():
-        acc[...] += branch
-
-    @pl.when(step == pl.num_programs(0) - 1)
-    def _():
-        total = (acc[...] + branch).astype(jnp.bfloat16)
-        size = rows[0].shape[0]
+def feed_kernel(*refs, count, chunk):
+    rows, weights, outs = (refs[:count], refs[count], refs[count + 1 : 2 * count + 1])
+    up, down, activation, sems = refs[2 * count + 1 :]
+    pieces, height, units = up.shape
+    size, steps = (rows[0].shape[0], units // chunk)
+    part = pieces // steps
+    width = part * height
+
+    def up_copy(k):
+        cols = pl.ds(pl.multiple_of(k * chunk, chunk), chunk)
+        return pltpu.make_async_copy(weights.at[:, 0, :, cols], up.at[:, :, cols], sems.at[k])
+
+    def down_copy(k):
+        span = pl.ds(k * part, part)
+        return pltpu.make_async_copy(weights.at[span, 1], down.at[span], sems.at[steps + k])
+
+    for k in range(steps):
+        up_copy(k).start()
+    for k in range(steps):
+        down_copy(k).start()
+
+    @pl.loop(0, steps)
+    def _(k):
+        up_copy(k).wait()
+        cols = pl.ds(pl.multiple_of(k * chunk, chunk), chunk)
+        hidden = jnp.dot(
+            jnp.concatenate([ref[...] for ref in rows], axis=0),
+            up[:, :, cols].reshape(pieces * height, chunk),
+            preferred_element_type=jnp.float32,
+        )
+        activation[:, cols] = jnp.square(jnp.maximum(hidden, 0.0)).astype(jnp.bfloat16)
+
+    @pl.loop(0, steps)
+    def _(k):
+        down_copy(k).wait()
+        branch = lax.dot_general(
+            activation[...],
+            down[pl.ds(k * part, part)].reshape(width, units),
+            (((1,), (1,)), ((), ())),
+            preferred_element_type=jnp.float32,
+        ).astype(jnp.bfloat16)
+        cols = pl.ds(pl.multiple_of(k * width, width), width)
         for index, out in enumerate(outs):
-            out[...] = total[index * size : (index + 1) * size]
-
-
-def feed_forward(rows, weights, block=512):
+            out[:, cols] = branch[index * size : (index + 1) * size]
+
+
+def feed_forward(rows, weights, chunk=512):
     size, width = rows[0].shape
     pieces, _, height, units = weights.shape
-    whole = pl.BlockSpec((size, width), lambda i: (0, 0))
+    whole = pl.BlockSpec(memory_space=pltpu.VMEM)
+    full = pltpu.VMEM((pieces, height, units), jnp.bfloat16)
     return pl.pallas_call(
-        functools.partial(feed_kernel, count=len(rows)),
-        grid=(units // block,),
-        in_specs=[whole] * len(rows)
-        + [
-            pl.BlockSpec((pieces, 1, height, block), lambda i: (0, 0, 0, i)),
-            pl.BlockSpec((pieces, 1, height, block), lambda i: (0, 1, 0, i)),
-        ],
+        functools.partial(feed_kernel, count=len(rows), chunk=chunk),
+        in_specs=[whole] * len(rows) + [pl.BlockSpec(memory_space=pl.ANY)],
         out_specs=[whole] * len(rows),
         out_shape=[jax.ShapeDtypeStruct((size, width), jnp.bfloat16)] * len(rows),
-        scratch_shapes=[pltpu.VMEM((size * len(rows), width), jnp.float32)],
-        compiler_params=pltpu.CompilerParams(vmem_limit_bytes=48 * 1024 * 1024),
+        scratch_shapes=[
+            full,
+            full,
+            pltpu.VMEM((size * len(rows), units), jnp.bfloat16),
+            pltpu.SemaphoreType.DMA((2 * (units // chunk),)),
+        ],
+        compiler_params=pltpu.CompilerParams(vmem_limit_bytes=54 * 1024 * 1024),
         name="feed",
-    )(*rows, weights, weights)
-
-
-def on_device(
+    )(*rows, weights)
+
+
+def layer(
     residual_in,
     queries,
     keys_values,
@@ -281,35 +294,35 @@
         attend, place, sink_logit, queries, before, keys_values, after, out_weight
     )
     far_top, far_bottom = run(1, lambda i: 2, n_tp, n_sp)
-    from_left = shift(far_top, "tp", 1)
-    from_right = shift(far_bottom, "tp", -1)
+    from_left = shift(far_top, 1)
+    from_right = shift(far_bottom, -1)
     right_top, right_bottom, left_top, left_bottom = run(2, lambda i: 1 + 2 * i, n_tp, n_sp)
-    left_plain = shift(right_bottom, "tp", 1)
-    right_plain = shift(left_top, "tp", -1)
+    left_plain = shift(right_bottom, 1)
+    right_plain = shift(left_top, -1)
     own_top, own_bottom = run(1, lambda i: 0, n_tp, n_sp)
-    left_sum = shift(added(right_top, from_left), "tp", 1)
-    right_sum = shift(added(left_bottom, from_right), "tp", -1)
+    left_sum = shift(added(right_top, from_left), 1)
+    right_sum = shift(added(left_bottom, from_right), -1)
     norm1 = (norm1_gain, norm1_bias)
     first_top = norm_half(residual_in, 0, (own_top, left_sum, right_plain), *norm1)
     first_bottom = norm_half(residual_in, 1, (own_bottom, left_plain, right_sum), *norm1)
 
-    row_lt = shift(first_top, "tp", 1)
-    row_rb = shift(first_bottom, "tp", -1)
-    row_lb = shift(first_bottom, "tp", 1)
-    row_rt = shift(first_top, "tp", -1)
-    row_ft = shift(row_lt, "tp", 1)
-    row_fb = shift(row_rb, "tp", -1)
+    row_lt = shift(first_top, 1)
+    row_rb = shift(first_bottom, -1)
+    row_lb = shift(first_bottom, 1)
+    row_rt = shift(first_top, -1)
+    row_ft = shift(row_lt, 1)
+    row_fb = shift(row_rb, -1)
     left_top, left_bottom, right_top, right_bottom = feed_forward(
         (row_lt, row_lb, row_rt, row_rb), weights
     )
-    left_plain = shift(right_bottom, "tp", 1)
-    right_plain = shift(left_top, "tp", -1)
+    left_plain = shift(right_bottom, 1)
+    right_plain = shift(left_top, -1)
     far_top, far_bottom = feed_forward((row_ft, row_fb), weights)
-    from_left = shift(far_top, "tp", 1)
-    from_right = shift(far_bottom, "tp", -1)
+    from_left = shift(far_top, 1)
+    from_right = shift(far_bottom, -1)
     own_top, own_bottom = feed_forward((first_top, first_bottom), weights)
-    left_sum = shift(added(right_top, from_left), "tp", 1)
-    right_sum = shift(added(left_bottom, from_right), "tp", -1)
+    left_sum = shift(added(right_top, from_left), 1)
+    right_sum = shift(added(left_bottom, from_right), -1)
     return norm_both(
         (first_top, first_bottom, own_top, own_bottom, left_sum, left_plain, right_plain, right_sum),
         norm2_gain,
@@ -319,7 +332,7 @@
 
 def solution(mesh):
     return jax.shard_map(
-        on_device,
+        layer,
         mesh=mesh,
         in_specs=(
             P(("sp", "tp"), None),

time: 167 us -> 171 us (1.024)
  Pallas kernels: 63.9 us -> 66.3 us
  other arithmetic: 4.93 us -> 7.13 us
    pallas_call x3, Pallas kernels: 31.6 us -> 34 us  [feed_forward(): pl.pallas_call(functools.partial(feed_kernel, count=len(rows), chunk=chun...]
    convert_element_type x4, other arithmetic: 2.58 us -> 4.67 us  [added(): (part.astype(jnp.float32) + arrived.astype(jnp.float32)).astype(jnp.bfloa...]
    unnamed x26 -> x30, local copies, waits for them, and re-layouts: 4.08 us -> 4.81 us
  transfers between devices with their start and end apart: 21 -> 21, of which waited for: 10 -> 9; matrix products, arithmetic and copies ran while one was open for 2% -> 4% of each run, Pallas kernels for 36% -> 37%
where the time goes in v3:
time: 171 us; the launch traced here: 168 us
  Pallas kernels  66.3 us (39%)
  waiting for transfers between devices  46.1 us (27%)
  starting transfers between devices  28.6 us (17%)
  between operations  13.6 us (8%)
  other arithmetic  7.13 us (4%)
  local copies, waits for them, and re-layouts  5.8 us (3%)
    ppermute x18, waiting for transfers between devices, shift(): lax.ppermute(value, axis, [(i, (i + step) % devices) for i in range(devic...  42.3 us
    pallas_call x3, Pallas kernels, feed_forward(): pl.pallas_call(functools.partial(feed_kernel, count=len(rows), chunk=chun...  34 us
    pallas_call x3, Pallas kernels, attend(): pl.pallas_call(functools.partial(attend_kernel, rel=rel, n_sp=n_sp, tok_r...  22.7 us
    ppermute x18, starting transfers between devices, shift(): lax.ppermute(value, axis, [(i, (i + step) % devices) for i in range(devic...  22.1 us
    pallas_call x2, Pallas kernels, norm_half(): pl.pallas_call(norm_kernel, grid=(steps,), in_specs=[pl.BlockSpec((block,...  5.43 us
    unnamed x30, local copies, waits for them, and re-layouts  4.81 us
    convert_element_type x4, other arithmetic, added(): (part.astype(jnp.float32) + arrived.astype(jnp.float32)).astype(jnp.bfloa...  4.67 us
    ppermute x1, starting transfers between devices, halo(): before = lax.ppermute(shard[:, length - width:], axis, up)  4.58 us
  transfers between devices with their start and end apart: 21, of which 9 were waited for; matrix products, arithmetic and copies ran while one was open for 4% of the time, Pallas kernels for 37%

profile of v3, /device:TPU:1, one launch (start us, length us, event | category | flops | bytes accessed | tf_op | source)
XLA Modules:
  0.0 167.5 jit_solution(5882680958246976356)
XLA Ops:
  6.5 1.9 %pad_maximum_fusion = bf16[128,2048]{1,0:T(8,128)(2,1)} fusion(bf16[64,2048]{1,0:T(8,128)(2,1)} %bitcast.9, bf16[64,2048]{1,0:T(8,128)(2,1)} %param.18), kind=kLoop, calls=%fused_computation.4 | loop fusion | flops 1048576 | bytes 1048576 | tf_op jit(solution)/shard_map/concatenate | solution.py:286
  9.4 4.6 %collective-permute-start = (bf16[2,128,256]{2,1,0:T(8,128)(2,1)S(1)}, bf16[2,128,256]{2,1,0:T(8,128)(2,1)S(1)}, u32[]{:S(2)}, u32[]{:S(2)}) collective-permute-start(bf16[2,128,256]{2,1,0:T(8,128)(2,1)S(1)} %get-tuple-element.38), channel_id=1, source_target_pairs={{0,4},{4,8},{8,12},{12,16},{16,20},{20,24},{24,28},{28,32},{32,36}... | collective-permute-start | bytes 393224 | tf_op jit(solution)/shard_map/ppermute | solution.py:26
  14.0 1.9 %collective-permute-start.1 = (bf16[2,128,256]{2,1,0:T(8,128)(2,1)S(1)}, bf16[2,128,256]{2,1,0:T(8,128)(2,1)S(1)}, u32[]{:S(2)}, u32[]{:S(2)}) collective-permute-start(bf16[2,128,256]{2,1,0:T(8,128)(2,1)S(1)} %get-tuple-element.37), channel_id=1, source_target_pairs={{4,0},{8,4},{12,8},{16,12},{20,16},{24,20},{28,24},{32,28},{36,32}... | collective-permute-start | bytes 393224 | tf_op jit(solution)/shard_map/ppermute | solution.py:27
  16.6 3.8 %collective-permute-done.1.after_ref = bf16[2,128,256]{2,1,0:T(8,128)(2,1)S(1)} collective-permute-done((bf16[2,128,256]{2,1,0:T(8,128)(2,1)S(1)}, bf16[2,128,256]{2,1,0:T(8,128)(2,1)S(1)}, u32[]{:S(2)}, u32[]{:S(2)}) %collective-permute-start.1) | collective-permute-done | bytes 131104 | tf_op jit(solution)/shard_map/ppermute | solution.py:27
  21.0 6.6 %attend.5 = (bf16[128,2048]{1,0:T(8,128)(2,1)}, bf16[128,2048]{1,0:T(8,128)(2,1)}) custom-call(s32[2]{0:T(128)} %compare_select_fusion.place, f32[8]{0:T(128)} %sink.5, bf16[1024,512]{1,0:T(8,128)(2,1)} %q_ref.5, bf16[2,128,256]{2,1,0:T(8,128)(2,1)} %copy-done, bf16[2,1024,256]{2,1,0:T(8,128)(2,1)} %mid_ref.5, bf16[2,128,256]{2,1,0:T(8,128)(2,1)} %copy-done.1, ...), custom_call_target="tpu_custom_call" | custom-call | tf_op jit(solution)/shard_map/attend/pallas_call | solution.py:123
  27.6 2.5 %collective-permute-start.6 = (bf16[128,2048]{1,0:T(8,128)(2,1)}, bf16[128,2048]{1,0:T(8,128)(2,1)S(1)}, u32[]{:S(2)}, u32[]{:S(2)}) collective-permute-start(bf16[128,2048]{1,0:T(8,128)(2,1)} %get-tuple-element.28), channel_id=1, source_target_pairs={{0,3},{1,0},{2,1},{3,2},{4,7},{5,4},{6,5},{7,6},{8,11},{9,8},{10,9... | collective-permute-start | bytes 1572872 | tf_op jit(solution)/shard_map/ppermute | solution.py:19
  30.1 9.6 %attend.4 = (bf16[128,2048]{1,0:T(8,128)(2,1)}, bf16[128,2048]{1,0:T(8,128)(2,1)}, bf16[128,2048]{1,0:T(8,128)(2,1)}, bf16[128,2048]{1,0:T(8,128)(2,1)}) custom-call(s32[2]{0:T(128)} %compare_select_fusion.place, f32[8]{0:T(128)} %sink.5, bf16[1024,512]{1,0:T(8,128)(2,1)} %q_ref.5, bf16[2,128,256]{2,1,0:T(8,128)(2,1)} %copy-done, ...), custom_call_target="tpu_custom_call" | custom-call | tf_op jit(solution)/shard_map/attend/pallas_call | solution.py:123
  39.9 2.4 %collective-permute-start.4 = (bf16[128,2048]{1,0:T(8,128)(2,1)}, bf16[128,2048]{1,0:T(8,128)(2,1)S(1)}, u32[]{:S(2)}, u32[]{:S(2)}) collective-permute-start(bf16[128,2048]{1,0:T(8,128)(2,1)} %get-tuple-element.24), channel_id=1, source_target_pairs={{0,3},{1,0},{2,1},{3,2},{4,7},{5,4},{6,5},{7,6},{8,11},{9,8},{10,9... | collective-permute-start | bytes 1572872 | tf_op jit(solution)/shard_map/ppermute | solution.py:19
  42.3 1.2 add_convert_fusion.2
  43.5 1.5 collective-permute-start.7
  45.0 1.2 add_convert_fusion.3
  46.3 6.5 %attend.3 = (bf16[128,2048]{1,0:T(8,128)(2,1)}, bf16[128,2048]{1,0:T(8,128)(2,1)}) custom-call(s32[2]{0:T(128)} %compare_select_fusion.place, f32[8]{0:T(128)} %sink.5, bf16[1024,512]{1,0:T(8,128)(2,1)} %q_ref.5, bf16[2,128,256]{2,1,0:T(8,128)(2,1)} %copy-done, bf16[2,1024,256]{2,1,0:T(8,128)(2,1)} %mid_ref.5, bf16[2,128,256]{2,1,0:T(8,128)(2,1)} %copy-done.1, ...), custom_call_target="tpu_custom_call" | custom-call | tf_op jit(solution)/shard_map/attend/pallas_call | solution.py:123
  52.8 3.0 %collective-permute-done.5.refs_2_ = bf16[128,2048]{1,0:T(8,128)(2,1)S(1)} collective-permute-done((bf16[128,2048]{1,0:T(8,128)(2,1)}, bf16[128,2048]{1,0:T(8,128)(2,1)S(1)}, u32[]{:S(2)}, u32[]{:S(2)}) %collective-permute-start.5) | collective-permute-done | bytes 524320 | tf_op jit(solution)/shard_map/ppermute | solution.py:19
  55.8 7.6 %collective-permute-done.7.refs_3_ = bf16[128,2048]{1,0:T(8,128)(2,1)} collective-permute-done((bf16[128,2048]{1,0:T(8,128)(2,1)S(1)}, bf16[128,2048]{1,0:T(8,128)(2,1)}, u32[]{:S(2)}, u32[]{:S(2)}) %collective-permute-start.7) | collective-permute-done | bytes 524320 | tf_op jit(solution)/shard_map/ppermute | solution.py:19
  63.4 2.8 %norm.3.refs_1_ = bf16[128,2048]{1,0:T(8,128)(2,1)} custom-call(bf16[256,2048]{1,0:T(8,128)(2,1)} %refs_0_.3, bf16[128,2048]{1,0:T(8,128)(2,1)} %get-tuple-element.25.refs_1_, bf16[128,2048]{1,0:T(8,128)(2,1)} %copy-done.13, bf16[128,2048]{1,0:T(8,128)(2,1)} %collective-permute-done.7.refs_3_, f32[1,2048]{1,0:T(1,128)} %bitcast.10, f32[1,2048]{1,0:T(1,128)} %bitcast.12), custom_call_target="tpu_custom_call" | custom-call | tf_op jit(solution)/shard_map/norm/pallas_call | solution.py:165
  66.2 3.4 %collective-permute-start.11 = (bf16[128,2048]{1,0:T(8,128)(2,1)}, bf16[128,2048]{1,0:T(8,128)(2,1)S(1)}, u32[]{:S(2)}, u32[]{:S(2)}) collective-permute-start(bf16[128,2048]{1,0:T(8,128)(2,1)} %norm.3.refs_1_), channel_id=1, source_target_pairs={{0,3},{1,0},{2,1},{3,2},{4,7},{5,4},{6,5},{7,6},{8,11},{9,8},{10,9... | collective-permute-start | bytes 1572872 | tf_op jit(solution)/shard_map/ppermute | solution.py:19
  70.5 2.7 %norm.2.refs_0_ = bf16[128,2048]{1,0:T(8,128)(2,1)} custom-call(bf16[256,2048]{1,0:T(8,128)(2,1)} %refs_0_.3, bf16[128,2048]{1,0:T(8,128)(2,1)} %get-tuple-element.21.refs_1_, bf16[128,2048]{1,0:T(8,128)(2,1)} %copy-done.14, bf16[128,2048]{1,0:T(8,128)(2,1)} %copy-done.12, f32[1,2048]{1,0:T(1,128)} %bitcast.11, f32[1,2048]{1,0:T(1,128)} %bitcast.13), custom_call_target="tpu_custom_call" | custom-call | tf_op jit(solution)/shard_map/norm/pallas_call | solution.py:165
  73.2 7.0 %collective-permute-done.11.refs_3_ = bf16[128,2048]{1,0:T(8,128)(2,1)S(1)} collective-permute-done((bf16[128,2048]{1,0:T(8,128)(2,1)}, bf16[128,2048]{1,0:T(8,128)(2,1)S(1)}, u32[]{:S(2)}, u32[]{:S(2)}) %collective-permute-start.11) | collective-permute-done | bytes 524320 | tf_op jit(solution)/shard_map/ppermute | solution.py:19
  80.2 3.4 %collective-permute-start.13 = (bf16[128,2048]{1,0:T(8,128)(2,1)S(1)}, bf16[128,2048]{1,0:T(8,128)(2,1)S(1)}, u32[]{:S(2)}, u32[]{:S(2)}) collective-permute-start(bf16[128,2048]{1,0:T(8,128)(2,1)S(1)} %collective-permute-done.11.refs_3_), channel_id=1, source_target_pairs={{0,3},{1,0},{2,1},{3,2},{4,7},{5,4},{6,5},{7,6},{8,11},{9,8},{10,9... | collective-permute-start | bytes 1572872 | tf_op jit(solution)/shard_map/ppermute | solution.py:19
  83.6 3.5 %collective-permute-done.8.refs_0_ = bf16[128,2048]{1,0:T(8,128)(2,1)S(1)} collective-permute-done((bf16[128,2048]{1,0:T(8,128)(2,1)}, bf16[128,2048]{1,0:T(8,128)(2,1)S(1)}, u32[]{:S(2)}, u32[]{:S(2)}) %collective-permute-start.8) | collective-permute-done | bytes 524320 | tf_op jit(solution)/shard_map/ppermute | solution.py:19
  87.1 2.7 %collective-permute-start.10 = (bf16[128,2048]{1,0:T(8,128)(2,1)}, bf16[128,2048]{1,0:T(8,128)(2,1)S(1)}, u32[]{:S(2)}, u32[]{:S(2)}) collective-permute-start(bf16[128,2048]{1,0:T(8,128)(2,1)} %norm.2.refs_0_), channel_id=1, source_target_pairs={{0,3},{1,0},{2,1},{3,2},{4,7},{5,4},{6,5},{7,6},{8,11},{9,8},{10,9... | collective-permute-start | bytes 1572872 | tf_op jit(solution)/shard_map/ppermute | solution.py:19
  89.8 5.5 %collective-permute-done.13.refs_1_ = bf16[128,2048]{1,0:T(8,128)(2,1)S(1)} collective-permute-done((bf16[128,2048]{1,0:T(8,128)(2,1)S(1)}, bf16[128,2048]{1,0:T(8,128)(2,1)S(1)}, u32[]{:S(2)}, u32[]{:S(2)}) %collective-permute-start.13) | collective-permute-done | bytes 524320 | tf_op jit(solution)/shard_map/ppermute | solution.py:19
  95.4 6.9 %collective-permute-done.12.refs_0_ = bf16[128,2048]{1,0:T(8,128)(2,1)S(1)} collective-permute-done((bf16[128,2048]{1,0:T(8,128)(2,1)S(1)}, bf16[128,2048]{1,0:T(8,128)(2,1)S(1)}, u32[]{:S(2)}, u32[]{:S(2)}) %collective-permute-start.12) | collective-permute-done | bytes 524320 | tf_op jit(solution)/shard_map/ppermute | solution.py:19
  103.0 9.7 %feed.5 = (bf16[128,2048]{1,0:T(8,128)(2,1)}, bf16[128,2048]{1,0:T(8,128)(2,1)}) custom-call(bf16[128,2048]{1,0:T(8,128)(2,1)} %copy-done.11, bf16[128,2048]{1,0:T(8,128)(2,1)} %copy-done.9, bf16[32,2,64,2048]{3,2,1,0:T(8,128)(2,1)} %bitcast.6), custom_call_target="tpu_custom_call" | custom-call | tf_op jit(solution)/shard_map/feed/pallas_call | solution.py:255
  112.8 1.5 collective-permute-start.14
  115.9 14.6 %feed.4 = (bf16[128,2048]{1,0:T(8,128)(2,1)}, bf16[128,2048]{1,0:T(8,128)(2,1)}, bf16[128,2048]{1,0:T(8,128)(2,1)}, bf16[128,2048]{1,0:T(8,128)(2,1)}) custom-call(bf16[128,2048]{1,0:T(8,128)(2,1)} %copy-done.3, bf16[128,2048]{1,0:T(8,128)(2,1)} %copy-done.6, bf16[128,2048]{1,0:T(8,128)(2,1)} %copy-done.7, bf16[128,2048]{1,0:T(8,128)(2,1)} %copy-done.2, ...), custom_call_target="tpu_custom_call" | custom-call | tf_op jit(solution)/shard_map/feed/pallas_call | solution.py:255
  130.6 2.7 %collective-permute-start.17 = (bf16[128,2048]{1,0:T(8,128)(2,1)}, bf16[128,2048]{1,0:T(8,128)(2,1)S(1)}, u32[]{:S(2)}, u32[]{:S(2)}) collective-permute-start(bf16[128,2048]{1,0:T(8,128)(2,1)} %get-tuple-element.34), channel_id=1, source_target_pairs={{0,3},{1,0},{2,1},{3,2},{4,7},{5,4},{6,5},{7,6},{8,11},{9,8},{10,9... | collective-permute-start | bytes 1572872 | tf_op jit(solution)/shard_map/ppermute | solution.py:19
  133.2 1.2 add_convert_fusion
  135.7 1.5 collective-permute-start.15
  137.2 9.7 %feed.3 = (bf16[128,2048]{1,0:T(8,128)(2,1)}, bf16[128,2048]{1,0:T(8,128)(2,1)}) custom-call(bf16[128,2048]{1,0:T(8,128)(2,1)} %norm.2.refs_0_, bf16[128,2048]{1,0:T(8,128)(2,1)} %norm.3.refs_1_, bf16[32,2,64,2048]{3,2,1,0:T(8,128)(2,1)} %bitcast.8), custom_call_target="tpu_custom_call" | custom-call | tf_op jit(solution)/shard_map/feed/pallas_call | solution.py:255
  146.9 7.7 %collective-permute-done.19.refs_7_ = bf16[128,2048]{1,0:T(8,128)(2,1)S(1)} collective-permute-done((bf16[128,2048]{1,0:T(8,128)(2,1)S(1)}, bf16[128,2048]{1,0:T(8,128)(2,1)S(1)}, u32[]{:S(2)}, u32[]{:S(2)}) %collective-permute-start.19) | collective-permute-done | bytes 524320 | tf_op jit(solution)/shard_map/ppermute | solution.py:19
  156.4 4.2 %norm_both.1 = bf16[256,2048]{1,0:T(8,128)(2,1)} custom-call(bf16[128,2048]{1,0:T(8,128)(2,1)} %norm.2.refs_0_, bf16[128,2048]{1,0:T(8,128)(2,1)} %norm.3.refs_1_, bf16[128,2048]{1,0:T(8,128)(2,1)} %get-tuple-element.29.refs_2_, bf16[128,2048]{1,0:T(8,128)(2,1)} %get-tuple-element.30.refs_3_, bf16[128,2048]{1,0:T(8,128)(2,1)} %copy-done.10, ...), custom_call_target="tpu_custom_call" | custom-call | tf_op jit(solution)/shard_map/norm_both/pallas_call | solution.py:190
  (57 shorter events, 9.3 us)
Async XLA Ops:
  6.5 95.7 %all-gather.2.cloned.1.call-start = ((), (), s32[]{:S(2)}) async-start(), calls=%async_computation | async-start | bytes 17301504 | tf_op jit(solution)/shard_map/all_gather | solution.py:287
  9.4 7.1 %collective-permute-start = (bf16[2,128,256]{2,1,0:T(8,128)(2,1)S(1)}, bf16[2,128,256]{2,1,0:T(8,128)(2,1)S(1)}, u32[]{:S(2)}, u32[]{:S(2)}) collective-permute-start(bf16[2,128,256]{2,1,0:T(8,128)(2,1)S(1)} %get-tuple-element.38), channel_id=1, source_target_pairs={{0,4},{4,8},{8,12},{12,16},{16,20},{20,24},{24,28},{28,32},{32,36}... | collective-permute-start | bytes 393224 | tf_op jit(solution)/shard_map/ppermute | solution.py:26
  14.0 6.3 %collective-permute-start.1 = (bf16[2,128,256]{2,1,0:T(8,128)(2,1)S(1)}, bf16[2,128,256]{2,1,0:T(8,128)(2,1)S(1)}, u32[]{:S(2)}, u32[]{:S(2)}) collective-permute-start(bf16[2,128,256]{2,1,0:T(8,128)(2,1)S(1)} %get-tuple-element.37), channel_id=1, source_target_pairs={{4,0},{8,4},{12,8},{16,12},{20,16},{24,20},{28,24},{32,28},{36,32}... | collective-permute-start | bytes 393224 | tf_op jit(solution)/shard_map/ppermute | solution.py:27
  16.6 3.8 %copy-start = (bf16[2,128,256]{2,1,0:T(8,128)(2,1)}, bf16[2,128,256]{2,1,0:T(8,128)(2,1)S(1)}, u32[]{:S(2)}) copy-start(bf16[2,128,256]{2,1,0:T(8,128)(2,1)S(1)} %collective-permute-done.before_ref) | copy-start | bytes 393220
  27.6 14.7 %collective-permute-start.6 = (bf16[128,2048]{1,0:T(8,128)(2,1)}, bf16[128,2048]{1,0:T(8,128)(2,1)S(1)}, u32[]{:S(2)}, u32[]{:S(2)}) collective-permute-start(bf16[128,2048]{1,0:T(8,128)(2,1)} %get-tuple-element.28), channel_id=1, source_target_pairs={{0,3},{1,0},{2,1},{3,2},{4,7},{5,4},{6,5},{7,6},{8,11},{9,8},{10,9... | collective-permute-start | bytes 1572872 | tf_op jit(solution)/shard_map/ppermute | solution.py:19
  30.1 15.0 %collective-permute-start.2 = (bf16[128,2048]{1,0:T(8,128)(2,1)}, bf16[128,2048]{1,0:T(8,128)(2,1)S(1)}, u32[]{:S(2)}, u32[]{:S(2)}) collective-permute-start(bf16[128,2048]{1,0:T(8,128)(2,1)} %get-tuple-element.23), channel_id=1, source_target_pairs={{0,1},{1,2},{2,3},{3,0},{4,5},{5,6},{6,7},{7,4},{8,9},{9,10},{10,1... | collective-permute-start | bytes 1572872 | tf_op jit(solution)/shard_map/ppermute | solution.py:19
  39.7 16.2 %collective-permute-start.5 = (bf16[128,2048]{1,0:T(8,128)(2,1)}, bf16[128,2048]{1,0:T(8,128)(2,1)S(1)}, u32[]{:S(2)}, u32[]{:S(2)}) collective-permute-start(bf16[128,2048]{1,0:T(8,128)(2,1)} %get-tuple-element.26), channel_id=1, source_target_pairs={{0,1},{1,2},{2,3},{3,0},{4,5},{5,6},{6,7},{7,4},{8,9},{9,10},{10,1... | collective-permute-start | bytes 1572872 | tf_op jit(solution)/shard_map/ppermute | solution.py:19
  39.9 29.6 %collective-permute-start.4 = (bf16[128,2048]{1,0:T(8,128)(2,1)}, bf16[128,2048]{1,0:T(8,128)(2,1)S(1)}, u32[]{:S(2)}, u32[]{:S(2)}) collective-permute-start(bf16[128,2048]{1,0:T(8,128)(2,1)} %get-tuple-element.24), channel_id=1, source_target_pairs={{0,3},{1,0},{2,1},{3,2},{4,7},{5,4},{6,5},{7,6},{8,11},{9,8},{10,9... | collective-permute-start | bytes 1572872 | tf_op jit(solution)/shard_map/ppermute | solution.py:19
  43.5 19.9 %collective-permute-start.7 = (bf16[128,2048]{1,0:T(8,128)(2,1)S(1)}, bf16[128,2048]{1,0:T(8,128)(2,1)}, u32[]{:S(2)}, u32[]{:S(2)}) collective-permute-start(bf16[128,2048]{1,0:T(8,128)(2,1)S(1)} %add_convert_fusion.2), channel_id=1, source_target_pairs={{0,3},{1,0},{2,1},{3,2},{4,7},{5,4},{6,5},{7,6},{8,11},{9,8},{10,9... | collective-permute-start | bytes 1572872 | tf_op jit(solution)/shard_map/ppermute | solution.py:19
  46.2 23.3 %collective-permute-start.3 = (bf16[128,2048]{1,0:T(8,128)(2,1)S(1)}, bf16[128,2048]{1,0:T(8,128)(2,1)S(1)}, u32[]{:S(2)}, u32[]{:S(2)}) collective-permute-start(bf16[128,2048]{1,0:T(8,128)(2,1)S(1)} %add_convert_fusion.3), channel_id=1, source_target_pairs={{0,1},{1,2},{2,3},{3,0},{4,5},{5,6},{6,7},{7,4},{8,9},{9,10},{10,1... | collective-permute-start | bytes 1572872 | tf_op jit(solution)/shard_map/ppermute | solution.py:19
  55.8 7.6 %copy-start.13 = (bf16[128,2048]{1,0:T(8,128)(2,1)}, bf16[128,2048]{1,0:T(8,128)(2,1)S(1)}, u32[]{:S(2)}) copy-start(bf16[128,2048]{1,0:T(8,128)(2,1)S(1)} %collective-permute-done.5.refs_2_) | copy-start | bytes 1572868
  66.2 14.0 %collective-permute-start.11 = (bf16[128,2048]{1,0:T(8,128)(2,1)}, bf16[128,2048]{1,0:T(8,128)(2,1)S(1)}, u32[]{:S(2)}, u32[]{:S(2)}) collective-permute-start(bf16[128,2048]{1,0:T(8,128)(2,1)} %norm.3.refs_1_), channel_id=1, source_target_pairs={{0,3},{1,0},{2,1},{3,2},{4,7},{5,4},{6,5},{7,6},{8,11},{9,8},{10,9... | collective-permute-start | bytes 1572872 | tf_op jit(solution)/shard_map/ppermute | solution.py:19
  69.5 0.8 copy-start.12
  69.5 1.0 copy-start.14
  73.2 14.0 %collective-permute-start.8 = (bf16[128,2048]{1,0:T(8,128)(2,1)}, bf16[128,2048]{1,0:T(8,128)(2,1)S(1)}, u32[]{:S(2)}, u32[]{:S(2)}) collective-permute-start(bf16[128,2048]{1,0:T(8,128)(2,1)} %norm.2.refs_0_), channel_id=1, source_target_pairs={{0,1},{1,2},{2,3},{3,0},{4,5},{5,6},{6,7},{7,4},{8,9},{9,10},{10,1... | collective-permute-start | bytes 1572872 | tf_op jit(solution)/shard_map/ppermute | solution.py:19
  80.2 34.1 %copy-start.2 = (bf16[128,2048]{1,0:T(8,128)(2,1)}, bf16[128,2048]{1,0:T(8,128)(2,1)S(1)}, u32[]{:S(2)}) copy-start(bf16[128,2048]{1,0:T(8,128)(2,1)S(1)} %collective-permute-done.11.refs_3_) | copy-start | bytes 1572868
  80.2 15.2 %collective-permute-start.13 = (bf16[128,2048]{1,0:T(8,128)(2,1)S(1)}, bf16[128,2048]{1,0:T(8,128)(2,1)S(1)}, u32[]{:S(2)}, u32[]{:S(2)}) collective-permute-start(bf16[128,2048]{1,0:T(8,128)(2,1)S(1)} %collective-permute-done.11.refs_3_), channel_id=1, source_target_pairs={{0,3},{1,0},{2,1},{3,2},{4,7},{5,4},{6,5},{7,6},{8,11},{9,8},{10,9... | collective-permute-start | bytes 1572872 | tf_op jit(solution)/shard_map/ppermute | solution.py:19
  87.1 27.2 %copy-start.3 = (bf16[128,2048]{1,0:T(8,128)(2,1)}, bf16[128,2048]{1,0:T(8,128)(2,1)S(1)}, u32[]{:S(2)}) copy-start(bf16[128,2048]{1,0:T(8,128)(2,1)S(1)} %collective-permute-done.8.refs_0_) | copy-start | bytes 1572868
  87.1 15.1 %collective-permute-start.12 = (bf16[128,2048]{1,0:T(8,128)(2,1)S(1)}, bf16[128,2048]{1,0:T(8,128)(2,1)S(1)}, u32[]{:S(2)}, u32[]{:S(2)}) collective-permute-start(bf16[128,2048]{1,0:T(8,128)(2,1)S(1)} %collective-permute-done.8.refs_0_), channel_id=1, source_target_pairs={{0,1},{1,2},{2,3},{3,0},{4,5},{5,6},{6,7},{7,4},{8,9},{9,10},{10,1... | collective-permute-start | bytes 1572872 | tf_op jit(solution)/shard_map/ppermute | solution.py:19
  87.1 27.1 %collective-permute-start.9 = (bf16[128,2048]{1,0:T(8,128)(2,1)}, bf16[128,2048]{1,0:T(8,128)(2,1)S(1)}, u32[]{:S(2)}, u32[]{:S(2)}) collective-permute-start(bf16[128,2048]{1,0:T(8,128)(2,1)} %norm.3.refs_1_), channel_id=1, source_target_pairs={{0,1},{1,2},{2,3},{3,0},{4,5},{5,6},{6,7},{7,4},{8,9},{9,10},{10,1... | collective-permute-start | bytes 1572872 | tf_op jit(solution)/shard_map/ppermute | solution.py:19
  87.1 27.1 %collective-permute-start.10 = (bf16[128,2048]{1,0:T(8,128)(2,1)}, bf16[128,2048]{1,0:T(8,128)(2,1)S(1)}, u32[]{:S(2)}, u32[]{:S(2)}) collective-permute-start(bf16[128,2048]{1,0:T(8,128)(2,1)} %norm.2.refs_0_), channel_id=1, source_target_pairs={{0,3},{1,0},{2,1},{3,2},{4,7},{5,4},{6,5},{7,6},{8,11},{9,8},{10,9... | collective-permute-start | bytes 1572872 | tf_op jit(solution)/shard_map/ppermute | solution.py:19
  95.4 6.9 %copy-start.9 = (bf16[128,2048]{1,0:T(8,128)(2,1)}, bf16[128,2048]{1,0:T(8,128)(2,1)S(1)}, u32[]{:S(2)}) copy-start(bf16[128,2048]{1,0:T(8,128)(2,1)S(1)} %collective-permute-done.13.refs_1_) | copy-start | bytes 1572868
  112.7 20.5 %collective-permute-start.18 = (bf16[128,2048]{1,0:T(8,128)(2,1)}, bf16[128,2048]{1,0:T(8,128)(2,1)S(1)}, u32[]{:S(2)}, u32[]{:S(2)}) collective-permute-start(bf16[128,2048]{1,0:T(8,128)(2,1)} %get-tuple-element.36), channel_id=1, source_target_pairs={{0,3},{1,0},{2,1},{3,2},{4,7},{5,4},{6,5},{7,6},{8,11},{9,8},{10,9... | collective-permute-start | bytes 1572872 | tf_op jit(solution)/shard_map/ppermute | solution.py:19
  112.8 21.7 %collective-permute-start.14 = (bf16[128,2048]{1,0:T(8,128)(2,1)}, bf16[128,2048]{1,0:T(8,128)(2,1)S(1)}, u32[]{:S(2)}, u32[]{:S(2)}) collective-permute-start(bf16[128,2048]{1,0:T(8,128)(2,1)} %get-tuple-element.32), channel_id=1, source_target_pairs={{0,1},{1,2},{2,3},{3,0},{4,5},{5,6},{6,7},{7,4},{8,9},{9,10},{10,1... | collective-permute-start | bytes 1572872 | tf_op jit(solution)/shard_map/ppermute | solution.py:19
  130.5 16.4 %collective-permute-start.16 = (bf16[128,2048]{1,0:T(8,128)(2,1)}, bf16[128,2048]{1,0:T(8,128)(2,1)S(1)}, u32[]{:S(2)}, u32[]{:S(2)}) collective-permute-start(bf16[128,2048]{1,0:T(8,128)(2,1)} %get-tuple-element.33), channel_id=1, source_target_pairs={{0,1},{1,2},{2,3},{3,0},{4,5},{5,6},{6,7},{7,4},{8,9},{9,10},{10,1... | collective-permute-start | bytes 1572872 | tf_op jit(solution)/shard_map/ppermute | solution.py:19
  130.6 16.3 %collective-permute-start.17 = (bf16[128,2048]{1,0:T(8,128)(2,1)}, bf16[128,2048]{1,0:T(8,128)(2,1)S(1)}, u32[]{:S(2)}, u32[]{:S(2)}) collective-permute-start(bf16[128,2048]{1,0:T(8,128)(2,1)} %get-tuple-element.34), channel_id=1, source_target_pairs={{0,3},{1,0},{2,1},{3,2},{4,7},{5,4},{6,5},{7,6},{8,11},{9,8},{10,9... | collective-permute-start | bytes 1572872 | tf_op jit(solution)/shard_map/ppermute | solution.py:19
  134.4 20.2 %collective-permute-start.19 = (bf16[128,2048]{1,0:T(8,128)(2,1)S(1)}, bf16[128,2048]{1,0:T(8,128)(2,1)S(1)}, u32[]{:S(2)}, u32[]{:S(2)}) collective-permute-start(bf16[128,2048]{1,0:T(8,128)(2,1)S(1)} %add_convert_fusion), channel_id=1, source_target_pairs={{0,3},{1,0},{2,1},{3,2},{4,7},{5,4},{6,5},{7,6},{8,11},{9,8},{10,9... | collective-permute-start | bytes 1572872 | tf_op jit(solution)/shard_map/ppermute | solution.py:19
  135.7 19.9 %collective-permute-start.15 = (bf16[128,2048]{1,0:T(8,128)(2,1)S(1)}, bf16[128,2048]{1,0:T(8,128)(2,1)S(1)}, u32[]{:S(2)}, u32[]{:S(2)}) collective-permute-start(bf16[128,2048]{1,0:T(8,128)(2,1)S(1)} %add_convert_fusion.1), channel_id=1, source_target_pairs={{0,1},{1,2},{2,3},{3,0},{4,5},{5,6},{6,7},{7,4},{8,9},{9,10},{10,1... | collective-permute-start | bytes 1572872 | tf_op jit(solution)/shard_map/ppermute | solution.py:19
  146.9 8.7 %copy-start.4 = (bf16[128,2048]{1,0:T(8,128)(2,1)}, bf16[128,2048]{1,0:T(8,128)(2,1)S(1)}, u32[]{:S(2)}) copy-start(bf16[128,2048]{1,0:T(8,128)(2,1)S(1)} %collective-permute-done.16.refs_5_) | copy-start | bytes 1572868
  146.9 8.7 %copy-start.5 = (bf16[128,2048]{1,0:T(8,128)(2,1)}, bf16[128,2048]{1,0:T(8,128)(2,1)S(1)}, u32[]{:S(2)}) copy-start(bf16[128,2048]{1,0:T(8,128)(2,1)S(1)} %collective-permute-done.17.refs_6_) | copy-start | bytes 1572868
  154.6 1.0 copy-start.8
  155.6 0.8 copy-start.10
  (4 other events, 3.0 us)
Sparse Core Ops, SparseCore 0:
  9.6 76.2 all-gather.1

commit v4 on v3

--- a/solution.py
+++ b/solution.py
@@ -153,61 +153,49 @@
     return (centred * lax.rsqrt(variance + 1e-06) * gain[...] + bias[...]).astype(jnp.bfloat16)
 
 
-def norm_kernel(*refs):
-    refs[-1][...] = normed(refs[:-3], *refs[-3:-1])
-
-
-def norm_half(residual, side, parts, gain, bias, block=64):
-    rows, width = parts[0].shape
+def norm_kernel(*refs, whole):
+    *parts, gain, bias, out_ref = refs
+    for side in range(2):
+
+        @pl.when(pl.program_id(0) // (pl.num_programs(0) // 2) == side)
+        def _():
+            out_ref[...] = normed(parts[:whole] + parts[whole + side :: 2], gain, bias)
+
+
+def norm_rows(wholes, halves, gain, bias, block=64):
+    rows, width = wholes[0].shape
     steps = rows // block
+    half = steps // 2
     tile = pl.BlockSpec((block, width), lambda i: (i, 0))
+    tops = pl.BlockSpec((block, width), lambda i: (jnp.minimum(i, half - 1), 0))
+    bottoms = pl.BlockSpec((block, width), lambda i: (jnp.maximum(i - half, 0), 0))
     line = pl.BlockSpec((1, width), lambda i: (0, 0))
     return pl.pallas_call(
-        norm_kernel,
+        functools.partial(norm_kernel, whole=len(wholes)),
         grid=(steps,),
-        in_specs=[pl.BlockSpec((block, width), lambda i: (side * steps + i, 0))]
-        + [tile] * len(parts)
-        + [line, line],
+        in_specs=[tile] * len(wholes) + [tops, bottoms] * (len(halves) // 2) + [line, line],
         out_specs=tile,
         out_shape=jax.ShapeDtypeStruct((rows, width), jnp.bfloat16),
         name="norm",
-    )(residual, *parts, gain[None], bias[None])
-
-
-def norm_both_kernel(*refs):
-    *halves, gain, bias, out_ref = refs
-    for side in range(2):
-
-        @pl.when(pl.program_id(0) == side)
-        def _():
-            out_ref[...] = normed(halves[side::2], gain, bias)
-
-
-def norm_both(halves, gain, bias):
-    rows, width = halves[0].shape
-    whole = pl.BlockSpec((rows, width), lambda i: (0, 0))
-    line = pl.BlockSpec((1, width), lambda i: (0, 0))
-    return pl.pallas_call(
-        norm_both_kernel,
-        grid=(2,),
-        in_specs=[whole] * len(halves) + [line, line],
-        out_specs=pl.BlockSpec((rows, width), lambda i: (i, 0)),
-        out_shape=jax.ShapeDtypeStruct((2 * rows, width), jnp.bfloat16),
-        name="norm_both",
-    )(*halves, gain[None], bias[None])
+    )(*wholes, *halves, gain[None], bias[None])
 
 
 def added(part, arrived):
     return (part.astype(jnp.float32) + arrived.astype(jnp.float32)).astype(jnp.bfloat16)
 
 
-def feed_kernel(*refs, count, chunk):
-    rows, weights, outs = (refs[:count], refs[count], refs[count + 1 : 2 * count + 1])
-    up, down, activation, sems = refs[2 * count + 1 :]
+def feed_kernel(*refs, count, outs, chunk):
+    rows, weights, results = (refs[:count], refs[count], refs[count + 1 : count + 1 + outs])
+    tokens, up, down, activation, branch, sems = refs[count + 1 + outs :]
     pieces, height, units = up.shape
     size, steps = (rows[0].shape[0], units // chunk)
+    height_out = results[0].shape[0]
     part = pieces // steps
     width = part * height
+
+    def row_copy(index):
+        span = pl.ds(index * size, size)
+        return pltpu.make_async_copy(rows[index], tokens.at[span], sems.at[2 * steps + index])
 
     def up_copy(k):
         cols = pl.ds(pl.multiple_of(k * chunk, chunk), chunk)
@@ -217,17 +205,30 @@
         span = pl.ds(k * part, part)
         return pltpu.make_async_copy(weights.at[span, 1], down.at[span], sems.at[steps + k])
 
+    def out_copy(index, k):
+        cols = pl.ds(pl.multiple_of(k * width, width), width)
+        span = pl.ds(index * height_out, height_out)
+        return pltpu.make_async_copy(
+            branch.at[span, cols],
+            results[index].at[:, cols],
+            sems.at[2 * steps + count + index * steps + k],
+        )
+
+    for index in range(count):
+        row_copy(index).start()
     for k in range(steps):
         up_copy(k).start()
     for k in range(steps):
         down_copy(k).start()
+    for index in range(count):
+        row_copy(index).wait()
 
     @pl.loop(0, steps)
     def _(k):
         up_copy(k).wait()
         cols = pl.ds(pl.multiple_of(k * chunk, chunk), chunk)
         hidden = jnp.dot(
-            jnp.concatenate([ref[...] for ref in rows], axis=0),
+            tokens[...],
             up[:, :, cols].reshape(pieces * height, chunk),
             preferred_element_type=jnp.float32,
         )
@@ -236,34 +237,44 @@
     @pl.loop(0, steps)
     def _(k):
         down_copy(k).wait()
-        branch = lax.dot_general(
+        cols = pl.ds(pl.multiple_of(k * width, width), width)
+        branch[:, cols] = lax.dot_general(
             activation[...],
             down[pl.ds(k * part, part)].reshape(width, units),
             (((1,), (1,)), ((), ())),
             preferred_element_type=jnp.float32,
         ).astype(jnp.bfloat16)
-        cols = pl.ds(pl.multiple_of(k * width, width), width)
-        for index, out in enumerate(outs):
-            out[:, cols] = branch[index * size : (index + 1) * size]
-
-
-def feed_forward(rows, weights, chunk=512):
+        for index in range(outs):
+            out_copy(index, k).start()
+
+    @pl.loop(0, steps)
+    def _(k):
+        for index in range(outs):
+            out_copy(index, k).wait()
+
+
+def feed_forward(rows, weights, height_out, chunk=512):
     size, width = rows[0].shape
     pieces, _, height, units = weights.shape
-    whole = pl.BlockSpec(memory_space=pltpu.VMEM)
+    count, total = (len(rows), len(rows) * size)
+    outs = total // height_out
+    anywhere = pl.BlockSpec(memory_space=pl.ANY)
     full = pltpu.VMEM((pieces, height, units), jnp.bfloat16)
+    steps = units // chunk
     return pl.pallas_call(
-        functools.partial(feed_kernel, count=len(rows), chunk=chunk),
-        in_specs=[whole] * len(rows) + [pl.BlockSpec(memory_space=pl.ANY)],
-        out_specs=[whole] * len(rows),
-        out_shape=[jax.ShapeDtypeStruct((size, width), jnp.bfloat16)] * len(rows),
+        functools.partial(feed_kernel, count=count, outs=outs, chunk=chunk),
+        in_specs=[anywhere] * (count + 1),
+        out_specs=[anywhere] * outs,
+        out_shape=[jax.ShapeDtypeStruct((height_out, width), jnp.bfloat16)] * outs,
         scratch_shapes=[
+            pltpu.VMEM((total, width), jnp.bfloat16),
             full,
             full,
-            pltpu.VMEM((size * len(rows), units), jnp.bfloat16),
-            pltpu.SemaphoreType.DMA((2 * (units // chunk),)),
+            pltpu.VMEM((total, units), jnp.bfloat16),
+            pltpu.VMEM((total, width), jnp.bfloat16),
+            pltpu.SemaphoreType.DMA((2 * steps + count + outs * steps,)),
         ],
-        compiler_params=pltpu.CompilerParams(vmem_limit_bytes=54 * 1024 * 1024),
+        compiler_params=pltpu.CompilerParams(vmem_limit_bytes=40 * 1024 * 1024),
         name="feed",
     )(*rows, weights)
 
@@ -302,31 +313,31 @@
     own_top, own_bottom = run(1, lambda i: 0, n_tp, n_sp)
     left_sum = shift(added(right_top, from_left), 1)
     right_sum = shift(added(left_bottom, from_right), -1)
-    norm1 = (norm1_gain, norm1_bias)
-    first_top = norm_half(residual_in, 0, (own_top, left_sum, right_plain), *norm1)
-    first_bottom = norm_half(residual_in, 1, (own_bottom, left_plain, right_sum), *norm1)
-
-    row_lt = shift(first_top, 1)
-    row_rb = shift(first_bottom, -1)
-    row_lb = shift(first_bottom, 1)
-    row_rt = shift(first_top, -1)
-    row_ft = shift(row_lt, 1)
-    row_fb = shift(row_rb, -1)
+    first = norm_rows(
+        (residual_in,),
+        (own_top, own_bottom, left_sum, left_plain, right_plain, right_sum),
+        norm1_gain,
+        norm1_bias,
+    )
+
+    half = first.shape[0] // 2
+    row_left = shift(first, 1)
+    row_right = shift(first, -1)
+    row_ft = shift(row_left[:half], 1)
+    row_fb = shift(row_right[half:], -1)
     left_top, left_bottom, right_top, right_bottom = feed_forward(
-        (row_lt, row_lb, row_rt, row_rb), weights
+        (row_left, row_right), weights, half
     )
     left_plain = shift(right_bottom, 1)
     right_plain = shift(left_top, -1)
-    far_top, far_bottom = feed_forward((row_ft, row_fb), weights)
+    far_top, far_bottom = feed_forward((row_ft, row_fb), weights, half)
     from_left = shift(far_top, 1)
     from_right = shift(far_bottom, -1)
-    own_top, own_bottom = feed_forward((first_top, first_bottom), weights)
+    (own,) = feed_forward((first,), weights, 2 * half)
     left_sum = shift(added(right_top, from_left), 1)
     right_sum = shift(added(left_bottom, from_right), -1)
-    return norm_both(
-        (first_top, first_bottom, own_top, own_bottom, left_sum, left_plain, right_plain, right_sum),
-        norm2_gain,
-        norm2_bias,
+    return norm_rows(
+        (first, own), (left_sum, left_plain, right_plain, right_sum), norm2_gain, norm2_bias
     )
 
 

time: 171 us -> 179 us (1.047)
  the two profiles are of different devices: /device:TPU:1 before, /device:TPU:14 now
where the time goes in v4:
time: 179 us; the launch traced here: 178 us
  waiting for transfers between devices  63.1 us (35%)
  Pallas kernels  60.3 us (34%)
  starting transfers between devices  27.8 us (16%)
  between operations  13.6 us (8%)
  local copies, waits for them, and re-layouts  8.32 us (5%)
  other arithmetic  4.94 us (3%)
    ppermute x16, waiting for transfers between devices, shift(): lax.ppermute(value, axis, [(i, (i + step) % devices) for i in range(devic...  61.1 us
    pallas_call x3, Pallas kernels, feed_forward(): pl.pallas_call(functools.partial(feed_kernel, count=count, outs=outs, chu...  28.4 us
    pallas_call x3, Pallas kernels, attend(): pl.pallas_call(functools.partial(attend_kernel, rel=rel, n_sp=n_sp, tok_r...  22.4 us
    ppermute x16, starting transfers between devices, shift(): lax.ppermute(value, axis, [(i, (i + step) % devices) for i in range(devic...  22.3 us
    pallas_call x2, Pallas kernels, norm_rows(): pl.pallas_call(functools.partial(norm_kernel, whole=len(wholes)), grid=(s...  9.52 us
    unnamed x32, local copies, waits for them, and re-layouts  7.24 us
    ppermute x1, starting transfers between devices, halo(): after = lax.ppermute(shard[:, :width], axis, down)  3.64 us
  transfers between devices with their start and end apart: 19, of which 12 were waited for; matrix products, arithmetic and copies ran while one was open for 2% of the time, Pallas kernels for 27%

profile of v4, /device:TPU:14, one launch (start us, length us, event | category | flops | bytes accessed | tf_op | source)
XLA Modules:
  0.0 178.1 jit_solution(10779397396377029538)
XLA Ops:
  6.5 1.9 %pad_maximum_fusion = bf16[128,2048]{1,0:T(8,128)(2,1)} fusion(bf16[64,2048]{1,0:T(8,128)(2,1)} %bitcast.9, bf16[64,2048]{1,0:T(8,128)(2,1)} %param.18), kind=kLoop, calls=%fused_computation.4 | loop fusion | flops 1048576 | bytes 1048576 | tf_op jit(solution)/shard_map/concatenate | solution.py:297
  8.4 1.0 fusion
  9.4 1.9 %collective-permute-start = (bf16[2,128,256]{2,1,0:T(8,128)(2,1)S(1)}, bf16[2,128,256]{2,1,0:T(8,128)(2,1)S(1)}, u32[]{:S(2)}, u32[]{:S(2)}) collective-permute-start(bf16[2,128,256]{2,1,0:T(8,128)(2,1)S(1)} %get-tuple-element.34), channel_id=1, source_target_pairs={{0,4},{4,8},{8,12},{12,16},{16,20},{20,24},{24,28},{28,32},{32,36}... | collective-permute-start | bytes 393224 | tf_op jit(solution)/shard_map/ppermute | solution.py:26
  11.4 3.6 %collective-permute-start.1 = (bf16[2,128,256]{2,1,0:T(8,128)(2,1)S(1)}, bf16[2,128,256]{2,1,0:T(8,128)(2,1)S(1)}, u32[]{:S(2)}, u32[]{:S(2)}) collective-permute-start(bf16[2,128,256]{2,1,0:T(8,128)(2,1)S(1)} %get-tuple-element.33), channel_id=1, source_target_pairs={{4,0},{8,4},{12,8},{16,12},{20,16},{24,20},{28,24},{32,28},{36,32}... | collective-permute-start | bytes 393224 | tf_op jit(solution)/shard_map/ppermute | solution.py:27
  15.7 1.8 %collective-permute-done.1.after_ref = bf16[2,128,256]{2,1,0:T(8,128)(2,1)S(1)} collective-permute-done((bf16[2,128,256]{2,1,0:T(8,128)(2,1)S(1)}, bf16[2,128,256]{2,1,0:T(8,128)(2,1)S(1)}, u32[]{:S(2)}, u32[]{:S(2)}) %collective-permute-start.1) | collective-permute-done | bytes 131104 | tf_op jit(solution)/shard_map/ppermute | solution.py:27
  18.2 6.3 %attend.5 = (bf16[128,2048]{1,0:T(8,128)(2,1)}, bf16[128,2048]{1,0:T(8,128)(2,1)}) custom-call(s32[2]{0:T(128)} %compare_select_fusion.place, f32[8]{0:T(128)} %sink.5, bf16[1024,512]{1,0:T(8,128)(2,1)} %q_ref.5, bf16[2,128,256]{2,1,0:T(8,128)(2,1)} %copy-done.6, bf16[2,1024,256]{2,1,0:T(8,128)(2,1)} %mid_ref.5, bf16[2,128,256]{2,1,0:T(8,128)(2,1)} %copy-done.7, ...), custom_call_target="tpu_custom_call" | custom-call | tf_op jit(solution)/shard_map/attend/pallas_call | solution.py:123
  25.3 2.4 %collective-permute-start.2 = (bf16[128,2048]{1,0:T(8,128)(2,1)}, bf16[128,2048]{1,0:T(8,128)(2,1)S(1)}, u32[]{:S(2)}, u32[]{:S(2)}) collective-permute-start(bf16[128,2048]{1,0:T(8,128)(2,1)} %get-tuple-element.22), channel_id=1, source_target_pairs={{0,1},{1,2},{2,3},{3,0},{4,5},{5,6},{6,7},{7,4},{8,9},{9,10},{10,1... | collective-permute-start | bytes 1572872 | tf_op jit(solution)/shard_map/ppermute | solution.py:19
  27.7 9.7 %attend.4 = (bf16[128,2048]{1,0:T(8,128)(2,1)}, bf16[128,2048]{1,0:T(8,128)(2,1)}, bf16[128,2048]{1,0:T(8,128)(2,1)}, bf16[128,2048]{1,0:T(8,128)(2,1)}) custom-call(s32[2]{0:T(128)} %compare_select_fusion.place, f32[8]{0:T(128)} %sink.5, bf16[1024,512]{1,0:T(8,128)(2,1)} %q_ref.5, bf16[2,128,256]{2,1,0:T(8,128)(2,1)} %copy-done.6, ...), custom_call_target="tpu_custom_call" | custom-call | tf_op jit(solution)/shard_map/attend/pallas_call | solution.py:123
  37.4 2.0 %collective-permute-start.5 = (bf16[128,2048]{1,0:T(8,128)(2,1)}, bf16[128,2048]{1,0:T(8,128)(2,1)S(1)}, u32[]{:S(2)}, u32[]{:S(2)}) collective-permute-start(bf16[128,2048]{1,0:T(8,128)(2,1)} %get-tuple-element.24), channel_id=1, source_target_pairs={{0,3},{1,0},{2,1},{3,2},{4,7},{5,4},{6,5},{7,6},{8,11},{9,8},{10,9... | collective-permute-start | bytes 1572872 | tf_op jit(solution)/shard_map/ppermute | solution.py:19
  39.6 1.2 add_convert_fusion.2
  40.9 1.2 add_convert_fusion.3
  42.0 3.3 %collective-permute-start.3 = (bf16[128,2048]{1,0:T(8,128)(2,1)S(1)}, bf16[128,2048]{1,0:T(8,128)(2,1)S(1)}, u32[]{:S(2)}, u32[]{:S(2)}) collective-permute-start(bf16[128,2048]{1,0:T(8,128)(2,1)S(1)} %add_convert_fusion.3), channel_id=1, source_target_pairs={{0,1},{1,2},{2,3},{3,0},{4,5},{5,6},{6,7},{7,4},{8,9},{9,10},{10,1... | collective-permute-start | bytes 1572872 | tf_op jit(solution)/shard_map/ppermute | solution.py:19
  45.3 6.4 %attend.3 = (bf16[128,2048]{1,0:T(8,128)(2,1)}, bf16[128,2048]{1,0:T(8,128)(2,1)}) custom-call(s32[2]{0:T(128)} %compare_select_fusion.place, f32[8]{0:T(128)} %sink.5, bf16[1024,512]{1,0:T(8,128)(2,1)} %q_ref.5, bf16[2,128,256]{2,1,0:T(8,128)(2,1)} %copy-done.6, bf16[2,1024,256]{2,1,0:T(8,128)(2,1)} %mid_ref.5, bf16[2,128,256]{2,1,0:T(8,128)(2,1)} %copy-done.7, ...), custom_call_target="tpu_custom_call" | custom-call | tf_op jit(solution)/shard_map/attend/pallas_call | solution.py:123
  51.9 1.2 collective-permute-done.5.refs_5_
  53.1 11.2 %collective-permute-done.7.refs_6_ = bf16[128,2048]{1,0:T(8,128)(2,1)S(1)} collective-permute-done((bf16[128,2048]{1,0:T(8,128)(2,1)S(1)}, bf16[128,2048]{1,0:T(8,128)(2,1)S(1)}, u32[]{:S(2)}, u32[]{:S(2)}) %collective-permute-start.7) | collective-permute-done | bytes 524320 | tf_op jit(solution)/shard_map/ppermute | solution.py:19
  65.3 4.9 %norm.2.refs_0_ = bf16[256,2048]{1,0:T(8,128)(2,1)} custom-call(bf16[256,2048]{1,0:T(8,128)(2,1)} %refs_0_.1, bf16[128,2048]{1,0:T(8,128)(2,1)} %get-tuple-element.19.refs_1_, bf16[128,2048]{1,0:T(8,128)(2,1)} %get-tuple-element.20.refs_2_, bf16[128,2048]{1,0:T(8,128)(2,1)} %copy-done.14, bf16[128,2048]{1,0:T(8,128)(2,1)} %copy-done.8, ...), custom_call_target="tpu_custom_call" | custom-call | tf_op jit(solution)/shard_map/norm/pallas_call | solution.py:173
  70.2 1.3 collective-permute-start.8
  72.2 24.1 %collective-permute-done.8.refs_0_ = bf16[256,2048]{1,0:T(8,128)(2,1)S(1)} collective-permute-done((bf16[256,2048]{1,0:T(8,128)(2,1)}, bf16[256,2048]{1,0:T(8,128)(2,1)S(1)}, u32[]{:S(2)}, u32[]{:S(2)}) %collective-permute-start.8) | collective-permute-done | bytes 1048608 | tf_op jit(solution)/shard_map/ppermute | solution.py:19
  96.3 2.8 %collective-permute-start.10 = (bf16[128,2048]{1,0:T(8,128)(2,1)S(1)}, bf16[128,2048]{1,0:T(8,128)(2,1)S(1)}, u32[]{:S(2)}, u32[]{:S(2)}) collective-permute-start(bf16[128,2048]{1,0:T(8,128)(2,1)S(1)} %slice.16), channel_id=1, source_target_pairs={{0,1},{1,2},{2,3},{3,0},{4,5},{5,6},{6,7},{7,4},{8,9},{9,10},{10,1... | collective-permute-start | bytes 1572872 | tf_op jit(solution)/shard_map/ppermute | solution.py:19
  99.3 11.3 %collective-permute-done.10.refs_0_ = bf16[128,2048]{1,0:T(8,128)(2,1)S(1)} collective-permute-done((bf16[128,2048]{1,0:T(8,128)(2,1)S(1)}, bf16[128,2048]{1,0:T(8,128)(2,1)S(1)}, u32[]{:S(2)}, u32[]{:S(2)}) %collective-permute-start.10) | collective-permute-done | bytes 524320 | tf_op jit(solution)/shard_map/ppermute | solution.py:19
  111.3 2.7 %collective-permute-done.11.refs_1_ = bf16[128,2048]{1,0:T(8,128)(2,1)S(1)} collective-permute-done((bf16[128,2048]{1,0:T(8,128)(2,1)S(1)}, bf16[128,2048]{1,0:T(8,128)(2,1)S(1)}, u32[]{:S(2)}, u32[]{:S(2)}) %collective-permute-start.11) | collective-permute-done | bytes 524320 | tf_op jit(solution)/shard_map/ppermute | solution.py:19
  114.8 1.0 copy-done.3
  115.9 1.0 copy-done.5
  116.9 8.0 %feed.5 = (bf16[128,2048]{1,0:T(8,128)(2,1)S(1)}, bf16[128,2048]{1,0:T(8,128)(2,1)S(1)}) custom-call(bf16[128,2048]{1,0:T(8,128)(2,1)S(1)} %copy-done.3, bf16[128,2048]{1,0:T(8,128)(2,1)S(1)} %copy-done.5, bf16[32,2,64,2048]{3,2,1,0:T(8,128)(2,1)} %bitcast.6), custom_call_target="tpu_custom_call" | custom-call | tf_op jit(solution)/shard_map/feed/pallas_call | solution.py:264
  125.0 3.2 %collective-permute-start.12 = (bf16[128,2048]{1,0:T(8,128)(2,1)S(1)}, bf16[128,2048]{1,0:T(8,128)(2,1)S(1)}, u32[]{:S(2)}, u32[]{:S(2)}) collective-permute-start(bf16[128,2048]{1,0:T(8,128)(2,1)S(1)} %get-tuple-element.28), channel_id=1, source_target_pairs={{0,1},{1,2},{2,3},{3,0},{4,5},{5,6},{6,7},{7,4},{8,9},{9,10},{10,1... | collective-permute-start | bytes 1572872 | tf_op jit(solution)/shard_map/ppermute | solution.py:19
  128.2 12.6 %feed.4 = (bf16[128,2048]{1,0:T(8,128)(2,1)S(1)}, bf16[128,2048]{1,0:T(8,128)(2,1)S(1)}, bf16[128,2048]{1,0:T(8,128)(2,1)S(1)}, bf16[128,2048]{1,0:T(8,128)(2,1)S(1)}) custom-call(bf16[256,2048]{1,0:T(8,128)(2,1)S(1)} %collective-permute-done.8.refs_0_, bf16[256,2048]{1,0:T(8,128)(2,1)S(1)} %collective-permute-done.9.refs_1_, bf16[32,2,64,2048]{3,2,1,0:T(8,128)(2,1)} %bitcast.7), custom_call_target="tpu_custom_call" | custom-call | tf_op jit(solution)/shard_map/feed/pallas_call | solution.py:264
  140.9 2.0 %collective-permute-start.15 = (bf16[128,2048]{1,0:T(8,128)(2,1)S(1)}, bf16[128,2048]{1,0:T(8,128)(2,1)S(1)}, u32[]{:S(2)}, u32[]{:S(2)}) collective-permute-start(bf16[128,2048]{1,0:T(8,128)(2,1)S(1)} %get-tuple-element.30), channel_id=1, source_target_pairs={{0,3},{1,0},{2,1},{3,2},{4,7},{5,4},{6,5},{7,6},{8,11},{9,8},{10,9... | collective-permute-start | bytes 1572872 | tf_op jit(solution)/shard_map/ppermute | solution.py:19
  143.3 3.3 %collective-permute-start.13 = (bf16[128,2048]{1,0:T(8,128)(2,1)S(1)}, bf16[128,2048]{1,0:T(8,128)(2,1)S(1)}, u32[]{:S(2)}, u32[]{:S(2)}) collective-permute-start(bf16[128,2048]{1,0:T(8,128)(2,1)S(1)} %add_convert_fusion.1), channel_id=1, source_target_pairs={{0,1},{1,2},{2,3},{3,0},{4,5},{5,6},{6,7},{7,4},{8,9},{9,10},{10,1... | collective-permute-start | bytes 1572872 | tf_op jit(solution)/shard_map/ppermute | solution.py:19
  146.6 7.8 %feed.3.refs_1_ = bf16[256,2048]{1,0:T(8,128)(2,1)S(1)} custom-call(bf16[256,2048]{1,0:T(8,128)(2,1)S(1)} %copy-done, bf16[32,2,64,2048]{3,2,1,0:T(8,128)(2,1)} %bitcast.8), custom_call_target="tpu_custom_call" | custom-call | tf_op jit(solution)/shard_map/feed/pallas_call | solution.py:264
  155.7 1.3 collective-permute-done.15.refs_4_
  157.0 8.6 %collective-permute-done.17.refs_5_ = bf16[128,2048]{1,0:T(8,128)(2,1)S(1)} collective-permute-done((bf16[128,2048]{1,0:T(8,128)(2,1)S(1)}, bf16[128,2048]{1,0:T(8,128)(2,1)S(1)}, u32[]{:S(2)}, u32[]{:S(2)}) %collective-permute-start.17) | collective-permute-done | bytes 524320 | tf_op jit(solution)/shard_map/ppermute | solution.py:19
  166.6 4.7 %norm.3 = bf16[256,2048]{1,0:T(8,128)(2,1)} custom-call(bf16[256,2048]{1,0:T(8,128)(2,1)} %norm.2.refs_0_, bf16[256,2048]{1,0:T(8,128)(2,1)} %copy-done.1, bf16[128,2048]{1,0:T(8,128)(2,1)} %copy-done.15, bf16[128,2048]{1,0:T(8,128)(2,1)} %copy-done.10, bf16[128,2048]{1,0:T(8,128)(2,1)} %copy-done.11, bf16[128,2048]{1,0:T(8,128)(2,1)} %copy-done.13, ...), custom_call_target="tpu_custom_call" | custom-call | tf_op jit(solution)/shard_map/norm/pallas_call | solution.py:173
  (56 shorter events, 8.9 us)
Async XLA Ops:
  6.5 108.3 %all-gather.2.cloned.1.call-start = ((), (), s32[]{:S(2)}) async-start(), calls=%async_computation | async-start | bytes 17301504 | tf_op jit(solution)/shard_map/all_gather | solution.py:298
  9.4 6.3 %collective-permute-start = (bf16[2,128,256]{2,1,0:T(8,128)(2,1)S(1)}, bf16[2,128,256]{2,1,0:T(8,128)(2,1)S(1)}, u32[]{:S(2)}, u32[]{:S(2)}) collective-permute-start(bf16[2,128,256]{2,1,0:T(8,128)(2,1)S(1)} %get-tuple-element.34), channel_id=1, source_target_pairs={{0,4},{4,8},{8,12},{12,16},{16,20},{20,24},{24,28},{28,32},{32,36}... | collective-permute-start | bytes 393224 | tf_op jit(solution)/shard_map/ppermute | solution.py:26
  11.4 6.1 %collective-permute-start.1 = (bf16[2,128,256]{2,1,0:T(8,128)(2,1)S(1)}, bf16[2,128,256]{2,1,0:T(8,128)(2,1)S(1)}, u32[]{:S(2)}, u32[]{:S(2)}) collective-permute-start(bf16[2,128,256]{2,1,0:T(8,128)(2,1)S(1)} %get-tuple-element.33), channel_id=1, source_target_pairs={{4,0},{8,4},{12,8},{16,12},{20,16},{24,20},{28,24},{32,28},{36,32}... | collective-permute-start | bytes 393224 | tf_op jit(solution)/shard_map/ppermute | solution.py:27
  15.7 1.8 %copy-start.6 = (bf16[2,128,256]{2,1,0:T(8,128)(2,1)}, bf16[2,128,256]{2,1,0:T(8,128)(2,1)S(1)}, u32[]{:S(2)}) copy-start(bf16[2,128,256]{2,1,0:T(8,128)(2,1)S(1)} %collective-permute-done.before_ref) | copy-start | bytes 393220
  24.5 15.1 %collective-permute-start.6 = (bf16[128,2048]{1,0:T(8,128)(2,1)}, bf16[128,2048]{1,0:T(8,128)(2,1)S(1)}, u32[]{:S(2)}, u32[]{:S(2)}) collective-permute-start(bf16[128,2048]{1,0:T(8,128)(2,1)} %get-tuple-element.26), channel_id=1, source_target_pairs={{0,3},{1,0},{2,1},{3,2},{4,7},{5,4},{6,5},{7,6},{8,11},{9,8},{10,9... | collective-permute-start | bytes 1572872 | tf_op jit(solution)/shard_map/ppermute | solution.py:19
  25.3 15.5 %collective-permute-start.2 = (bf16[128,2048]{1,0:T(8,128)(2,1)}, bf16[128,2048]{1,0:T(8,128)(2,1)S(1)}, u32[]{:S(2)}, u32[]{:S(2)}) collective-permute-start(bf16[128,2048]{1,0:T(8,128)(2,1)} %get-tuple-element.22), channel_id=1, source_target_pairs={{0,1},{1,2},{2,3},{3,0},{4,5},{5,6},{6,7},{7,4},{8,9},{9,10},{10,1... | collective-permute-start | bytes 1572872 | tf_op jit(solution)/shard_map/ppermute | solution.py:19
  37.4 14.5 %collective-permute-start.4 = (bf16[128,2048]{1,0:T(8,128)(2,1)}, bf16[128,2048]{1,0:T(8,128)(2,1)S(1)}, u32[]{:S(2)}, u32[]{:S(2)}) collective-permute-start(bf16[128,2048]{1,0:T(8,128)(2,1)} %get-tuple-element.23), channel_id=1, source_target_pairs={{0,1},{1,2},{2,3},{3,0},{4,5},{5,6},{6,7},{7,4},{8,9},{9,10},{10,1... | collective-permute-start | bytes 1572872 | tf_op jit(solution)/shard_map/ppermute | solution.py:19
  37.4 15.7 %collective-permute-start.5 = (bf16[128,2048]{1,0:T(8,128)(2,1)}, bf16[128,2048]{1,0:T(8,128)(2,1)S(1)}, u32[]{:S(2)}, u32[]{:S(2)}) collective-permute-start(bf16[128,2048]{1,0:T(8,128)(2,1)} %get-tuple-element.24), channel_id=1, source_target_pairs={{0,3},{1,0},{2,1},{3,2},{4,7},{5,4},{6,5},{7,6},{8,11},{9,8},{10,9... | collective-permute-start | bytes 1572872 | tf_op jit(solution)/shard_map/ppermute | solution.py:19
  40.8 23.6 %collective-permute-start.7 = (bf16[128,2048]{1,0:T(8,128)(2,1)S(1)}, bf16[128,2048]{1,0:T(8,128)(2,1)S(1)}, u32[]{:S(2)}, u32[]{:S(2)}) collective-permute-start(bf16[128,2048]{1,0:T(8,128)(2,1)S(1)} %add_convert_fusion.2), channel_id=1, source_target_pairs={{0,3},{1,0},{2,1},{3,2},{4,7},{5,4},{6,5},{7,6},{8,11},{9,8},{10,9... | collective-permute-start | bytes 1572872 | tf_op jit(solution)/shard_map/ppermute | solution.py:19
  42.0 22.3 %collective-permute-start.3 = (bf16[128,2048]{1,0:T(8,128)(2,1)S(1)}, bf16[128,2048]{1,0:T(8,128)(2,1)S(1)}, u32[]{:S(2)}, u32[]{:S(2)}) collective-permute-start(bf16[128,2048]{1,0:T(8,128)(2,1)S(1)} %add_convert_fusion.3), channel_id=1, source_target_pairs={{0,1},{1,2},{2,3},{3,0},{4,5},{5,6},{6,7},{7,4},{8,9},{9,10},{10,1... | collective-permute-start | bytes 1572872 | tf_op jit(solution)/shard_map/ppermute | solution.py:19
  51.9 12.5 %copy-start.8 = (bf16[128,2048]{1,0:T(8,128)(2,1)}, bf16[128,2048]{1,0:T(8,128)(2,1)S(1)}, u32[]{:S(2)}) copy-start(bf16[128,2048]{1,0:T(8,128)(2,1)S(1)} %collective-permute-done.4.refs_4_) | copy-start | bytes 1572868
  53.1 11.3 %copy-start.9 = (bf16[128,2048]{1,0:T(8,128)(2,1)}, bf16[128,2048]{1,0:T(8,128)(2,1)S(1)}, u32[]{:S(2)}) copy-start(bf16[128,2048]{1,0:T(8,128)(2,1)S(1)} %collective-permute-done.5.refs_5_) | copy-start | bytes 1572868
  64.3 0.8 copy-start.12
  64.4 1.0 copy-start.14
  70.2 26.1 %collective-permute-start.8 = (bf16[256,2048]{1,0:T(8,128)(2,1)}, bf16[256,2048]{1,0:T(8,128)(2,1)S(1)}, u32[]{:S(2)}, u32[]{:S(2)}) collective-permute-start(bf16[256,2048]{1,0:T(8,128)(2,1)} %norm.2.refs_0_), channel_id=1, source_target_pairs={{0,1},{1,2},{2,3},{3,0},{4,5},{5,6},{6,7},{7,4},{8,9},{9,10},{10,1... | collective-permute-start | bytes 3145736 | tf_op jit(solution)/shard_map/ppermute | solution.py:19
  71.4 27.7 %collective-permute-start.9 = (bf16[256,2048]{1,0:T(8,128)(2,1)}, bf16[256,2048]{1,0:T(8,128)(2,1)S(1)}, u32[]{:S(2)}, u32[]{:S(2)}) collective-permute-start(bf16[256,2048]{1,0:T(8,128)(2,1)} %norm.2.refs_0_), channel_id=1, source_target_pairs={{0,3},{1,0},{2,1},{3,2},{4,7},{5,4},{6,5},{7,6},{8,11},{9,8},{10,9... | collective-permute-start | bytes 3145736 | tf_op jit(solution)/shard_map/ppermute | solution.py:19
  96.3 14.2 %collective-permute-start.10 = (bf16[128,2048]{1,0:T(8,128)(2,1)S(1)}, bf16[128,2048]{1,0:T(8,128)(2,1)S(1)}, u32[]{:S(2)}, u32[]{:S(2)}) collective-permute-start(bf16[128,2048]{1,0:T(8,128)(2,1)S(1)} %slice.16), channel_id=1, source_target_pairs={{0,1},{1,2},{2,3},{3,0},{4,5},{5,6},{6,7},{7,4},{8,9},{9,10},{10,1... | collective-permute-start | bytes 1572872 | tf_op jit(solution)/shard_map/ppermute | solution.py:19
  99.2 14.9 %collective-permute-start.11 = (bf16[128,2048]{1,0:T(8,128)(2,1)S(1)}, bf16[128,2048]{1,0:T(8,128)(2,1)S(1)}, u32[]{:S(2)}, u32[]{:S(2)}) collective-permute-start(bf16[128,2048]{1,0:T(8,128)(2,1)S(1)} %slice.17), channel_id=1, source_target_pairs={{0,3},{1,0},{2,1},{3,2},{4,7},{5,4},{6,5},{7,6},{8,11},{9,8},{10,9... | collective-permute-start | bytes 1572872 | tf_op jit(solution)/shard_map/ppermute | solution.py:19
  114.8 1.0 copy-start.3
  115.9 1.0 copy-start.5
  116.9 29.7 %copy-start = (bf16[256,2048]{1,0:T(8,128)(2,1)S(1)}, bf16[256,2048]{1,0:T(8,128)(2,1)}, u32[]{:S(2)}) copy-start(bf16[256,2048]{1,0:T(8,128)(2,1)} %norm.2.refs_0_) | copy-start | bytes 3145732
  124.9 18.0 %collective-permute-start.16 = (bf16[128,2048]{1,0:T(8,128)(2,1)S(1)}, bf16[128,2048]{1,0:T(8,128)(2,1)S(1)}, u32[]{:S(2)}, u32[]{:S(2)}) collective-permute-start(bf16[128,2048]{1,0:T(8,128)(2,1)S(1)} %get-tuple-element.32), channel_id=1, source_target_pairs={{0,3},{1,0},{2,1},{3,2},{4,7},{5,4},{6,5},{7,6},{8,11},{9,8},{10,9... | collective-permute-start | bytes 1572872 | tf_op jit(solution)/shard_map/ppermute | solution.py:19
  125.0 18.1 %collective-permute-start.12 = (bf16[128,2048]{1,0:T(8,128)(2,1)S(1)}, bf16[128,2048]{1,0:T(8,128)(2,1)S(1)}, u32[]{:S(2)}, u32[]{:S(2)}) collective-permute-start(bf16[128,2048]{1,0:T(8,128)(2,1)S(1)} %get-tuple-element.28), channel_id=1, source_target_pairs={{0,1},{1,2},{2,3},{3,0},{4,5},{5,6},{6,7},{7,4},{8,9},{9,10},{10,1... | collective-permute-start | bytes 1572872 | tf_op jit(solution)/shard_map/ppermute | solution.py:19
  140.9 14.9 %collective-permute-start.14 = (bf16[128,2048]{1,0:T(8,128)(2,1)S(1)}, bf16[128,2048]{1,0:T(8,128)(2,1)S(1)}, u32[]{:S(2)}, u32[]{:S(2)}) collective-permute-start(bf16[128,2048]{1,0:T(8,128)(2,1)S(1)} %get-tuple-element.29), channel_id=1, source_target_pairs={{0,1},{1,2},{2,3},{3,0},{4,5},{5,6},{6,7},{7,4},{8,9},{9,10},{10,1... | collective-permute-start | bytes 1572872 | tf_op jit(solution)/shard_map/ppermute | solution.py:19
  140.9 16.1 %collective-permute-start.15 = (bf16[128,2048]{1,0:T(8,128)(2,1)S(1)}, bf16[128,2048]{1,0:T(8,128)(2,1)S(1)}, u32[]{:S(2)}, u32[]{:S(2)}) collective-permute-start(bf16[128,2048]{1,0:T(8,128)(2,1)S(1)} %get-tuple-element.30), channel_id=1, source_target_pairs={{0,3},{1,0},{2,1},{3,2},{4,7},{5,4},{6,5},{7,6},{8,11},{9,8},{10,9... | collective-permute-start | bytes 1572872 | tf_op jit(solution)/shard_map/ppermute | solution.py:19
  143.1 22.5 %collective-permute-start.17 = (bf16[128,2048]{1,0:T(8,128)(2,1)S(1)}, bf16[128,2048]{1,0:T(8,128)(2,1)S(1)}, u32[]{:S(2)}, u32[]{:S(2)}) collective-permute-start(bf16[128,2048]{1,0:T(8,128)(2,1)S(1)} %add_convert_fusion), channel_id=1, source_target_pairs={{0,3},{1,0},{2,1},{3,2},{4,7},{5,4},{6,5},{7,6},{8,11},{9,8},{10,9... | collective-permute-start | bytes 1572872 | tf_op jit(solution)/shard_map/ppermute | solution.py:19
  143.3 22.3 %collective-permute-start.13 = (bf16[128,2048]{1,0:T(8,128)(2,1)S(1)}, bf16[128,2048]{1,0:T(8,128)(2,1)S(1)}, u32[]{:S(2)}, u32[]{:S(2)}) collective-permute-start(bf16[128,2048]{1,0:T(8,128)(2,1)S(1)} %add_convert_fusion.1), channel_id=1, source_target_pairs={{0,1},{1,2},{2,3},{3,0},{4,5},{5,6},{6,7},{7,4},{8,9},{9,10},{10,1... | collective-permute-start | bytes 1572872 | tf_op jit(solution)/shard_map/ppermute | solution.py:19
  154.4 1.0 copy-start.1
  155.7 9.9 %copy-start.10 = (bf16[128,2048]{1,0:T(8,128)(2,1)}, bf16[128,2048]{1,0:T(8,128)(2,1)S(1)}, u32[]{:S(2)}) copy-start(bf16[128,2048]{1,0:T(8,128)(2,1)S(1)} %collective-permute-done.14.refs_3_) | copy-start | bytes 1572868
  157.0 8.6 %copy-start.11 = (bf16[128,2048]{1,0:T(8,128)(2,1)}, bf16[128,2048]{1,0:T(8,128)(2,1)S(1)}, u32[]{:S(2)}) copy-start(bf16[128,2048]{1,0:T(8,128)(2,1)S(1)} %collective-permute-done.15.refs_4_) | copy-start | bytes 1572868
  165.6 0.8 copy-start.13
  165.6 1.0 copy-start.15
  (3 other events, 2.2 us)
Sparse Core Ops, SparseCore 0:
  9.6 74.8 all-gather.1

commit v5 on v4

--- a/solution.py
+++ b/solution.py
@@ -31,14 +31,23 @@
 def attend_kernel(
     place, sink, q_ref, before_ref, mid_ref, after_ref, w_ref, *refs, rel, n_sp, tok_rows
 ):
-    *out_refs, kv_ref = refs
+    *out_refs, kv_ref, weight_ref, sems = refs
     step = pl.program_id(0)
+    kv_copies = [
+        pltpu.make_async_copy(ref, kv_ref.at[:, pl.ds(at, ref.shape[1])], sems.at[index])
+        for index, (ref, at) in enumerate(
+            ((before_ref, 0), (mid_ref, WINDOW), (after_ref, WINDOW + tok_rows))
+        )
+    ]
+    weight_copy = pltpu.make_async_copy(w_ref, weight_ref, sems.at[3])
 
     @pl.when(step == 0)
     def _():
-        kv_ref[:, :WINDOW] = before_ref[...]
-        kv_ref[:, WINDOW : WINDOW + tok_rows] = mid_ref[...]
-        kv_ref[:, WINDOW + tok_rows :] = after_ref[...]
+        for copy in kv_copies:
+            copy.start()
+        weight_copy.start()
+        for copy in kv_copies:
+            copy.wait()
 
     rows = q_ref.shape[0]
     quarter = (place[0] + rel(step)) % (tok_rows // rows)
@@ -100,7 +109,12 @@
             mixed.append(jnp.where(low, first, second).astype(jnp.bfloat16))
         finished.append(jnp.concatenate(mixed, axis=1))
     attended = jnp.concatenate(finished, axis=0)
-    projected = jnp.dot(attended, w_ref[...], preferred_element_type=jnp.float32).astype(
+
+    @pl.when(step == 0)
+    def _():
+        weight_copy.wait()
+
+    projected = jnp.dot(attended, weight_ref[...], preferred_element_type=jnp.float32).astype(
         jnp.bfloat16
     )
     half = rows // 2
@@ -117,9 +131,7 @@
     rows = tok_rows // n_tp
     cols = out_weight.shape[1]
 
-    def whole(array):
-        return pl.BlockSpec(array.shape, lambda i, place, sink: (0,) * array.ndim)
-
+    anywhere = pl.BlockSpec(memory_space=pl.ANY)
     return pl.pallas_call(
         functools.partial(attend_kernel, rel=rel, n_sp=n_sp, tok_rows=tok_rows),
         grid_spec=pltpu.PrefetchScalarGridSpec(
@@ -127,57 +139,90 @@
             grid=(steps,),
             in_specs=[
                 pl.BlockSpec((rows, width), lambda i, place, sink: ((place[0] + rel(i)) % n_tp, 0)),
-                whole(before),
-                whole(middle),
-                whole(after),
-                whole(out_weight),
+                anywhere,
+                anywhere,
+                anywhere,
+                anywhere,
             ],
             out_specs=[pl.BlockSpec((rows // 2, cols), lambda i, place, sink: (0, 0))] * (2 * steps),
             scratch_shapes=[
-                pltpu.VMEM((2, tok_rows + 2 * WINDOW, middle.shape[2]), jnp.bfloat16)
+                pltpu.VMEM((2, tok_rows + 2 * WINDOW, middle.shape[2]), jnp.bfloat16),
+                pltpu.VMEM(out_weight.shape, jnp.bfloat16),
+                pltpu.SemaphoreType.DMA((4,)),
             ],
         ),
         out_shape=[jax.ShapeDtypeStruct((rows // 2, cols), jnp.bfloat16)] * (2 * steps),
+        compiler_params=pltpu.CompilerParams(vmem_limit_bytes=24 * 1024 * 1024),
         name="attend",
     )(place, sink, queries, before, middle, after, out_weight)
 
 
-def normed(refs, gain, bias):
-    values = refs[0][...].astype(jnp.float32)
-    for ref in refs[1:]:
-        values = values + ref[...].astype(jnp.float32)
-    width = values.shape[1]
-    mean = jnp.sum(values, axis=-1, keepdims=True) * (1.0 / width)
-    centred = values - mean
-    variance = jnp.sum(centred * centred, axis=-1, keepdims=True) * (1.0 / width)
-    return (centred * lax.rsqrt(variance + 1e-06) * gain[...] + bias[...]).astype(jnp.bfloat16)
-
-
-def norm_kernel(*refs, whole):
-    *parts, gain, bias, out_ref = refs
-    for side in range(2):
-
-        @pl.when(pl.program_id(0) // (pl.num_programs(0) // 2) == side)
-        def _():
-            out_ref[...] = normed(parts[:whole] + parts[whole + side :: 2], gain, bias)
-
-
-def norm_rows(wholes, halves, gain, bias, block=64):
-    rows, width = wholes[0].shape
+def norm_kernel(*refs, tops, bottoms, outs, block):
+    count = max(max(tops), max(bottoms)) + 1
+    sources, (gain, bias), results = (refs[:count], refs[count : count + 2], refs[count + 2 : -3])
+    parts, out, sems = refs[-3:]
+    rows, width = out.shape
     steps = rows // block
     half = steps // 2
-    tile = pl.BlockSpec((block, width), lambda i: (i, 0))
-    tops = pl.BlockSpec((block, width), lambda i: (jnp.minimum(i, half - 1), 0))
-    bottoms = pl.BlockSpec((block, width), lambda i: (jnp.maximum(i - half, 0), 0))
-    line = pl.BlockSpec((1, width), lambda i: (0, 0))
+
+    def in_copy(step, place):
+        ref = sources[(tops if step < half else bottoms)[place]]
+        at = step * block % ref.shape[0]
+        return pltpu.make_async_copy(
+            ref.at[pl.ds(at, block)],
+            parts.at[place, pl.ds(step * block, block)],
+            sems.at[step * (len(tops) + 1) + place],
+        )
+
+    def out_copy(step):
+        ref = results[step * block // (rows // outs)]
+        at = step * block % ref.shape[0]
+        return pltpu.make_async_copy(
+            out.at[pl.ds(step * block, block)],
+            ref.at[pl.ds(at, block)],
+            sems.at[step * (len(tops) + 1) + len(tops)],
+        )
+
+    for step in range(steps):
+        for place in range(len(tops)):
+            in_copy(step, place).start()
+    for step in range(steps):
+        span = slice(step * block, (step + 1) * block)
+        values = None
+        for place in range(len(tops)):
+            in_copy(step, place).wait()
+        for place in range(len(tops)):
+            part = parts[place, span].astype(jnp.float32)
+            values = part if values is None else values + part
+        mean = jnp.sum(values, axis=-1, keepdims=True) * (1.0 / width)
+        centred = values - mean
+        variance = jnp.sum(centred * centred, axis=-1, keepdims=True) * (1.0 / width)
+        out[span] = (centred * lax.rsqrt(variance + 1e-06) * gain[...] + bias[...]).astype(
+            jnp.bfloat16
+        )
+        out_copy(step).start()
+    for step in range(steps):
+        out_copy(step).wait()
+
+
+def norm_rows(sources, tops, bottoms, outs, gain, bias, rows, block=64):
+    width = sources[0].shape[1]
+    anywhere = pl.BlockSpec(memory_space=pl.ANY)
+    vmem = pl.BlockSpec(memory_space=pltpu.VMEM)
+    steps = rows // block
     return pl.pallas_call(
-        functools.partial(norm_kernel, whole=len(wholes)),
-        grid=(steps,),
-        in_specs=[tile] * len(wholes) + [tops, bottoms] * (len(halves) // 2) + [line, line],
-        out_specs=tile,
-        out_shape=jax.ShapeDtypeStruct((rows, width), jnp.bfloat16),
+        functools.partial(norm_kernel, tops=tops, bottoms=bottoms, outs=outs, block=block),
+        in_specs=[anywhere] * len(sources) + [vmem, vmem],
+        out_specs=[anywhere] * outs,
+        out_shape=[jax.ShapeDtypeStruct((rows // outs, width), jnp.bfloat16)] * outs,
+        scratch_shapes=[
+            pltpu.VMEM((len(tops), rows, width), jnp.bfloat16),
+            pltpu.VMEM((rows, width), jnp.bfloat16),
+            pltpu.SemaphoreType.DMA((steps * (len(tops) + 1),)),
+        ],
+        compiler_params=pltpu.CompilerParams(vmem_limit_bytes=16 * 1024 * 1024),
         name="norm",
-    )(*wholes, *halves, gain[None], bias[None])
+    )(*sources, gain[None], bias[None])
 
 
 def added(part, arrived):
@@ -313,32 +358,52 @@
     own_top, own_bottom = run(1, lambda i: 0, n_tp, n_sp)
     left_sum = shift(added(right_top, from_left), 1)
     right_sum = shift(added(left_bottom, from_right), -1)
-    first = norm_rows(
-        (residual_in,),
-        (own_top, own_bottom, left_sum, left_plain, right_plain, right_sum),
+    rows, half = (2 * own_top.shape[0], own_top.shape[0])
+    first_top, first_bottom = norm_rows(
+        (residual_in, own_top, own_bottom, left_sum, left_plain, right_plain, right_sum),
+        (0, 1, 3, 5),
+        (0, 2, 4, 6),
+        2,
         norm1_gain,
         norm1_bias,
-    )
-
-    half = first.shape[0] // 2
-    row_left = shift(first, 1)
-    row_right = shift(first, -1)
-    row_ft = shift(row_left[:half], 1)
-    row_fb = shift(row_right[half:], -1)
-    left_top, left_bottom, right_top, right_bottom = feed_forward(
-        (row_left, row_right), weights, half
-    )
+        rows,
+    )
+
+    row_lt = shift(first_top, 1)
+    row_rb = shift(first_bottom, -1)
+    row_lb = shift(first_bottom, 1)
+    row_rt = shift(first_top, -1)
+    row_ft = shift(row_lt, 1)
+    row_fb = shift(row_rb, -1)
+    left_top, right_bottom = feed_forward((row_lt, row_rb), weights, half)
     left_plain = shift(right_bottom, 1)
     right_plain = shift(left_top, -1)
     far_top, far_bottom = feed_forward((row_ft, row_fb), weights, half)
     from_left = shift(far_top, 1)
     from_right = shift(far_bottom, -1)
-    (own,) = feed_forward((first,), weights, 2 * half)
+    left_bottom, right_top = feed_forward((row_lb, row_rt), weights, half)
     left_sum = shift(added(right_top, from_left), 1)
     right_sum = shift(added(left_bottom, from_right), -1)
-    return norm_rows(
-        (first, own), (left_sum, left_plain, right_plain, right_sum), norm2_gain, norm2_bias
-    )
+    own_top, own_bottom = feed_forward((first_top, first_bottom), weights, half)
+    (out,) = norm_rows(
+        (
+            first_top,
+            first_bottom,
+            own_top,
+            own_bottom,
+            left_sum,
+            left_plain,
+            right_plain,
+            right_sum,
+        ),
+        (0, 2, 4, 6),
+        (1, 3, 5, 7),
+        1,
+        norm2_gain,
+        norm2_bias,
+        rows,
+    )
+    return out
 
 
 def solution(mesh):

time: 179 us -> 156 us (0.87)
  the two profiles are of different devices: /device:TPU:14 before, /device:TPU:1 now
where the time goes in v5:
time: 156 us; the launch traced here: 153 us
  Pallas kernels  50.1 us (32%)
  waiting for transfers between devices  49.2 us (32%)
  starting transfers between devices  28.2 us (18%)
  between operations  13.6 us (9%)
  local copies, waits for them, and re-layouts  9.4 us (6%)
  other arithmetic  2.46 us (2%)
    ppermute x18, waiting for transfers between devices, shift(): lax.ppermute(value, axis, [(i, (i + step) % devices) for i in range(devic...  47.3 us
    pallas_call x4, Pallas kernels, feed_forward(): pl.pallas_call(functools.partial(feed_kernel, count=count, outs=outs, chu...  31.7 us
    ppermute x18, starting transfers between devices, shift(): lax.ppermute(value, axis, [(i, (i + step) % devices) for i in range(devic...  21.7 us
    pallas_call x3, Pallas kernels, attend(): pl.pallas_call(functools.partial(attend_kernel, rel=rel, n_sp=n_sp, tok_r...  14 us
    unnamed x26, local copies, waits for them, and re-layouts  8.41 us
    pallas_call x2, Pallas kernels, norm_rows(): pl.pallas_call(functools.partial(norm_kernel, tops=tops, bottoms=bottoms,...  4.43 us
    ppermute x1, starting transfers between devices, halo(): after = lax.ppermute(shard[:, :width], axis, down)  3.29 us
    ppermute x1, starting transfers between devices, halo(): before = lax.ppermute(shard[:, length - width:], axis, up)  3.21 us
  transfers between devices with their start and end apart: 21, of which 10 were waited for; matrix products, arithmetic and copies ran while one was open for 1% of the time, Pallas kernels for 31%

profile of v5, /device:TPU:1, one launch (start us, length us, event | category | flops | bytes accessed | tf_op | source)
XLA Modules:
  0.0 153.0 jit_solution(5497186023106239403)
XLA Ops:
  6.5 2.0 %pad_maximum_fusion = bf16[128,2048]{1,0:T(8,128)(2,1)} fusion(bf16[64,2048]{1,0:T(8,128)(2,1)} %bitcast.14, bf16[64,2048]{1,0:T(8,128)(2,1)} %param.18), kind=kLoop, calls=%fused_computation.4 | loop fusion | flops 1048576 | bytes 1048576 | tf_op jit(solution)/shard_map/concatenate | solution.py:342
  9.5 3.3 %collective-permute-start.1 = (bf16[2,128,256]{2,1,0:T(8,128)(2,1)S(1)}, bf16[2,128,256]{2,1,0:T(8,128)(2,1)S(1)}, u32[]{:S(2)}, u32[]{:S(2)}) collective-permute-start(bf16[2,128,256]{2,1,0:T(8,128)(2,1)S(1)} %get-tuple-element.41), channel_id=1, source_target_pairs={{4,0},{8,4},{12,8},{16,12},{20,16},{24,20},{28,24},{32,28},{36,32}... | collective-permute-start | bytes 393224 | tf_op jit(solution)/shard_map/ppermute | solution.py:27
  12.8 3.2 %collective-permute-start = (bf16[2,128,256]{2,1,0:T(8,128)(2,1)S(1)}, bf16[2,128,256]{2,1,0:T(8,128)(2,1)S(1)}, u32[]{:S(2)}, u32[]{:S(2)}) collective-permute-start(bf16[2,128,256]{2,1,0:T(8,128)(2,1)S(1)} %get-tuple-element.42), channel_id=1, source_target_pairs={{0,4},{4,8},{8,12},{12,16},{16,20},{20,24},{24,28},{28,32},{32,36}... | collective-permute-start | bytes 393224 | tf_op jit(solution)/shard_map/ppermute | solution.py:26
  18.0 1.6 %copy-done = bf16[512,2048]{1,0:T(8,128)(2,1)S(1)} copy-done((bf16[512,2048]{1,0:T(8,128)(2,1)S(1)}, bf16[512,2048]{1,0:T(8,128)(2,1)}, u32[]{:S(2)}) %copy-start) | copy-done | bytes 2097176
  19.6 1.2 copy-done.1
  20.8 1.2 copy-done.2
  22.7 3.7 %attend.5 = (bf16[128,2048]{1,0:T(8,128)(2,1)S(1)}, bf16[128,2048]{1,0:T(8,128)(2,1)S(1)}) custom-call(s32[2]{0:T(128)S(1)} %compare_select_fusion.place, f32[8]{0:T(128)S(1)} %copy-done.12, bf16[1024,512]{1,0:T(8,128)(2,1)S(1)} %copy-done.2, bf16[2,128,256]{2,1,0:T(8,128)(2,1)S(1)} %collective-permute-done.before_ref, bf16[2,1024,256]{2,1,0:T(8,128)(2,1)S(1)} %copy-done.1, ...), custom_call_target="tpu_custom_call" | custom-call | tf_op jit(solution)/shard_map/attend/pallas_call | solution.py:135
  26.3 1.3 collective-permute-start.2
  27.6 1.5 collective-permute-start.6
  29.1 6.6 %attend.4 = (bf16[128,2048]{1,0:T(8,128)(2,1)S(1)}, bf16[128,2048]{1,0:T(8,128)(2,1)S(1)}, bf16[128,2048]{1,0:T(8,128)(2,1)S(1)}, bf16[128,2048]{1,0:T(8,128)(2,1)S(1)}) custom-call(s32[2]{0:T(128)S(1)} %compare_select_fusion.place, f32[8]{0:T(128)S(1)} %copy-done.12, bf16[1024,512]{1,0:T(8,128)(2,1)S(1)} %copy-done.2, ...), custom_call_target="tpu_custom_call" | custom-call | tf_op jit(solution)/shard_map/attend/pallas_call | solution.py:135
  35.8 2.7 %collective-permute-start.5 = (bf16[128,2048]{1,0:T(8,128)(2,1)S(1)}, bf16[128,2048]{1,0:T(8,128)(2,1)S(1)}, u32[]{:S(2)}, u32[]{:S(2)}) collective-permute-start(bf16[128,2048]{1,0:T(8,128)(2,1)S(1)} %get-tuple-element.28), channel_id=1, source_target_pairs={{0,3},{1,0},{2,1},{3,2},{4,7},{5,4},{6,5},{7,6},{8,11},{9,8},{10,9... | collective-permute-start | bytes 1572872 | tf_op jit(solution)/shard_map/ppermute | solution.py:19
  38.5 3.1 %collective-permute-done.2 = bf16[128,2048]{1,0:T(8,128)(2,1)S(1)} collective-permute-done((bf16[128,2048]{1,0:T(8,128)(2,1)S(1)}, bf16[128,2048]{1,0:T(8,128)(2,1)S(1)}, u32[]{:S(2)}, u32[]{:S(2)}) %collective-permute-start.2) | collective-permute-done | bytes 524320 | tf_op jit(solution)/shard_map/ppermute | solution.py:19
  41.9 2.9 %collective-permute-start.7 = (bf16[128,2048]{1,0:T(8,128)(2,1)S(1)}, bf16[128,2048]{1,0:T(8,128)(2,1)S(1)}, u32[]{:S(2)}, u32[]{:S(2)}) collective-permute-start(bf16[128,2048]{1,0:T(8,128)(2,1)S(1)} %add_convert_fusion.2), channel_id=1, source_target_pairs={{0,3},{1,0},{2,1},{3,2},{4,7},{5,4},{6,5},{7,6},{8,11},{9,8},{10,9... | collective-permute-start | bytes 1572872 | tf_op jit(solution)/shard_map/ppermute | solution.py:19
  44.8 3.7 %attend.3 = (bf16[128,2048]{1,0:T(8,128)(2,1)S(1)}, bf16[128,2048]{1,0:T(8,128)(2,1)S(1)}) custom-call(s32[2]{0:T(128)S(1)} %compare_select_fusion.place, f32[8]{0:T(128)S(1)} %copy-done.12, bf16[1024,512]{1,0:T(8,128)(2,1)S(1)} %copy-done.2, bf16[2,128,256]{2,1,0:T(8,128)(2,1)S(1)} %collective-permute-done.before_ref, bf16[2,1024,256]{2,1,0:T(8,128)(2,1)S(1)} %copy-done.1, ...), custom_call_target="tpu_custom_call" | custom-call | tf_op jit(solution)/shard_map/attend/pallas_call | solution.py:135
  48.5 4.4 %collective-permute-done.4.refs_4_ = bf16[128,2048]{1,0:T(8,128)(2,1)S(1)} collective-permute-done((bf16[128,2048]{1,0:T(8,128)(2,1)S(1)}, bf16[128,2048]{1,0:T(8,128)(2,1)S(1)}, u32[]{:S(2)}, u32[]{:S(2)}) %collective-permute-start.4) | collective-permute-done | bytes 524320 | tf_op jit(solution)/shard_map/ppermute | solution.py:19
  52.9 9.9 %collective-permute-done.3.refs_3_ = bf16[128,2048]{1,0:T(8,128)(2,1)S(1)} collective-permute-done((bf16[128,2048]{1,0:T(8,128)(2,1)S(1)}, bf16[128,2048]{1,0:T(8,128)(2,1)S(1)}, u32[]{:S(2)}, u32[]{:S(2)}) %collective-permute-start.3) | collective-permute-done | bytes 524320 | tf_op jit(solution)/shard_map/ppermute | solution.py:19
  63.2 1.9 %norm.2 = (bf16[128,2048]{1,0:T(8,128)(2,1)S(1)}, bf16[128,2048]{1,0:T(8,128)(2,1)S(1)}) custom-call(bf16[256,2048]{1,0:T(8,128)(2,1)S(1)} %copy-done.3, bf16[128,2048]{1,0:T(8,128)(2,1)S(1)} %get-tuple-element.23.refs_1_, bf16[128,2048]{1,0:T(8,128)(2,1)S(1)} %get-tuple-element.24.refs_2_, bf16[128,2048]{1,0:T(8,128)(2,1)S(1)} %collective-permute-done.3.refs_3_, ...), custom_call_target="tpu_custom_call" | custom-call | tf_op jit(solution)/shard_map/norm/pallas_call | solution.py:213
  65.2 1.3 collective-permute-start.10
  66.4 1.5 collective-permute-start.12
  67.9 12.4 %collective-permute-done.10.refs_0_ = bf16[128,2048]{1,0:T(8,128)(2,1)S(1)} collective-permute-done((bf16[128,2048]{1,0:T(8,128)(2,1)S(1)}, bf16[128,2048]{1,0:T(8,128)(2,1)S(1)}, u32[]{:S(2)}, u32[]{:S(2)}) %collective-permute-start.10) | collective-permute-done | bytes 524320 | tf_op jit(solution)/shard_map/ppermute | solution.py:19
  80.4 2.7 %collective-permute-start.13 = (bf16[128,2048]{1,0:T(8,128)(2,1)S(1)}, bf16[128,2048]{1,0:T(8,128)(2,1)S(1)}, u32[]{:S(2)}, u32[]{:S(2)}) collective-permute-start(bf16[128,2048]{1,0:T(8,128)(2,1)S(1)} %collective-permute-done.12.refs_1_), channel_id=1, source_target_pairs={{0,3},{1,0},{2,1},{3,2},{4,7},{5,4},{6,5},{7,6},{8,11},{9,8},{10,9... | collective-permute-start | bytes 1572872 | tf_op jit(solution)/shard_map/ppermute | solution.py:19
  84.5 10.4 %collective-permute-done.11.refs_0_ = bf16[128,2048]{1,0:T(8,128)(2,1)S(1)} collective-permute-done((bf16[128,2048]{1,0:T(8,128)(2,1)S(1)}, bf16[128,2048]{1,0:T(8,128)(2,1)S(1)}, u32[]{:S(2)}, u32[]{:S(2)}) %collective-permute-start.11) | collective-permute-done | bytes 524320 | tf_op jit(solution)/shard_map/ppermute | solution.py:19
  98.6 7.9 %feed.6 = (bf16[128,2048]{1,0:T(8,128)(2,1)S(1)}, bf16[128,2048]{1,0:T(8,128)(2,1)S(1)}) custom-call(bf16[128,2048]{1,0:T(8,128)(2,1)S(1)} %copy-done.5, bf16[128,2048]{1,0:T(8,128)(2,1)S(1)} %copy-done.7, bf16[32,2,64,2048]{3,2,1,0:T(8,128)(2,1)} %bitcast.10), custom_call_target="tpu_custom_call" | custom-call | tf_op jit(solution)/shard_map/feed/pallas_call | solution.py:309
  106.5 1.7 %collective-permute-start.18 = (bf16[128,2048]{1,0:T(8,128)(2,1)S(1)}, bf16[128,2048]{1,0:T(8,128)(2,1)S(1)}, u32[]{:S(2)}, u32[]{:S(2)}) collective-permute-start(bf16[128,2048]{1,0:T(8,128)(2,1)S(1)} %get-tuple-element.40), channel_id=1, source_target_pairs={{0,3},{1,0},{2,1},{3,2},{4,7},{5,4},{6,5},{7,6},{8,11},{9,8},{10,9... | collective-permute-start | bytes 1572872 | tf_op jit(solution)/shard_map/ppermute | solution.py:19
  108.2 7.9 %feed.7 = (bf16[128,2048]{1,0:T(8,128)(2,1)S(1)}, bf16[128,2048]{1,0:T(8,128)(2,1)S(1)}) custom-call(bf16[128,2048]{1,0:T(8,128)(2,1)S(1)} %collective-permute-done.10.refs_0_, bf16[128,2048]{1,0:T(8,128)(2,1)S(1)} %collective-permute-done.12.refs_1_, bf16[32,2,64,2048]{3,2,1,0:T(8,128)(2,1)} %bitcast.11), custom_call_target="tpu_custom_call" | custom-call | tf_op jit(solution)/shard_map/feed/pallas_call | solution.py:309
  116.3 2.7 %collective-permute-start.17 = (bf16[128,2048]{1,0:T(8,128)(2,1)S(1)}, bf16[128,2048]{1,0:T(8,128)(2,1)S(1)}, u32[]{:S(2)}, u32[]{:S(2)}) collective-permute-start(bf16[128,2048]{1,0:T(8,128)(2,1)S(1)} %get-tuple-element.38), channel_id=1, source_target_pairs={{0,3},{1,0},{2,1},{3,2},{4,7},{5,4},{6,5},{7,6},{8,11},{9,8},{10,9... | collective-permute-start | bytes 1572872 | tf_op jit(solution)/shard_map/ppermute | solution.py:19
  119.0 7.9 %feed.5 = (bf16[128,2048]{1,0:T(8,128)(2,1)S(1)}, bf16[128,2048]{1,0:T(8,128)(2,1)S(1)}) custom-call(bf16[128,2048]{1,0:T(8,128)(2,1)S(1)} %collective-permute-done.8.refs_0_, bf16[128,2048]{1,0:T(8,128)(2,1)S(1)} %collective-permute-done.9.refs_1_, bf16[32,2,64,2048]{3,2,1,0:T(8,128)(2,1)} %bitcast.12), custom_call_target="tpu_custom_call" | custom-call | tf_op jit(solution)/shard_map/feed/pallas_call | solution.py:309
  127.1 1.4 collective-permute-start.19
  129.0 7.9 %feed.4 = (bf16[128,2048]{1,0:T(8,128)(2,1)S(1)}, bf16[128,2048]{1,0:T(8,128)(2,1)S(1)}) custom-call(bf16[128,2048]{1,0:T(8,128)(2,1)S(1)} %get-tuple-element.31.refs_0_, bf16[128,2048]{1,0:T(8,128)(2,1)S(1)} %get-tuple-element.32.refs_1_, bf16[32,2,64,2048]{3,2,1,0:T(8,128)(2,1)} %bitcast.13), custom_call_target="tpu_custom_call" | custom-call | tf_op jit(solution)/shard_map/feed/pallas_call | solution.py:309
  137.0 4.5 %collective-permute-done.19.refs_7_ = bf16[128,2048]{1,0:T(8,128)(2,1)S(1)} collective-permute-done((bf16[128,2048]{1,0:T(8,128)(2,1)S(1)}, bf16[128,2048]{1,0:T(8,128)(2,1)S(1)}, u32[]{:S(2)}, u32[]{:S(2)}) %collective-permute-start.19) | collective-permute-done | bytes 524320 | tf_op jit(solution)/shard_map/ppermute | solution.py:19
  141.5 2.1 %collective-permute-done.15.refs_4_ = bf16[128,2048]{1,0:T(8,128)(2,1)S(1)} collective-permute-done((bf16[128,2048]{1,0:T(8,128)(2,1)S(1)}, bf16[128,2048]{1,0:T(8,128)(2,1)S(1)}, u32[]{:S(2)}, u32[]{:S(2)}) %collective-permute-start.15) | collective-permute-done | bytes 524320 | tf_op jit(solution)/shard_map/ppermute | solution.py:19
  143.6 2.5 %norm.3 = bf16[256,2048]{1,0:T(8,128)(2,1)} custom-call(bf16[128,2048]{1,0:T(8,128)(2,1)S(1)} %get-tuple-element.31.refs_0_, bf16[128,2048]{1,0:T(8,128)(2,1)S(1)} %get-tuple-element.32.refs_1_, bf16[128,2048]{1,0:T(8,128)(2,1)S(1)} %get-tuple-element.33.refs_2_, bf16[128,2048]{1,0:T(8,128)(2,1)S(1)} %get-tuple-element.34.refs_3_, ...), custom_call_target="tpu_custom_call" | custom-call | tf_op jit(solution)/shard_map/norm/pallas_call | solution.py:213
  (53 shorter events, 10.3 us)
Async XLA Ops:
  6.5 56.7 %copy-start.9 = (f32[2048]{0:T(1024)S(1)}, f32[2048]{0:T(1024)}, u32[]{:S(2)}) copy-start(f32[2048]{0:T(1024)} %param.17) | copy-start | bytes 24580
  6.5 56.7 %copy-start.8 = (f32[2048]{0:T(1024)S(1)}, f32[2048]{0:T(1024)}, u32[]{:S(2)}) copy-start(f32[2048]{0:T(1024)} %param.16) | copy-start | bytes 24580
  6.5 56.7 %copy-start.3 = (bf16[256,2048]{1,0:T(8,128)(2,1)S(1)}, bf16[256,2048]{1,0:T(8,128)(2,1)}, u32[]{:S(2)}) copy-start(bf16[256,2048]{1,0:T(8,128)(2,1)} %refs_0_.1) | copy-start | bytes 3145732
  6.5 90.0 %all-gather.2.cloned.1.call-start = ((), (), s32[]{:S(2)}) async-start(), calls=%async_computation | async-start | bytes 17301504 | tf_op jit(solution)/shard_map/all_gather | solution.py:343
  9.5 7.2 %collective-permute-start.1 = (bf16[2,128,256]{2,1,0:T(8,128)(2,1)S(1)}, bf16[2,128,256]{2,1,0:T(8,128)(2,1)S(1)}, u32[]{:S(2)}, u32[]{:S(2)}) collective-permute-start(bf16[2,128,256]{2,1,0:T(8,128)(2,1)S(1)} %get-tuple-element.41), channel_id=1, source_target_pairs={{4,0},{8,4},{12,8},{16,12},{20,16},{24,20},{28,24},{32,28},{36,32}... | collective-permute-start | bytes 393224 | tf_op jit(solution)/shard_map/ppermute | solution.py:27
  12.8 5.1 %collective-permute-start = (bf16[2,128,256]{2,1,0:T(8,128)(2,1)S(1)}, bf16[2,128,256]{2,1,0:T(8,128)(2,1)S(1)}, u32[]{:S(2)}, u32[]{:S(2)}) collective-permute-start(bf16[2,128,256]{2,1,0:T(8,128)(2,1)S(1)} %get-tuple-element.42), channel_id=1, source_target_pairs={{0,4},{4,8},{8,12},{12,16},{16,20},{20,24},{24,28},{28,32},{32,36}... | collective-permute-start | bytes 393224 | tf_op jit(solution)/shard_map/ppermute | solution.py:26
  18.0 1.6 %copy-start = (bf16[512,2048]{1,0:T(8,128)(2,1)S(1)}, bf16[512,2048]{1,0:T(8,128)(2,1)}, u32[]{:S(2)}) copy-start(bf16[512,2048]{1,0:T(8,128)(2,1)} %w_ref.5) | copy-start | bytes 6291460
  19.6 1.2 copy-start.1
  20.8 1.2 copy-start.2
  26.3 15.2 %collective-permute-start.2 = (bf16[128,2048]{1,0:T(8,128)(2,1)S(1)}, bf16[128,2048]{1,0:T(8,128)(2,1)S(1)}, u32[]{:S(2)}, u32[]{:S(2)}) collective-permute-start(bf16[128,2048]{1,0:T(8,128)(2,1)S(1)} %get-tuple-element.26), channel_id=1, source_target_pairs={{0,1},{1,2},{2,3},{3,0},{4,5},{5,6},{6,7},{7,4},{8,9},{9,10},{10,1... | collective-permute-start | bytes 1572872 | tf_op jit(solution)/shard_map/ppermute | solution.py:19
  27.6 14.2 %collective-permute-start.6 = (bf16[128,2048]{1,0:T(8,128)(2,1)S(1)}, bf16[128,2048]{1,0:T(8,128)(2,1)S(1)}, u32[]{:S(2)}, u32[]{:S(2)}) collective-permute-start(bf16[128,2048]{1,0:T(8,128)(2,1)S(1)} %get-tuple-element.30), channel_id=1, source_target_pairs={{0,3},{1,0},{2,1},{3,2},{4,7},{5,4},{6,5},{7,6},{8,11},{9,8},{10,9... | collective-permute-start | bytes 1572872 | tf_op jit(solution)/shard_map/ppermute | solution.py:19
  35.7 17.2 %collective-permute-start.4 = (bf16[128,2048]{1,0:T(8,128)(2,1)S(1)}, bf16[128,2048]{1,0:T(8,128)(2,1)S(1)}, u32[]{:S(2)}, u32[]{:S(2)}) collective-permute-start(bf16[128,2048]{1,0:T(8,128)(2,1)S(1)} %get-tuple-element.27), channel_id=1, source_target_pairs={{0,1},{1,2},{2,3},{3,0},{4,5},{5,6},{6,7},{7,4},{8,9},{9,10},{10,1... | collective-permute-start | bytes 1572872 | tf_op jit(solution)/shard_map/ppermute | solution.py:19
  35.8 17.1 %collective-permute-start.5 = (bf16[128,2048]{1,0:T(8,128)(2,1)S(1)}, bf16[128,2048]{1,0:T(8,128)(2,1)S(1)}, u32[]{:S(2)}, u32[]{:S(2)}) collective-permute-start(bf16[128,2048]{1,0:T(8,128)(2,1)S(1)} %get-tuple-element.28), channel_id=1, source_target_pairs={{0,3},{1,0},{2,1},{3,2},{4,7},{5,4},{6,5},{7,6},{8,11},{9,8},{10,9... | collective-permute-start | bytes 1572872 | tf_op jit(solution)/shard_map/ppermute | solution.py:19
  41.7 21.1 %collective-permute-start.3 = (bf16[128,2048]{1,0:T(8,128)(2,1)S(1)}, bf16[128,2048]{1,0:T(8,128)(2,1)S(1)}, u32[]{:S(2)}, u32[]{:S(2)}) collective-permute-start(bf16[128,2048]{1,0:T(8,128)(2,1)S(1)} %add_convert_fusion.3), channel_id=1, source_target_pairs={{0,1},{1,2},{2,3},{3,0},{4,5},{5,6},{6,7},{7,4},{8,9},{9,10},{10,1... | collective-permute-start | bytes 1572872 | tf_op jit(solution)/shard_map/ppermute | solution.py:19
  41.9 21.3 %collective-permute-start.7 = (bf16[128,2048]{1,0:T(8,128)(2,1)S(1)}, bf16[128,2048]{1,0:T(8,128)(2,1)S(1)}, u32[]{:S(2)}, u32[]{:S(2)}) collective-permute-start(bf16[128,2048]{1,0:T(8,128)(2,1)S(1)} %add_convert_fusion.2), channel_id=1, source_target_pairs={{0,3},{1,0},{2,1},{3,2},{4,7},{5,4},{6,5},{7,6},{8,11},{9,8},{10,9... | collective-permute-start | bytes 1572872 | tf_op jit(solution)/shard_map/ppermute | solution.py:19
  65.2 15.2 %collective-permute-start.10 = (bf16[128,2048]{1,0:T(8,128)(2,1)S(1)}, bf16[128,2048]{1,0:T(8,128)(2,1)S(1)}, u32[]{:S(2)}, u32[]{:S(2)}) collective-permute-start(bf16[128,2048]{1,0:T(8,128)(2,1)S(1)} %get-tuple-element.31.refs_0_), channel_id=1, source_target_pairs={{0,1},{1,2},{2,3},{3,0},{4,5},{5,6},{6,7},{7,4},{8,9},{9,10},{10,1... | collective-permute-start | bytes 1572872 | tf_op jit(solution)/shard_map/ppermute | solution.py:19
  66.4 13.9 %collective-permute-start.12 = (bf16[128,2048]{1,0:T(8,128)(2,1)S(1)}, bf16[128,2048]{1,0:T(8,128)(2,1)S(1)}, u32[]{:S(2)}, u32[]{:S(2)}) collective-permute-start(bf16[128,2048]{1,0:T(8,128)(2,1)S(1)} %get-tuple-element.32.refs_1_), channel_id=1, source_target_pairs={{0,3},{1,0},{2,1},{3,2},{4,7},{5,4},{6,5},{7,6},{8,11},{9,8},{10,9... | collective-permute-start | bytes 1572872 | tf_op jit(solution)/shard_map/ppermute | solution.py:19
  80.3 14.6 %collective-permute-start.11 = (bf16[128,2048]{1,0:T(8,128)(2,1)S(1)}, bf16[128,2048]{1,0:T(8,128)(2,1)S(1)}, u32[]{:S(2)}, u32[]{:S(2)}) collective-permute-start(bf16[128,2048]{1,0:T(8,128)(2,1)S(1)} %collective-permute-done.10.refs_0_), channel_id=1, source_target_pairs={{0,1},{1,2},{2,3},{3,0},{4,5},{5,6},{6,7},{7,4},{8,9},{9,10},{10,1... | collective-permute-start | bytes 1572872 | tf_op jit(solution)/shard_map/ppermute | solution.py:19
  80.4 15.3 %collective-permute-start.13 = (bf16[128,2048]{1,0:T(8,128)(2,1)S(1)}, bf16[128,2048]{1,0:T(8,128)(2,1)S(1)}, u32[]{:S(2)}, u32[]{:S(2)}) collective-permute-start(bf16[128,2048]{1,0:T(8,128)(2,1)S(1)} %collective-permute-done.12.refs_1_), channel_id=1, source_target_pairs={{0,3},{1,0},{2,1},{3,2},{4,7},{5,4},{6,5},{7,6},{8,11},{9,8},{10,9... | collective-permute-start | bytes 1572872 | tf_op jit(solution)/shard_map/ppermute | solution.py:19
  83.0 33.2 %collective-permute-start.9 = (bf16[128,2048]{1,0:T(8,128)(2,1)S(1)}, bf16[128,2048]{1,0:T(8,128)(2,1)S(1)}, u32[]{:S(2)}, u32[]{:S(2)}) collective-permute-start(bf16[128,2048]{1,0:T(8,128)(2,1)S(1)} %get-tuple-element.31.refs_0_), channel_id=1, source_target_pairs={{0,3},{1,0},{2,1},{3,2},{4,7},{5,4},{6,5},{7,6},{8,11},{9,8},{10,9... | collective-permute-start | bytes 1572872 | tf_op jit(solution)/shard_map/ppermute | solution.py:19
  83.3 35.7 %collective-permute-start.8 = (bf16[128,2048]{1,0:T(8,128)(2,1)S(1)}, bf16[128,2048]{1,0:T(8,128)(2,1)S(1)}, u32[]{:S(2)}, u32[]{:S(2)}) collective-permute-start(bf16[128,2048]{1,0:T(8,128)(2,1)S(1)} %get-tuple-element.32.refs_1_), channel_id=1, source_target_pairs={{0,1},{1,2},{2,3},{3,0},{4,5},{5,6},{6,7},{7,4},{8,9},{9,10},{10,1... | collective-permute-start | bytes 1572872 | tf_op jit(solution)/shard_map/ppermute | solution.py:19
  95.7 0.8 copy-start.6
  96.5 1.0 copy-start.5
  97.6 1.0 copy-start.7
  106.5 20.4 %collective-permute-start.18 = (bf16[128,2048]{1,0:T(8,128)(2,1)S(1)}, bf16[128,2048]{1,0:T(8,128)(2,1)S(1)}, u32[]{:S(2)}, u32[]{:S(2)}) collective-permute-start(bf16[128,2048]{1,0:T(8,128)(2,1)S(1)} %get-tuple-element.40), channel_id=1, source_target_pairs={{0,3},{1,0},{2,1},{3,2},{4,7},{5,4},{6,5},{7,6},{8,11},{9,8},{10,9... | collective-permute-start | bytes 1572872 | tf_op jit(solution)/shard_map/ppermute | solution.py:19
  108.2 20.3 %collective-permute-start.14 = (bf16[128,2048]{1,0:T(8,128)(2,1)S(1)}, bf16[128,2048]{1,0:T(8,128)(2,1)S(1)}, u32[]{:S(2)}, u32[]{:S(2)}) collective-permute-start(bf16[128,2048]{1,0:T(8,128)(2,1)S(1)} %get-tuple-element.36), channel_id=1, source_target_pairs={{0,1},{1,2},{2,3},{3,0},{4,5},{5,6},{6,7},{7,4},{8,9},{9,10},{10,1... | collective-permute-start | bytes 1572872 | tf_op jit(solution)/shard_map/ppermute | solution.py:19
  116.2 20.8 %collective-permute-start.16 = (bf16[128,2048]{1,0:T(8,128)(2,1)S(1)}, bf16[128,2048]{1,0:T(8,128)(2,1)S(1)}, u32[]{:S(2)}, u32[]{:S(2)}) collective-permute-start(bf16[128,2048]{1,0:T(8,128)(2,1)S(1)} %get-tuple-element.37), channel_id=1, source_target_pairs={{0,1},{1,2},{2,3},{3,0},{4,5},{5,6},{6,7},{7,4},{8,9},{9,10},{10,1... | collective-permute-start | bytes 1572872 | tf_op jit(solution)/shard_map/ppermute | solution.py:19
  116.2 27.4 %copy-start.10 = (f32[2048]{0:T(1024)S(1)}, f32[2048]{0:T(1024)}, u32[]{:S(2)}) copy-start(f32[2048]{0:T(1024)} %param.20) | copy-start | bytes 24580
  116.3 27.4 %copy-start.11 = (f32[2048]{0:T(1024)S(1)}, f32[2048]{0:T(1024)}, u32[]{:S(2)}) copy-start(f32[2048]{0:T(1024)} %param.21) | copy-start | bytes 24580
  116.3 20.7 %collective-permute-start.17 = (bf16[128,2048]{1,0:T(8,128)(2,1)S(1)}, bf16[128,2048]{1,0:T(8,128)(2,1)S(1)}, u32[]{:S(2)}, u32[]{:S(2)}) collective-permute-start(bf16[128,2048]{1,0:T(8,128)(2,1)S(1)} %get-tuple-element.38), channel_id=1, source_target_pairs={{0,3},{1,0},{2,1},{3,2},{4,7},{5,4},{6,5},{7,6},{8,11},{9,8},{10,9... | collective-permute-start | bytes 1572872 | tf_op jit(solution)/shard_map/ppermute | solution.py:19
  127.1 14.4 %collective-permute-start.19 = (bf16[128,2048]{1,0:T(8,128)(2,1)S(1)}, bf16[128,2048]{1,0:T(8,128)(2,1)S(1)}, u32[]{:S(2)}, u32[]{:S(2)}) collective-permute-start(bf16[128,2048]{1,0:T(8,128)(2,1)S(1)} %add_convert_fusion), channel_id=1, source_target_pairs={{0,3},{1,0},{2,1},{3,2},{4,7},{5,4},{6,5},{7,6},{8,11},{9,8},{10,9... | collective-permute-start | bytes 1572872 | tf_op jit(solution)/shard_map/ppermute | solution.py:19
  128.7 15.0 %collective-permute-start.15 = (bf16[128,2048]{1,0:T(8,128)(2,1)S(1)}, bf16[128,2048]{1,0:T(8,128)(2,1)S(1)}, u32[]{:S(2)}, u32[]{:S(2)}) collective-permute-start(bf16[128,2048]{1,0:T(8,128)(2,1)S(1)} %add_convert_fusion.1), channel_id=1, source_target_pairs={{0,1},{1,2},{2,3},{3,0},{4,5},{5,6},{6,7},{7,4},{8,9},{9,10},{10,1... | collective-permute-start | bytes 1572872 | tf_op jit(solution)/shard_map/ppermute | solution.py:19
  (2 other events, 1.5 us)
Sparse Core Ops, SparseCore 0:
  9.6 76.2 all-gather.1

commit v6 on v5

--- a/solution.py
+++ b/solution.py
@@ -19,40 +19,88 @@
     return lax.ppermute(value, axis, [(i, (i + step) % devices) for i in range(devices)])
 
 
-def halo(shard, axis, width):
-    devices, length = (lax.axis_size(axis), shard.shape[1])
+def prepare_kernel(up, down, keys_values, joined, last, first, sems):
+    height, tok_rows = (up.shape[0], keys_values.shape[1])
+    copies = [
+        pltpu.make_async_copy(source, target, sems.at[index])
+        for index, (source, target) in enumerate(
+            (
+                (keys_values.at[:, pl.ds(tok_rows - WINDOW, WINDOW)], last),
+                (keys_values.at[:, pl.ds(0, WINDOW)], first),
+                (up, joined.at[pl.ds(0, height)]),
+                (down, joined.at[pl.ds(height, height)]),
+            )
+        )
+    ]
+    for copy in copies:
+        copy.start()
+    for copy in copies:
+        copy.wait()
+
+
+def prepare(up, down, keys_values):
+    anywhere = pl.BlockSpec(memory_space=pl.ANY)
+    edge = jax.ShapeDtypeStruct((2, WINDOW, keys_values.shape[2]), jnp.bfloat16)
+    return pl.pallas_call(
+        prepare_kernel,
+        in_specs=[pl.BlockSpec(memory_space=pltpu.HBM)] * 3,
+        out_specs=[pl.BlockSpec(memory_space=pltpu.HBM), anywhere, anywhere],
+        out_shape=[
+            jax.ShapeDtypeStruct((2 * up.shape[0], up.shape[1]), jnp.bfloat16),
+            edge,
+            edge,
+        ],
+        scratch_shapes=[pltpu.SemaphoreType.DMA((4,))],
+        compiler_params=pltpu.CompilerParams(vmem_limit_bytes=60 * 1024 * 1024),
+        name="prepare",
+    )(up, down, keys_values)
+
+
+def halo(last, first, axis):
+    devices = lax.axis_size(axis)
     up = [(i, i + 1) for i in range(devices - 1)]
     down = [(j, i) for i, j in up]
-    before = lax.ppermute(shard[:, length - width :], axis, up)
-    after = lax.ppermute(shard[:, :width], axis, down)
+    before = lax.ppermute(last, axis, up)
+    after = lax.ppermute(first, axis, down)
     return before, after
 
 
-def attend_kernel(
-    place, sink, q_ref, before_ref, mid_ref, after_ref, w_ref, *refs, rel, n_sp, tok_rows
-):
-    *out_refs, kv_ref, weight_ref, sems = refs
+def attend_kernel(sink, q_hbm, before_ref, mid_ref, after_ref, w_ref, *refs, rels):
+    *out_refs, q_ref, kv_ref, weight_ref, sems = refs
     step = pl.program_id(0)
-    kv_copies = [
+    rows, tok_rows = (q_ref.shape[1], mid_ref.shape[1])
+    count = tok_rows // rows
+    n_sp = lax.axis_size("sp")
+    token_group, head_group = (lax.axis_index("sp"), lax.axis_index("tp"))
+    rel = rels[-1]
+    for turn in reversed(range(len(rels) - 1)):
+        rel = jnp.where(step == turn, rels[turn], rel)
+    quarter = (head_group + rel) % count
+    copies = [
         pltpu.make_async_copy(ref, kv_ref.at[:, pl.ds(at, ref.shape[1])], sems.at[index])
         for index, (ref, at) in enumerate(
             ((before_ref, 0), (mid_ref, WINDOW), (after_ref, WINDOW + tok_rows))
         )
+    ] + [
+        pltpu.make_async_copy(
+            q_hbm.at[pl.ds(pl.multiple_of((head_group + turn) % count * rows, rows), rows)],
+            q_ref.at[index],
+            sems.at[4 + index],
+        )
+        for index, turn in enumerate(rels)
     ]
     weight_copy = pltpu.make_async_copy(w_ref, weight_ref, sems.at[3])
 
     @pl.when(step == 0)
     def _():
-        for copy in kv_copies:
+        for copy in copies:
             copy.start()
         weight_copy.start()
-        for copy in kv_copies:
+        for copy in copies:
             copy.wait()
 
-    rows = q_ref.shape[0]
-    quarter = (place[0] + rel(step)) % (tok_rows // rows)
     blocks = rows // WINDOW
-    pairs = q_ref.shape[1] // LANES
+    pairs = q_ref.shape[2] // LANES
     row = lax.broadcasted_iota(jnp.int32, (2 * WINDOW, WINDOW), 0) % WINDOW
     col = lax.broadcasted_iota(jnp.int32, (2 * WINDOW, WINDOW), 1)
     low = lax.broadcasted_iota(jnp.int32, (WINDOW, LANES), 1) < HEAD_DIM
@@ -61,8 +109,8 @@
     finished = []
     for block in range(blocks):
         index = quarter * blocks + block
-        at_start = jnp.where((place[1] == 0) & (index == 0), 4 * WINDOW, 0)
-        at_end = jnp.where((place[1] == n_sp - 1) & (index == tok_rows // WINDOW - 1), 4 * WINDOW, 0)
+        at_start = jnp.where((token_group == 0) & (index == 0), 4 * WINDOW, 0)
+        at_end = jnp.where((token_group == n_sp - 1) & (index == tok_rows // WINDOW - 1), 4 * WINDOW, 0)
         before_ok = col - row >= at_start
         after_ok = row - col >= at_end
         start = pl.multiple_of(index * WINDOW, WINDOW)
@@ -70,7 +118,7 @@
         for pair in range(pairs):
             tile, half = (pair // 2, pair % 2)
             lanes = slice(tile * LANES, (tile + 1) * LANES)
-            query = q_ref[block * WINDOW : (block + 1) * WINDOW, pair * LANES : (pair + 1) * LANES]
+            query = q_ref[step, block * WINDOW : (block + 1) * WINDOW, pair * LANES : (pair + 1) * LANES]
             query = query.astype(jnp.float32) * HEAD_DIM**-0.5
             turned = pltpu.roll(query, HEAD_DIM, 1)
             if half == 0:
@@ -126,35 +174,34 @@
             out_refs[2 * turn + 1][...] = projected[half:]
 
 
-def attend(place, sink, queries, before, middle, after, out_weight, steps, rel, n_tp, n_sp):
+def attend(sink, queries, before, middle, after, out_weight, rels, n_tp):
     tok_rows, width = queries.shape
-    rows = tok_rows // n_tp
+    rows, steps = (tok_rows // n_tp, len(rels))
     cols = out_weight.shape[1]
-
     anywhere = pl.BlockSpec(memory_space=pl.ANY)
+    hbm = pl.BlockSpec(memory_space=pltpu.HBM)
     return pl.pallas_call(
-        functools.partial(attend_kernel, rel=rel, n_sp=n_sp, tok_rows=tok_rows),
-        grid_spec=pltpu.PrefetchScalarGridSpec(
-            num_scalar_prefetch=2,
-            grid=(steps,),
-            in_specs=[
-                pl.BlockSpec((rows, width), lambda i, place, sink: ((place[0] + rel(i)) % n_tp, 0)),
-                anywhere,
-                anywhere,
-                anywhere,
-                anywhere,
-            ],
-            out_specs=[pl.BlockSpec((rows // 2, cols), lambda i, place, sink: (0, 0))] * (2 * steps),
-            scratch_shapes=[
-                pltpu.VMEM((2, tok_rows + 2 * WINDOW, middle.shape[2]), jnp.bfloat16),
-                pltpu.VMEM(out_weight.shape, jnp.bfloat16),
-                pltpu.SemaphoreType.DMA((4,)),
-            ],
-        ),
+        functools.partial(attend_kernel, rels=rels),
+        grid=(steps,),
+        in_specs=[
+            pl.BlockSpec(memory_space=pltpu.SMEM),
+            hbm,
+            anywhere,
+            hbm,
+            anywhere,
+            hbm,
+        ],
+        out_specs=[pl.BlockSpec((rows // 2, cols), lambda i: (0, 0))] * (2 * steps),
+        scratch_shapes=[
+            pltpu.VMEM((steps, rows, width), jnp.bfloat16),
+            pltpu.VMEM((2, tok_rows + 2 * WINDOW, middle.shape[2]), jnp.bfloat16),
+            pltpu.VMEM(out_weight.shape, jnp.bfloat16),
+            pltpu.SemaphoreType.DMA((4 + steps,)),
+        ],
         out_shape=[jax.ShapeDtypeStruct((rows // 2, cols), jnp.bfloat16)] * (2 * steps),
-        compiler_params=pltpu.CompilerParams(vmem_limit_bytes=24 * 1024 * 1024),
+        compiler_params=pltpu.CompilerParams(vmem_limit_bytes=52 * 1024 * 1024),
         name="attend",
-    )(place, sink, queries, before, middle, after, out_weight)
+    )(sink, queries, before, middle, after, out_weight)
 
 
 def norm_kernel(*refs, tops, bottoms, outs, block):
@@ -338,24 +385,24 @@
     norm2_bias,
 ):
     n_tp, n_sp = (lax.axis_size("tp"), lax.axis_size("sp"))
-    before, after = halo(keys_values, "sp", WINDOW)
-    shards = jnp.concatenate([up_weight, down_weight.T], axis=0)
+    shards, last, edge = prepare(up_weight, down_weight.T, keys_values)
     weights = lax.all_gather(shards, "sp", axis=0, tiled=True).reshape(
         n_sp, 2, up_weight.shape[0], up_weight.shape[1]
     )
-    place = jnp.where(
-        jnp.arange(2, dtype=jnp.int32) == 0, lax.axis_index("tp"), lax.axis_index("sp")
-    )
-    run = functools.partial(
-        attend, place, sink_logit, queries, before, keys_values, after, out_weight
-    )
-    far_top, far_bottom = run(1, lambda i: 2, n_tp, n_sp)
+    before, after = halo(last, edge, "sp")
+
+    def run(*rels):
+        return attend(
+            sink_logit, queries, before, keys_values, after, out_weight, rels, n_tp
+        )
+
+    far_top, far_bottom = run(2)
     from_left = shift(far_top, 1)
     from_right = shift(far_bottom, -1)
-    right_top, right_bottom, left_top, left_bottom = run(2, lambda i: 1 + 2 * i, n_tp, n_sp)
+    right_top, right_bottom, left_top, left_bottom = run(1, 3)
     left_plain = shift(right_bottom, 1)
     right_plain = shift(left_top, -1)
-    own_top, own_bottom = run(1, lambda i: 0, n_tp, n_sp)
+    own_top, own_bottom = run(0)
     left_sum = shift(added(right_top, from_left), 1)
     right_sum = shift(added(left_bottom, from_right), -1)
     rows, half = (2 * own_top.shape[0], own_top.shape[0])

time: 156 us -> 177 us (1.13)
  Pallas kernels: 50.1 us -> 78.9 us
  local copies, waits for them, and re-layouts: 9.4 us -> 4.36 us
    pallas_call x3 -> x4, Pallas kernels: 14 us -> 42.8 us  [the longest x1 25 us: prepare(): pl.pallas_call(prepare_kernel, in_specs=[pl.BlockSpec(memory_space=pltpu....]
    ppermute x18, waiting for transfers between devices: 47.3 us -> 43.1 us  [shift(): lax.ppermute(value, axis, [(i, (i + step) % devices) for i in range(devic...]
    unnamed x26 -> x20, local copies, waits for them, and re-layouts: 8.41 us -> 4.36 us
    ppermute x2, waiting for transfers between devices: 1.91 us -> 4.57 us  [the longest x1 4.25 us: halo(): after = lax.ppermute(first, axis, down)]
    concatenate x1 -> x0, other arithmetic: 1.96 us -> none  [layer(): shards = jnp.concatenate([up_weight, down_weight.T], axis=0)]
  transfers between devices with their start and end apart: 21 -> 21, of which waited for: 10 -> 9; matrix products, arithmetic and copies ran while one was open for 1% -> 1% of each run, Pallas kernels for 31% -> 29%
where the time goes in v6:
time: 177 us; the launch traced here: 175 us
  Pallas kernels  78.9 us (45%)
  waiting for transfers between devices  47.7 us (27%)
  starting transfers between devices  29.1 us (16%)
  between operations  13.6 us (8%)
  local copies, waits for them, and re-layouts  4.36 us (2%)
    ppermute x18, waiting for transfers between devices, shift(): lax.ppermute(value, axis, [(i, (i + step) % devices) for i in range(devic...  43.1 us
    pallas_call x4, Pallas kernels, feed_forward(): pl.pallas_call(functools.partial(feed_kernel, count=count, outs=outs, chu...  31.7 us
    pallas_call x1, Pallas kernels, prepare(): pl.pallas_call(prepare_kernel, in_specs=[pl.BlockSpec(memory_space=pltpu....  25 us
    ppermute x18, starting transfers between devices, shift(): lax.ppermute(value, axis, [(i, (i + step) % devices) for i in range(devic...  22.6 us
    pallas_call x3, Pallas kernels, attend(): pl.pallas_call(functools.partial(attend_kernel, rels=rels), grid=(steps,)...  17.9 us
    ppermute x1, starting transfers between devices, halo(): before = lax.ppermute(last, axis, up)  4.58 us
    pallas_call x2, Pallas kernels, norm_rows(): pl.pallas_call(functools.partial(norm_kernel, tops=tops, bottoms=bottoms,...  4.43 us
    unnamed x20, local copies, waits for them, and re-layouts  4.36 us
  transfers between devices with their start and end apart: 21, of which 9 were waited for; matrix products, arithmetic and copies ran while one was open for 1% of the time, Pallas kernels for 29%

profile of v6, /device:TPU:1, one launch (start us, length us, event | category | flops | bytes accessed | tf_op | source)
XLA Modules:
  0.0 175.2 jit_solution(104837435125865618)
XLA Ops:
  6.5 25.0 %prepare.1 = (bf16[128,2048]{1,0:T(8,128)(2,1)}, bf16[2,128,256]{2,1,0:T(8,128)(2,1)}, bf16[2,128,256]{2,1,0:T(8,128)(2,1)}) custom-call(bf16[64,2048]{1,0:T(8,128)(2,1)} %up.1, bf16[64,2048]{1,0:T(8,128)(2,1)} %bitcast.14, bf16[2,1024,256]{2,1,0:T(8,128)(2,1)} %mid_ref.5), custom_call_target="tpu_custom_call" | custom-call | tf_op jit(solution)/shard_map/prepare/pallas_call | solution.py:44
  31.5 4.6 %collective-permute-start = (bf16[2,128,256]{2,1,0:T(8,128)(2,1)}, bf16[2,128,256]{2,1,0:T(8,128)(2,1)S(1)}, u32[]{:S(2)}, u32[]{:S(2)}) collective-permute-start(bf16[2,128,256]{2,1,0:T(8,128)(2,1)} %get-tuple-element.26), channel_id=1, source_target_pairs={{0,4},{4,8},{8,12},{12,16},{16,20},{20,24},{24,28},{28,32},{32,36}... | collective-permute-start | bytes 393224 | tf_op jit(solution)/shard_map/ppermute | solution.py:63
  36.1 1.9 %collective-permute-start.1 = (bf16[2,128,256]{2,1,0:T(8,128)(2,1)}, bf16[2,128,256]{2,1,0:T(8,128)(2,1)S(1)}, u32[]{:S(2)}, u32[]{:S(2)}) collective-permute-start(bf16[2,128,256]{2,1,0:T(8,128)(2,1)} %get-tuple-element.27), channel_id=1, source_target_pairs={{4,0},{8,4},{12,8},{16,12},{20,16},{24,20},{28,24},{32,28},{36,32}... | collective-permute-start | bytes 393224 | tf_op jit(solution)/shard_map/ppermute | solution.py:64
  38.4 4.3 %collective-permute-done.1.after_ref = bf16[2,128,256]{2,1,0:T(8,128)(2,1)S(1)} collective-permute-done((bf16[2,128,256]{2,1,0:T(8,128)(2,1)}, bf16[2,128,256]{2,1,0:T(8,128)(2,1)S(1)}, u32[]{:S(2)}, u32[]{:S(2)}) %collective-permute-start.1) | collective-permute-done | bytes 131104 | tf_op jit(solution)/shard_map/ppermute | solution.py:64
  43.3 4.7 %attend.5 = (bf16[128,2048]{1,0:T(8,128)(2,1)S(1)}, bf16[128,2048]{1,0:T(8,128)(2,1)S(1)}) custom-call(f32[8]{0:T(128)S(1)} %copy-done.9, bf16[1024,512]{1,0:T(8,128)(2,1)} %q_hbm.5, bf16[2,128,256]{2,1,0:T(8,128)(2,1)S(1)} %collective-permute-done.before_ref, bf16[2,1024,256]{2,1,0:T(8,128)(2,1)} %mid_ref.5, ...), custom_call_target="tpu_custom_call" | custom-call | tf_op jit(solution)/shard_map/attend/pallas_call | solution.py:183
  48.0 1.3 collective-permute-start.2
  49.3 1.5 collective-permute-start.6
  50.8 8.5 %attend.4 = (bf16[128,2048]{1,0:T(8,128)(2,1)S(1)}, bf16[128,2048]{1,0:T(8,128)(2,1)S(1)}, bf16[128,2048]{1,0:T(8,128)(2,1)S(1)}, bf16[128,2048]{1,0:T(8,128)(2,1)}) custom-call(f32[8]{0:T(128)S(1)} %copy-done.9, bf16[1024,512]{1,0:T(8,128)(2,1)} %q_hbm.5, bf16[2,128,256]{2,1,0:T(8,128)(2,1)S(1)} %collective-permute-done.before_ref, ...), custom_call_target="tpu_custom_call" | custom-call | tf_op jit(solution)/shard_map/attend/pallas_call | solution.py:183
  59.3 2.7 %collective-permute-start.5 = (bf16[128,2048]{1,0:T(8,128)(2,1)S(1)}, bf16[128,2048]{1,0:T(8,128)(2,1)S(1)}, u32[]{:S(2)}, u32[]{:S(2)}) collective-permute-start(bf16[128,2048]{1,0:T(8,128)(2,1)S(1)} %get-tuple-element.33), channel_id=1, source_target_pairs={{0,3},{1,0},{2,1},{3,2},{4,7},{5,4},{6,5},{7,6},{8,11},{9,8},{10,9... | collective-permute-start | bytes 1572872 | tf_op jit(solution)/shard_map/ppermute | solution.py:19
  62.2 1.2 add_convert_fusion.2
  63.4 2.9 %collective-permute-start.7 = (bf16[128,2048]{1,0:T(8,128)(2,1)S(1)}, bf16[128,2048]{1,0:T(8,128)(2,1)S(1)}, u32[]{:S(2)}, u32[]{:S(2)}) collective-permute-start(bf16[128,2048]{1,0:T(8,128)(2,1)S(1)} %add_convert_fusion.2), channel_id=1, source_target_pairs={{0,3},{1,0},{2,1},{3,2},{4,7},{5,4},{6,5},{7,6},{8,11},{9,8},{10,9... | collective-permute-start | bytes 1572872 | tf_op jit(solution)/shard_map/ppermute | solution.py:19
  66.3 4.7 %attend.3 = (bf16[128,2048]{1,0:T(8,128)(2,1)S(1)}, bf16[128,2048]{1,0:T(8,128)(2,1)S(1)}) custom-call(f32[8]{0:T(128)S(1)} %copy-done.9, bf16[1024,512]{1,0:T(8,128)(2,1)} %q_hbm.5, bf16[2,128,256]{2,1,0:T(8,128)(2,1)S(1)} %collective-permute-done.before_ref, bf16[2,1024,256]{2,1,0:T(8,128)(2,1)} %mid_ref.5, ...), custom_call_target="tpu_custom_call" | custom-call | tf_op jit(solution)/shard_map/attend/pallas_call | solution.py:183
  71.0 3.6 %collective-permute-done.4.refs_4_ = bf16[128,2048]{1,0:T(8,128)(2,1)S(1)} collective-permute-done((bf16[128,2048]{1,0:T(8,128)(2,1)S(1)}, bf16[128,2048]{1,0:T(8,128)(2,1)S(1)}, u32[]{:S(2)}, u32[]{:S(2)}) %collective-permute-start.4) | collective-permute-done | bytes 524320 | tf_op jit(solution)/shard_map/ppermute | solution.py:19
  74.6 9.1 %collective-permute-done.3.refs_3_ = bf16[128,2048]{1,0:T(8,128)(2,1)S(1)} collective-permute-done((bf16[128,2048]{1,0:T(8,128)(2,1)S(1)}, bf16[128,2048]{1,0:T(8,128)(2,1)S(1)}, u32[]{:S(2)}, u32[]{:S(2)}) %collective-permute-start.3) | collective-permute-done | bytes 524320 | tf_op jit(solution)/shard_map/ppermute | solution.py:19
  83.7 1.9 %norm.2 = (bf16[128,2048]{1,0:T(8,128)(2,1)S(1)}, bf16[128,2048]{1,0:T(8,128)(2,1)S(1)}) custom-call(bf16[256,2048]{1,0:T(8,128)(2,1)S(1)} %copy-done, bf16[128,2048]{1,0:T(8,128)(2,1)S(1)} %get-tuple-element.28.refs_1_, bf16[128,2048]{1,0:T(8,128)(2,1)S(1)} %get-tuple-element.29.refs_2_, bf16[128,2048]{1,0:T(8,128)(2,1)S(1)} %collective-permute-done.3.refs_3_, ...), custom_call_target="tpu_custom_call" | custom-call | tf_op jit(solution)/shard_map/norm/pallas_call | solution.py:260
  86.7 2.1 %collective-permute-start.12 = (bf16[128,2048]{1,0:T(8,128)(2,1)S(1)}, bf16[128,2048]{1,0:T(8,128)(2,1)S(1)}, u32[]{:S(2)}, u32[]{:S(2)}) collective-permute-start(bf16[128,2048]{1,0:T(8,128)(2,1)S(1)} %get-tuple-element.37.refs_1_), channel_id=1, source_target_pairs={{0,3},{1,0},{2,1},{3,2},{4,7},{5,4},{6,5},{7,6},{8,11},{9,8},{10,9... | collective-permute-start | bytes 1572872 | tf_op jit(solution)/shard_map/ppermute | solution.py:19
  88.7 11.5 %collective-permute-done.10.refs_0_ = bf16[128,2048]{1,0:T(8,128)(2,1)S(1)} collective-permute-done((bf16[128,2048]{1,0:T(8,128)(2,1)S(1)}, bf16[128,2048]{1,0:T(8,128)(2,1)S(1)}, u32[]{:S(2)}, u32[]{:S(2)}) %collective-permute-start.10) | collective-permute-done | bytes 524320 | tf_op jit(solution)/shard_map/ppermute | solution.py:19
  100.6 2.6 %collective-permute-start.13 = (bf16[128,2048]{1,0:T(8,128)(2,1)S(1)}, bf16[128,2048]{1,0:T(8,128)(2,1)S(1)}, u32[]{:S(2)}, u32[]{:S(2)}) collective-permute-start(bf16[128,2048]{1,0:T(8,128)(2,1)S(1)} %collective-permute-done.12.refs_1_), channel_id=1, source_target_pairs={{0,3},{1,0},{2,1},{3,2},{4,7},{5,4},{6,5},{7,6},{8,11},{9,8},{10,9... | collective-permute-start | bytes 1572872 | tf_op jit(solution)/shard_map/ppermute | solution.py:19
  103.4 1.3 collective-permute-start.8
  104.7 10.7 %collective-permute-done.11.refs_0_ = bf16[128,2048]{1,0:T(8,128)(2,1)S(1)} collective-permute-done((bf16[128,2048]{1,0:T(8,128)(2,1)S(1)}, bf16[128,2048]{1,0:T(8,128)(2,1)S(1)}, u32[]{:S(2)}, u32[]{:S(2)}) %collective-permute-start.11) | collective-permute-done | bytes 524320 | tf_op jit(solution)/shard_map/ppermute | solution.py:19
  117.0 1.0 copy-done.2
  118.0 1.0 copy-done.4
  119.1 7.9 %feed.6 = (bf16[128,2048]{1,0:T(8,128)(2,1)S(1)}, bf16[128,2048]{1,0:T(8,128)(2,1)S(1)}) custom-call(bf16[128,2048]{1,0:T(8,128)(2,1)S(1)} %copy-done.2, bf16[128,2048]{1,0:T(8,128)(2,1)S(1)} %copy-done.4, bf16[32,2,64,2048]{3,2,1,0:T(8,128)(2,1)} %bitcast.10), custom_call_target="tpu_custom_call" | custom-call | tf_op jit(solution)/shard_map/feed/pallas_call | solution.py:356
  127.0 2.2 %collective-permute-start.18 = (bf16[128,2048]{1,0:T(8,128)(2,1)S(1)}, bf16[128,2048]{1,0:T(8,128)(2,1)S(1)}, u32[]{:S(2)}, u32[]{:S(2)}) collective-permute-start(bf16[128,2048]{1,0:T(8,128)(2,1)S(1)} %get-tuple-element.46), channel_id=1, source_target_pairs={{0,3},{1,0},{2,1},{3,2},{4,7},{5,4},{6,5},{7,6},{8,11},{9,8},{10,9... | collective-permute-start | bytes 1572872 | tf_op jit(solution)/shard_map/ppermute | solution.py:19
  129.2 7.9 %feed.7 = (bf16[128,2048]{1,0:T(8,128)(2,1)S(1)}, bf16[128,2048]{1,0:T(8,128)(2,1)S(1)}) custom-call(bf16[128,2048]{1,0:T(8,128)(2,1)S(1)} %collective-permute-done.10.refs_0_, bf16[128,2048]{1,0:T(8,128)(2,1)S(1)} %collective-permute-done.12.refs_1_, bf16[32,2,64,2048]{3,2,1,0:T(8,128)(2,1)} %bitcast.11), custom_call_target="tpu_custom_call" | custom-call | tf_op jit(solution)/shard_map/feed/pallas_call | solution.py:356
  137.3 2.7 %collective-permute-start.17 = (bf16[128,2048]{1,0:T(8,128)(2,1)S(1)}, bf16[128,2048]{1,0:T(8,128)(2,1)S(1)}, u32[]{:S(2)}, u32[]{:S(2)}) collective-permute-start(bf16[128,2048]{1,0:T(8,128)(2,1)S(1)} %get-tuple-element.44), channel_id=1, source_target_pairs={{0,3},{1,0},{2,1},{3,2},{4,7},{5,4},{6,5},{7,6},{8,11},{9,8},{10,9... | collective-permute-start | bytes 1572872 | tf_op jit(solution)/shard_map/ppermute | solution.py:19
  140.0 7.9 %feed.5 = (bf16[128,2048]{1,0:T(8,128)(2,1)S(1)}, bf16[128,2048]{1,0:T(8,128)(2,1)S(1)}) custom-call(bf16[128,2048]{1,0:T(8,128)(2,1)S(1)} %collective-permute-done.8.refs_0_, bf16[128,2048]{1,0:T(8,128)(2,1)S(1)} %collective-permute-done.9.refs_1_, bf16[32,2,64,2048]{3,2,1,0:T(8,128)(2,1)} %bitcast.12), custom_call_target="tpu_custom_call" | custom-call | tf_op jit(solution)/shard_map/feed/pallas_call | solution.py:356
  148.1 1.4 collective-permute-start.19
  150.1 7.9 %feed.4 = (bf16[128,2048]{1,0:T(8,128)(2,1)S(1)}, bf16[128,2048]{1,0:T(8,128)(2,1)S(1)}) custom-call(bf16[128,2048]{1,0:T(8,128)(2,1)S(1)} %get-tuple-element.36.refs_0_, bf16[128,2048]{1,0:T(8,128)(2,1)S(1)} %get-tuple-element.37.refs_1_, bf16[32,2,64,2048]{3,2,1,0:T(8,128)(2,1)} %bitcast.13), custom_call_target="tpu_custom_call" | custom-call | tf_op jit(solution)/shard_map/feed/pallas_call | solution.py:356
  158.0 5.2 %collective-permute-done.19.refs_7_ = bf16[128,2048]{1,0:T(8,128)(2,1)S(1)} collective-permute-done((bf16[128,2048]{1,0:T(8,128)(2,1)S(1)}, bf16[128,2048]{1,0:T(8,128)(2,1)S(1)}, u32[]{:S(2)}, u32[]{:S(2)}) %collective-permute-start.19) | collective-permute-done | bytes 524320 | tf_op jit(solution)/shard_map/ppermute | solution.py:19
  163.2 2.7 %collective-permute-done.15.refs_4_ = bf16[128,2048]{1,0:T(8,128)(2,1)S(1)} collective-permute-done((bf16[128,2048]{1,0:T(8,128)(2,1)S(1)}, bf16[128,2048]{1,0:T(8,128)(2,1)S(1)}, u32[]{:S(2)}, u32[]{:S(2)}) %collective-permute-start.15) | collective-permute-done | bytes 524320 | tf_op jit(solution)/shard_map/ppermute | solution.py:19
  165.8 2.5 %norm.3 = bf16[256,2048]{1,0:T(8,128)(2,1)} custom-call(bf16[128,2048]{1,0:T(8,128)(2,1)S(1)} %get-tuple-element.36.refs_0_, bf16[128,2048]{1,0:T(8,128)(2,1)S(1)} %get-tuple-element.37.refs_1_, bf16[128,2048]{1,0:T(8,128)(2,1)S(1)} %get-tuple-element.39.refs_2_, bf16[128,2048]{1,0:T(8,128)(2,1)S(1)} %get-tuple-element.40.refs_3_, ...), custom_call_target="tpu_custom_call" | custom-call | tf_op jit(solution)/shard_map/norm/pallas_call | solution.py:260
  (45 shorter events, 5.2 us)
Async XLA Ops:
  6.5 77.2 %copy-start.6 = (f32[2048]{0:T(1024)S(1)}, f32[2048]{0:T(1024)}, u32[]{:S(2)}) copy-start(f32[2048]{0:T(1024)} %param.17) | copy-start | bytes 24580
  6.5 77.2 %copy-start.5 = (f32[2048]{0:T(1024)S(1)}, f32[2048]{0:T(1024)}, u32[]{:S(2)}) copy-start(f32[2048]{0:T(1024)} %param.16) | copy-start | bytes 24580
  6.5 77.2 %copy-start = (bf16[256,2048]{1,0:T(8,128)(2,1)S(1)}, bf16[256,2048]{1,0:T(8,128)(2,1)}, u32[]{:S(2)}) copy-start(bf16[256,2048]{1,0:T(8,128)(2,1)} %refs_0_.1) | copy-start | bytes 3145732
  6.5 110.5 %all-gather.2.cloned.1.call-start = ((), (), s32[]{:S(2)}) async-start(), calls=%async_computation | async-start | bytes 17301504 | tf_op jit(solution)/shard_map/all_gather | solution.py:389
  31.5 6.8 %collective-permute-start = (bf16[2,128,256]{2,1,0:T(8,128)(2,1)}, bf16[2,128,256]{2,1,0:T(8,128)(2,1)S(1)}, u32[]{:S(2)}, u32[]{:S(2)}) collective-permute-start(bf16[2,128,256]{2,1,0:T(8,128)(2,1)} %get-tuple-element.26), channel_id=1, source_target_pairs={{0,4},{4,8},{8,12},{12,16},{16,20},{20,24},{24,28},{28,32},{32,36}... | collective-permute-start | bytes 393224 | tf_op jit(solution)/shard_map/ppermute | solution.py:63
  36.1 6.5 %collective-permute-start.1 = (bf16[2,128,256]{2,1,0:T(8,128)(2,1)}, bf16[2,128,256]{2,1,0:T(8,128)(2,1)S(1)}, u32[]{:S(2)}, u32[]{:S(2)}) collective-permute-start(bf16[2,128,256]{2,1,0:T(8,128)(2,1)} %get-tuple-element.27), channel_id=1, source_target_pairs={{4,0},{8,4},{12,8},{16,12},{20,16},{24,20},{28,24},{32,28},{36,32}... | collective-permute-start | bytes 393224 | tf_op jit(solution)/shard_map/ppermute | solution.py:64
  42.6 0.7 copy-start.9
  48.0 14.0 %collective-permute-start.2 = (bf16[128,2048]{1,0:T(8,128)(2,1)S(1)}, bf16[128,2048]{1,0:T(8,128)(2,1)S(1)}, u32[]{:S(2)}, u32[]{:S(2)}) collective-permute-start(bf16[128,2048]{1,0:T(8,128)(2,1)S(1)} %get-tuple-element.31), channel_id=1, source_target_pairs={{0,1},{1,2},{2,3},{3,0},{4,5},{5,6},{6,7},{7,4},{8,9},{9,10},{10,1... | collective-permute-start | bytes 1572872 | tf_op jit(solution)/shard_map/ppermute | solution.py:19
  49.3 12.9 %collective-permute-start.6 = (bf16[128,2048]{1,0:T(8,128)(2,1)S(1)}, bf16[128,2048]{1,0:T(8,128)(2,1)S(1)}, u32[]{:S(2)}, u32[]{:S(2)}) collective-permute-start(bf16[128,2048]{1,0:T(8,128)(2,1)S(1)} %get-tuple-element.35), channel_id=1, source_target_pairs={{0,3},{1,0},{2,1},{3,2},{4,7},{5,4},{6,5},{7,6},{8,11},{9,8},{10,9... | collective-permute-start | bytes 1572872 | tf_op jit(solution)/shard_map/ppermute | solution.py:19
  59.2 15.3 %collective-permute-start.4 = (bf16[128,2048]{1,0:T(8,128)(2,1)S(1)}, bf16[128,2048]{1,0:T(8,128)(2,1)S(1)}, u32[]{:S(2)}, u32[]{:S(2)}) collective-permute-start(bf16[128,2048]{1,0:T(8,128)(2,1)S(1)} %get-tuple-element.32), channel_id=1, source_target_pairs={{0,1},{1,2},{2,3},{3,0},{4,5},{5,6},{6,7},{7,4},{8,9},{9,10},{10,1... | collective-permute-start | bytes 1572872 | tf_op jit(solution)/shard_map/ppermute | solution.py:19
  59.3 15.2 %collective-permute-start.5 = (bf16[128,2048]{1,0:T(8,128)(2,1)S(1)}, bf16[128,2048]{1,0:T(8,128)(2,1)S(1)}, u32[]{:S(2)}, u32[]{:S(2)}) collective-permute-start(bf16[128,2048]{1,0:T(8,128)(2,1)S(1)} %get-tuple-element.33), channel_id=1, source_target_pairs={{0,3},{1,0},{2,1},{3,2},{4,7},{5,4},{6,5},{7,6},{8,11},{9,8},{10,9... | collective-permute-start | bytes 1572872 | tf_op jit(solution)/shard_map/ppermute | solution.py:19
  62.1 21.6 %collective-permute-start.3 = (bf16[128,2048]{1,0:T(8,128)(2,1)S(1)}, bf16[128,2048]{1,0:T(8,128)(2,1)S(1)}, u32[]{:S(2)}, u32[]{:S(2)}) collective-permute-start(bf16[128,2048]{1,0:T(8,128)(2,1)S(1)} %add_convert_fusion.3), channel_id=1, source_target_pairs={{0,1},{1,2},{2,3},{3,0},{4,5},{5,6},{6,7},{7,4},{8,9},{9,10},{10,1... | collective-permute-start | bytes 1572872 | tf_op jit(solution)/shard_map/ppermute | solution.py:19
  63.4 20.3 %collective-permute-start.7 = (bf16[128,2048]{1,0:T(8,128)(2,1)S(1)}, bf16[128,2048]{1,0:T(8,128)(2,1)S(1)}, u32[]{:S(2)}, u32[]{:S(2)}) collective-permute-start(bf16[128,2048]{1,0:T(8,128)(2,1)S(1)} %add_convert_fusion.2), channel_id=1, source_target_pairs={{0,3},{1,0},{2,1},{3,2},{4,7},{5,4},{6,5},{7,6},{8,11},{9,8},{10,9... | collective-permute-start | bytes 1572872 | tf_op jit(solution)/shard_map/ppermute | solution.py:19
  85.6 14.6 %collective-permute-start.10 = (bf16[128,2048]{1,0:T(8,128)(2,1)S(1)}, bf16[128,2048]{1,0:T(8,128)(2,1)S(1)}, u32[]{:S(2)}, u32[]{:S(2)}) collective-permute-start(bf16[128,2048]{1,0:T(8,128)(2,1)S(1)} %get-tuple-element.36.refs_0_), channel_id=1, source_target_pairs={{0,1},{1,2},{2,3},{3,0},{4,5},{5,6},{6,7},{7,4},{8,9},{9,10},{10,1... | collective-permute-start | bytes 1572872 | tf_op jit(solution)/shard_map/ppermute | solution.py:19
  86.7 13.9 %collective-permute-start.12 = (bf16[128,2048]{1,0:T(8,128)(2,1)S(1)}, bf16[128,2048]{1,0:T(8,128)(2,1)S(1)}, u32[]{:S(2)}, u32[]{:S(2)}) collective-permute-start(bf16[128,2048]{1,0:T(8,128)(2,1)S(1)} %get-tuple-element.37.refs_1_), channel_id=1, source_target_pairs={{0,3},{1,0},{2,1},{3,2},{4,7},{5,4},{6,5},{7,6},{8,11},{9,8},{10,9... | collective-permute-start | bytes 1572872 | tf_op jit(solution)/shard_map/ppermute | solution.py:19
  100.2 15.2 %collective-permute-start.11 = (bf16[128,2048]{1,0:T(8,128)(2,1)S(1)}, bf16[128,2048]{1,0:T(8,128)(2,1)S(1)}, u32[]{:S(2)}, u32[]{:S(2)}) collective-permute-start(bf16[128,2048]{1,0:T(8,128)(2,1)S(1)} %collective-permute-done.10.refs_0_), channel_id=1, source_target_pairs={{0,1},{1,2},{2,3},{3,0},{4,5},{5,6},{6,7},{7,4},{8,9},{9,10},{10,1... | collective-permute-start | bytes 1572872 | tf_op jit(solution)/shard_map/ppermute | solution.py:19
  100.6 15.6 %collective-permute-start.13 = (bf16[128,2048]{1,0:T(8,128)(2,1)S(1)}, bf16[128,2048]{1,0:T(8,128)(2,1)S(1)}, u32[]{:S(2)}, u32[]{:S(2)}) collective-permute-start(bf16[128,2048]{1,0:T(8,128)(2,1)S(1)} %collective-permute-done.12.refs_1_), channel_id=1, source_target_pairs={{0,3},{1,0},{2,1},{3,2},{4,7},{5,4},{6,5},{7,6},{8,11},{9,8},{10,9... | collective-permute-start | bytes 1572872 | tf_op jit(solution)/shard_map/ppermute | solution.py:19
  103.2 34.1 %collective-permute-start.9 = (bf16[128,2048]{1,0:T(8,128)(2,1)S(1)}, bf16[128,2048]{1,0:T(8,128)(2,1)S(1)}, u32[]{:S(2)}, u32[]{:S(2)}) collective-permute-start(bf16[128,2048]{1,0:T(8,128)(2,1)S(1)} %get-tuple-element.36.refs_0_), channel_id=1, source_target_pairs={{0,3},{1,0},{2,1},{3,2},{4,7},{5,4},{6,5},{7,6},{8,11},{9,8},{10,9... | collective-permute-start | bytes 1572872 | tf_op jit(solution)/shard_map/ppermute | solution.py:19
  103.4 36.7 %collective-permute-start.8 = (bf16[128,2048]{1,0:T(8,128)(2,1)S(1)}, bf16[128,2048]{1,0:T(8,128)(2,1)S(1)}, u32[]{:S(2)}, u32[]{:S(2)}) collective-permute-start(bf16[128,2048]{1,0:T(8,128)(2,1)S(1)} %get-tuple-element.37.refs_1_), channel_id=1, source_target_pairs={{0,1},{1,2},{2,3},{3,0},{4,5},{5,6},{6,7},{7,4},{8,9},{9,10},{10,1... | collective-permute-start | bytes 1572872 | tf_op jit(solution)/shard_map/ppermute | solution.py:19
  115.4 0.8 copy-start.1
  116.2 0.8 copy-start.3
  117.0 1.0 copy-start.2
  118.0 1.0 copy-start.4
  127.0 21.0 %collective-permute-start.18 = (bf16[128,2048]{1,0:T(8,128)(2,1)S(1)}, bf16[128,2048]{1,0:T(8,128)(2,1)S(1)}, u32[]{:S(2)}, u32[]{:S(2)}) collective-permute-start(bf16[128,2048]{1,0:T(8,128)(2,1)S(1)} %get-tuple-element.46), channel_id=1, source_target_pairs={{0,3},{1,0},{2,1},{3,2},{4,7},{5,4},{6,5},{7,6},{8,11},{9,8},{10,9... | collective-permute-start | bytes 1572872 | tf_op jit(solution)/shard_map/ppermute | solution.py:19
  129.2 20.3 %collective-permute-start.14 = (bf16[128,2048]{1,0:T(8,128)(2,1)S(1)}, bf16[128,2048]{1,0:T(8,128)(2,1)S(1)}, u32[]{:S(2)}, u32[]{:S(2)}) collective-permute-start(bf16[128,2048]{1,0:T(8,128)(2,1)S(1)} %get-tuple-element.42), channel_id=1, source_target_pairs={{0,1},{1,2},{2,3},{3,0},{4,5},{5,6},{6,7},{7,4},{8,9},{9,10},{10,1... | collective-permute-start | bytes 1572872 | tf_op jit(solution)/shard_map/ppermute | solution.py:19
  137.2 20.8 %collective-permute-start.16 = (bf16[128,2048]{1,0:T(8,128)(2,1)S(1)}, bf16[128,2048]{1,0:T(8,128)(2,1)S(1)}, u32[]{:S(2)}, u32[]{:S(2)}) collective-permute-start(bf16[128,2048]{1,0:T(8,128)(2,1)S(1)} %get-tuple-element.43), channel_id=1, source_target_pairs={{0,1},{1,2},{2,3},{3,0},{4,5},{5,6},{6,7},{7,4},{8,9},{9,10},{10,1... | collective-permute-start | bytes 1572872 | tf_op jit(solution)/shard_map/ppermute | solution.py:19
  137.3 28.6 %copy-start.7 = (f32[2048]{0:T(1024)S(1)}, f32[2048]{0:T(1024)}, u32[]{:S(2)}) copy-start(f32[2048]{0:T(1024)} %param.20) | copy-start | bytes 24580
  137.3 28.6 %copy-start.8 = (f32[2048]{0:T(1024)S(1)}, f32[2048]{0:T(1024)}, u32[]{:S(2)}) copy-start(f32[2048]{0:T(1024)} %param.21) | copy-start | bytes 24580
  137.3 20.7 %collective-permute-start.17 = (bf16[128,2048]{1,0:T(8,128)(2,1)S(1)}, bf16[128,2048]{1,0:T(8,128)(2,1)S(1)}, u32[]{:S(2)}, u32[]{:S(2)}) collective-permute-start(bf16[128,2048]{1,0:T(8,128)(2,1)S(1)} %get-tuple-element.44), channel_id=1, source_target_pairs={{0,3},{1,0},{2,1},{3,2},{4,7},{5,4},{6,5},{7,6},{8,11},{9,8},{10,9... | collective-permute-start | bytes 1572872 | tf_op jit(solution)/shard_map/ppermute | solution.py:19
  148.1 15.1 %collective-permute-start.19 = (bf16[128,2048]{1,0:T(8,128)(2,1)S(1)}, bf16[128,2048]{1,0:T(8,128)(2,1)S(1)}, u32[]{:S(2)}, u32[]{:S(2)}) collective-permute-start(bf16[128,2048]{1,0:T(8,128)(2,1)S(1)} %add_convert_fusion), channel_id=1, source_target_pairs={{0,3},{1,0},{2,1},{3,2},{4,7},{5,4},{6,5},{7,6},{8,11},{9,8},{10,9... | collective-permute-start | bytes 1572872 | tf_op jit(solution)/shard_map/ppermute | solution.py:19
  149.7 16.2 %collective-permute-start.15 = (bf16[128,2048]{1,0:T(8,128)(2,1)S(1)}, bf16[128,2048]{1,0:T(8,128)(2,1)S(1)}, u32[]{:S(2)}, u32[]{:S(2)}) collective-permute-start(bf16[128,2048]{1,0:T(8,128)(2,1)S(1)} %add_convert_fusion.1), channel_id=1, source_target_pairs={{0,1},{1,2},{2,3},{3,0},{4,5},{5,6},{6,7},{7,4},{8,9},{9,10},{10,1... | collective-permute-start | bytes 1572872 | tf_op jit(solution)/shard_map/ppermute | solution.py:19
Sparse Core Ops, SparseCore 0:
  31.7 76.3 all-gather.1

commit v7 on v6

--- a/solution.py
+++ b/solution.py
@@ -19,18 +19,50 @@
     return lax.ppermute(value, axis, [(i, (i + step) % devices) for i in range(devices)])
 
 
-def prepare_kernel(up, down, keys_values, joined, last, first, sems):
+def prepare_kernel(up, down, keys_values, joined, last, first, weights, sems):
     height, tok_rows = (up.shape[0], keys_values.shape[1])
+    into = [
+        pltpu.make_async_copy(up, weights.at[pl.ds(0, height)], sems.at[0]),
+        pltpu.make_async_copy(down, weights.at[pl.ds(height, height)], sems.at[1]),
+    ]
+    edges = [
+        pltpu.make_async_copy(
+            keys_values.at[:, pl.ds(tok_rows - WINDOW, WINDOW)], last, sems.at[2]
+        ),
+        pltpu.make_async_copy(keys_values.at[:, pl.ds(0, WINDOW)], first, sems.at[3]),
+    ]
+    for copy in into + edges:
+        copy.start()
+    for copy in into:
+        copy.wait()
+    out = pltpu.make_async_copy(weights, joined, sems.at[4])
+    out.start()
+    for copy in edges + [out]:
+        copy.wait()
+
+
+def prepare(up, down, keys_values):
+    anywhere = pl.BlockSpec(memory_space=pl.ANY)
+    vmem = pl.BlockSpec(memory_space=pltpu.VMEM)
+    edge = jax.ShapeDtypeStruct((2, WINDOW, keys_values.shape[2]), jnp.bfloat16)
+    both = (2 * up.shape[0], up.shape[1])
+    return pl.pallas_call(
+        prepare_kernel,
+        in_specs=[anywhere] * 3,
+        out_specs=[anywhere, vmem, vmem],
+        out_shape=[jax.ShapeDtypeStruct(both, jnp.bfloat16), edge, edge],
+        scratch_shapes=[pltpu.VMEM(both, jnp.bfloat16), pltpu.SemaphoreType.DMA((5,))],
+        compiler_params=pltpu.CompilerParams(vmem_limit_bytes=60 * 1024 * 1024),
+        name="prepare",
+    )(up, down, keys_values)
+
+
+def fetch_kernel(*refs):
+    count = len(refs) // 2
+    sems = refs[-1]
     copies = [
-        pltpu.make_async_copy(source, target, sems.at[index])
-        for index, (source, target) in enumerate(
-            (
-                (keys_values.at[:, pl.ds(tok_rows - WINDOW, WINDOW)], last),
-                (keys_values.at[:, pl.ds(0, WINDOW)], first),
-                (up, joined.at[pl.ds(0, height)]),
-                (down, joined.at[pl.ds(height, height)]),
-            )
-        )
+        pltpu.make_async_copy(refs[index], refs[count + index], sems.at[index])
+        for index in range(count)
     ]
     for copy in copies:
         copy.start()
@@ -38,22 +70,18 @@
         copy.wait()
 
 
-def prepare(up, down, keys_values):
+def fetch(*arrays):
     anywhere = pl.BlockSpec(memory_space=pl.ANY)
-    edge = jax.ShapeDtypeStruct((2, WINDOW, keys_values.shape[2]), jnp.bfloat16)
+    vmem = pl.BlockSpec(memory_space=pltpu.VMEM)
     return pl.pallas_call(
-        prepare_kernel,
-        in_specs=[pl.BlockSpec(memory_space=pltpu.HBM)] * 3,
-        out_specs=[pl.BlockSpec(memory_space=pltpu.HBM), anywhere, anywhere],
-        out_shape=[
-            jax.ShapeDtypeStruct((2 * up.shape[0], up.shape[1]), jnp.bfloat16),
-            edge,
-            edge,
-        ],
-        scratch_shapes=[pltpu.SemaphoreType.DMA((4,))],
-        compiler_params=pltpu.CompilerParams(vmem_limit_bytes=60 * 1024 * 1024),
-        name="prepare",
-    )(up, down, keys_values)
+        fetch_kernel,
+        in_specs=[anywhere] * len(arrays),
+        out_specs=[anywhere] * len(arrays),
+        out_shape=[jax.ShapeDtypeStruct(a.shape, a.dtype) for a in arrays],
+        scratch_shapes=[pltpu.SemaphoreType.DMA((len(arrays),))],
+        compiler_params=pltpu.CompilerParams(vmem_limit_bytes=47 * 1024 * 1024),
+        name="fetch",
+    )(*arrays)
 
 
 def halo(last, first, axis):
@@ -199,7 +227,7 @@
             pltpu.SemaphoreType.DMA((4 + steps,)),
         ],
         out_shape=[jax.ShapeDtypeStruct((rows // 2, cols), jnp.bfloat16)] * (2 * steps),
-        compiler_params=pltpu.CompilerParams(vmem_limit_bytes=52 * 1024 * 1024),
+        compiler_params=pltpu.CompilerParams(vmem_limit_bytes=24 * 1024 * 1024),
         name="attend",
     )(sink, queries, before, middle, after, out_weight)
 
@@ -390,6 +418,7 @@
         n_sp, 2, up_weight.shape[0], up_weight.shape[1]
     )
     before, after = halo(last, edge, "sp")
+    queries, keys_values, out_weight = fetch(queries, keys_values, out_weight)
 
     def run(*rels):
         return attend(

time: 177 us -> 155 us (0.88)
  Pallas kernels: 78.9 us -> 54.6 us
  waiting for transfers between devices: 47.7 us -> 50.2 us
  starting transfers between devices: 29.1 us -> 31 us
    pallas_call x1 -> x2, Pallas kernels: 25 us -> 4.46 us  [the longest x1 2.7 us: prepare(): pl.pallas_call(prepare_kernel, in_specs=[anywhere] * 3, out_specs=[anywhe...]
    ppermute x18, waiting for transfers between devices: 43.1 us -> 47.4 us  [shift(): lax.ppermute(value, axis, [(i, (i + step) % devices) for i in range(devic...]
    pallas_call x3, Pallas kernels: 17.9 us -> 14.1 us  [attend(): pl.pallas_call(functools.partial(attend_kernel, rels=rels), grid=(steps,)...]
    ppermute x18, starting transfers between devices: 22.6 us -> 24.5 us  [shift(): lax.ppermute(value, axis, [(i, (i + step) % devices) for i in range(devic...]
    unnamed x20 -> x24, local copies, waits for them, and re-layouts: 4.36 us -> 3.74 us
  transfers between devices with their start and end apart: 21 -> 21, of which waited for: 9 -> 10; matrix products, arithmetic and copies ran while one was open for 1% -> 0% of each run, Pallas kernels for 29% -> 32%
where the time goes in v7:
time: 155 us; the launch traced here: 154 us
  Pallas kernels  54.6 us (35%)
  waiting for transfers between devices  50.2 us (32%)
  starting transfers between devices  31 us (20%)
  between operations  13.7 us (9%)
  local copies, waits for them, and re-layouts  3.74 us (2%)
    ppermute x18, waiting for transfers between devices, shift(): lax.ppermute(value, axis, [(i, (i + step) % devices) for i in range(devic...  47.4 us
    pallas_call x4, Pallas kernels, feed_forward(): pl.pallas_call(functools.partial(feed_kernel, count=count, outs=outs, chu...  31.6 us
    ppermute x18, starting transfers between devices, shift(): lax.ppermute(value, axis, [(i, (i + step) % devices) for i in range(devic...  24.5 us
    pallas_call x3, Pallas kernels, attend(): pl.pallas_call(functools.partial(attend_kernel, rels=rels), grid=(steps,)...  14.1 us
    ppermute x1, starting transfers between devices, halo(): before = lax.ppermute(last, axis, up)  4.58 us
    pallas_call x2, Pallas kernels, norm_rows(): pl.pallas_call(functools.partial(norm_kernel, tops=tops, bottoms=bottoms,...  4.43 us
    unnamed x24, local copies, waits for them, and re-layouts  3.74 us
  transfers between devices with their start and end apart: 21, of which 10 were waited for; matrix products, arithmetic and copies ran while one was open for 0% of the time, Pallas kernels for 32%

profile of v7, /device:TPU:1, one launch (start us, length us, event | category | flops | bytes accessed | tf_op | source)
XLA Modules:
  0.0 153.7 jit_solution(11626527916591053621)
XLA Ops:
  6.5 2.7 %prepare.1 = (bf16[128,2048]{1,0:T(8,128)(2,1)}, bf16[2,128,256]{2,1,0:T(8,128)(2,1)}, bf16[2,128,256]{2,1,0:T(8,128)(2,1)}) custom-call(bf16[64,2048]{1,0:T(8,128)(2,1)} %up.1, bf16[64,2048]{1,0:T(8,128)(2,1)} %bitcast.14, bf16[2,1024,256]{2,1,0:T(8,128)(2,1)} %keys_values.1), custom_call_target="tpu_custom_call" | custom-call | tf_op jit(solution)/shard_map/prepare/pallas_call | solution.py:49
  9.3 4.6 %collective-permute-start = (bf16[2,128,256]{2,1,0:T(8,128)(2,1)}, bf16[2,128,256]{2,1,0:T(8,128)(2,1)S(1)}, u32[]{:S(2)}, u32[]{:S(2)}) collective-permute-start(bf16[2,128,256]{2,1,0:T(8,128)(2,1)} %get-tuple-element.30), channel_id=1, source_target_pairs={{0,4},{4,8},{8,12},{12,16},{16,20},{20,24},{24,28},{28,32},{32,36}... | collective-permute-start | bytes 393224 | tf_op jit(solution)/shard_map/ppermute | solution.py:91
  13.9 1.9 %collective-permute-start.1 = (bf16[2,128,256]{2,1,0:T(8,128)(2,1)}, bf16[2,128,256]{2,1,0:T(8,128)(2,1)S(1)}, u32[]{:S(2)}, u32[]{:S(2)}) collective-permute-start(bf16[2,128,256]{2,1,0:T(8,128)(2,1)} %get-tuple-element.32), channel_id=1, source_target_pairs={{4,0},{8,4},{12,8},{16,12},{20,16},{24,20},{28,24},{32,28},{36,32}... | collective-permute-start | bytes 393224 | tf_op jit(solution)/shard_map/ppermute | solution.py:92
  15.8 1.8 %fetch.1 = (bf16[1024,512]{1,0:T(8,128)(2,1)S(1)}, bf16[2,1024,256]{2,1,0:T(8,128)(2,1)S(1)}, bf16[512,2048]{1,0:T(8,128)(2,1)S(1)}) custom-call(bf16[1024,512]{1,0:T(8,128)(2,1)S(1)} %copy-done.1, bf16[2,1024,256]{2,1,0:T(8,128)(2,1)S(1)} %copy-done, bf16[512,2048]{1,0:T(8,128)(2,1)} %refs_2_.1), custom_call_target="tpu_custom_call" | custom-call | tf_op jit(solution)/shard_map/fetch/pallas_call | solution.py:76
  17.6 2.8 %collective-permute-done.1.after_ref = bf16[2,128,256]{2,1,0:T(8,128)(2,1)S(1)} collective-permute-done((bf16[2,128,256]{2,1,0:T(8,128)(2,1)}, bf16[2,128,256]{2,1,0:T(8,128)(2,1)S(1)}, u32[]{:S(2)}, u32[]{:S(2)}) %collective-permute-start.1) | collective-permute-done | bytes 131104 | tf_op jit(solution)/shard_map/ppermute | solution.py:92
  20.4 3.7 %attend.5 = (bf16[128,2048]{1,0:T(8,128)(2,1)S(1)}, bf16[128,2048]{1,0:T(8,128)(2,1)S(1)}) custom-call(f32[8]{0:T(128)S(1)} %copy-done.11, bf16[1024,512]{1,0:T(8,128)(2,1)S(1)} %get-tuple-element.29.q_hbm, bf16[2,128,256]{2,1,0:T(8,128)(2,1)S(1)} %collective-permute-done.before_ref, bf16[2,1024,256]{2,1,0:T(8,128)(2,1)S(1)} %get-tuple-element.31.mid_ref, ...), custom_call_target="tpu_custom_call" | custom-call | tf_op jit(solution)/shard_map/attend/pallas_call | solution.py:211
  24.1 2.5 %collective-permute-start.6 = (bf16[128,2048]{1,0:T(8,128)(2,1)S(1)}, bf16[128,2048]{1,0:T(8,128)(2,1)S(1)}, u32[]{:S(2)}, u32[]{:S(2)}) collective-permute-start(bf16[128,2048]{1,0:T(8,128)(2,1)S(1)} %get-tuple-element.41), channel_id=1, source_target_pairs={{0,3},{1,0},{2,1},{3,2},{4,7},{5,4},{6,5},{7,6},{8,11},{9,8},{10,9... | collective-permute-start | bytes 1572872 | tf_op jit(solution)/shard_map/ppermute | solution.py:19
  26.6 6.7 %attend.4 = (bf16[128,2048]{1,0:T(8,128)(2,1)S(1)}, bf16[128,2048]{1,0:T(8,128)(2,1)S(1)}, bf16[128,2048]{1,0:T(8,128)(2,1)S(1)}, bf16[128,2048]{1,0:T(8,128)(2,1)S(1)}) custom-call(f32[8]{0:T(128)S(1)} %copy-done.11, bf16[1024,512]{1,0:T(8,128)(2,1)S(1)} %get-tuple-element.29.q_hbm, bf16[2,128,256]{2,1,0:T(8,128)(2,1)S(1)} %collective-permute-done.before_ref, ...), custom_call_target="tpu_custom_call" | custom-call | tf_op jit(solution)/shard_map/attend/pallas_call | solution.py:211
  33.6 2.6 %collective-permute-start.5 = (bf16[128,2048]{1,0:T(8,128)(2,1)S(1)}, bf16[128,2048]{1,0:T(8,128)(2,1)S(1)}, u32[]{:S(2)}, u32[]{:S(2)}) collective-permute-start(bf16[128,2048]{1,0:T(8,128)(2,1)S(1)} %get-tuple-element.39), channel_id=1, source_target_pairs={{0,3},{1,0},{2,1},{3,2},{4,7},{5,4},{6,5},{7,6},{8,11},{9,8},{10,9... | collective-permute-start | bytes 1572872 | tf_op jit(solution)/shard_map/ppermute | solution.py:19
  37.1 3.6 %collective-permute-start.7 = (bf16[128,2048]{1,0:T(8,128)(2,1)S(1)}, bf16[128,2048]{1,0:T(8,128)(2,1)S(1)}, u32[]{:S(2)}, u32[]{:S(2)}) collective-permute-start(bf16[128,2048]{1,0:T(8,128)(2,1)S(1)} %add_convert_fusion.2), channel_id=1, source_target_pairs={{0,3},{1,0},{2,1},{3,2},{4,7},{5,4},{6,5},{7,6},{8,11},{9,8},{10,9... | collective-permute-start | bytes 1572872 | tf_op jit(solution)/shard_map/ppermute | solution.py:19
  40.7 1.1 collective-permute-done.2
  42.2 3.7 %attend.3 = (bf16[128,2048]{1,0:T(8,128)(2,1)S(1)}, bf16[128,2048]{1,0:T(8,128)(2,1)S(1)}) custom-call(f32[8]{0:T(128)S(1)} %copy-done.11, bf16[1024,512]{1,0:T(8,128)(2,1)S(1)} %get-tuple-element.29.q_hbm, bf16[2,128,256]{2,1,0:T(8,128)(2,1)S(1)} %collective-permute-done.before_ref, bf16[2,1024,256]{2,1,0:T(8,128)(2,1)S(1)} %get-tuple-element.31.mid_ref, ...), custom_call_target="tpu_custom_call" | custom-call | tf_op jit(solution)/shard_map/attend/pallas_call | solution.py:211
  45.9 7.2 %collective-permute-done.4.refs_4_ = bf16[128,2048]{1,0:T(8,128)(2,1)S(1)} collective-permute-done((bf16[128,2048]{1,0:T(8,128)(2,1)S(1)}, bf16[128,2048]{1,0:T(8,128)(2,1)S(1)}, u32[]{:S(2)}, u32[]{:S(2)}) %collective-permute-start.4) | collective-permute-done | bytes 524320 | tf_op jit(solution)/shard_map/ppermute | solution.py:19
  53.1 5.1 %collective-permute-done.7.refs_6_ = bf16[128,2048]{1,0:T(8,128)(2,1)S(1)} collective-permute-done((bf16[128,2048]{1,0:T(8,128)(2,1)S(1)}, bf16[128,2048]{1,0:T(8,128)(2,1)S(1)}, u32[]{:S(2)}, u32[]{:S(2)}) %collective-permute-start.7) | collective-permute-done | bytes 524320 | tf_op jit(solution)/shard_map/ppermute | solution.py:19
  58.3 3.8 %collective-permute-done.3.refs_3_ = bf16[128,2048]{1,0:T(8,128)(2,1)S(1)} collective-permute-done((bf16[128,2048]{1,0:T(8,128)(2,1)S(1)}, bf16[128,2048]{1,0:T(8,128)(2,1)S(1)}, u32[]{:S(2)}, u32[]{:S(2)}) %collective-permute-start.3) | collective-permute-done | bytes 524320 | tf_op jit(solution)/shard_map/ppermute | solution.py:19
  62.1 1.9 %norm.2 = (bf16[128,2048]{1,0:T(8,128)(2,1)S(1)}, bf16[128,2048]{1,0:T(8,128)(2,1)S(1)}) custom-call(bf16[256,2048]{1,0:T(8,128)(2,1)S(1)} %copy-done.2, bf16[128,2048]{1,0:T(8,128)(2,1)S(1)} %get-tuple-element.34.refs_1_, bf16[128,2048]{1,0:T(8,128)(2,1)S(1)} %get-tuple-element.35.refs_2_, bf16[128,2048]{1,0:T(8,128)(2,1)S(1)} %collective-permute-done.3.refs_3_, ...), custom_call_target="tpu_custom_call" | custom-call | tf_op jit(solution)/shard_map/norm/pallas_call | solution.py:288
  64.1 2.7 %collective-permute-start.12 = (bf16[128,2048]{1,0:T(8,128)(2,1)S(1)}, bf16[128,2048]{1,0:T(8,128)(2,1)S(1)}, u32[]{:S(2)}, u32[]{:S(2)}) collective-permute-start(bf16[128,2048]{1,0:T(8,128)(2,1)S(1)} %get-tuple-element.43.refs_1_), channel_id=1, source_target_pairs={{0,3},{1,0},{2,1},{3,2},{4,7},{5,4},{6,5},{7,6},{8,11},{9,8},{10,9... | collective-permute-start | bytes 1572872 | tf_op jit(solution)/shard_map/ppermute | solution.py:19
  66.7 11.0 %collective-permute-done.10.refs_0_ = bf16[128,2048]{1,0:T(8,128)(2,1)S(1)} collective-permute-done((bf16[128,2048]{1,0:T(8,128)(2,1)S(1)}, bf16[128,2048]{1,0:T(8,128)(2,1)S(1)}, u32[]{:S(2)}, u32[]{:S(2)}) %collective-permute-start.10) | collective-permute-done | bytes 524320 | tf_op jit(solution)/shard_map/ppermute | solution.py:19
  77.8 3.0 %collective-permute-start.13 = (bf16[128,2048]{1,0:T(8,128)(2,1)S(1)}, bf16[128,2048]{1,0:T(8,128)(2,1)S(1)}, u32[]{:S(2)}, u32[]{:S(2)}) collective-permute-start(bf16[128,2048]{1,0:T(8,128)(2,1)S(1)} %collective-permute-done.12.refs_1_), channel_id=1, source_target_pairs={{0,3},{1,0},{2,1},{3,2},{4,7},{5,4},{6,5},{7,6},{8,11},{9,8},{10,9... | collective-permute-start | bytes 1572872 | tf_op jit(solution)/shard_map/ppermute | solution.py:19
  80.7 2.7 %collective-permute-start.9 = (bf16[128,2048]{1,0:T(8,128)(2,1)S(1)}, bf16[128,2048]{1,0:T(8,128)(2,1)S(1)}, u32[]{:S(2)}, u32[]{:S(2)}) collective-permute-start(bf16[128,2048]{1,0:T(8,128)(2,1)S(1)} %get-tuple-element.42.refs_0_), channel_id=1, source_target_pairs={{0,3},{1,0},{2,1},{3,2},{4,7},{5,4},{6,5},{7,6},{8,11},{9,8},{10,9... | collective-permute-start | bytes 1572872 | tf_op jit(solution)/shard_map/ppermute | solution.py:19
  83.4 9.5 %collective-permute-done.11.refs_0_ = bf16[128,2048]{1,0:T(8,128)(2,1)S(1)} collective-permute-done((bf16[128,2048]{1,0:T(8,128)(2,1)S(1)}, bf16[128,2048]{1,0:T(8,128)(2,1)S(1)}, u32[]{:S(2)}, u32[]{:S(2)}) %collective-permute-start.11) | collective-permute-done | bytes 524320 | tf_op jit(solution)/shard_map/ppermute | solution.py:19
  94.6 1.0 copy-done.4
  96.6 7.9 %feed.6 = (bf16[128,2048]{1,0:T(8,128)(2,1)S(1)}, bf16[128,2048]{1,0:T(8,128)(2,1)S(1)}) custom-call(bf16[128,2048]{1,0:T(8,128)(2,1)S(1)} %copy-done.4, bf16[128,2048]{1,0:T(8,128)(2,1)S(1)} %copy-done.6, bf16[32,2,64,2048]{3,2,1,0:T(8,128)(2,1)} %bitcast.10), custom_call_target="tpu_custom_call" | custom-call | tf_op jit(solution)/shard_map/feed/pallas_call | solution.py:384
  104.6 2.2 %collective-permute-start.18 = (bf16[128,2048]{1,0:T(8,128)(2,1)S(1)}, bf16[128,2048]{1,0:T(8,128)(2,1)S(1)}, u32[]{:S(2)}, u32[]{:S(2)}) collective-permute-start(bf16[128,2048]{1,0:T(8,128)(2,1)S(1)} %get-tuple-element.52), channel_id=1, source_target_pairs={{0,3},{1,0},{2,1},{3,2},{4,7},{5,4},{6,5},{7,6},{8,11},{9,8},{10,9... | collective-permute-start | bytes 1572872 | tf_op jit(solution)/shard_map/ppermute | solution.py:19
  106.8 7.9 %feed.7 = (bf16[128,2048]{1,0:T(8,128)(2,1)S(1)}, bf16[128,2048]{1,0:T(8,128)(2,1)S(1)}) custom-call(bf16[128,2048]{1,0:T(8,128)(2,1)S(1)} %collective-permute-done.10.refs_0_, bf16[128,2048]{1,0:T(8,128)(2,1)S(1)} %collective-permute-done.12.refs_1_, bf16[32,2,64,2048]{3,2,1,0:T(8,128)(2,1)} %bitcast.11), custom_call_target="tpu_custom_call" | custom-call | tf_op jit(solution)/shard_map/feed/pallas_call | solution.py:384
  114.8 2.7 %collective-permute-start.17 = (bf16[128,2048]{1,0:T(8,128)(2,1)S(1)}, bf16[128,2048]{1,0:T(8,128)(2,1)S(1)}, u32[]{:S(2)}, u32[]{:S(2)}) collective-permute-start(bf16[128,2048]{1,0:T(8,128)(2,1)S(1)} %get-tuple-element.50), channel_id=1, source_target_pairs={{0,3},{1,0},{2,1},{3,2},{4,7},{5,4},{6,5},{7,6},{8,11},{9,8},{10,9... | collective-permute-start | bytes 1572872 | tf_op jit(solution)/shard_map/ppermute | solution.py:19
  117.5 7.9 %feed.5 = (bf16[128,2048]{1,0:T(8,128)(2,1)S(1)}, bf16[128,2048]{1,0:T(8,128)(2,1)S(1)}) custom-call(bf16[128,2048]{1,0:T(8,128)(2,1)S(1)} %collective-permute-done.8.refs_0_, bf16[128,2048]{1,0:T(8,128)(2,1)S(1)} %collective-permute-done.9.refs_1_, bf16[32,2,64,2048]{3,2,1,0:T(8,128)(2,1)} %bitcast.12), custom_call_target="tpu_custom_call" | custom-call | tf_op jit(solution)/shard_map/feed/pallas_call | solution.py:384
  125.6 1.5 collective-permute-start.19
  127.6 7.9 %feed.4 = (bf16[128,2048]{1,0:T(8,128)(2,1)S(1)}, bf16[128,2048]{1,0:T(8,128)(2,1)S(1)}) custom-call(bf16[128,2048]{1,0:T(8,128)(2,1)S(1)} %get-tuple-element.42.refs_0_, bf16[128,2048]{1,0:T(8,128)(2,1)S(1)} %get-tuple-element.43.refs_1_, bf16[32,2,64,2048]{3,2,1,0:T(8,128)(2,1)} %bitcast.13), custom_call_target="tpu_custom_call" | custom-call | tf_op jit(solution)/shard_map/feed/pallas_call | solution.py:384
  135.5 5.2 %collective-permute-done.19.refs_7_ = bf16[128,2048]{1,0:T(8,128)(2,1)S(1)} collective-permute-done((bf16[128,2048]{1,0:T(8,128)(2,1)S(1)}, bf16[128,2048]{1,0:T(8,128)(2,1)S(1)}, u32[]{:S(2)}, u32[]{:S(2)}) %collective-permute-start.19) | collective-permute-done | bytes 524320 | tf_op jit(solution)/shard_map/ppermute | solution.py:19
  140.8 3.5 %collective-permute-done.15.refs_4_ = bf16[128,2048]{1,0:T(8,128)(2,1)S(1)} collective-permute-done((bf16[128,2048]{1,0:T(8,128)(2,1)S(1)}, bf16[128,2048]{1,0:T(8,128)(2,1)S(1)}, u32[]{:S(2)}, u32[]{:S(2)}) %collective-permute-start.15) | collective-permute-done | bytes 524320 | tf_op jit(solution)/shard_map/ppermute | solution.py:19
  144.3 2.5 %norm.3 = bf16[256,2048]{1,0:T(8,128)(2,1)} custom-call(bf16[128,2048]{1,0:T(8,128)(2,1)S(1)} %get-tuple-element.42.refs_0_, bf16[128,2048]{1,0:T(8,128)(2,1)S(1)} %get-tuple-element.43.refs_1_, bf16[128,2048]{1,0:T(8,128)(2,1)S(1)} %get-tuple-element.45.refs_2_, bf16[128,2048]{1,0:T(8,128)(2,1)S(1)} %get-tuple-element.46.refs_3_, ...), custom_call_target="tpu_custom_call" | custom-call | tf_op jit(solution)/shard_map/norm/pallas_call | solution.py:288
  (50 shorter events, 5.2 us)
Async XLA Ops:
  6.5 9.3 %copy-start = (bf16[2,1024,256]{2,1,0:T(8,128)(2,1)S(1)}, bf16[2,1024,256]{2,1,0:T(8,128)(2,1)}, u32[]{:S(2)}) copy-start(bf16[2,1024,256]{2,1,0:T(8,128)(2,1)} %keys_values.1) | copy-start | bytes 3145732
  6.5 9.3 %copy-start.1 = (bf16[1024,512]{1,0:T(8,128)(2,1)S(1)}, bf16[1024,512]{1,0:T(8,128)(2,1)}, u32[]{:S(2)}) copy-start(bf16[1024,512]{1,0:T(8,128)(2,1)} %refs_0_.2) | copy-start | bytes 3145732
  6.5 88.0 %all-gather.2.cloned.1.call-start = ((), (), s32[]{:S(2)}) async-start(), calls=%async_computation | async-start | bytes 17301504 | tf_op jit(solution)/shard_map/all_gather | solution.py:417
  9.3 8.3 %collective-permute-start = (bf16[2,128,256]{2,1,0:T(8,128)(2,1)}, bf16[2,128,256]{2,1,0:T(8,128)(2,1)S(1)}, u32[]{:S(2)}, u32[]{:S(2)}) collective-permute-start(bf16[2,128,256]{2,1,0:T(8,128)(2,1)} %get-tuple-element.30), channel_id=1, source_target_pairs={{0,4},{4,8},{8,12},{12,16},{16,20},{20,24},{24,28},{28,32},{32,36}... | collective-permute-start | bytes 393224 | tf_op jit(solution)/shard_map/ppermute | solution.py:91
  13.9 6.5 %copy-start.11 = (f32[8]{0:T(128)S(1)}, f32[8]{0:T(128)}, u32[]{:S(2)}) copy-start(f32[8]{0:T(128)} %sink.5) | copy-start | bytes 100
  13.9 6.5 %collective-permute-start.1 = (bf16[2,128,256]{2,1,0:T(8,128)(2,1)}, bf16[2,128,256]{2,1,0:T(8,128)(2,1)S(1)}, u32[]{:S(2)}, u32[]{:S(2)}) collective-permute-start(bf16[2,128,256]{2,1,0:T(8,128)(2,1)} %get-tuple-element.32), channel_id=1, source_target_pairs={{4,0},{8,4},{12,8},{16,12},{20,16},{24,20},{28,24},{32,28},{36,32}... | collective-permute-start | bytes 393224 | tf_op jit(solution)/shard_map/ppermute | solution.py:92
  24.1 12.9 %collective-permute-start.6 = (bf16[128,2048]{1,0:T(8,128)(2,1)S(1)}, bf16[128,2048]{1,0:T(8,128)(2,1)S(1)}, u32[]{:S(2)}, u32[]{:S(2)}) collective-permute-start(bf16[128,2048]{1,0:T(8,128)(2,1)S(1)} %get-tuple-element.41), channel_id=1, source_target_pairs={{0,3},{1,0},{2,1},{3,2},{4,7},{5,4},{6,5},{7,6},{8,11},{9,8},{10,9... | collective-permute-start | bytes 1572872 | tf_op jit(solution)/shard_map/ppermute | solution.py:19
  26.6 15.1 %collective-permute-start.2 = (bf16[128,2048]{1,0:T(8,128)(2,1)S(1)}, bf16[128,2048]{1,0:T(8,128)(2,1)S(1)}, u32[]{:S(2)}, u32[]{:S(2)}) collective-permute-start(bf16[128,2048]{1,0:T(8,128)(2,1)S(1)} %get-tuple-element.37), channel_id=1, source_target_pairs={{0,1},{1,2},{2,3},{3,0},{4,5},{5,6},{6,7},{7,4},{8,9},{9,10},{10,1... | collective-permute-start | bytes 1572872 | tf_op jit(solution)/shard_map/ppermute | solution.py:19
  33.3 19.8 %collective-permute-start.4 = (bf16[128,2048]{1,0:T(8,128)(2,1)S(1)}, bf16[128,2048]{1,0:T(8,128)(2,1)S(1)}, u32[]{:S(2)}, u32[]{:S(2)}) collective-permute-start(bf16[128,2048]{1,0:T(8,128)(2,1)S(1)} %get-tuple-element.38), channel_id=1, source_target_pairs={{0,1},{1,2},{2,3},{3,0},{4,5},{5,6},{6,7},{7,4},{8,9},{9,10},{10,1... | collective-permute-start | bytes 1572872 | tf_op jit(solution)/shard_map/ppermute | solution.py:19
  33.6 19.6 %collective-permute-start.5 = (bf16[128,2048]{1,0:T(8,128)(2,1)S(1)}, bf16[128,2048]{1,0:T(8,128)(2,1)S(1)}, u32[]{:S(2)}, u32[]{:S(2)}) collective-permute-start(bf16[128,2048]{1,0:T(8,128)(2,1)S(1)} %get-tuple-element.39), channel_id=1, source_target_pairs={{0,3},{1,0},{2,1},{3,2},{4,7},{5,4},{6,5},{7,6},{8,11},{9,8},{10,9... | collective-permute-start | bytes 1572872 | tf_op jit(solution)/shard_map/ppermute | solution.py:19
  37.1 21.1 %collective-permute-start.7 = (bf16[128,2048]{1,0:T(8,128)(2,1)S(1)}, bf16[128,2048]{1,0:T(8,128)(2,1)S(1)}, u32[]{:S(2)}, u32[]{:S(2)}) collective-permute-start(bf16[128,2048]{1,0:T(8,128)(2,1)S(1)} %add_convert_fusion.2), channel_id=1, source_target_pairs={{0,3},{1,0},{2,1},{3,2},{4,7},{5,4},{6,5},{7,6},{8,11},{9,8},{10,9... | collective-permute-start | bytes 1572872 | tf_op jit(solution)/shard_map/ppermute | solution.py:19
  41.9 20.2 %copy-start.2 = (bf16[256,2048]{1,0:T(8,128)(2,1)S(1)}, bf16[256,2048]{1,0:T(8,128)(2,1)}, u32[]{:S(2)}) copy-start(bf16[256,2048]{1,0:T(8,128)(2,1)} %refs_0_.3) | copy-start | bytes 3145732
  41.9 20.1 %copy-start.7 = (f32[2048]{0:T(1024)S(1)}, f32[2048]{0:T(1024)}, u32[]{:S(2)}) copy-start(f32[2048]{0:T(1024)} %param.16) | copy-start | bytes 24580
  41.9 20.1 %copy-start.8 = (f32[2048]{0:T(1024)S(1)}, f32[2048]{0:T(1024)}, u32[]{:S(2)}) copy-start(f32[2048]{0:T(1024)} %param.17) | copy-start | bytes 24580
  42.0 20.1 %collective-permute-start.3 = (bf16[128,2048]{1,0:T(8,128)(2,1)S(1)}, bf16[128,2048]{1,0:T(8,128)(2,1)S(1)}, u32[]{:S(2)}, u32[]{:S(2)}) collective-permute-start(bf16[128,2048]{1,0:T(8,128)(2,1)S(1)} %add_convert_fusion.3), channel_id=1, source_target_pairs={{0,1},{1,2},{2,3},{3,0},{4,5},{5,6},{6,7},{7,4},{8,9},{9,10},{10,1... | collective-permute-start | bytes 1572872 | tf_op jit(solution)/shard_map/ppermute | solution.py:19
  64.0 13.8 %collective-permute-start.10 = (bf16[128,2048]{1,0:T(8,128)(2,1)S(1)}, bf16[128,2048]{1,0:T(8,128)(2,1)S(1)}, u32[]{:S(2)}, u32[]{:S(2)}) collective-permute-start(bf16[128,2048]{1,0:T(8,128)(2,1)S(1)} %get-tuple-element.42.refs_0_), channel_id=1, source_target_pairs={{0,1},{1,2},{2,3},{3,0},{4,5},{5,6},{6,7},{7,4},{8,9},{9,10},{10,1... | collective-permute-start | bytes 1572872 | tf_op jit(solution)/shard_map/ppermute | solution.py:19
  64.1 13.7 %collective-permute-start.12 = (bf16[128,2048]{1,0:T(8,128)(2,1)S(1)}, bf16[128,2048]{1,0:T(8,128)(2,1)S(1)}, u32[]{:S(2)}, u32[]{:S(2)}) collective-permute-start(bf16[128,2048]{1,0:T(8,128)(2,1)S(1)} %get-tuple-element.43.refs_1_), channel_id=1, source_target_pairs={{0,3},{1,0},{2,1},{3,2},{4,7},{5,4},{6,5},{7,6},{8,11},{9,8},{10,9... | collective-permute-start | bytes 1572872 | tf_op jit(solution)/shard_map/ppermute | solution.py:19
  77.8 15.2 %collective-permute-start.11 = (bf16[128,2048]{1,0:T(8,128)(2,1)S(1)}, bf16[128,2048]{1,0:T(8,128)(2,1)S(1)}, u32[]{:S(2)}, u32[]{:S(2)}) collective-permute-start(bf16[128,2048]{1,0:T(8,128)(2,1)S(1)} %collective-permute-done.10.refs_0_), channel_id=1, source_target_pairs={{0,1},{1,2},{2,3},{3,0},{4,5},{5,6},{6,7},{7,4},{8,9},{9,10},{10,1... | collective-permute-start | bytes 1572872 | tf_op jit(solution)/shard_map/ppermute | solution.py:19
  77.8 15.9 %collective-permute-start.13 = (bf16[128,2048]{1,0:T(8,128)(2,1)S(1)}, bf16[128,2048]{1,0:T(8,128)(2,1)S(1)}, u32[]{:S(2)}, u32[]{:S(2)}) collective-permute-start(bf16[128,2048]{1,0:T(8,128)(2,1)S(1)} %collective-permute-done.12.refs_1_), channel_id=1, source_target_pairs={{0,3},{1,0},{2,1},{3,2},{4,7},{5,4},{6,5},{7,6},{8,11},{9,8},{10,9... | collective-permute-start | bytes 1572872 | tf_op jit(solution)/shard_map/ppermute | solution.py:19
  80.7 34.0 %collective-permute-start.8 = (bf16[128,2048]{1,0:T(8,128)(2,1)S(1)}, bf16[128,2048]{1,0:T(8,128)(2,1)S(1)}, u32[]{:S(2)}, u32[]{:S(2)}) collective-permute-start(bf16[128,2048]{1,0:T(8,128)(2,1)S(1)} %get-tuple-element.43.refs_1_), channel_id=1, source_target_pairs={{0,1},{1,2},{2,3},{3,0},{4,5},{5,6},{6,7},{7,4},{8,9},{9,10},{10,1... | collective-permute-start | bytes 1572872 | tf_op jit(solution)/shard_map/ppermute | solution.py:19
  80.7 36.8 %collective-permute-start.9 = (bf16[128,2048]{1,0:T(8,128)(2,1)S(1)}, bf16[128,2048]{1,0:T(8,128)(2,1)S(1)}, u32[]{:S(2)}, u32[]{:S(2)}) collective-permute-start(bf16[128,2048]{1,0:T(8,128)(2,1)S(1)} %get-tuple-element.42.refs_0_), channel_id=1, source_target_pairs={{0,3},{1,0},{2,1},{3,2},{4,7},{5,4},{6,5},{7,6},{8,11},{9,8},{10,9... | collective-permute-start | bytes 1572872 | tf_op jit(solution)/shard_map/ppermute | solution.py:19
  93.7 0.8 copy-start.5
  94.6 1.0 copy-start.4
  95.6 1.0 copy-start.6
  104.6 20.9 %collective-permute-start.18 = (bf16[128,2048]{1,0:T(8,128)(2,1)S(1)}, bf16[128,2048]{1,0:T(8,128)(2,1)S(1)}, u32[]{:S(2)}, u32[]{:S(2)}) collective-permute-start(bf16[128,2048]{1,0:T(8,128)(2,1)S(1)} %get-tuple-element.52), channel_id=1, source_target_pairs={{0,3},{1,0},{2,1},{3,2},{4,7},{5,4},{6,5},{7,6},{8,11},{9,8},{10,9... | collective-permute-start | bytes 1572872 | tf_op jit(solution)/shard_map/ppermute | solution.py:19
  106.8 20.3 %collective-permute-start.14 = (bf16[128,2048]{1,0:T(8,128)(2,1)S(1)}, bf16[128,2048]{1,0:T(8,128)(2,1)S(1)}, u32[]{:S(2)}, u32[]{:S(2)}) collective-permute-start(bf16[128,2048]{1,0:T(8,128)(2,1)S(1)} %get-tuple-element.48), channel_id=1, source_target_pairs={{0,1},{1,2},{2,3},{3,0},{4,5},{5,6},{6,7},{7,4},{8,9},{9,10},{10,1... | collective-permute-start | bytes 1572872 | tf_op jit(solution)/shard_map/ppermute | solution.py:19
  114.7 20.8 %collective-permute-start.16 = (bf16[128,2048]{1,0:T(8,128)(2,1)S(1)}, bf16[128,2048]{1,0:T(8,128)(2,1)S(1)}, u32[]{:S(2)}, u32[]{:S(2)}) collective-permute-start(bf16[128,2048]{1,0:T(8,128)(2,1)S(1)} %get-tuple-element.49), channel_id=1, source_target_pairs={{0,1},{1,2},{2,3},{3,0},{4,5},{5,6},{6,7},{7,4},{8,9},{9,10},{10,1... | collective-permute-start | bytes 1572872 | tf_op jit(solution)/shard_map/ppermute | solution.py:19
  114.8 20.7 %collective-permute-start.17 = (bf16[128,2048]{1,0:T(8,128)(2,1)S(1)}, bf16[128,2048]{1,0:T(8,128)(2,1)S(1)}, u32[]{:S(2)}, u32[]{:S(2)}) collective-permute-start(bf16[128,2048]{1,0:T(8,128)(2,1)S(1)} %get-tuple-element.50), channel_id=1, source_target_pairs={{0,3},{1,0},{2,1},{3,2},{4,7},{5,4},{6,5},{7,6},{8,11},{9,8},{10,9... | collective-permute-start | bytes 1572872 | tf_op jit(solution)/shard_map/ppermute | solution.py:19
  125.6 15.2 %collective-permute-start.19 = (bf16[128,2048]{1,0:T(8,128)(2,1)S(1)}, bf16[128,2048]{1,0:T(8,128)(2,1)S(1)}, u32[]{:S(2)}, u32[]{:S(2)}) collective-permute-start(bf16[128,2048]{1,0:T(8,128)(2,1)S(1)} %add_convert_fusion), channel_id=1, source_target_pairs={{0,3},{1,0},{2,1},{3,2},{4,7},{5,4},{6,5},{7,6},{8,11},{9,8},{10,9... | collective-permute-start | bytes 1572872 | tf_op jit(solution)/shard_map/ppermute | solution.py:19
  127.2 17.1 %copy-start.9 = (f32[2048]{0:T(1024)S(1)}, f32[2048]{0:T(1024)}, u32[]{:S(2)}) copy-start(f32[2048]{0:T(1024)} %param.20) | copy-start | bytes 24580
  127.2 17.1 %copy-start.10 = (f32[2048]{0:T(1024)S(1)}, f32[2048]{0:T(1024)}, u32[]{:S(2)}) copy-start(f32[2048]{0:T(1024)} %param.21) | copy-start | bytes 24580
  127.2 17.1 %collective-permute-start.15 = (bf16[128,2048]{1,0:T(8,128)(2,1)S(1)}, bf16[128,2048]{1,0:T(8,128)(2,1)S(1)}, u32[]{:S(2)}, u32[]{:S(2)}) collective-permute-start(bf16[128,2048]{1,0:T(8,128)(2,1)S(1)} %add_convert_fusion.1), channel_id=1, source_target_pairs={{0,1},{1,2},{2,3},{3,0},{4,5},{5,6},{6,7},{7,4},{8,9},{9,10},{10,1... | collective-permute-start | bytes 1572872 | tf_op jit(solution)/shard_map/ppermute | solution.py:19
  (1 other events, 0.8 us)
Sparse Core Ops, SparseCore 0:
  9.6 76.3 all-gather.1

commit v8 on v7

--- a/solution.py
+++ b/solution.py
@@ -304,48 +304,58 @@
     return (part.astype(jnp.float32) + arrived.astype(jnp.float32)).astype(jnp.bfloat16)
 
 
-def feed_kernel(*refs, count, outs, chunk):
-    rows, weights, results = (refs[:count], refs[count], refs[count + 1 : count + 1 + outs])
-    tokens, up, down, activation, branch, sems = refs[count + 1 + outs :]
+def feed_kernel(*refs, count, chunk, resident):
+    rows, rest = (refs[:count], refs[count:])
+    if resident:
+        up, down, *rest = rest
+    else:
+        weights, *rest = rest
+    results, rest = (rest[:count], rest[count:])
+    if not resident:
+        up, down, *rest = rest
+    tokens, activation, branch, sems, *load_sems = rest
     pieces, height, units = up.shape
     size, steps = (rows[0].shape[0], units // chunk)
-    height_out = results[0].shape[0]
     part = pieces // steps
     width = part * height
 
     def row_copy(index):
         span = pl.ds(index * size, size)
-        return pltpu.make_async_copy(rows[index], tokens.at[span], sems.at[2 * steps + index])
+        return pltpu.make_async_copy(rows[index], tokens.at[span], sems.at[index])
 
     def up_copy(k):
         cols = pl.ds(pl.multiple_of(k * chunk, chunk), chunk)
-        return pltpu.make_async_copy(weights.at[:, 0, :, cols], up.at[:, :, cols], sems.at[k])
+        return pltpu.make_async_copy(
+            weights.at[:, 0, :, cols], up.at[:, :, cols], load_sems[0].at[k]
+        )
 
     def down_copy(k):
         span = pl.ds(k * part, part)
-        return pltpu.make_async_copy(weights.at[span, 1], down.at[span], sems.at[steps + k])
+        return pltpu.make_async_copy(
+            weights.at[span, 1], down.at[span], load_sems[0].at[steps + k]
+        )
 
     def out_copy(index, k):
         cols = pl.ds(pl.multiple_of(k * width, width), width)
-        span = pl.ds(index * height_out, height_out)
+        span = pl.ds(index * size, size)
         return pltpu.make_async_copy(
-            branch.at[span, cols],
-            results[index].at[:, cols],
-            sems.at[2 * steps + count + index * steps + k],
+            branch.at[span, cols], results[index].at[:, cols], sems.at[count + index * steps + k]
         )
 
     for index in range(count):
         row_copy(index).start()
-    for k in range(steps):
-        up_copy(k).start()
-    for k in range(steps):
-        down_copy(k).start()
+    if not resident:
+        for k in range(steps):
+            up_copy(k).start()
+        for k in range(steps):
+            down_copy(k).start()
     for index in range(count):
         row_copy(index).wait()
 
     @pl.loop(0, steps)
     def _(k):
-        up_copy(k).wait()
+        if not resident:
+            up_copy(k).wait()
         cols = pl.ds(pl.multiple_of(k * chunk, chunk), chunk)
         hidden = jnp.dot(
             tokens[...],
@@ -356,7 +366,8 @@
 
     @pl.loop(0, steps)
     def _(k):
-        down_copy(k).wait()
+        if not resident:
+            down_copy(k).wait()
         cols = pl.ds(pl.multiple_of(k * width, width), width)
         branch[:, cols] = lax.dot_general(
             activation[...],
@@ -364,39 +375,46 @@
             (((1,), (1,)), ((), ())),
             preferred_element_type=jnp.float32,
         ).astype(jnp.bfloat16)
-        for index in range(outs):
+        for index in range(count):
             out_copy(index, k).start()
 
     @pl.loop(0, steps)
     def _(k):
-        for index in range(outs):
+        for index in range(count):
             out_copy(index, k).wait()
 
 
-def feed_forward(rows, weights, height_out, chunk=512):
+def feed_forward(rows, weights):
+    resident = len(weights) == 2
+    chunk = 1024 if resident else 512
     size, width = rows[0].shape
-    pieces, _, height, units = weights.shape
-    count, total = (len(rows), len(rows) * size)
-    outs = total // height_out
+    count, total = (len(rows), len(rows) * rows[0].shape[0])
+    if resident:
+        pieces, height, units = weights[0].shape
+    else:
+        pieces, _, height, units = weights[0].shape
+    steps = units // chunk
     anywhere = pl.BlockSpec(memory_space=pl.ANY)
-    full = pltpu.VMEM((pieces, height, units), jnp.bfloat16)
-    steps = units // chunk
+    vmem = pl.BlockSpec(memory_space=pltpu.VMEM)
+    held = [] if resident else [jax.ShapeDtypeStruct((pieces, height, units), jnp.bfloat16)] * 2
+    load_sems = [] if resident else [pltpu.SemaphoreType.DMA((2 * steps,))]
     return pl.pallas_call(
-        functools.partial(feed_kernel, count=count, outs=outs, chunk=chunk),
-        in_specs=[anywhere] * (count + 1),
-        out_specs=[anywhere] * outs,
-        out_shape=[jax.ShapeDtypeStruct((height_out, width), jnp.bfloat16)] * outs,
+        functools.partial(feed_kernel, count=count, chunk=chunk, resident=resident),
+        in_specs=[anywhere] * count + ([vmem] * 2 if resident else [anywhere]),
+        out_specs=[anywhere] * count + [vmem] * len(held),
+        out_shape=[jax.ShapeDtypeStruct((size, width), jnp.bfloat16)] * count + held,
         scratch_shapes=[
             pltpu.VMEM((total, width), jnp.bfloat16),
-            full,
-            full,
             pltpu.VMEM((total, units), jnp.bfloat16),
             pltpu.VMEM((total, width), jnp.bfloat16),
-            pltpu.SemaphoreType.DMA((2 * steps + count + outs * steps,)),
+            pltpu.SemaphoreType.DMA((count + count * steps,)),
+            *load_sems,
         ],
-        compiler_params=pltpu.CompilerParams(vmem_limit_bytes=40 * 1024 * 1024),
+        compiler_params=pltpu.CompilerParams(
+            vmem_limit_bytes=(12 if resident else 32) * 1024 * 1024
+        ),
         name="feed",
-    )(*rows, weights)
+    )(*rows, *weights)
 
 
 def layer(
@@ -434,7 +452,7 @@
     own_top, own_bottom = run(0)
     left_sum = shift(added(right_top, from_left), 1)
     right_sum = shift(added(left_bottom, from_right), -1)
-    rows, half = (2 * own_top.shape[0], own_top.shape[0])
+    rows = 2 * own_top.shape[0]
     first_top, first_bottom = norm_rows(
         (residual_in, own_top, own_bottom, left_sum, left_plain, right_plain, right_sum),
         (0, 1, 3, 5),
@@ -451,16 +469,16 @@
     row_rt = shift(first_top, -1)
     row_ft = shift(row_lt, 1)
     row_fb = shift(row_rb, -1)
-    left_top, right_bottom = feed_forward((row_lt, row_rb), weights, half)
+    left_top, right_bottom, *held = feed_forward((row_lt, row_rb), (weights,))
     left_plain = shift(right_bottom, 1)
     right_plain = shift(left_top, -1)
-    far_top, far_bottom = feed_forward((row_ft, row_fb), weights, half)
+    far_top, far_bottom = feed_forward((row_ft, row_fb), held)
     from_left = shift(far_top, 1)
     from_right = shift(far_bottom, -1)
-    left_bottom, right_top = feed_forward((row_lb, row_rt), weights, half)
+    left_bottom, right_top = feed_forward((row_lb, row_rt), held)
     left_sum = shift(added(right_top, from_left), 1)
     right_sum = shift(added(left_bottom, from_right), -1)
-    own_top, own_bottom = feed_forward((first_top, first_bottom), weights, half)
+    own_top, own_bottom = feed_forward((first_top, first_bottom), held)
     (out,) = norm_rows(
         (
             first_top,

time: 155 us -> 153 us (0.987)
  the two profiles are of different devices: /device:TPU:1 before, /device:TPU:24 now
where the time goes in v8:
time: 153 us
  waiting for transfers between devices  51.8 us (34%)
  Pallas kernels  47.7 us (31%)
  starting transfers between devices  35.9 us (23%)
  between operations  13.7 us (9%)
  local copies, waits for them, and re-layouts  3.2 us (2%)
    ppermute x18, waiting for transfers between devices, shift(): lax.ppermute(value, axis, [(i, (i + step) % devices) for i in range(devic...  51.8 us
    ppermute x18, starting transfers between devices, shift(): lax.ppermute(value, axis, [(i, (i + step) % devices) for i in range(devic...  30.3 us
    pallas_call x4, Pallas kernels, feed_forward(): pl.pallas_call(functools.partial(feed_kernel, count=count, chunk=chunk, r...  24.9 us
    pallas_call x3, Pallas kernels, attend(): pl.pallas_call(functools.partial(attend_kernel, rels=rels), grid=(steps,)...  14.1 us
    pallas_call x2, Pallas kernels, norm_rows(): pl.pallas_call(functools.partial(norm_kernel, tops=tops, bottoms=bottoms,...  4.43 us
    ppermute x1, starting transfers between devices, halo(): after = lax.ppermute(first, axis, down)  3.64 us
    unnamed x16, local copies, waits for them, and re-layouts  3.2 us
  transfers between devices with their start and end apart: 21, of which 12 were waited for; matrix products, arithmetic and copies ran while one was open for 0% of the time, Pallas kernels for 28%

profile of v8, /device:TPU:24, one launch (start us, length us, event | category | flops | bytes accessed | tf_op | source)
XLA Modules:
  0.0 152.8 jit_solution(4013280037411478103)
XLA Ops:
  6.5 2.6 %prepare.1 = (bf16[128,2048]{1,0:T(8,128)(2,1)}, bf16[2,128,256]{2,1,0:T(8,128)(2,1)}, bf16[2,128,256]{2,1,0:T(8,128)(2,1)}) custom-call(bf16[64,2048]{1,0:T(8,128)(2,1)} %up.1, bf16[64,2048]{1,0:T(8,128)(2,1)} %bitcast.11, bf16[2,1024,256]{2,1,0:T(8,128)(2,1)} %keys_values.1), custom_call_target="tpu_custom_call" | custom-call | tf_op jit(solution)/shard_map/prepare/pallas_call | solution.py:49
  9.1 1.9 %collective-permute-start = (bf16[2,128,256]{2,1,0:T(8,128)(2,1)}, bf16[2,128,256]{2,1,0:T(8,128)(2,1)S(1)}, u32[]{:S(2)}, u32[]{:S(2)}) collective-permute-start(bf16[2,128,256]{2,1,0:T(8,128)(2,1)} %get-tuple-element.32), channel_id=1, source_target_pairs={{0,4},{4,8},{8,12},{12,16},{16,20},{20,24},{24,28},{28,32},{32,36}... | collective-permute-start | bytes 393224 | tf_op jit(solution)/shard_map/ppermute | solution.py:91
  11.1 3.6 %collective-permute-start.1 = (bf16[2,128,256]{2,1,0:T(8,128)(2,1)}, bf16[2,128,256]{2,1,0:T(8,128)(2,1)S(1)}, u32[]{:S(2)}, u32[]{:S(2)}) collective-permute-start(bf16[2,128,256]{2,1,0:T(8,128)(2,1)} %get-tuple-element.34), channel_id=1, source_target_pairs={{4,0},{8,4},{12,8},{16,12},{20,16},{24,20},{28,24},{32,28},{36,32}... | collective-permute-start | bytes 393224 | tf_op jit(solution)/shard_map/ppermute | solution.py:92
  15.9 1.2 copy-done.1
  17.2 1.8 %fetch.1 = (bf16[1024,512]{1,0:T(8,128)(2,1)S(1)}, bf16[2,1024,256]{2,1,0:T(8,128)(2,1)S(1)}, bf16[512,2048]{1,0:T(8,128)(2,1)S(1)}) custom-call(bf16[1024,512]{1,0:T(8,128)(2,1)S(1)} %copy-done.1, bf16[2,1024,256]{2,1,0:T(8,128)(2,1)S(1)} %copy-done, bf16[512,2048]{1,0:T(8,128)(2,1)} %refs_2_.1), custom_call_target="tpu_custom_call" | custom-call | tf_op jit(solution)/shard_map/fetch/pallas_call | solution.py:76
  19.7 3.7 %attend.5 = (bf16[128,2048]{1,0:T(8,128)(2,1)S(1)}, bf16[128,2048]{1,0:T(8,128)(2,1)S(1)}) custom-call(f32[8]{0:T(128)S(1)} %copy-done.7, bf16[1024,512]{1,0:T(8,128)(2,1)S(1)} %get-tuple-element.31.q_hbm, bf16[2,128,256]{2,1,0:T(8,128)(2,1)S(1)} %collective-permute-done.before_ref, bf16[2,1024,256]{2,1,0:T(8,128)(2,1)S(1)} %get-tuple-element.33.mid_ref, ...), custom_call_target="tpu_custom_call" | custom-call | tf_op jit(solution)/shard_map/attend/pallas_call | solution.py:211
  23.4 2.8 %collective-permute-start.6 = (bf16[128,2048]{1,0:T(8,128)(2,1)S(1)}, bf16[128,2048]{1,0:T(8,128)(2,1)S(1)}, u32[]{:S(2)}, u32[]{:S(2)}) collective-permute-start(bf16[128,2048]{1,0:T(8,128)(2,1)S(1)} %get-tuple-element.43), channel_id=1, source_target_pairs={{0,3},{1,0},{2,1},{3,2},{4,7},{5,4},{6,5},{7,6},{8,11},{9,8},{10,9... | collective-permute-start | bytes 1572872 | tf_op jit(solution)/shard_map/ppermute | solution.py:19
  26.3 6.7 %attend.4 = (bf16[128,2048]{1,0:T(8,128)(2,1)S(1)}, bf16[128,2048]{1,0:T(8,128)(2,1)S(1)}, bf16[128,2048]{1,0:T(8,128)(2,1)S(1)}, bf16[128,2048]{1,0:T(8,128)(2,1)S(1)}) custom-call(f32[8]{0:T(128)S(1)} %copy-done.7, bf16[1024,512]{1,0:T(8,128)(2,1)S(1)} %get-tuple-element.31.q_hbm, bf16[2,128,256]{2,1,0:T(8,128)(2,1)S(1)} %collective-permute-done.before_ref, ...), custom_call_target="tpu_custom_call" | custom-call | tf_op jit(solution)/shard_map/attend/pallas_call | solution.py:211
  33.8 2.6 %collective-permute-start.5 = (bf16[128,2048]{1,0:T(8,128)(2,1)S(1)}, bf16[128,2048]{1,0:T(8,128)(2,1)S(1)}, u32[]{:S(2)}, u32[]{:S(2)}) collective-permute-start(bf16[128,2048]{1,0:T(8,128)(2,1)S(1)} %get-tuple-element.41), channel_id=1, source_target_pairs={{0,3},{1,0},{2,1},{3,2},{4,7},{5,4},{6,5},{7,6},{8,11},{9,8},{10,9... | collective-permute-start | bytes 1572872 | tf_op jit(solution)/shard_map/ppermute | solution.py:19
  37.4 3.8 %collective-permute-start.7 = (bf16[128,2048]{1,0:T(8,128)(2,1)S(1)}, bf16[128,2048]{1,0:T(8,128)(2,1)S(1)}, u32[]{:S(2)}, u32[]{:S(2)}) collective-permute-start(bf16[128,2048]{1,0:T(8,128)(2,1)S(1)} %add_convert_fusion.2), channel_id=1, source_target_pairs={{0,3},{1,0},{2,1},{3,2},{4,7},{5,4},{6,5},{7,6},{8,11},{9,8},{10,9... | collective-permute-start | bytes 1572872 | tf_op jit(solution)/shard_map/ppermute | solution.py:19
  41.6 3.7 %attend.3 = (bf16[128,2048]{1,0:T(8,128)(2,1)S(1)}, bf16[128,2048]{1,0:T(8,128)(2,1)S(1)}) custom-call(f32[8]{0:T(128)S(1)} %copy-done.7, bf16[1024,512]{1,0:T(8,128)(2,1)S(1)} %get-tuple-element.31.q_hbm, bf16[2,128,256]{2,1,0:T(8,128)(2,1)S(1)} %collective-permute-done.before_ref, bf16[2,1024,256]{2,1,0:T(8,128)(2,1)S(1)} %get-tuple-element.33.mid_ref, ...), custom_call_target="tpu_custom_call" | custom-call | tf_op jit(solution)/shard_map/attend/pallas_call | solution.py:211
  45.3 7.1 %collective-permute-done.4.refs_4_ = bf16[128,2048]{1,0:T(8,128)(2,1)S(1)} collective-permute-done((bf16[128,2048]{1,0:T(8,128)(2,1)S(1)}, bf16[128,2048]{1,0:T(8,128)(2,1)S(1)}, u32[]{:S(2)}, u32[]{:S(2)}) %collective-permute-start.4) | collective-permute-done | bytes 524320 | tf_op jit(solution)/shard_map/ppermute | solution.py:19
  52.5 7.4 %collective-permute-done.7.refs_6_ = bf16[128,2048]{1,0:T(8,128)(2,1)S(1)} collective-permute-done((bf16[128,2048]{1,0:T(8,128)(2,1)S(1)}, bf16[128,2048]{1,0:T(8,128)(2,1)S(1)}, u32[]{:S(2)}, u32[]{:S(2)}) %collective-permute-start.7) | collective-permute-done | bytes 524320 | tf_op jit(solution)/shard_map/ppermute | solution.py:19
  59.9 3.8 %collective-permute-done.3.refs_3_ = bf16[128,2048]{1,0:T(8,128)(2,1)S(1)} collective-permute-done((bf16[128,2048]{1,0:T(8,128)(2,1)S(1)}, bf16[128,2048]{1,0:T(8,128)(2,1)S(1)}, u32[]{:S(2)}, u32[]{:S(2)}) %collective-permute-start.3) | collective-permute-done | bytes 524320 | tf_op jit(solution)/shard_map/ppermute | solution.py:19
  63.7 1.9 %norm.2 = (bf16[128,2048]{1,0:T(8,128)(2,1)S(1)}, bf16[128,2048]{1,0:T(8,128)(2,1)S(1)}) custom-call(bf16[256,2048]{1,0:T(8,128)(2,1)S(1)} %copy-done.2, bf16[128,2048]{1,0:T(8,128)(2,1)S(1)} %get-tuple-element.36.refs_1_, bf16[128,2048]{1,0:T(8,128)(2,1)S(1)} %get-tuple-element.37.refs_2_, bf16[128,2048]{1,0:T(8,128)(2,1)S(1)} %collective-permute-done.3.refs_3_, ...), custom_call_target="tpu_custom_call" | custom-call | tf_op jit(solution)/shard_map/norm/pallas_call | solution.py:288
  65.7 3.2 %collective-permute-start.9 = (bf16[128,2048]{1,0:T(8,128)(2,1)S(1)}, bf16[128,2048]{1,0:T(8,128)(2,1)S(1)}, u32[]{:S(2)}, u32[]{:S(2)}) collective-permute-start(bf16[128,2048]{1,0:T(8,128)(2,1)S(1)} %get-tuple-element.45.refs_1_), channel_id=1, source_target_pairs={{0,3},{1,0},{2,1},{3,2},{4,7},{5,4},{6,5},{7,6},{8,11},{9,8},{10,9... | collective-permute-start | bytes 1572872 | tf_op jit(solution)/shard_map/ppermute | solution.py:19
  68.9 12.5 %collective-permute-done.8.refs_0_ = bf16[128,2048]{1,0:T(8,128)(2,1)S(1)} collective-permute-done((bf16[128,2048]{1,0:T(8,128)(2,1)S(1)}, bf16[128,2048]{1,0:T(8,128)(2,1)S(1)}, u32[]{:S(2)}, u32[]{:S(2)}) %collective-permute-start.8) | collective-permute-done | bytes 524320 | tf_op jit(solution)/shard_map/ppermute | solution.py:19
  81.4 3.5 %collective-permute-start.13 = (bf16[128,2048]{1,0:T(8,128)(2,1)S(1)}, bf16[128,2048]{1,0:T(8,128)(2,1)}, u32[]{:S(2)}, u32[]{:S(2)}) collective-permute-start(bf16[128,2048]{1,0:T(8,128)(2,1)S(1)} %collective-permute-done.9.refs_1_), channel_id=1, source_target_pairs={{0,3},{1,0},{2,1},{3,2},{4,7},{5,4},{6,5},{7,6},{8,11},{9,8},{10,9... | collective-permute-start | bytes 1572872 | tf_op jit(solution)/shard_map/ppermute | solution.py:19
  84.9 3.2 %collective-permute-start.11 = (bf16[128,2048]{1,0:T(8,128)(2,1)S(1)}, bf16[128,2048]{1,0:T(8,128)(2,1)S(1)}, u32[]{:S(2)}, u32[]{:S(2)}) collective-permute-start(bf16[128,2048]{1,0:T(8,128)(2,1)S(1)} %get-tuple-element.44.refs_0_), channel_id=1, source_target_pairs={{0,3},{1,0},{2,1},{3,2},{4,7},{5,4},{6,5},{7,6},{8,11},{9,8},{10,9... | collective-permute-start | bytes 1572872 | tf_op jit(solution)/shard_map/ppermute | solution.py:19
  88.2 7.9 %feed.4 = (bf16[128,2048]{1,0:T(8,128)(2,1)S(1)}, bf16[128,2048]{1,0:T(8,128)(2,1)S(1)}, bf16[32,64,2048]{2,1,0:T(8,128)(2,1)S(1)}, bf16[32,64,2048]{2,1,0:T(8,128)(2,1)S(1)}) custom-call(bf16[128,2048]{1,0:T(8,128)(2,1)S(1)} %collective-permute-done.8.refs_0_, bf16[128,2048]{1,0:T(8,128)(2,1)S(1)} %collective-permute-done.9.refs_1_, ...), custom_call_target="tpu_custom_call" | custom-call | tf_op jit(solution)/shard_map/feed/pallas_call | solution.py:401
  96.1 1.4 collective-permute-done.12.refs_0_
  97.5 6.4 %feed.7 = (bf16[128,2048]{1,0:T(8,128)(2,1)S(1)}, bf16[128,2048]{1,0:T(8,128)(2,1)S(1)}) custom-call(bf16[128,2048]{1,0:T(8,128)(2,1)} %collective-permute-done.12.refs_0_, bf16[128,2048]{1,0:T(8,128)(2,1)} %collective-permute-done.13.refs_1_, bf16[32,64,2048]{2,1,0:T(8,128)(2,1)S(1)} %get-tuple-element.47.refs_2_, ...), custom_call_target="tpu_custom_call" | custom-call | tf_op jit(solution)/shard_map/feed/pallas_call | solution.py:401
  104.0 3.6 %collective-permute-start.18 = (bf16[128,2048]{1,0:T(8,128)(2,1)S(1)}, bf16[128,2048]{1,0:T(8,128)(2,1)S(1)}, u32[]{:S(2)}, u32[]{:S(2)}) collective-permute-start(bf16[128,2048]{1,0:T(8,128)(2,1)S(1)} %get-tuple-element.56), channel_id=1, source_target_pairs={{0,3},{1,0},{2,1},{3,2},{4,7},{5,4},{6,5},{7,6},{8,11},{9,8},{10,9... | collective-permute-start | bytes 1572872 | tf_op jit(solution)/shard_map/ppermute | solution.py:19
  108.2 2.6 %collective-permute-start.17 = (bf16[128,2048]{1,0:T(8,128)(2,1)S(1)}, bf16[128,2048]{1,0:T(8,128)(2,1)S(1)}, u32[]{:S(2)}, u32[]{:S(2)}) collective-permute-start(bf16[128,2048]{1,0:T(8,128)(2,1)S(1)} %get-tuple-element.54), channel_id=1, source_target_pairs={{0,3},{1,0},{2,1},{3,2},{4,7},{5,4},{6,5},{7,6},{8,11},{9,8},{10,9... | collective-permute-start | bytes 1572872 | tf_op jit(solution)/shard_map/ppermute | solution.py:19
  110.8 5.3 %feed.6 = (bf16[128,2048]{1,0:T(8,128)(2,1)S(1)}, bf16[128,2048]{1,0:T(8,128)(2,1)S(1)}) custom-call(bf16[128,2048]{1,0:T(8,128)(2,1)S(1)} %collective-permute-done.10.refs_0_, bf16[128,2048]{1,0:T(8,128)(2,1)S(1)} %collective-permute-done.11.refs_1_, bf16[32,64,2048]{2,1,0:T(8,128)(2,1)S(1)} %get-tuple-element.47.refs_2_, ...), custom_call_target="tpu_custom_call" | custom-call | tf_op jit(solution)/shard_map/feed/pallas_call | solution.py:401
  116.1 3.7 %collective-permute-done.18 = bf16[128,2048]{1,0:T(8,128)(2,1)S(1)} collective-permute-done((bf16[128,2048]{1,0:T(8,128)(2,1)S(1)}, bf16[128,2048]{1,0:T(8,128)(2,1)S(1)}, u32[]{:S(2)}, u32[]{:S(2)}) %collective-permute-start.18) | collective-permute-done | bytes 524320 | tf_op jit(solution)/shard_map/ppermute | solution.py:19
  120.0 3.8 %collective-permute-start.19 = (bf16[128,2048]{1,0:T(8,128)(2,1)S(1)}, bf16[128,2048]{1,0:T(8,128)(2,1)S(1)}, u32[]{:S(2)}, u32[]{:S(2)}) collective-permute-start(bf16[128,2048]{1,0:T(8,128)(2,1)S(1)} %add_convert_fusion), channel_id=1, source_target_pairs={{0,3},{1,0},{2,1},{3,2},{4,7},{5,4},{6,5},{7,6},{8,11},{9,8},{10,9... | collective-permute-start | bytes 1572872 | tf_op jit(solution)/shard_map/ppermute | solution.py:19
  124.0 5.3 %feed.5 = (bf16[128,2048]{1,0:T(8,128)(2,1)S(1)}, bf16[128,2048]{1,0:T(8,128)(2,1)S(1)}) custom-call(bf16[128,2048]{1,0:T(8,128)(2,1)S(1)} %get-tuple-element.44.refs_0_, bf16[128,2048]{1,0:T(8,128)(2,1)S(1)} %get-tuple-element.45.refs_1_, bf16[32,64,2048]{2,1,0:T(8,128)(2,1)S(1)} %get-tuple-element.47.refs_2_, ...), custom_call_target="tpu_custom_call" | custom-call | tf_op jit(solution)/shard_map/feed/pallas_call | solution.py:401
  129.3 5.5 %collective-permute-done.16.refs_5_ = bf16[128,2048]{1,0:T(8,128)(2,1)S(1)} collective-permute-done((bf16[128,2048]{1,0:T(8,128)(2,1)S(1)}, bf16[128,2048]{1,0:T(8,128)(2,1)S(1)}, u32[]{:S(2)}, u32[]{:S(2)}) %collective-permute-start.16) | collective-permute-done | bytes 524320 | tf_op jit(solution)/shard_map/ppermute | solution.py:19
  134.8 6.7 %collective-permute-done.19.refs_7_ = bf16[128,2048]{1,0:T(8,128)(2,1)S(1)} collective-permute-done((bf16[128,2048]{1,0:T(8,128)(2,1)S(1)}, bf16[128,2048]{1,0:T(8,128)(2,1)S(1)}, u32[]{:S(2)}, u32[]{:S(2)}) %collective-permute-start.19) | collective-permute-done | bytes 524320 | tf_op jit(solution)/shard_map/ppermute | solution.py:19
  141.5 1.9 %collective-permute-done.15.refs_4_ = bf16[128,2048]{1,0:T(8,128)(2,1)S(1)} collective-permute-done((bf16[128,2048]{1,0:T(8,128)(2,1)S(1)}, bf16[128,2048]{1,0:T(8,128)(2,1)S(1)}, u32[]{:S(2)}, u32[]{:S(2)}) %collective-permute-start.15) | collective-permute-done | bytes 524320 | tf_op jit(solution)/shard_map/ppermute | solution.py:19
  143.4 2.5 %norm.3 = bf16[256,2048]{1,0:T(8,128)(2,1)} custom-call(bf16[128,2048]{1,0:T(8,128)(2,1)S(1)} %get-tuple-element.44.refs_0_, bf16[128,2048]{1,0:T(8,128)(2,1)S(1)} %get-tuple-element.45.refs_1_, bf16[128,2048]{1,0:T(8,128)(2,1)S(1)} %get-tuple-element.49.refs_2_, bf16[128,2048]{1,0:T(8,128)(2,1)S(1)} %get-tuple-element.50.refs_3_, ...), custom_call_target="tpu_custom_call" | custom-call | tf_op jit(solution)/shard_map/norm/pallas_call | solution.py:288
  (42 shorter events, 5.5 us)
Async XLA Ops:
  6.5 81.6 %all-gather.2.cloned.1.call-start = ((), (), s32[]{:S(2)}) async-start(), calls=%async_computation | async-start | bytes 17301504 | tf_op jit(solution)/shard_map/all_gather | solution.py:435
  9.1 9.8 %collective-permute-start = (bf16[2,128,256]{2,1,0:T(8,128)(2,1)}, bf16[2,128,256]{2,1,0:T(8,128)(2,1)S(1)}, u32[]{:S(2)}, u32[]{:S(2)}) collective-permute-start(bf16[2,128,256]{2,1,0:T(8,128)(2,1)} %get-tuple-element.32), channel_id=1, source_target_pairs={{0,4},{4,8},{8,12},{12,16},{16,20},{20,24},{24,28},{28,32},{32,36}... | collective-permute-start | bytes 393224 | tf_op jit(solution)/shard_map/ppermute | solution.py:91
  11.1 7.9 %collective-permute-start.1 = (bf16[2,128,256]{2,1,0:T(8,128)(2,1)}, bf16[2,128,256]{2,1,0:T(8,128)(2,1)S(1)}, u32[]{:S(2)}, u32[]{:S(2)}) collective-permute-start(bf16[2,128,256]{2,1,0:T(8,128)(2,1)} %get-tuple-element.34), channel_id=1, source_target_pairs={{4,0},{8,4},{12,8},{16,12},{20,16},{24,20},{28,24},{32,28},{36,32}... | collective-permute-start | bytes 393224 | tf_op jit(solution)/shard_map/ppermute | solution.py:92
  14.7 1.2 copy-start
  15.9 1.2 copy-start.1
  18.9 44.8 %copy-start.2 = (bf16[256,2048]{1,0:T(8,128)(2,1)S(1)}, bf16[256,2048]{1,0:T(8,128)(2,1)}, u32[]{:S(2)}) copy-start(bf16[256,2048]{1,0:T(8,128)(2,1)} %refs_0_.3) | copy-start | bytes 3145732
  18.9 44.8 %copy-start.3 = (f32[2048]{0:T(1024)S(1)}, f32[2048]{0:T(1024)}, u32[]{:S(2)}) copy-start(f32[2048]{0:T(1024)} %param.16) | copy-start | bytes 24580
  19.0 44.8 %copy-start.4 = (f32[2048]{0:T(1024)S(1)}, f32[2048]{0:T(1024)}, u32[]{:S(2)}) copy-start(f32[2048]{0:T(1024)} %param.17) | copy-start | bytes 24580
  19.0 0.7 copy-start.7
  23.4 13.8 %collective-permute-start.6 = (bf16[128,2048]{1,0:T(8,128)(2,1)S(1)}, bf16[128,2048]{1,0:T(8,128)(2,1)S(1)}, u32[]{:S(2)}, u32[]{:S(2)}) collective-permute-start(bf16[128,2048]{1,0:T(8,128)(2,1)S(1)} %get-tuple-element.43), channel_id=1, source_target_pairs={{0,3},{1,0},{2,1},{3,2},{4,7},{5,4},{6,5},{7,6},{8,11},{9,8},{10,9... | collective-permute-start | bytes 1572872 | tf_op jit(solution)/shard_map/ppermute | solution.py:19
  26.3 15.0 %collective-permute-start.2 = (bf16[128,2048]{1,0:T(8,128)(2,1)S(1)}, bf16[128,2048]{1,0:T(8,128)(2,1)S(1)}, u32[]{:S(2)}, u32[]{:S(2)}) collective-permute-start(bf16[128,2048]{1,0:T(8,128)(2,1)S(1)} %get-tuple-element.39), channel_id=1, source_target_pairs={{0,1},{1,2},{2,3},{3,0},{4,5},{5,6},{6,7},{7,4},{8,9},{9,10},{10,1... | collective-permute-start | bytes 1572872 | tf_op jit(solution)/shard_map/ppermute | solution.py:19
  32.9 19.5 %collective-permute-start.4 = (bf16[128,2048]{1,0:T(8,128)(2,1)S(1)}, bf16[128,2048]{1,0:T(8,128)(2,1)S(1)}, u32[]{:S(2)}, u32[]{:S(2)}) collective-permute-start(bf16[128,2048]{1,0:T(8,128)(2,1)S(1)} %get-tuple-element.40), channel_id=1, source_target_pairs={{0,1},{1,2},{2,3},{3,0},{4,5},{5,6},{6,7},{7,4},{8,9},{9,10},{10,1... | collective-permute-start | bytes 1572872 | tf_op jit(solution)/shard_map/ppermute | solution.py:19
  33.8 18.7 %collective-permute-start.5 = (bf16[128,2048]{1,0:T(8,128)(2,1)S(1)}, bf16[128,2048]{1,0:T(8,128)(2,1)S(1)}, u32[]{:S(2)}, u32[]{:S(2)}) collective-permute-start(bf16[128,2048]{1,0:T(8,128)(2,1)S(1)} %get-tuple-element.41), channel_id=1, source_target_pairs={{0,3},{1,0},{2,1},{3,2},{4,7},{5,4},{6,5},{7,6},{8,11},{9,8},{10,9... | collective-permute-start | bytes 1572872 | tf_op jit(solution)/shard_map/ppermute | solution.py:19
  37.4 22.5 %collective-permute-start.7 = (bf16[128,2048]{1,0:T(8,128)(2,1)S(1)}, bf16[128,2048]{1,0:T(8,128)(2,1)S(1)}, u32[]{:S(2)}, u32[]{:S(2)}) collective-permute-start(bf16[128,2048]{1,0:T(8,128)(2,1)S(1)} %add_convert_fusion.2), channel_id=1, source_target_pairs={{0,3},{1,0},{2,1},{3,2},{4,7},{5,4},{6,5},{7,6},{8,11},{9,8},{10,9... | collective-permute-start | bytes 1572872 | tf_op jit(solution)/shard_map/ppermute | solution.py:19
  41.4 22.3 %collective-permute-start.3 = (bf16[128,2048]{1,0:T(8,128)(2,1)S(1)}, bf16[128,2048]{1,0:T(8,128)(2,1)S(1)}, u32[]{:S(2)}, u32[]{:S(2)}) collective-permute-start(bf16[128,2048]{1,0:T(8,128)(2,1)S(1)} %add_convert_fusion.3), channel_id=1, source_target_pairs={{0,1},{1,2},{2,3},{3,0},{4,5},{5,6},{6,7},{7,4},{8,9},{9,10},{10,1... | collective-permute-start | bytes 1572872 | tf_op jit(solution)/shard_map/ppermute | solution.py:19
  65.6 15.8 %collective-permute-start.8 = (bf16[128,2048]{1,0:T(8,128)(2,1)S(1)}, bf16[128,2048]{1,0:T(8,128)(2,1)S(1)}, u32[]{:S(2)}, u32[]{:S(2)}) collective-permute-start(bf16[128,2048]{1,0:T(8,128)(2,1)S(1)} %get-tuple-element.44.refs_0_), channel_id=1, source_target_pairs={{0,1},{1,2},{2,3},{3,0},{4,5},{5,6},{6,7},{7,4},{8,9},{9,10},{10,1... | collective-permute-start | bytes 1572872 | tf_op jit(solution)/shard_map/ppermute | solution.py:19
  65.7 15.7 %collective-permute-start.9 = (bf16[128,2048]{1,0:T(8,128)(2,1)S(1)}, bf16[128,2048]{1,0:T(8,128)(2,1)S(1)}, u32[]{:S(2)}, u32[]{:S(2)}) collective-permute-start(bf16[128,2048]{1,0:T(8,128)(2,1)S(1)} %get-tuple-element.45.refs_1_), channel_id=1, source_target_pairs={{0,3},{1,0},{2,1},{3,2},{4,7},{5,4},{6,5},{7,6},{8,11},{9,8},{10,9... | collective-permute-start | bytes 1572872 | tf_op jit(solution)/shard_map/ppermute | solution.py:19
  81.4 16.1 %collective-permute-start.12 = (bf16[128,2048]{1,0:T(8,128)(2,1)S(1)}, bf16[128,2048]{1,0:T(8,128)(2,1)}, u32[]{:S(2)}, u32[]{:S(2)}) collective-permute-start(bf16[128,2048]{1,0:T(8,128)(2,1)S(1)} %collective-permute-done.8.refs_0_), channel_id=1, source_target_pairs={{0,1},{1,2},{2,3},{3,0},{4,5},{5,6},{6,7},{7,4},{8,9},{9,10},{10,1... | collective-permute-start | bytes 1572872 | tf_op jit(solution)/shard_map/ppermute | solution.py:19
  81.4 16.1 %collective-permute-start.13 = (bf16[128,2048]{1,0:T(8,128)(2,1)S(1)}, bf16[128,2048]{1,0:T(8,128)(2,1)}, u32[]{:S(2)}, u32[]{:S(2)}) collective-permute-start(bf16[128,2048]{1,0:T(8,128)(2,1)S(1)} %collective-permute-done.9.refs_1_), channel_id=1, source_target_pairs={{0,3},{1,0},{2,1},{3,2},{4,7},{5,4},{6,5},{7,6},{8,11},{9,8},{10,9... | collective-permute-start | bytes 1572872 | tf_op jit(solution)/shard_map/ppermute | solution.py:19
  84.9 23.3 %collective-permute-start.10 = (bf16[128,2048]{1,0:T(8,128)(2,1)S(1)}, bf16[128,2048]{1,0:T(8,128)(2,1)S(1)}, u32[]{:S(2)}, u32[]{:S(2)}) collective-permute-start(bf16[128,2048]{1,0:T(8,128)(2,1)S(1)} %get-tuple-element.45.refs_1_), channel_id=1, source_target_pairs={{0,1},{1,2},{2,3},{3,0},{4,5},{5,6},{6,7},{7,4},{8,9},{9,10},{10,1... | collective-permute-start | bytes 1572872 | tf_op jit(solution)/shard_map/ppermute | solution.py:19
  84.9 25.9 %collective-permute-start.11 = (bf16[128,2048]{1,0:T(8,128)(2,1)S(1)}, bf16[128,2048]{1,0:T(8,128)(2,1)S(1)}, u32[]{:S(2)}, u32[]{:S(2)}) collective-permute-start(bf16[128,2048]{1,0:T(8,128)(2,1)S(1)} %get-tuple-element.44.refs_0_), channel_id=1, source_target_pairs={{0,3},{1,0},{2,1},{3,2},{4,7},{5,4},{6,5},{7,6},{8,11},{9,8},{10,9... | collective-permute-start | bytes 1572872 | tf_op jit(solution)/shard_map/ppermute | solution.py:19
  104.0 15.9 %collective-permute-start.18 = (bf16[128,2048]{1,0:T(8,128)(2,1)S(1)}, bf16[128,2048]{1,0:T(8,128)(2,1)S(1)}, u32[]{:S(2)}, u32[]{:S(2)}) collective-permute-start(bf16[128,2048]{1,0:T(8,128)(2,1)S(1)} %get-tuple-element.56), channel_id=1, source_target_pairs={{0,3},{1,0},{2,1},{3,2},{4,7},{5,4},{6,5},{7,6},{8,11},{9,8},{10,9... | collective-permute-start | bytes 1572872 | tf_op jit(solution)/shard_map/ppermute | solution.py:19
  107.5 16.2 %collective-permute-start.14 = (bf16[128,2048]{1,0:T(8,128)(2,1)S(1)}, bf16[128,2048]{1,0:T(8,128)(2,1)S(1)}, u32[]{:S(2)}, u32[]{:S(2)}) collective-permute-start(bf16[128,2048]{1,0:T(8,128)(2,1)S(1)} %get-tuple-element.52), channel_id=1, source_target_pairs={{0,1},{1,2},{2,3},{3,0},{4,5},{5,6},{6,7},{7,4},{8,9},{9,10},{10,1... | collective-permute-start | bytes 1572872 | tf_op jit(solution)/shard_map/ppermute | solution.py:19
  107.5 27.2 %collective-permute-start.16 = (bf16[128,2048]{1,0:T(8,128)(2,1)S(1)}, bf16[128,2048]{1,0:T(8,128)(2,1)S(1)}, u32[]{:S(2)}, u32[]{:S(2)}) collective-permute-start(bf16[128,2048]{1,0:T(8,128)(2,1)S(1)} %get-tuple-element.53), channel_id=1, source_target_pairs={{0,1},{1,2},{2,3},{3,0},{4,5},{5,6},{6,7},{7,4},{8,9},{9,10},{10,1... | collective-permute-start | bytes 1572872 | tf_op jit(solution)/shard_map/ppermute | solution.py:19
  108.2 26.6 %collective-permute-start.17 = (bf16[128,2048]{1,0:T(8,128)(2,1)S(1)}, bf16[128,2048]{1,0:T(8,128)(2,1)S(1)}, u32[]{:S(2)}, u32[]{:S(2)}) collective-permute-start(bf16[128,2048]{1,0:T(8,128)(2,1)S(1)} %get-tuple-element.54), channel_id=1, source_target_pairs={{0,3},{1,0},{2,1},{3,2},{4,7},{5,4},{6,5},{7,6},{8,11},{9,8},{10,9... | collective-permute-start | bytes 1572872 | tf_op jit(solution)/shard_map/ppermute | solution.py:19
  120.0 21.5 %collective-permute-start.19 = (bf16[128,2048]{1,0:T(8,128)(2,1)S(1)}, bf16[128,2048]{1,0:T(8,128)(2,1)S(1)}, u32[]{:S(2)}, u32[]{:S(2)}) collective-permute-start(bf16[128,2048]{1,0:T(8,128)(2,1)S(1)} %add_convert_fusion), channel_id=1, source_target_pairs={{0,3},{1,0},{2,1},{3,2},{4,7},{5,4},{6,5},{7,6},{8,11},{9,8},{10,9... | collective-permute-start | bytes 1572872 | tf_op jit(solution)/shard_map/ppermute | solution.py:19
  123.9 19.5 %copy-start.5 = (f32[2048]{0:T(1024)S(1)}, f32[2048]{0:T(1024)}, u32[]{:S(2)}) copy-start(f32[2048]{0:T(1024)} %param.20) | copy-start | bytes 24580
  123.9 19.5 %copy-start.6 = (f32[2048]{0:T(1024)S(1)}, f32[2048]{0:T(1024)}, u32[]{:S(2)}) copy-start(f32[2048]{0:T(1024)} %param.21) | copy-start | bytes 24580
  123.9 19.5 %collective-permute-start.15 = (bf16[128,2048]{1,0:T(8,128)(2,1)S(1)}, bf16[128,2048]{1,0:T(8,128)(2,1)S(1)}, u32[]{:S(2)}, u32[]{:S(2)}) collective-permute-start(bf16[128,2048]{1,0:T(8,128)(2,1)S(1)} %add_convert_fusion.1), channel_id=1, source_target_pairs={{0,1},{1,2},{2,3},{3,0},{4,5},{5,6},{6,7},{7,4},{8,9},{9,10},{10,1... | collective-permute-start | bytes 1572872 | tf_op jit(solution)/shard_map/ppermute | solution.py:19
Sparse Core Ops, SparseCore 0:
  9.6 74.7 all-gather.1

commit v9 on v8

--- a/solution.py
+++ b/solution.py
@@ -232,41 +232,38 @@
     )(sink, queries, before, middle, after, out_weight)
 
 
-def norm_kernel(*refs, tops, bottoms, outs, block):
-    count = max(max(tops), max(bottoms)) + 1
-    sources, (gain, bias), results = (refs[:count], refs[count : count + 2], refs[count + 2 : -3])
-    parts, out, sems = refs[-3:]
+def norm_kernel(*refs, count, base, block):
+    sources, (gain, bias) = (refs[:count], refs[count : count + 2])
+    result, parts, out, sems = refs[-4:]
     rows, width = out.shape
     steps = rows // block
-    half = steps // 2
 
     def in_copy(step, place):
-        ref = sources[(tops if step < half else bottoms)[place]]
-        at = step * block % ref.shape[0]
+        ref = sources[place]
+        at = (base + step * block) % ref.shape[0]
         return pltpu.make_async_copy(
             ref.at[pl.ds(at, block)],
             parts.at[place, pl.ds(step * block, block)],
-            sems.at[step * (len(tops) + 1) + place],
+            sems.at[step * (count + 1) + place],
         )
 
     def out_copy(step):
-        ref = results[step * block // (rows // outs)]
-        at = step * block % ref.shape[0]
+        at = (base + step * block) % result.shape[0]
         return pltpu.make_async_copy(
             out.at[pl.ds(step * block, block)],
-            ref.at[pl.ds(at, block)],
-            sems.at[step * (len(tops) + 1) + len(tops)],
+            result.at[pl.ds(at, block)],
+            sems.at[step * (count + 1) + count],
         )
 
     for step in range(steps):
-        for place in range(len(tops)):
+        for place in range(count):
             in_copy(step, place).start()
     for step in range(steps):
         span = slice(step * block, (step + 1) * block)
         values = None
-        for place in range(len(tops)):
+        for place in range(count):
             in_copy(step, place).wait()
-        for place in range(len(tops)):
+        for place in range(count):
             part = parts[place, span].astype(jnp.float32)
             values = part if values is None else values + part
         mean = jnp.sum(values, axis=-1, keepdims=True) * (1.0 / width)
@@ -280,24 +277,26 @@
         out_copy(step).wait()
 
 
-def norm_rows(sources, tops, bottoms, outs, gain, bias, rows, block=64):
-    width = sources[0].shape[1]
+def norm_half(sources, base, gain, bias, rows, out_rows, into=None, block=64):
+    count, width = (len(sources), sources[0].shape[1])
     anywhere = pl.BlockSpec(memory_space=pl.ANY)
     vmem = pl.BlockSpec(memory_space=pltpu.VMEM)
     steps = rows // block
+    extra = () if into is None else (into,)
     return pl.pallas_call(
-        functools.partial(norm_kernel, tops=tops, bottoms=bottoms, outs=outs, block=block),
-        in_specs=[anywhere] * len(sources) + [vmem, vmem],
-        out_specs=[anywhere] * outs,
-        out_shape=[jax.ShapeDtypeStruct((rows // outs, width), jnp.bfloat16)] * outs,
+        functools.partial(norm_kernel, count=count, base=base, block=block),
+        in_specs=[anywhere] * count + [vmem, vmem] + [anywhere] * len(extra),
+        out_specs=anywhere,
+        out_shape=jax.ShapeDtypeStruct((out_rows, width), jnp.bfloat16),
         scratch_shapes=[
-            pltpu.VMEM((len(tops), rows, width), jnp.bfloat16),
+            pltpu.VMEM((count, rows, width), jnp.bfloat16),
             pltpu.VMEM((rows, width), jnp.bfloat16),
-            pltpu.SemaphoreType.DMA((steps * (len(tops) + 1),)),
+            pltpu.SemaphoreType.DMA((steps * (count + 1),)),
         ],
+        input_output_aliases={count + 2: 0} if extra else {},
         compiler_params=pltpu.CompilerParams(vmem_limit_bytes=16 * 1024 * 1024),
         name="norm",
-    )(*sources, gain[None], bias[None])
+    )(*sources, gain[None], bias[None], *extra)
 
 
 def added(part, arrived):
@@ -411,7 +410,7 @@
             *load_sems,
         ],
         compiler_params=pltpu.CompilerParams(
-            vmem_limit_bytes=(12 if resident else 32) * 1024 * 1024
+            vmem_limit_bytes=(24 if resident else 32) * 1024 * 1024
         ),
         name="feed",
     )(*rows, *weights)
@@ -452,15 +451,12 @@
     own_top, own_bottom = run(0)
     left_sum = shift(added(right_top, from_left), 1)
     right_sum = shift(added(left_bottom, from_right), -1)
-    rows = 2 * own_top.shape[0]
-    first_top, first_bottom = norm_rows(
-        (residual_in, own_top, own_bottom, left_sum, left_plain, right_plain, right_sum),
-        (0, 1, 3, 5),
-        (0, 2, 4, 6),
-        2,
-        norm1_gain,
-        norm1_bias,
-        rows,
+    rows, half = (2 * own_top.shape[0], own_top.shape[0])
+    first_top = norm_half(
+        (residual_in, own_top, left_sum, right_plain), 0, norm1_gain, norm1_bias, half, half
+    )
+    first_bottom = norm_half(
+        (residual_in, own_bottom, left_plain, right_sum), half, norm1_gain, norm1_bias, half, half
     )
 
     row_lt = shift(first_top, 1)
@@ -479,25 +475,18 @@
     left_sum = shift(added(right_top, from_left), 1)
     right_sum = shift(added(left_bottom, from_right), -1)
     own_top, own_bottom = feed_forward((first_top, first_bottom), held)
-    (out,) = norm_rows(
-        (
-            first_top,
-            first_bottom,
-            own_top,
-            own_bottom,
-            left_sum,
-            left_plain,
-            right_plain,
-            right_sum,
-        ),
-        (0, 2, 4, 6),
-        (1, 3, 5, 7),
-        1,
+    out = norm_half(
+        (first_top, own_top, left_sum, right_plain), 0, norm2_gain, norm2_bias, half, rows
+    )
+    return norm_half(
+        (first_bottom, own_bottom, left_plain, right_sum),
+        half,
         norm2_gain,
         norm2_bias,
+        half,
         rows,
-    )
-    return out
+        out,
+    )
 
 
 def solution(mesh):

time: 153 us -> 149 us (0.974)
  the two profiles are of different devices: /device:TPU:24 before, /device:TPU:1 now
where the time goes in v9:
time: 149 us; the launch traced here: 147 us
  waiting for transfers between devices  50.5 us (34%)
  Pallas kernels  48.4 us (32%)
  starting transfers between devices  30.7 us (21%)
  between operations  13.7 us (9%)
  local copies, waits for them, and re-layouts  3.13 us (2%)
    ppermute x18, waiting for transfers between devices, shift(): lax.ppermute(value, axis, [(i, (i + step) % devices) for i in range(devic...  46.7 us
    pallas_call x4, Pallas kernels, feed_forward(): pl.pallas_call(functools.partial(feed_kernel, count=count, chunk=chunk, r...  24.9 us
    ppermute x18, starting transfers between devices, shift(): lax.ppermute(value, axis, [(i, (i + step) % devices) for i in range(devic...  24.2 us
    pallas_call x3, Pallas kernels, attend(): pl.pallas_call(functools.partial(attend_kernel, rels=rels), grid=(steps,)...  14.1 us
    pallas_call x4, Pallas kernels, norm_half(): pl.pallas_call(functools.partial(norm_kernel, count=count, base=base, blo...  5.14 us
    ppermute x1, starting transfers between devices, halo(): before = lax.ppermute(last, axis, up)  4.58 us
    all_gather x1, waiting for transfers between devices, layer(): lax.all_gather(shards, 'sp', axis=0, tiled=True)  3.44 us
    unnamed x18, local copies, waits for them, and re-layouts  3.13 us
  transfers between devices with their start and end apart: 21, of which 11 were waited for; matrix products, arithmetic and copies ran while one was open for 0% of the time, Pallas kernels for 30%

profile of v9, /device:TPU:1, one launch (start us, length us, event | category | flops | bytes accessed | tf_op | source)
XLA Modules:
  0.0 146.9 jit_solution(17319813135997029581)
XLA Ops:
  6.5 2.6 %prepare.1 = (bf16[128,2048]{1,0:T(8,128)(2,1)}, bf16[2,128,256]{2,1,0:T(8,128)(2,1)}, bf16[2,128,256]{2,1,0:T(8,128)(2,1)}) custom-call(bf16[64,2048]{1,0:T(8,128)(2,1)} %up.1, bf16[64,2048]{1,0:T(8,128)(2,1)} %bitcast.15, bf16[2,1024,256]{2,1,0:T(8,128)(2,1)} %keys_values.1), custom_call_target="tpu_custom_call" | custom-call | tf_op jit(solution)/shard_map/prepare/pallas_call | solution.py:49
  9.1 4.6 %collective-permute-start = (bf16[2,128,256]{2,1,0:T(8,128)(2,1)}, bf16[2,128,256]{2,1,0:T(8,128)(2,1)S(1)}, u32[]{:S(2)}, u32[]{:S(2)}) collective-permute-start(bf16[2,128,256]{2,1,0:T(8,128)(2,1)} %get-tuple-element.30), channel_id=1, source_target_pairs={{0,4},{4,8},{8,12},{12,16},{16,20},{20,24},{24,28},{28,32},{32,36}... | collective-permute-start | bytes 393224 | tf_op jit(solution)/shard_map/ppermute | solution.py:91
  13.7 1.9 %collective-permute-start.1 = (bf16[2,128,256]{2,1,0:T(8,128)(2,1)}, bf16[2,128,256]{2,1,0:T(8,128)(2,1)S(1)}, u32[]{:S(2)}, u32[]{:S(2)}) collective-permute-start(bf16[2,128,256]{2,1,0:T(8,128)(2,1)} %get-tuple-element.32), channel_id=1, source_target_pairs={{4,0},{8,4},{12,8},{16,12},{20,16},{24,20},{28,24},{32,28},{36,32}... | collective-permute-start | bytes 393224 | tf_op jit(solution)/shard_map/ppermute | solution.py:92
  18.1 1.8 %fetch.1 = (bf16[1024,512]{1,0:T(8,128)(2,1)S(1)}, bf16[2,1024,256]{2,1,0:T(8,128)(2,1)S(1)}, bf16[512,2048]{1,0:T(8,128)(2,1)S(1)}) custom-call(bf16[1024,512]{1,0:T(8,128)(2,1)S(1)} %copy-done.2, bf16[2,1024,256]{2,1,0:T(8,128)(2,1)S(1)} %copy-done.1, bf16[512,2048]{1,0:T(8,128)(2,1)} %refs_2_.1), custom_call_target="tpu_custom_call" | custom-call | tf_op jit(solution)/shard_map/fetch/pallas_call | solution.py:76
  20.9 3.7 %attend.5 = (bf16[128,2048]{1,0:T(8,128)(2,1)S(1)}, bf16[128,2048]{1,0:T(8,128)(2,1)S(1)}) custom-call(f32[8]{0:T(128)S(1)} %copy-done.7, bf16[1024,512]{1,0:T(8,128)(2,1)S(1)} %get-tuple-element.29.q_hbm, bf16[2,128,256]{2,1,0:T(8,128)(2,1)S(1)} %collective-permute-done.before_ref, bf16[2,1024,256]{2,1,0:T(8,128)(2,1)S(1)} %get-tuple-element.31.mid_ref, ...), custom_call_target="tpu_custom_call" | custom-call | tf_op jit(solution)/shard_map/attend/pallas_call | solution.py:211
  24.6 1.3 collective-permute-start.5
  25.9 1.5 collective-permute-start.3
  27.4 6.7 %attend.4 = (bf16[128,2048]{1,0:T(8,128)(2,1)S(1)}, bf16[128,2048]{1,0:T(8,128)(2,1)S(1)}, bf16[128,2048]{1,0:T(8,128)(2,1)S(1)}, bf16[128,2048]{1,0:T(8,128)(2,1)S(1)}) custom-call(f32[8]{0:T(128)S(1)} %copy-done.8, bf16[1024,512]{1,0:T(8,128)(2,1)S(1)} %get-tuple-element.29.q_hbm, bf16[2,128,256]{2,1,0:T(8,128)(2,1)S(1)} %collective-permute-done.before_ref, ...), custom_call_target="tpu_custom_call" | custom-call | tf_op jit(solution)/shard_map/attend/pallas_call | solution.py:211
  34.0 1.3 collective-permute-start.7
  35.6 2.2 %collective-permute-done.5 = bf16[128,2048]{1,0:T(8,128)(2,1)S(1)} collective-permute-done((bf16[128,2048]{1,0:T(8,128)(2,1)S(1)}, bf16[128,2048]{1,0:T(8,128)(2,1)S(1)}, u32[]{:S(2)}, u32[]{:S(2)}) %collective-permute-start.5) | collective-permute-done | bytes 524320 | tf_op jit(solution)/shard_map/ppermute | solution.py:19
  37.9 1.7 %collective-permute-start.6 = (bf16[128,2048]{1,0:T(8,128)(2,1)S(1)}, bf16[128,2048]{1,0:T(8,128)(2,1)S(1)}, u32[]{:S(2)}, u32[]{:S(2)}) collective-permute-start(bf16[128,2048]{1,0:T(8,128)(2,1)S(1)} %add_convert_fusion.2), channel_id=1, source_target_pairs={{0,1},{1,2},{2,3},{3,0},{4,5},{5,6},{6,7},{7,4},{8,9},{9,10},{10,1... | collective-permute-start | bytes 1572872 | tf_op jit(solution)/shard_map/ppermute | solution.py:19
  40.0 2.8 %collective-permute-start.4 = (bf16[128,2048]{1,0:T(8,128)(2,1)S(1)}, bf16[128,2048]{1,0:T(8,128)(2,1)S(1)}, u32[]{:S(2)}, u32[]{:S(2)}) collective-permute-start(bf16[128,2048]{1,0:T(8,128)(2,1)S(1)} %add_convert_fusion.3), channel_id=1, source_target_pairs={{0,3},{1,0},{2,1},{3,2},{4,7},{5,4},{6,5},{7,6},{8,11},{9,8},{10,9... | collective-permute-start | bytes 1572872 | tf_op jit(solution)/shard_map/ppermute | solution.py:19
  42.7 3.7 %attend.3 = (bf16[128,2048]{1,0:T(8,128)(2,1)S(1)}, bf16[128,2048]{1,0:T(8,128)(2,1)S(1)}) custom-call(f32[8]{0:T(128)S(1)} %copy-done.8, bf16[1024,512]{1,0:T(8,128)(2,1)S(1)} %get-tuple-element.29.q_hbm, bf16[2,128,256]{2,1,0:T(8,128)(2,1)S(1)} %collective-permute-done.before_ref, bf16[2,1024,256]{2,1,0:T(8,128)(2,1)S(1)} %get-tuple-element.31.mid_ref, ...), custom_call_target="tpu_custom_call" | custom-call | tf_op jit(solution)/shard_map/attend/pallas_call | solution.py:211
  46.4 4.7 %collective-permute-done.7.refs_3_ = bf16[128,2048]{1,0:T(8,128)(2,1)S(1)} collective-permute-done((bf16[128,2048]{1,0:T(8,128)(2,1)S(1)}, bf16[128,2048]{1,0:T(8,128)(2,1)S(1)}, u32[]{:S(2)}, u32[]{:S(2)}) %collective-permute-start.7) | collective-permute-done | bytes 524320 | tf_op jit(solution)/shard_map/ppermute | solution.py:19
  51.2 9.8 %collective-permute-done.6.refs_2_ = bf16[128,2048]{1,0:T(8,128)(2,1)S(1)} collective-permute-done((bf16[128,2048]{1,0:T(8,128)(2,1)S(1)}, bf16[128,2048]{1,0:T(8,128)(2,1)S(1)}, u32[]{:S(2)}, u32[]{:S(2)}) %collective-permute-start.6) | collective-permute-done | bytes 524320 | tf_op jit(solution)/shard_map/ppermute | solution.py:19
  63.2 2.7 %collective-permute-start.9 = (bf16[128,2048]{1,0:T(8,128)(2,1)S(1)}, bf16[128,2048]{1,0:T(8,128)(2,1)S(1)}, u32[]{:S(2)}, u32[]{:S(2)}) collective-permute-start(bf16[128,2048]{1,0:T(8,128)(2,1)S(1)} %norm.4.refs_1_.refs_0_), channel_id=1, source_target_pairs={{0,3},{1,0},{2,1},{3,2},{4,7},{5,4},{6,5},{7,6},{8,11},{9,8},{10,9... | collective-permute-start | bytes 1572872 | tf_op jit(solution)/shard_map/ppermute | solution.py:19
  65.9 11.4 %collective-permute-done.8.refs_0_ = bf16[128,2048]{1,0:T(8,128)(2,1)S(1)} collective-permute-done((bf16[128,2048]{1,0:T(8,128)(2,1)S(1)}, bf16[128,2048]{1,0:T(8,128)(2,1)S(1)}, u32[]{:S(2)}, u32[]{:S(2)}) %collective-permute-start.8) | collective-permute-done | bytes 524320 | tf_op jit(solution)/shard_map/ppermute | solution.py:19
  77.5 3.5 %collective-permute-start.14 = (bf16[128,2048]{1,0:T(8,128)(2,1)S(1)}, bf16[128,2048]{1,0:T(8,128)(2,1)}, u32[]{:S(2)}, u32[]{:S(2)}) collective-permute-start(bf16[128,2048]{1,0:T(8,128)(2,1)S(1)} %collective-permute-done.9.refs_1_), channel_id=1, source_target_pairs={{0,3},{1,0},{2,1},{3,2},{4,7},{5,4},{6,5},{7,6},{8,11},{9,8},{10,9... | collective-permute-start | bytes 1572872 | tf_op jit(solution)/shard_map/ppermute | solution.py:19
  81.0 1.4 collective-permute-start.11
  82.5 3.4 %all-gather.2.cloned.1.call-done = bf16[4096,2048]{1,0:T(8,128)(2,1)} async-done(((bf16[128,2048]{1,0:T(8,128)(2,1)}), bf16[4096,2048]{1,0:T(8,128)(2,1)}) %all-gather.2.cloned.1.call-update) | async-done | bytes 16777232 | tf_op jit(solution)/shard_map/all_gather | solution.py:434
  85.9 7.9 %feed.4 = (bf16[128,2048]{1,0:T(8,128)(2,1)S(1)}, bf16[128,2048]{1,0:T(8,128)(2,1)S(1)}, bf16[32,64,2048]{2,1,0:T(8,128)(2,1)S(1)}, bf16[32,64,2048]{2,1,0:T(8,128)(2,1)S(1)}) custom-call(bf16[128,2048]{1,0:T(8,128)(2,1)S(1)} %collective-permute-done.8.refs_0_, bf16[128,2048]{1,0:T(8,128)(2,1)S(1)} %collective-permute-done.9.refs_1_, ...), custom_call_target="tpu_custom_call" | custom-call | tf_op jit(solution)/shard_map/feed/pallas_call | solution.py:400
  93.9 6.4 %feed.7 = (bf16[128,2048]{1,0:T(8,128)(2,1)S(1)}, bf16[128,2048]{1,0:T(8,128)(2,1)S(1)}) custom-call(bf16[128,2048]{1,0:T(8,128)(2,1)} %collective-permute-done.13.refs_0_, bf16[128,2048]{1,0:T(8,128)(2,1)} %collective-permute-done.14.refs_1_, bf16[32,64,2048]{2,1,0:T(8,128)(2,1)S(1)} %get-tuple-element.43.refs_2_, ...), custom_call_target="tpu_custom_call" | custom-call | tf_op jit(solution)/shard_map/feed/pallas_call | solution.py:400
  100.3 1.3 collective-permute-start.17
  101.6 1.5 %collective-permute-start.15 = (bf16[128,2048]{1,0:T(8,128)(2,1)S(1)}, bf16[128,2048]{1,0:T(8,128)(2,1)S(1)}, u32[]{:S(2)}, u32[]{:S(2)}) collective-permute-start(bf16[128,2048]{1,0:T(8,128)(2,1)S(1)} %get-tuple-element.48), channel_id=1, source_target_pairs={{0,3},{1,0},{2,1},{3,2},{4,7},{5,4},{6,5},{7,6},{8,11},{9,8},{10,9... | collective-permute-start | bytes 1572872 | tf_op jit(solution)/shard_map/ppermute | solution.py:19
  104.5 5.3 %feed.6 = (bf16[128,2048]{1,0:T(8,128)(2,1)S(1)}, bf16[128,2048]{1,0:T(8,128)(2,1)S(1)}) custom-call(bf16[128,2048]{1,0:T(8,128)(2,1)S(1)} %collective-permute-done.11.refs_0_, bf16[128,2048]{1,0:T(8,128)(2,1)S(1)} %collective-permute-done.12.refs_1_, bf16[32,64,2048]{2,1,0:T(8,128)(2,1)S(1)} %get-tuple-element.43.refs_2_, ...), custom_call_target="tpu_custom_call" | custom-call | tf_op jit(solution)/shard_map/feed/pallas_call | solution.py:400
  109.8 4.5 %collective-permute-done.17 = bf16[128,2048]{1,0:T(8,128)(2,1)S(1)} collective-permute-done((bf16[128,2048]{1,0:T(8,128)(2,1)S(1)}, bf16[128,2048]{1,0:T(8,128)(2,1)S(1)}, u32[]{:S(2)}, u32[]{:S(2)}) %collective-permute-start.17) | collective-permute-done | bytes 524320 | tf_op jit(solution)/shard_map/ppermute | solution.py:19
  115.1 2.9 %collective-permute-start.16 = (bf16[128,2048]{1,0:T(8,128)(2,1)S(1)}, bf16[128,2048]{1,0:T(8,128)(2,1)S(1)}, u32[]{:S(2)}, u32[]{:S(2)}) collective-permute-start(bf16[128,2048]{1,0:T(8,128)(2,1)S(1)} %add_convert_fusion.1), channel_id=1, source_target_pairs={{0,3},{1,0},{2,1},{3,2},{4,7},{5,4},{6,5},{7,6},{8,11},{9,8},{10,9... | collective-permute-start | bytes 1572872 | tf_op jit(solution)/shard_map/ppermute | solution.py:19
  118.0 5.3 %feed.5 = (bf16[128,2048]{1,0:T(8,128)(2,1)S(1)}, bf16[128,2048]{1,0:T(8,128)(2,1)S(1)}) custom-call(bf16[128,2048]{1,0:T(8,128)(2,1)S(1)} %norm.5.refs_0_, bf16[128,2048]{1,0:T(8,128)(2,1)S(1)} %norm.4.refs_1_.refs_0_, bf16[32,64,2048]{2,1,0:T(8,128)(2,1)S(1)} %get-tuple-element.43.refs_2_, bf16[32,64,2048]{2,1,0:T(8,128)(2,1)S(1)} %get-tuple-element.44.refs_3_), custom_call_target="tpu_custom_call" | custom-call | tf_op jit(solution)/shard_map/feed/pallas_call | solution.py:400
  123.3 2.4 %collective-permute-done.19.refs_3_ = bf16[128,2048]{1,0:T(8,128)(2,1)S(1)} collective-permute-done((bf16[128,2048]{1,0:T(8,128)(2,1)S(1)}, bf16[128,2048]{1,0:T(8,128)(2,1)S(1)}, u32[]{:S(2)}, u32[]{:S(2)}) %collective-permute-start.19) | collective-permute-done | bytes 524320 | tf_op jit(solution)/shard_map/ppermute | solution.py:19
  125.7 11.1 %collective-permute-done.18.refs_2_ = bf16[128,2048]{1,0:T(8,128)(2,1)S(1)} collective-permute-done((bf16[128,2048]{1,0:T(8,128)(2,1)S(1)}, bf16[128,2048]{1,0:T(8,128)(2,1)S(1)}, u32[]{:S(2)}, u32[]{:S(2)}) %collective-permute-start.18) | collective-permute-done | bytes 524320 | tf_op jit(solution)/shard_map/ppermute | solution.py:19
  136.8 1.6 %norm.6.refs_6_ = bf16[256,2048]{1,0:T(8,128)(2,1)} custom-call(bf16[128,2048]{1,0:T(8,128)(2,1)S(1)} %norm.5.refs_0_, bf16[128,2048]{1,0:T(8,128)(2,1)S(1)} %get-tuple-element.49.refs_1_, bf16[128,2048]{1,0:T(8,128)(2,1)S(1)} %collective-permute-done.18.refs_2_, bf16[128,2048]{1,0:T(8,128)(2,1)S(1)} %collective-permute-done.19.refs_3_, ...), custom_call_target="tpu_custom_call" | custom-call | tf_op jit(solution)/shard_map/norm/pallas_call | solution.py:286
  138.5 1.6 %norm.7 = bf16[256,2048]{1,0:T(8,128)(2,1)} custom-call(bf16[128,2048]{1,0:T(8,128)(2,1)S(1)} %norm.4.refs_1_.refs_0_, bf16[128,2048]{1,0:T(8,128)(2,1)S(1)} %get-tuple-element.45.refs_1_, bf16[128,2048]{1,0:T(8,128)(2,1)S(1)} %collective-permute-done.10.refs_2_, ...), custom_call_target="tpu_custom_call", output_to_operand_aliasing={{}: (6, {})} | custom-call | tf_op jit(solution)/shard_map/norm/pallas_call | solution.py:286
  (46 shorter events, 8.8 us)
Async XLA Ops:
  6.5 20.8 %copy-start.8 = (f32[8]{0:T(128)S(1)}, f32[8]{0:T(128)}, u32[]{:S(2)}) copy-start(f32[8]{0:T(128)} %sink.5) | copy-start | bytes 100
  6.5 79.4 %all-gather.2.cloned.1.call-start = ((), (), s32[]{:S(2)}) async-start(), calls=%async_computation | async-start | bytes 17301504 | tf_op jit(solution)/shard_map/all_gather | solution.py:434
  9.1 10.8 %collective-permute-start = (bf16[2,128,256]{2,1,0:T(8,128)(2,1)}, bf16[2,128,256]{2,1,0:T(8,128)(2,1)S(1)}, u32[]{:S(2)}, u32[]{:S(2)}) collective-permute-start(bf16[2,128,256]{2,1,0:T(8,128)(2,1)} %get-tuple-element.30), channel_id=1, source_target_pairs={{0,4},{4,8},{8,12},{12,16},{16,20},{20,24},{24,28},{28,32},{32,36}... | collective-permute-start | bytes 393224 | tf_op jit(solution)/shard_map/ppermute | solution.py:91
  13.7 6.5 %collective-permute-start.1 = (bf16[2,128,256]{2,1,0:T(8,128)(2,1)}, bf16[2,128,256]{2,1,0:T(8,128)(2,1)S(1)}, u32[]{:S(2)}, u32[]{:S(2)}) collective-permute-start(bf16[2,128,256]{2,1,0:T(8,128)(2,1)} %get-tuple-element.32), channel_id=1, source_target_pairs={{4,0},{8,4},{12,8},{16,12},{20,16},{24,20},{28,24},{32,28},{36,32}... | collective-permute-start | bytes 393224 | tf_op jit(solution)/shard_map/ppermute | solution.py:92
  15.7 1.2 copy-start.1
  16.9 1.2 copy-start.2
  19.9 41.1 %copy-start = (bf16[256,2048]{1,0:T(8,128)(2,1)S(1)}, bf16[256,2048]{1,0:T(8,128)(2,1)}, u32[]{:S(2)}) copy-start(bf16[256,2048]{1,0:T(8,128)(2,1)} %refs_0_.5) | copy-start | bytes 3145732
  19.9 41.1 %copy-start.3 = (f32[2048]{0:T(1024)S(1)}, f32[2048]{0:T(1024)}, u32[]{:S(2)}) copy-start(f32[2048]{0:T(1024)} %param.16) | copy-start | bytes 24580
  19.9 41.1 %copy-start.4 = (f32[2048]{0:T(1024)S(1)}, f32[2048]{0:T(1024)}, u32[]{:S(2)}) copy-start(f32[2048]{0:T(1024)} %param.17) | copy-start | bytes 24580
  20.2 0.7 copy-start.7
  24.6 13.1 %collective-permute-start.5 = (bf16[128,2048]{1,0:T(8,128)(2,1)S(1)}, bf16[128,2048]{1,0:T(8,128)(2,1)S(1)}, u32[]{:S(2)}, u32[]{:S(2)}) collective-permute-start(bf16[128,2048]{1,0:T(8,128)(2,1)S(1)} %get-tuple-element.40), channel_id=1, source_target_pairs={{0,1},{1,2},{2,3},{3,0},{4,5},{5,6},{6,7},{7,4},{8,9},{9,10},{10,1... | collective-permute-start | bytes 1572872 | tf_op jit(solution)/shard_map/ppermute | solution.py:19
  25.9 13.9 %collective-permute-start.3 = (bf16[128,2048]{1,0:T(8,128)(2,1)S(1)}, bf16[128,2048]{1,0:T(8,128)(2,1)S(1)}, u32[]{:S(2)}, u32[]{:S(2)}) collective-permute-start(bf16[128,2048]{1,0:T(8,128)(2,1)S(1)} %get-tuple-element.37), channel_id=1, source_target_pairs={{0,3},{1,0},{2,1},{3,2},{4,7},{5,4},{6,5},{7,6},{8,11},{9,8},{10,9... | collective-permute-start | bytes 1572872 | tf_op jit(solution)/shard_map/ppermute | solution.py:19
  34.0 17.1 %collective-permute-start.7 = (bf16[128,2048]{1,0:T(8,128)(2,1)S(1)}, bf16[128,2048]{1,0:T(8,128)(2,1)S(1)}, u32[]{:S(2)}, u32[]{:S(2)}) collective-permute-start(bf16[128,2048]{1,0:T(8,128)(2,1)S(1)} %get-tuple-element.41), channel_id=1, source_target_pairs={{0,3},{1,0},{2,1},{3,2},{4,7},{5,4},{6,5},{7,6},{8,11},{9,8},{10,9... | collective-permute-start | bytes 1572872 | tf_op jit(solution)/shard_map/ppermute | solution.py:19
  35.4 26.8 %collective-permute-start.2 = (bf16[128,2048]{1,0:T(8,128)(2,1)S(1)}, bf16[128,2048]{1,0:T(8,128)(2,1)S(1)}, u32[]{:S(2)}, u32[]{:S(2)}) collective-permute-start(bf16[128,2048]{1,0:T(8,128)(2,1)S(1)} %get-tuple-element.35), channel_id=1, source_target_pairs={{0,1},{1,2},{2,3},{3,0},{4,5},{5,6},{6,7},{7,4},{8,9},{9,10},{10,1... | collective-permute-start | bytes 1572872 | tf_op jit(solution)/shard_map/ppermute | solution.py:19
  37.9 23.1 %collective-permute-start.6 = (bf16[128,2048]{1,0:T(8,128)(2,1)S(1)}, bf16[128,2048]{1,0:T(8,128)(2,1)S(1)}, u32[]{:S(2)}, u32[]{:S(2)}) collective-permute-start(bf16[128,2048]{1,0:T(8,128)(2,1)S(1)} %add_convert_fusion.2), channel_id=1, source_target_pairs={{0,1},{1,2},{2,3},{3,0},{4,5},{5,6},{6,7},{7,4},{8,9},{9,10},{10,1... | collective-permute-start | bytes 1572872 | tf_op jit(solution)/shard_map/ppermute | solution.py:19
  40.0 22.3 %collective-permute-start.4 = (bf16[128,2048]{1,0:T(8,128)(2,1)S(1)}, bf16[128,2048]{1,0:T(8,128)(2,1)S(1)}, u32[]{:S(2)}, u32[]{:S(2)}) collective-permute-start(bf16[128,2048]{1,0:T(8,128)(2,1)S(1)} %add_convert_fusion.3), channel_id=1, source_target_pairs={{0,3},{1,0},{2,1},{3,2},{4,7},{5,4},{6,5},{7,6},{8,11},{9,8},{10,9... | collective-permute-start | bytes 1572872 | tf_op jit(solution)/shard_map/ppermute | solution.py:19
  61.9 15.4 %collective-permute-start.8 = (bf16[128,2048]{1,0:T(8,128)(2,1)S(1)}, bf16[128,2048]{1,0:T(8,128)(2,1)S(1)}, u32[]{:S(2)}, u32[]{:S(2)}) collective-permute-start(bf16[128,2048]{1,0:T(8,128)(2,1)S(1)} %norm.5.refs_0_), channel_id=1, source_target_pairs={{0,1},{1,2},{2,3},{3,0},{4,5},{5,6},{6,7},{7,4},{8,9},{9,10},{10,1... | collective-permute-start | bytes 1572872 | tf_op jit(solution)/shard_map/ppermute | solution.py:19
  63.2 14.3 %collective-permute-start.9 = (bf16[128,2048]{1,0:T(8,128)(2,1)S(1)}, bf16[128,2048]{1,0:T(8,128)(2,1)S(1)}, u32[]{:S(2)}, u32[]{:S(2)}) collective-permute-start(bf16[128,2048]{1,0:T(8,128)(2,1)S(1)} %norm.4.refs_1_.refs_0_), channel_id=1, source_target_pairs={{0,3},{1,0},{2,1},{3,2},{4,7},{5,4},{6,5},{7,6},{8,11},{9,8},{10,9... | collective-permute-start | bytes 1572872 | tf_op jit(solution)/shard_map/ppermute | solution.py:19
  77.3 16.6 %collective-permute-start.13 = (bf16[128,2048]{1,0:T(8,128)(2,1)S(1)}, bf16[128,2048]{1,0:T(8,128)(2,1)}, u32[]{:S(2)}, u32[]{:S(2)}) collective-permute-start(bf16[128,2048]{1,0:T(8,128)(2,1)S(1)} %collective-permute-done.8.refs_0_), channel_id=1, source_target_pairs={{0,1},{1,2},{2,3},{3,0},{4,5},{5,6},{6,7},{7,4},{8,9},{9,10},{10,1... | collective-permute-start | bytes 1572872 | tf_op jit(solution)/shard_map/ppermute | solution.py:19
  77.5 16.4 %collective-permute-start.14 = (bf16[128,2048]{1,0:T(8,128)(2,1)S(1)}, bf16[128,2048]{1,0:T(8,128)(2,1)}, u32[]{:S(2)}, u32[]{:S(2)}) collective-permute-start(bf16[128,2048]{1,0:T(8,128)(2,1)S(1)} %collective-permute-done.9.refs_1_), channel_id=1, source_target_pairs={{0,3},{1,0},{2,1},{3,2},{4,7},{5,4},{6,5},{7,6},{8,11},{9,8},{10,9... | collective-permute-start | bytes 1572872 | tf_op jit(solution)/shard_map/ppermute | solution.py:19
  81.0 23.2 %collective-permute-start.12 = (bf16[128,2048]{1,0:T(8,128)(2,1)S(1)}, bf16[128,2048]{1,0:T(8,128)(2,1)S(1)}, u32[]{:S(2)}, u32[]{:S(2)}) collective-permute-start(bf16[128,2048]{1,0:T(8,128)(2,1)S(1)} %norm.5.refs_0_), channel_id=1, source_target_pairs={{0,3},{1,0},{2,1},{3,2},{4,7},{5,4},{6,5},{7,6},{8,11},{9,8},{10,9... | collective-permute-start | bytes 1572872 | tf_op jit(solution)/shard_map/ppermute | solution.py:19
  81.0 23.5 %collective-permute-start.11 = (bf16[128,2048]{1,0:T(8,128)(2,1)S(1)}, bf16[128,2048]{1,0:T(8,128)(2,1)S(1)}, u32[]{:S(2)}, u32[]{:S(2)}) collective-permute-start(bf16[128,2048]{1,0:T(8,128)(2,1)S(1)} %norm.4.refs_1_.refs_0_), channel_id=1, source_target_pairs={{0,1},{1,2},{2,3},{3,0},{4,5},{5,6},{6,7},{7,4},{8,9},{9,10},{10,1... | collective-permute-start | bytes 1572872 | tf_op jit(solution)/shard_map/ppermute | solution.py:19
  100.3 14.0 %collective-permute-start.17 = (bf16[128,2048]{1,0:T(8,128)(2,1)S(1)}, bf16[128,2048]{1,0:T(8,128)(2,1)S(1)}, u32[]{:S(2)}, u32[]{:S(2)}) collective-permute-start(bf16[128,2048]{1,0:T(8,128)(2,1)S(1)} %get-tuple-element.51), channel_id=1, source_target_pairs={{0,1},{1,2},{2,3},{3,0},{4,5},{5,6},{6,7},{7,4},{8,9},{9,10},{10,1... | collective-permute-start | bytes 1572872 | tf_op jit(solution)/shard_map/ppermute | solution.py:19
  101.6 13.4 %collective-permute-start.15 = (bf16[128,2048]{1,0:T(8,128)(2,1)S(1)}, bf16[128,2048]{1,0:T(8,128)(2,1)S(1)}, u32[]{:S(2)}, u32[]{:S(2)}) collective-permute-start(bf16[128,2048]{1,0:T(8,128)(2,1)S(1)} %get-tuple-element.48), channel_id=1, source_target_pairs={{0,3},{1,0},{2,1},{3,2},{4,7},{5,4},{6,5},{7,6},{8,11},{9,8},{10,9... | collective-permute-start | bytes 1572872 | tf_op jit(solution)/shard_map/ppermute | solution.py:19
  103.0 22.7 %collective-permute-start.19 = (bf16[128,2048]{1,0:T(8,128)(2,1)S(1)}, bf16[128,2048]{1,0:T(8,128)(2,1)S(1)}, u32[]{:S(2)}, u32[]{:S(2)}) collective-permute-start(bf16[128,2048]{1,0:T(8,128)(2,1)S(1)} %get-tuple-element.52), channel_id=1, source_target_pairs={{0,3},{1,0},{2,1},{3,2},{4,7},{5,4},{6,5},{7,6},{8,11},{9,8},{10,9... | collective-permute-start | bytes 1572872 | tf_op jit(solution)/shard_map/ppermute | solution.py:19
  104.2 34.2 %collective-permute-start.10 = (bf16[128,2048]{1,0:T(8,128)(2,1)S(1)}, bf16[128,2048]{1,0:T(8,128)(2,1)S(1)}, u32[]{:S(2)}, u32[]{:S(2)}) collective-permute-start(bf16[128,2048]{1,0:T(8,128)(2,1)S(1)} %get-tuple-element.46), channel_id=1, source_target_pairs={{0,1},{1,2},{2,3},{3,0},{4,5},{5,6},{6,7},{7,4},{8,9},{9,10},{10,1... | collective-permute-start | bytes 1572872 | tf_op jit(solution)/shard_map/ppermute | solution.py:19
  114.5 22.3 %collective-permute-start.18 = (bf16[128,2048]{1,0:T(8,128)(2,1)S(1)}, bf16[128,2048]{1,0:T(8,128)(2,1)S(1)}, u32[]{:S(2)}, u32[]{:S(2)}) collective-permute-start(bf16[128,2048]{1,0:T(8,128)(2,1)S(1)} %add_convert_fusion), channel_id=1, source_target_pairs={{0,1},{1,2},{2,3},{3,0},{4,5},{5,6},{6,7},{7,4},{8,9},{9,10},{10,1... | collective-permute-start | bytes 1572872 | tf_op jit(solution)/shard_map/ppermute | solution.py:19
  115.1 21.7 %copy-start.5 = (f32[2048]{0:T(1024)S(1)}, f32[2048]{0:T(1024)}, u32[]{:S(2)}) copy-start(f32[2048]{0:T(1024)} %param.20) | copy-start | bytes 24580
  115.1 21.7 %copy-start.6 = (f32[2048]{0:T(1024)S(1)}, f32[2048]{0:T(1024)}, u32[]{:S(2)}) copy-start(f32[2048]{0:T(1024)} %param.21) | copy-start | bytes 24580
  115.1 23.3 %collective-permute-start.16 = (bf16[128,2048]{1,0:T(8,128)(2,1)S(1)}, bf16[128,2048]{1,0:T(8,128)(2,1)S(1)}, u32[]{:S(2)}, u32[]{:S(2)}) collective-permute-start(bf16[128,2048]{1,0:T(8,128)(2,1)S(1)} %add_convert_fusion.1), channel_id=1, source_target_pairs={{0,3},{1,0},{2,1},{3,2},{4,7},{5,4},{6,5},{7,6},{8,11},{9,8},{10,9... | collective-permute-start | bytes 1572872 | tf_op jit(solution)/shard_map/ppermute | solution.py:19
Sparse Core Ops, SparseCore 0:
  9.6 76.2 all-gather.1
